TPU v7x, 128 devices: a whole 4x4x4 slice. The times are simulated.
128 devices in a mesh: rep: 2 (over z_hi), fs: 32 (over z_lo, y, x), tp: 2 (over core).
Axes of the slice: x: 4, y: 4, z: 4 (z_hi: 2, z_lo: 2; z = z_hi * 2 + z_lo), core: 2. Of those that a mesh axis runs over, the one named last changes fastest.
Arguments:
- tokens: bfloat16 [40960, 2048], P(('rep', 'fs'), 'tp'), may hold values from -6 to 6
- norm_first: float32 [2048], replicated, may hold values from 0.1 to 1.9
- norm_mix: float32 [2048], replicated, may hold values from 0.1 to 1.9
- norm_second: float32 [2048], replicated, may hold values from 0.1 to 1.9
- gate_weight: float32 [2048, 2816], P('fs', 'tp'), may hold values from -0.125 to 0.125
- up_weight: float32 [2048, 2816], P('fs', 'tp'), may hold values from -0.125 to 0.125
- down_weight: float32 [2816, 2048], P('tp', 'fs'), may hold values from -0.109375 to 0.109375
- gate_scale: float32 [2816], P('tp'), may hold values from 0.3 to 3
- up_scale: float32 [2816], P('tp'), may hold values from 0.3 to 3
- down_scale: float32 [2048], P('fs'), may hold values from 0.3 to 3
- u_weight: float32 [2048, 1024], P('fs', 'tp'), may hold values from -0.125 to 0.125
- v_weight: float32 [2048, 1024], P('fs', 'tp'), may hold values from -0.125 to 0.125
- u_scale: float32 [1024], P('tp'), may hold values from 0.3 to 3
- v_scale: float32 [1024], P('tp'), may hold values from 0.15 to 6
- ln_gain: float32 [1024], P('tp'), may hold values from 0.1 to 1.9
- ln_bias: float32 [1024], P('tp'), may hold values from -3 to 3
- spatial_weight: bfloat16 [8, 128, 128], P('tp'), may hold values from -0.25 to 0.25
- spatial_bias: float32 [8, 128], P('tp'), may hold values from 0.1 to 1.9
- out_weight: float32 [1024, 2048], P('tp', 'fs'), may hold values from -0.1875 to 0.1875
- out_scale: float32 [2048], P('fs'), may hold values from 0.3 to 3
Outputs:
- layer_out: bfloat16 [40960, 2048], P(('rep', 'fs'), 'tp')
All inputs are finite; a program needn't handle non-finite values.
Results may differ from a plain program's by a relative error of at most 0.019.
Values may be sent and summed in bfloat16 or wider, within the bound.
No kernel may reach another device: no remote copies, remote signals or barrier semaphores. Data moves between devices by JAX's collectives and lax.ppermute only.
A program may use at most 128 MiB of HBM per device.

v0:
```python
import functools

import jax
import jax.numpy as jnp
from jax import lax
from jax.experimental import pallas as pl
from jax.experimental.pallas import tpu as pltpu
from jax.sharding import Mesh
from jax.sharding import PartitionSpec as P


BW = 1024
SPAN = 128
FS = ("fs_0", "fs_1", "fs_2")
REP_FS = ("rep", "fs_0", "fs_1", "fs_2")
LANES = 128
WIDE = 512
HALF_ROWS = 32
FIRST = (4, 4, 4, 4, 3, 3)
OTHERS = (4, 4, 4, 3, 4, 4)
RINGS = (("fs_2", 1), ("fs_1", 1), ("z", 1), ("fs_2", 3), ("fs_1", 3), ("z", 3))
PLACES = (2, 8, 32, 6, 24, 33)

EPS = 1e-06


def other_core(x):
    return lax.ppermute(x, "tp", [(0, 1), (1, 0)])


def normed_rows(values, gain):
    factor = lax.rsqrt(jnp.mean(values * values, axis=1, keepdims=True) + EPS)
    return (values * factor * gain).astype(jnp.bfloat16)


def dot(left, right):
    return jnp.dot(left, right, preferred_element_type=jnp.float32)


def dot_rows(left, rows):
    return lax.dot_general(
        left, rows, (((1,), (1,)), ((), ())), preferred_element_type=jnp.float32
    )


def gelu(a):
    return 0.5 * a * (1.0 + jnp.tanh(0.7978845608028654 * (a + 0.044715 * a * a * a)))


def spec(block, index):
    return pl.BlockSpec(block, index)


def whole(shape):
    return pl.BlockSpec(shape, lambda *_: (0,) * len(shape))


ANY = pl.BlockSpec(memory_space=pl.ANY)


def params(steps):
    return pltpu.CompilerParams(
        dimension_semantics=("arbitrary",) * steps, vmem_limit_bytes=60 * 1024 * 1024
    )


def cost(flops, moved, special):
    return pl.CostEstimate(flops=flops, bytes_accessed=moved, transcendentals=special)


def exchange(x, color, turn):
    name, flip = RINGS[(color + turn) % 6]
    axis = ("rep", "fs_0") if name == "z" else name
    return lax.ppermute(x, axis, [(i, i ^ flip) for i in range(4)])


def place(color, slot):
    at = 0
    for turn in range(6):
        if slot >> turn & 1:
            at ^= PLACES[(color + turn) % 6]
    return at


def starts(widths):
    ends = [0]
    for n in widths:
        ends.append(ends[-1] + n * LANES)
    return ends


PAIRS = [(p, t + k) for t in (0, 2, 4, 6) for p in (0, 1) for k in (0, 1)]
PAIRS += [(0, 8), (0, 9), (1, 8), (1, 9), (0, 10), (1, 10)]


def prepare_kernel(
    rep, gate, up, down, u, v, out, gate_s, up_s, down_s, u_s, v_s, out_s, *colors
):
    rows = pl.ds(pl.multiple_of(rep[0] * HALF_ROWS, HALF_ROWS), HALF_ROWS)
    low = jnp.bfloat16

    def across(scale):
        return scale[...][None, :]

    def down_rows(scale):
        size = scale.shape[0]
        row = lax.broadcasted_iota(jnp.int32, (HALF_ROWS, size), 0) + rep[0] * HALF_ROWS
        column = lax.broadcasted_iota(jnp.int32, (HALF_ROWS, size), 1)
        return jnp.sum(jnp.where(row == column, across(scale), 0.0), axis=1, keepdims=True)

    pair = ((gate[rows, :] * across(gate_s)).astype(low), (up[rows, :] * across(up_s)).astype(low))
    firsts = [pair[p][:, t * LANES : (t + 1) * LANES] for p, t in PAIRS]
    rest = jnp.concatenate(
        [
            (out[rows, :] * down_rows(out_s)).astype(low),
            (u[rows, :] * across(u_s)).astype(low),
            (v[rows, :] * across(v_s)).astype(low),
            (down[rows, :] * down_rows(down_s)).astype(low),
        ],
        axis=1,
    )
    at, begin = 0, starts(OTHERS)
    for c, ref in enumerate(colors):
        mine = firsts[at : at + FIRST[c]] + [rest[:, begin[c] : begin[c + 1]]]
        ref[...] = jnp.concatenate(mine, axis=1)
        at += FIRST[c]


def prepare(rep, *arrays):
    return pl.pallas_call(
        prepare_kernel,
        out_shape=[
            jax.ShapeDtypeStruct((HALF_ROWS, (a + b) * LANES), jnp.bfloat16)
            for a, b in zip(FIRST, OTHERS)
        ],
        grid_spec=pltpu.PrefetchScalarGridSpec(
            num_scalar_prefetch=1,
            grid=(1,),
            in_specs=[whole(a.shape) for a in arrays],
            out_specs=[whole((HALF_ROWS, (a + b) * LANES)) for a, b in zip(FIRST, OTHERS)],
        ),
        compiler_params=params(1),
        name="prepare",
    )(rep, *arrays)


VMEM = pl.BlockSpec(memory_space=pltpu.VMEM)


def join_kernel(cuts, *refs):
    held, arrived, joined = refs[:6], refs[6:12], refs[12:]
    for c in range(6):
        begin, end = cuts[c]
        rows = held[c].shape[0]
        joined[c][pl.ds(0, rows), :] = held[c][:, begin:end]
        joined[c][pl.ds(rows, rows), :] = arrived[c][:, begin:end]


def join(held, arrived, cuts=None):
    rows, low = held[0].shape[0], jnp.bfloat16
    if cuts is None:
        cuts = [(0, x.shape[1]) for x in held]
    return pl.pallas_call(
        functools.partial(join_kernel, cuts),
        out_shape=[jax.ShapeDtypeStruct((2 * rows, b - a), low) for a, b in cuts],
        in_specs=[VMEM] * 12,
        out_specs=[VMEM] * 6,
        compiler_params=pltpu.CompilerParams(vmem_limit_bytes=32 * 1024 * 1024),
        name="join",
    )(*held, *arrived)


def gather(colors):
    held = list(colors)
    for turn in range(5):
        arrived = [exchange(x, c, turn) for c, x in enumerate(held)]
        if turn < 4:
            held = join(held, arrived)
    groups = []
    for g in range(2):
        edge = [n * LANES for n in FIRST]
        cuts = [(e, x.shape[1]) if g else (0, e) for e, x in zip(edge, held)]
        group = join(held, arrived, cuts)
        last = []
        for c, x in enumerate(group):
            last.append(exchange(x, c, 5))
        groups.append([piece[c] for c in range(6) for piece in (group, last)])
    return groups


def place_blocks(at, pieces, weight, sems, widths, colors):
    begin = starts(widths)
    for c in colors:
        columns = pl.ds(begin[c], widths[c] * LANES)
        for k in range(2):

            def copy_four(high, carry, c=c, k=k, columns=columns):
                moved = at ^ place(c, 32 * k)
                for bit in range(3):
                    moved = moved ^ ((high >> bit & 1) * place(c, 4 << bit))
                for low in range(4):
                    to = (moved ^ place(c, low)) * HALF_ROWS
                    origin = (high * 4 + low) * HALF_ROWS
                    pltpu.make_async_copy(
                        pieces[2 * c + k].at[
                            pl.ds(pl.multiple_of(origin, HALF_ROWS), HALF_ROWS), :
                        ],
                        weight.at[pl.ds(pl.multiple_of(to, HALF_ROWS), HALF_ROWS), columns],
                        sems.at[c],
                    ).start()
                return carry

            lax.fori_loop(0, 8, copy_four, 0)


def wait_color(weight, sems, widths, c):
    columns = pl.ds(starts(widths)[c], widths[c] * LANES)
    part = weight.at[:, columns]
    pltpu.make_async_copy(part, part, sems.at[c]).wait()


def silu_product(gate, up):
    return (gate / (1.0 + jnp.exp(-gate)) * up).astype(jnp.bfloat16)


def narrow_step(normed, weight):
    both = dot(normed, weight)
    tile = [both[:, k * LANES : (k + 1) * LANES] for k in range(6)]
    gate = jnp.concatenate([tile[0], tile[1], tile[4]], axis=1)
    up = jnp.concatenate([tile[2], tile[3], tile[5]], axis=1)
    return silu_product(gate, up)


def hidden_step(step, normed, weight, hidden):
    @pl.when(step < 4)
    def _():
        columns = pl.ds(pl.multiple_of(step * WIDE, WIDE), WIDE)
        both = dot(normed[...], weight[:, columns])
        to = pl.ds(pl.multiple_of(step * (WIDE // 2), WIDE // 2), WIDE // 2)
        hidden[:, to] = silu_product(both[:, : WIDE // 2], both[:, WIDE // 2 :])

    @pl.when(step == 4)
    def _():
        hidden[:, 2 * WIDE :] = narrow_step(normed[...], weight[:, 4 * WIDE :])


def first_kernel(core, at, own, other, gain, *rest):
    pieces, (hidden, kept, weight, normed, sems, out_sem) = rest[:12], rest[12:]
    step = pl.program_id(0)

    @pl.when(step == 0)
    def _():
        place_blocks(at[0], pieces, weight, sems, FIRST, range(6))
        left = jnp.where(core[0] == 0, own[...], other[...])
        right = jnp.where(core[0] == 0, other[...], own[...])
        values = jnp.concatenate([left, right], axis=1).astype(jnp.float32)
        normed[...] = normed_rows(values, gain[...])

    for c in range(6):

        @pl.when(step == min(c, 4))
        def _():
            wait_color(weight, sems, FIRST, c)

    hidden_step(step, normed, weight, hidden)

    @pl.when(step == 4)
    def _():
        copy = pltpu.make_async_copy(weight, kept, out_sem)
        copy.start()
        copy.wait()


def first_hidden(core, at, own, other, gain, pieces):
    count, half = own.shape
    width = 2 * half
    columns = sum(FIRST) * LANES
    units = columns // 2
    return pl.pallas_call(
        first_kernel,
        out_shape=[
            jax.ShapeDtypeStruct((count, units), jnp.bfloat16),
            jax.ShapeDtypeStruct((width, columns), jnp.bfloat16),
        ],
        grid_spec=pltpu.PrefetchScalarGridSpec(
            num_scalar_prefetch=2,
            grid=(5,),
            in_specs=[whole((count, half)), whole((count, half)), whole((1, width))] + [ANY] * 12,
            out_specs=[whole((count, units)), ANY],
            scratch_shapes=[
                pltpu.VMEM((width, columns), jnp.bfloat16),
                pltpu.VMEM((count, width), jnp.bfloat16),
                pltpu.SemaphoreType.DMA((6,)),
                pltpu.SemaphoreType.DMA,
            ],
        ),
        compiler_params=params(1),
        cost_estimate=cost(2 * count * width * columns, 4 * width * columns, count * units),
        name="first_hidden",
    )(core, at, own, other, gain, *pieces)


def down_kernel(at, hidden, *rest):
    pieces, (term, kept, weight, sems, out_sem) = rest[:12], rest[12:]
    step = pl.program_id(0)
    begin = starts(OTHERS)
    copy = pltpu.make_async_copy(weight, kept, out_sem)

    @pl.when(step == 0)
    def _():
        place_blocks(at[0], pieces, weight, sems, OTHERS, (3, 4, 5, 0, 1, 2))
        for c in (3, 4, 5):
            wait_color(weight, sems, OTHERS, c)

    rows = pl.ds(pl.multiple_of(step * WIDE, WIDE), WIDE)
    term[...] = dot_rows(hidden[...], weight[rows, begin[3] :]).astype(jnp.bfloat16)

    @pl.when(step == 0)
    def _():
        for c in (0, 1, 2):
            wait_color(weight, sems, OTHERS, c)
        copy.start()

    @pl.when(step == pl.num_programs(0) - 1)
    def _():
        copy.wait()


def first_down(at, hidden, width, pieces):
    count, units = hidden.shape
    columns = sum(OTHERS) * LANES
    return pl.pallas_call(
        down_kernel,
        out_shape=[
            jax.ShapeDtypeStruct((count, width), jnp.bfloat16),
            jax.ShapeDtypeStruct((width, columns), jnp.bfloat16),
        ],
        grid_spec=pltpu.PrefetchScalarGridSpec(
            num_scalar_prefetch=1,
            grid=(width // WIDE,),
            in_specs=[whole((count, units))] + [ANY] * 12,
            out_specs=[spec((count, WIDE), lambda j, a: (0, j)), ANY],
            scratch_shapes=[
                pltpu.VMEM((width, columns), jnp.bfloat16),
                pltpu.SemaphoreType.DMA((6,)),
                pltpu.SemaphoreType.DMA,
            ],
        ),
        compiler_params=params(1),
        cost_estimate=cost(2 * count * width * units, 4 * width * columns, 0),
        name="first_down",
    )(at, hidden, *pieces)


def gates_kernel(core, own, other, term, far, gain, rows, middle, act, sums, normed):
    @pl.when(pl.program_id(0) == 0)
    def _():
        left = jnp.where(core[0] == 0, own[...], other[...])
        right = jnp.where(core[0] == 0, other[...], own[...])
        values = jnp.concatenate([left, right], axis=1).astype(jnp.float32)
        values = values + 0.5 * (term[...].astype(jnp.float32) + far[...].astype(jnp.float32))
        mid = values.astype(jnp.bfloat16)
        middle[...] = mid
        normed[...] = normed_rows(mid.astype(jnp.float32), gain[...])

    acted = gelu(dot(normed[...], rows[...]))
    act[0] = acted

    @pl.when(pl.program_id(0) == 0)
    def _():
        lane = lax.broadcasted_iota(jnp.int32, sums.shape, 1)
        total = jnp.sum(acted, axis=1, keepdims=True)
        squares = jnp.sum(acted * acted, axis=1, keepdims=True)
        sums[...] = jnp.where(lane == 0, total, squares)


def gates(core, own, other, term, far, gain, weight, chans):
    count, half = own.shape
    width = 2 * half
    return pl.pallas_call(
        gates_kernel,
        out_shape=[
            jax.ShapeDtypeStruct((count, width), jnp.bfloat16),
            jax.ShapeDtypeStruct((2, count, chans), jnp.float32),
            jax.ShapeDtypeStruct((count, LANES), jnp.float32),
        ],
        grid_spec=pltpu.PrefetchScalarGridSpec(
            num_scalar_prefetch=1,
            grid=(2,),
            in_specs=[
                whole((count, half)),
                whole((count, half)),
                whole((count, width)),
                whole((count, width)),
                whole((1, width)),
                spec((width, chans), lambda i, c: (0, 2 - i)),
            ],
            out_specs=[
                whole((count, width)),
                spec((1, count, chans), lambda i, c: (i, 0, 0)),
                whole((count, LANES)),
            ],
            scratch_shapes=[pltpu.VMEM((count, width), jnp.bfloat16)],
        ),
        compiler_params=params(1),
        cost_estimate=cost(4 * count * width * chans, 4 * width * chans, 2 * count * chans),
        name="gates",
    )(core, own, other, term, far, gain, weight)


def mix_kernel(act, sums, far, gain, bias, weight, shift, rows, term, mixed):
    groups = weight.shape[0]

    @pl.when(pl.program_id(0) == 0)
    def _():
        at = lax.broadcasted_iota(jnp.int32, (SPAN, SPAN), 0)
        source = lax.broadcasted_iota(jnp.int32, (SPAN, SPAN), 1)
        masked = [
            jnp.where(source <= at, weight[g], jnp.zeros_like(weight[g])) for g in range(groups)
        ]
        count, chans = mixed.shape
        wide = chans // groups
        for n in range(count // SPAN):
            block = pl.ds(n * SPAN, SPAN)
            totals = (sums[block, :] + far[block, :]) / BW
            v_mean = totals[:, 0:1]
            v_var = totals[:, 1:2] - v_mean * v_mean
            v_normed = (act[0, block, :] - v_mean) * lax.rsqrt(v_var + EPS) * gain[...] + bias[...]
            v_normed = v_normed.astype(jnp.bfloat16)
            spatial = [
                dot(masked[g], v_normed[:, g * wide : (g + 1) * wide]) + shift[:, g : g + 1]
                for g in range(groups)
            ]
            product = act[1, block, :] * jnp.concatenate(spatial, axis=1)
            mixed[block, :] = product.astype(jnp.bfloat16)

    term[...] = dot_rows(mixed[...], rows[...]).astype(jnp.bfloat16)


def mix(act, sums, far, gain, bias, weight, shift, rows):
    _, count, chans = act.shape
    width = rows.shape[0]
    groups = weight.shape[0]
    return pl.pallas_call(
        mix_kernel,
        out_shape=jax.ShapeDtypeStruct((count, width), jnp.bfloat16),
        grid=(width // WIDE,),
        in_specs=[
            whole(act.shape),
            whole((count, LANES)),
            whole((count, LANES)),
            whole((1, chans)),
            whole((1, chans)),
            whole((groups, SPAN, SPAN)),
            whole((SPAN, groups)),
            spec((WIDE, chans), lambda j: (j, 0)),
        ],
        out_specs=spec((count, WIDE), lambda j: (0, j)),
        scratch_shapes=[pltpu.VMEM((count, chans), jnp.bfloat16)],
        compiler_params=params(1),
        cost_estimate=cost(2 * count * width * chans, 2 * width * chans, count),
        name="mix",
    )(act, sums, far, gain, bias, weight, shift, rows)


def second_kernel(
    core, middle, term, far, gain, first, others, send, keep, base, normed, hidden, wide, down, sems
):
    step = pl.program_id(0)
    steps = 5
    outs = down.shape[0] // WIDE
    begin = starts(OTHERS)[3]
    cuts = [pl.ds(k * WIDE, WIDE) for k in range(4)] + [pl.ds(4 * WIDE, 6 * LANES)]
    copies = [
        pltpu.make_async_copy(first.at[:, cut], wide.at[:, cut], sems.at[k])
        for k, cut in enumerate(cuts)
    ]
    copies.append(
        pltpu.make_async_copy(others.at[:, pl.ds(begin, down.shape[1])], down, sems.at[steps])
    )

    @pl.when(step == 0)
    def _():
        for copy in copies:
            copy.start()
        values = middle[...].astype(jnp.float32) + (
            term[...].astype(jnp.float32) + far[...].astype(jnp.float32)
        )
        second = values.astype(jnp.bfloat16)
        half = second.shape[1] // 2
        base[...] = jnp.where(core[0] == 0, second[:, :half], second[:, half:])
        normed[...] = normed_rows(second.astype(jnp.float32), gain[...])

    for k, copy in enumerate(copies):

        @pl.when(step == k)
        def _():
            copy.wait()

    hidden_step(step, normed, wide, hidden)

    @pl.when(step >= steps)
    def _():
        n = step - steps
        mine = jnp.where(n < outs // 2, 1 - core[0], core[0])
        row = mine * (outs // 2) + lax.rem(n, outs // 2)
        rows = pl.ds(pl.multiple_of(row * WIDE, WIDE), WIDE)
        part = dot_rows(hidden[...], down[rows, :]).astype(jnp.bfloat16)

        @pl.when(n < outs // 2)
        def _():
            send[...] = part

        @pl.when(n >= outs // 2)
        def _():
            keep[...] = part


def second_pass(core, middle, term, far, gain, first, others):
    count, width = middle.shape
    half = width // 2
    columns = first.shape[1]
    units = columns // 2
    outs = width // WIDE
    sent = outs // 2
    return pl.pallas_call(
        second_kernel,
        out_shape=[jax.ShapeDtypeStruct((count, half), jnp.bfloat16)] * 3,
        grid_spec=pltpu.PrefetchScalarGridSpec(
            num_scalar_prefetch=1,
            grid=(5 + outs,),
            in_specs=[
                whole((count, width)),
                whole((count, width)),
                whole((count, width)),
                whole((1, width)),
                ANY,
                ANY,
            ],
            out_specs=[
                spec((count, WIDE), lambda j, c: (0, jnp.clip(j - 5, 0, sent - 1))),
                spec((count, WIDE), lambda j, c: (0, jnp.maximum(j - 5 - sent, 0))),
                whole((count, half)),
            ],
            scratch_shapes=[
                pltpu.VMEM((count, width), jnp.bfloat16),
                pltpu.VMEM((count, units), jnp.bfloat16),
                pltpu.VMEM((width, columns), jnp.bfloat16),
                pltpu.VMEM((width, units), jnp.bfloat16),
                pltpu.SemaphoreType.DMA((6,)),
            ],
        ),
        compiler_params=params(1),
        cost_estimate=cost(6 * count * width * units, 6 * width * units, count * units),
        name="second_pass",
    )(core, middle, term, far, gain, first, others)


def layer(
    tokens,
    norm_first,
    norm_mix,
    norm_second,
    gate_weight,
    up_weight,
    down_weight,
    gate_scale,
    up_scale,
    down_scale,
    u_weight,
    v_weight,
    u_scale,
    v_scale,
    ln_gain,
    ln_bias,
    spatial_weight,
    spatial_bias,
    out_weight,
    out_scale,
):
    chans = u_weight.shape[1]
    width = 2 * tokens.shape[1]

    def number(x):
        return x.reshape(1).astype(jnp.int32)

    core = number(lax.axis_index("tp"))
    rep = lax.axis_index("rep")
    at = number(2 * lax.axis_index(FS) + rep)

    colors = prepare(
        number(rep),
        gate_weight,
        up_weight,
        down_weight.T,
        u_weight,
        v_weight,
        out_weight.T,
        gate_scale,
        up_scale,
        down_scale,
        u_scale,
        v_scale,
        out_scale,
    )
    one, two = gather(colors)

    own, other = tokens, other_core(tokens)
    hidden, first = first_hidden(core, at, own, other, norm_first[None], one)
    term, others = first_down(at, hidden, width, two)
    middle, act, sums = gates(
        core, own, other, term, other_core(term), norm_mix[None], others, chans
    )
    term = mix(
        act,
        sums,
        other_core(sums),
        ln_gain[None],
        ln_bias[None],
        spatial_weight,
        spatial_bias.T,
        others,
    )
    send, keep, base = second_pass(
        core, middle, term, other_core(term), norm_second[None], first, others
    )
    last = keep.astype(jnp.float32) + other_core(send).astype(jnp.float32)
    return (base.astype(jnp.float32) + 0.5 * last).astype(jnp.bfloat16)


def solution(mesh):
    torus = Mesh(
        mesh.devices.reshape(mesh.shape["rep"], 2, 4, 4, mesh.shape["tp"]),
        ("rep", "fs_0", "fs_1", "fs_2", "tp"),
    )
    in_specs = (
        P(REP_FS, "tp"),
        P(),
        P(),
        P(),
        P(FS, "tp"),
        P(FS, "tp"),
        P("tp", FS),
        P("tp"),
        P("tp"),
        P(FS),
        P(FS, "tp"),
        P(FS, "tp"),
        P("tp"),
        P("tp"),
        P("tp"),
        P("tp"),
        P("tp", None, None),
        P("tp", None),
        P("tp", FS),
        P(FS),
    )
    out_specs = P(REP_FS, "tp")
    return jax.shard_map(layer, mesh=torus, in_specs=in_specs, out_specs=out_specs, check_vma=False)
```

profile of v0, /device:TPU:1, one launch (start us, length us, event | category | flops | bytes accessed | tf_op | source)
XLA Modules:
  0.0 245.1 jit_solution(3447113297747584969)
XLA Ops:
  0.0 2.2 prepare.1
  2.2 3.4 %collective-permute-start.4 = (bf16[32,896]{1,0:T(8,128)(2,1)}, bf16[32,896]{1,0:T(8,128)(2,1)S(1)}, u32[]{:S(2)}, u32[]{:S(2)}) collective-permute-start(bf16[32,896]{1,0:T(8,128)(2,1)} %get-tuple-element.60.refs_3_), channel_id=1, source_target_pairs={{0,6},{2,4},{4,2},{6,0},{1,7},{3,5},{5,3},{7,1},{8,14},{10,12},{12... | collective-permute-start | bytes 172040 | tf_op jit(solution)/shard_map/ppermute | solution.py:74
  8.5 1.9 collective-permute-start.5
  10.4 2.2 collective-permute-start.6
  13.0 2.2 collective-permute-done.6.refs_11_
  21.1 2.3 collective-permute-start.9
  23.4 2.7 %collective-permute-start.11 = (bf16[64,896]{1,0:T(8,128)(2,1)S(1)}, bf16[64,896]{1,0:T(8,128)(2,1)S(1)}, u32[]{:S(2)}, u32[]{:S(2)}) collective-permute-start(bf16[64,896]{1,0:T(8,128)(2,1)S(1)} %get-tuple-element.67.refs_4_), channel_id=1, source_target_pairs={{0,96},{32,64},{64,32},{96,0},{1,97},{33,65},{65,33},{97,1},{2,98}... | collective-permute-start | bytes 344072 | tf_op jit(solution)/shard_map/ppermute | solution.py:74
  26.6 2.0 collective-permute-done.11.refs_10_
  32.4 2.7 %collective-permute-start.15 = (bf16[128,1024]{1,0:T(8,128)(2,1)S(1)}, bf16[128,1024]{1,0:T(8,128)(2,1)S(1)}, u32[]{:S(2)}, u32[]{:S(2)}) collective-permute-start(bf16[128,1024]{1,0:T(8,128)(2,1)S(1)} %get-tuple-element.71.refs_2_), channel_id=1, source_target_pairs={{0,24},{8,16},{16,8},{24,0},{1,25},{9,17},{17,9},{25,1},{2,26},{10... | collective-permute-start | bytes 786440 | tf_op jit(solution)/shard_map/ppermute | solution.py:74
  37.8 2.5 %collective-permute-done.17.refs_10_ = bf16[128,896]{1,0:T(8,128)(2,1)S(1)} collective-permute-done((bf16[128,896]{1,0:T(8,128)(2,1)S(1)}, bf16[128,896]{1,0:T(8,128)(2,1)S(1)}, u32[]{:S(2)}, u32[]{:S(2)}) %collective-permute-start.17) | collective-permute-done | bytes 229408 | tf_op jit(solution)/shard_map/ppermute | solution.py:74
  44.5 2.3 collective-permute-start.21
  47.1 4.1 %collective-permute-done.22.refs_9_ = bf16[256,896]{1,0:T(8,128)(2,1)S(1)} collective-permute-done((bf16[256,896]{1,0:T(8,128)(2,1)S(1)}, bf16[256,896]{1,0:T(8,128)(2,1)S(1)}, u32[]{:S(2)}, u32[]{:S(2)}) %collective-permute-start.22) | collective-permute-done | bytes 458784 | tf_op jit(solution)/shard_map/ppermute | solution.py:74
  51.9 2.5 %collective-permute-done.23.refs_10_ = bf16[256,896]{1,0:T(8,128)(2,1)S(1)} collective-permute-done((bf16[256,896]{1,0:T(8,128)(2,1)S(1)}, bf16[256,896]{1,0:T(8,128)(2,1)S(1)}, u32[]{:S(2)}, u32[]{:S(2)}) %collective-permute-start.23) | collective-permute-done | bytes 458784 | tf_op jit(solution)/shard_map/ppermute | solution.py:74
  54.4 4.4 %collective-permute-done.24.refs_11_ = bf16[256,896]{1,0:T(8,128)(2,1)S(1)} collective-permute-done((bf16[256,896]{1,0:T(8,128)(2,1)S(1)}, bf16[256,896]{1,0:T(8,128)(2,1)S(1)}, u32[]{:S(2)}, u32[]{:S(2)}) %collective-permute-start.24) | collective-permute-done | bytes 458784 | tf_op jit(solution)/shard_map/ppermute | solution.py:74
  63.1 9.1 %collective-permute-done.28.refs_9_ = bf16[512,896]{1,0:T(8,128)(2,1)S(1)} collective-permute-done((bf16[512,896]{1,0:T(8,128)(2,1)S(1)}, bf16[512,896]{1,0:T(8,128)(2,1)S(1)}, u32[]{:S(2)}, u32[]{:S(2)}) %collective-permute-start.28) | collective-permute-done | bytes 917536 | tf_op jit(solution)/shard_map/ppermute | solution.py:74
  73.9 3.4 %collective-permute-done.29.refs_10_ = bf16[512,896]{1,0:T(8,128)(2,1)S(1)} collective-permute-done((bf16[512,896]{1,0:T(8,128)(2,1)S(1)}, bf16[512,896]{1,0:T(8,128)(2,1)S(1)}, u32[]{:S(2)}, u32[]{:S(2)}) %collective-permute-start.29) | collective-permute-done | bytes 917536 | tf_op jit(solution)/shard_map/ppermute | solution.py:74
  77.3 9.1 %collective-permute-start = (bf16[640,1024]{1,0:T(8,128)(2,1)S(1)}, bf16[640,1024]{1,0:T(8,128)(2,1)S(1)}, u32[]{:S(2)}, u32[]{:S(2)}) collective-permute-start(bf16[640,1024]{1,0:T(8,128)(2,1)S(1)} %copy-done.17), channel_id=1, source_target_pairs={{0,1},{1,0},{2,3},{3,2},{4,5},{5,4},{6,7},{7,6},{8,9},{9,8},{10,11... | collective-permute-start | bytes 3932168 | tf_op jit(solution)/shard_map/ppermute | solution.py:28
  88.2 1.8 collective-permute-start.40
  93.5 6.2 %collective-permute-done.40.rest_7_ = bf16[1024,384]{1,0:T(8,128)(2,1)S(1)} collective-permute-done((bf16[1024,384]{1,0:T(8,128)(2,1)S(1)}, bf16[1024,384]{1,0:T(8,128)(2,1)S(1)}, u32[]{:S(2)}, u32[]{:S(2)}) %collective-permute-start.40) | collective-permute-done | bytes 786464 | tf_op jit(solution)/shard_map/ppermute | solution.py:74
  101.1 6.0 %collective-permute-done.35.rest_9_ = bf16[1024,384]{1,0:T(8,128)(2,1)S(1)} collective-permute-done((bf16[1024,384]{1,0:T(8,128)(2,1)S(1)}, bf16[1024,384]{1,0:T(8,128)(2,1)S(1)}, u32[]{:S(2)}, u32[]{:S(2)}) %collective-permute-start.35) | collective-permute-done | bytes 786464 | tf_op jit(solution)/shard_map/ppermute | solution.py:74
  107.1 12.3 %collective-permute-done.36.rest_11_ = bf16[1024,384]{1,0:T(8,128)(2,1)S(1)} collective-permute-done((bf16[1024,384]{1,0:T(8,128)(2,1)S(1)}, bf16[1024,384]{1,0:T(8,128)(2,1)S(1)}, u32[]{:S(2)}, u32[]{:S(2)}) %collective-permute-start.36) | collective-permute-done | bytes 786464 | tf_op jit(solution)/shard_map/ppermute | solution.py:74
  123.9 16.5 %first_hidden.1 = (bf16[640,1408]{1,0:T(8,128)(2,1)}, bf16[2048,2816]{1,0:T(8,128)(2,1)}) custom-call(s32[1]{0:T(128)} %bitcast.core, s32[1]{0:T(128)} %bitcast.1.at, bf16[640,1024]{1,0:T(8,128)(2,1)} %own.3, bf16[640,1024]{1,0:T(8,128)(2,1)} %copy-done.18, f32[1,2048]{1,0:T(1,128)} %bitcast.17, bf16[1024,512]{1,0:T(8,128)(2,1)} %copy-done.10, ...), custom_call_target="tpu_custom_call" | custom-call | flops 7381975040 | bytes 23068672 | tf_op jit(solution)/shard_map/first_hidden/pallas_call | solution.py:279
  140.4 6.3 %collective-permute-done.42.rest_11_ = bf16[1024,512]{1,0:T(8,128)(2,1)} collective-permute-done((bf16[1024,512]{1,0:T(8,128)(2,1)}, bf16[1024,512]{1,0:T(8,128)(2,1)}, u32[]{:S(2)}, u32[]{:S(2)}) %collective-permute-start.42) | collective-permute-done | bytes 1048608 | tf_op jit(solution)/shard_map/ppermute | solution.py:74
  146.7 13.9 %first_down.1 = (bf16[640,2048]{1,0:T(8,128)(2,1)}, bf16[2048,2944]{1,0:T(8,128)(2,1)}) custom-call(s32[1]{0:T(128)} %bitcast.1.at, bf16[640,1408]{1,0:T(8,128)(2,1)} %get-tuple-element.93.hidden, bf16[1024,512]{1,0:T(8,128)(2,1)} %copy-done, bf16[1024,512]{1,0:T(8,128)(2,1)} %collective-permute-done.37.rest_1_, bf16[1024,512]{1,0:T(8,128)(2,1)} %copy-done.1, ...), custom_call_target="tpu_custom_call" | custom-call | flops 3690987520 | bytes 24117248 | tf_op jit(solution)/shard_map/first_down/pallas_call | solution.py:332
  160.6 22.2 %collective-permute-start.43 = (bf16[640,2048]{1,0:T(8,128)(2,1)}, bf16[640,2048]{1,0:T(8,128)(2,1)S(1)}, u32[]{:S(2)}, u32[]{:S(2)}) collective-permute-start(bf16[640,2048]{1,0:T(8,128)(2,1)} %get-tuple-element.100.term), channel_id=1, source_target_pairs={{0,1},{1,0},{2,3},{3,2},{4,5},{5,4},{6,7},{7,6},{8,9},{9,8},{10,11... | collective-permute-start | bytes 7864328 | tf_op jit(solution)/shard_map/ppermute | solution.py:28
  182.9 4.7 %collective-permute-done.43.far = bf16[640,2048]{1,0:T(8,128)(2,1)S(1)} collective-permute-done((bf16[640,2048]{1,0:T(8,128)(2,1)}, bf16[640,2048]{1,0:T(8,128)(2,1)S(1)}, u32[]{:S(2)}, u32[]{:S(2)}) %collective-permute-start.43) | collective-permute-done | bytes 2621472 | tf_op jit(solution)/shard_map/ppermute | solution.py:28
  189.1 11.9 %gates.1 = (bf16[640,2048]{1,0:T(8,128)(2,1)}, f32[2,640,512]{2,1,0:T(8,128)}, f32[640,128]{1,0:T(8,128)}) custom-call(s32[1]{0:T(128)} %bitcast.core, bf16[640,1024]{1,0:T(8,128)(2,1)} %own.3, bf16[640,1024]{1,0:T(8,128)(2,1)} %copy-done.18, bf16[640,2048]{1,0:T(8,128)(2,1)} %get-tuple-element.100.term, bf16[640,2048]{1,0:T(8,128)(2,1)} %copy-done.16, ...), custom_call_target="tpu_custom_call" | custom-call | flops 2684354560 | bytes 4194304 | tf_op jit(solution)/shard_map/gates/pallas_call | solution.py:380
  203.6 7.3 %mix.1.term = bf16[640,2048]{1,0:T(8,128)(2,1)} custom-call(f32[2,640,512]{2,1,0:T(8,128)} %get-tuple-element.103.act, f32[640,128]{1,0:T(8,128)} %get-tuple-element.104.sums, f32[640,128]{1,0:T(8,128)} %copy-done.20, f32[1,512]{1,0:T(1,128)} %bitcast.15, f32[1,512]{1,0:T(1,128)} %bitcast.16, bf16[4,128,128]{2,1,0:T(8,128)(2,1)} %weight.1, ...), custom_call_target="tpu_custom_call" | custom-call | flops 1342177280 | bytes 2097152 | tf_op jit(solution)/shard_map/mix/pallas_call | solution.py:444
  211.2 4.7 %collective-permute-done.45.far = bf16[640,2048]{1,0:T(8,128)(2,1)S(1)} collective-permute-done((bf16[640,2048]{1,0:T(8,128)(2,1)}, bf16[640,2048]{1,0:T(8,128)(2,1)S(1)}, u32[]{:S(2)}, u32[]{:S(2)}) %collective-permute-start.45) | collective-permute-done | bytes 2621472 | tf_op jit(solution)/shard_map/ppermute | solution.py:28
  217.4 20.7 %second_pass.1 = (bf16[640,1024]{1,0:T(8,128)(2,1)}, bf16[640,1024]{1,0:T(8,128)(2,1)}, bf16[640,1024]{1,0:T(8,128)(2,1)}) custom-call(s32[1]{0:T(128)} %bitcast.core, bf16[640,2048]{1,0:T(8,128)(2,1)} %get-tuple-element.102.middle, bf16[640,2048]{1,0:T(8,128)(2,1)} %mix.1.term, bf16[640,2048]{1,0:T(8,128)(2,1)} %copy-done.22, f32[1,2048]{1,0:T(1,128)} %bitcast.18, ...), custom_call_target="tpu_custom_call" | custom-call | flops 11072962560 | bytes 17301504 | tf_op jit(solution)/shard_map/second_pass/pallas_call | solution.py:526
  238.6 2.9 %collective-permute-done.46 = bf16[640,1024]{1,0:T(8,128)(2,1)S(1)} collective-permute-done((bf16[640,1024]{1,0:T(8,128)(2,1)}, bf16[640,1024]{1,0:T(8,128)(2,1)S(1)}, u32[]{:S(2)}, u32[]{:S(2)}) %collective-permute-start.46) | collective-permute-done | bytes 1310752 | tf_op jit(solution)/shard_map/ppermute | solution.py:28
  241.4 3.6 %add_convert_fusion = bf16[640,1024]{1,0:T(8,128)(2,1)} fusion(bf16[640,1024]{1,0:T(8,128)(2,1)S(1)} %collective-permute-done.46, bf16[640,1024]{1,0:T(8,128)(2,1)} %get-tuple-element.107, bf16[640,1024]{1,0:T(8,128)(2,1)} %get-tuple-element.106), kind=kLoop, calls=%fused_computation | loop fusion | flops 4587520 | bytes 5242880 | tf_op jit(solution)/shard_map/convert_element_type | solution.py:628
  (134 shorter events, 44.6 us)
Async XLA Ops:
  5.6 9.6 %collective-permute-start.1 = (bf16[32,1024]{1,0:T(8,128)(2,1)}, bf16[32,1024]{1,0:T(8,128)(2,1)S(1)}, u32[]{:S(2)}, u32[]{:S(2)}) collective-permute-start(bf16[32,1024]{1,0:T(8,128)(2,1)} %get-tuple-element.57.refs_0_), channel_id=1, source_target_pairs={{0,2},{2,0},{4,6},{6,4},{1,3},{3,1},{5,7},{7,5},{8,10},{10,8},{12,... | collective-permute-start | bytes 196616 | tf_op jit(solution)/shard_map/ppermute | solution.py:74
  5.6 9.6 %collective-permute-start.2 = (bf16[32,1024]{1,0:T(8,128)(2,1)}, bf16[32,1024]{1,0:T(8,128)(2,1)S(1)}, u32[]{:S(2)}, u32[]{:S(2)}) collective-permute-start(bf16[32,1024]{1,0:T(8,128)(2,1)} %get-tuple-element.58.refs_1_), channel_id=1, source_target_pairs={{0,8},{8,0},{16,24},{24,16},{1,9},{9,1},{17,25},{25,17},{2,10},{10... | collective-permute-start | bytes 196616 | tf_op jit(solution)/shard_map/ppermute | solution.py:74
  21.0 9.1 %collective-permute-start.7 = (bf16[64,1024]{1,0:T(8,128)(2,1)S(1)}, bf16[64,1024]{1,0:T(8,128)(2,1)S(1)}, u32[]{:S(2)}, u32[]{:S(2)}) collective-permute-start(bf16[64,1024]{1,0:T(8,128)(2,1)S(1)} %get-tuple-element.63.refs_0_), channel_id=1, source_target_pairs={{0,8},{8,0},{16,24},{24,16},{1,9},{9,1},{17,25},{25,17},{2,10},{10... | collective-permute-start | bytes 393224 | tf_op jit(solution)/shard_map/ppermute | solution.py:74
  21.0 9.1 %collective-permute-start.8 = (bf16[64,1024]{1,0:T(8,128)(2,1)S(1)}, bf16[64,1024]{1,0:T(8,128)(2,1)S(1)}, u32[]{:S(2)}, u32[]{:S(2)}) collective-permute-start(bf16[64,1024]{1,0:T(8,128)(2,1)S(1)} %get-tuple-element.64.refs_1_), channel_id=1, source_target_pairs={{0,32},{32,0},{64,96},{96,64},{1,33},{33,1},{65,97},{97,65},{2,34}... | collective-permute-start | bytes 393224 | tf_op jit(solution)/shard_map/ppermute | solution.py:74
  21.1 9.0 %collective-permute-start.9 = (bf16[64,1024]{1,0:T(8,128)(2,1)S(1)}, bf16[64,1024]{1,0:T(8,128)(2,1)S(1)}, u32[]{:S(2)}, u32[]{:S(2)}) collective-permute-start(bf16[64,1024]{1,0:T(8,128)(2,1)S(1)} %get-tuple-element.65.refs_2_), channel_id=1, source_target_pairs={{0,6},{2,4},{4,2},{6,0},{1,7},{3,5},{5,3},{7,1},{8,14},{10,12},{12... | collective-permute-start | bytes 393224 | tf_op jit(solution)/shard_map/ppermute | solution.py:74
  31.5 10.0 %collective-permute-start.13 = (bf16[128,1024]{1,0:T(8,128)(2,1)S(1)}, bf16[128,1024]{1,0:T(8,128)(2,1)S(1)}, u32[]{:S(2)}, u32[]{:S(2)}) collective-permute-start(bf16[128,1024]{1,0:T(8,128)(2,1)S(1)} %get-tuple-element.69.refs_0_), channel_id=1, source_target_pairs={{0,32},{32,0},{64,96},{96,64},{1,33},{33,1},{65,97},{97,65},{2,34}... | collective-permute-start | bytes 786440 | tf_op jit(solution)/shard_map/ppermute | solution.py:74
  31.6 10.0 %collective-permute-start.14 = (bf16[128,1024]{1,0:T(8,128)(2,1)S(1)}, bf16[128,1024]{1,0:T(8,128)(2,1)S(1)}, u32[]{:S(2)}, u32[]{:S(2)}) collective-permute-start(bf16[128,1024]{1,0:T(8,128)(2,1)S(1)} %get-tuple-element.70.refs_1_), channel_id=1, source_target_pairs={{0,6},{2,4},{4,2},{6,0},{1,7},{3,5},{5,3},{7,1},{8,14},{10,12},{12... | collective-permute-start | bytes 786440 | tf_op jit(solution)/shard_map/ppermute | solution.py:74
  32.4 9.1 %collective-permute-start.15 = (bf16[128,1024]{1,0:T(8,128)(2,1)S(1)}, bf16[128,1024]{1,0:T(8,128)(2,1)S(1)}, u32[]{:S(2)}, u32[]{:S(2)}) collective-permute-start(bf16[128,1024]{1,0:T(8,128)(2,1)S(1)} %get-tuple-element.71.refs_2_), channel_id=1, source_target_pairs={{0,24},{8,16},{16,8},{24,0},{1,25},{9,17},{17,9},{25,1},{2,26},{10... | collective-permute-start | bytes 786440 | tf_op jit(solution)/shard_map/ppermute | solution.py:74
  41.7 9.4 %collective-permute-start.22 = (bf16[256,896]{1,0:T(8,128)(2,1)S(1)}, bf16[256,896]{1,0:T(8,128)(2,1)S(1)}, u32[]{:S(2)}, u32[]{:S(2)}) collective-permute-start(bf16[256,896]{1,0:T(8,128)(2,1)S(1)} %get-tuple-element.78.refs_3_), channel_id=1, source_target_pairs={{0,2},{2,0},{4,6},{6,4},{1,3},{3,1},{5,7},{7,5},{8,10},{10,8},{12,... | collective-permute-start | bytes 1376264 | tf_op jit(solution)/shard_map/ppermute | solution.py:74
  42.3 16.5 %collective-permute-start.19 = (bf16[256,1024]{1,0:T(8,128)(2,1)S(1)}, bf16[256,1024]{1,0:T(8,128)(2,1)S(1)}, u32[]{:S(2)}, u32[]{:S(2)}) collective-permute-start(bf16[256,1024]{1,0:T(8,128)(2,1)S(1)} %get-tuple-element.75.refs_0_), channel_id=1, source_target_pairs={{0,6},{2,4},{4,2},{6,0},{1,7},{3,5},{5,3},{7,1},{8,14},{10,12},{12... | collective-permute-start | bytes 1572872 | tf_op jit(solution)/shard_map/ppermute | solution.py:74
  42.9 16.0 %collective-permute-start.20 = (bf16[256,1024]{1,0:T(8,128)(2,1)S(1)}, bf16[256,1024]{1,0:T(8,128)(2,1)S(1)}, u32[]{:S(2)}, u32[]{:S(2)}) collective-permute-start(bf16[256,1024]{1,0:T(8,128)(2,1)S(1)} %get-tuple-element.76.refs_1_), channel_id=1, source_target_pairs={{0,24},{8,16},{16,8},{24,0},{1,25},{9,17},{17,9},{25,1},{2,26},{10... | collective-permute-start | bytes 1572872 | tf_op jit(solution)/shard_map/ppermute | solution.py:74
  44.5 14.3 %collective-permute-start.21 = (bf16[256,1024]{1,0:T(8,128)(2,1)S(1)}, bf16[256,1024]{1,0:T(8,128)(2,1)S(1)}, u32[]{:S(2)}, u32[]{:S(2)}) collective-permute-start(bf16[256,1024]{1,0:T(8,128)(2,1)S(1)} %get-tuple-element.77.refs_2_), channel_id=1, source_target_pairs={{0,96},{32,64},{64,32},{96,0},{1,97},{33,65},{65,33},{97,1},{2,98}... | collective-permute-start | bytes 1572872 | tf_op jit(solution)/shard_map/ppermute | solution.py:74
  59.2 13.0 %collective-permute-start.28 = (bf16[512,896]{1,0:T(8,128)(2,1)S(1)}, bf16[512,896]{1,0:T(8,128)(2,1)S(1)}, u32[]{:S(2)}, u32[]{:S(2)}) collective-permute-start(bf16[512,896]{1,0:T(8,128)(2,1)S(1)} %get-tuple-element.84.refs_3_), channel_id=1, source_target_pairs={{0,8},{8,0},{16,24},{24,16},{1,9},{9,1},{17,25},{25,17},{2,10},{10... | collective-permute-start | bytes 2752520 | tf_op jit(solution)/shard_map/ppermute | solution.py:74
  59.4 17.9 %collective-permute-start.29 = (bf16[512,896]{1,0:T(8,128)(2,1)S(1)}, bf16[512,896]{1,0:T(8,128)(2,1)S(1)}, u32[]{:S(2)}, u32[]{:S(2)}) collective-permute-start(bf16[512,896]{1,0:T(8,128)(2,1)S(1)} %get-tuple-element.85.refs_4_), channel_id=1, source_target_pairs={{0,32},{32,0},{64,96},{96,64},{1,33},{33,1},{65,97},{97,65},{2,34}... | collective-permute-start | bytes 2752520 | tf_op jit(solution)/shard_map/ppermute | solution.py:74
  60.8 25.5 %collective-permute-start.25 = (bf16[512,1024]{1,0:T(8,128)(2,1)S(1)}, bf16[512,1024]{1,0:T(8,128)(2,1)S(1)}, u32[]{:S(2)}, u32[]{:S(2)}) collective-permute-start(bf16[512,1024]{1,0:T(8,128)(2,1)S(1)} %get-tuple-element.81.refs_0_), channel_id=1, source_target_pairs={{0,24},{8,16},{16,8},{24,0},{1,25},{9,17},{17,9},{25,1},{2,26},{10... | collective-permute-start | bytes 3145736 | tf_op jit(solution)/shard_map/ppermute | solution.py:74
  61.1 25.3 %collective-permute-start.26 = (bf16[512,1024]{1,0:T(8,128)(2,1)S(1)}, bf16[512,1024]{1,0:T(8,128)(2,1)S(1)}, u32[]{:S(2)}, u32[]{:S(2)}) collective-permute-start(bf16[512,1024]{1,0:T(8,128)(2,1)S(1)} %get-tuple-element.82.refs_1_), channel_id=1, source_target_pairs={{0,96},{32,64},{64,32},{96,0},{1,97},{33,65},{65,33},{97,1},{2,98}... | collective-permute-start | bytes 3145736 | tf_op jit(solution)/shard_map/ppermute | solution.py:74
  62.8 23.6 %collective-permute-start.27 = (bf16[512,1024]{1,0:T(8,128)(2,1)S(1)}, bf16[512,1024]{1,0:T(8,128)(2,1)S(1)}, u32[]{:S(2)}, u32[]{:S(2)}) collective-permute-start(bf16[512,1024]{1,0:T(8,128)(2,1)S(1)} %get-tuple-element.83.refs_2_), channel_id=1, source_target_pairs={{0,2},{2,0},{4,6},{6,4},{1,3},{3,1},{5,7},{7,5},{8,10},{10,8},{12,... | collective-permute-start | bytes 3145736 | tf_op jit(solution)/shard_map/ppermute | solution.py:74
  72.2 14.2 %collective-permute-start.30 = (bf16[512,896]{1,0:T(8,128)(2,1)S(1)}, bf16[512,896]{1,0:T(8,128)(2,1)S(1)}, u32[]{:S(2)}, u32[]{:S(2)}) collective-permute-start(bf16[512,896]{1,0:T(8,128)(2,1)S(1)} %get-tuple-element.86.refs_5_), channel_id=1, source_target_pairs={{0,6},{2,4},{4,2},{6,0},{1,7},{3,5},{5,3},{7,1},{8,14},{10,12},{12... | collective-permute-start | bytes 2752520 | tf_op jit(solution)/shard_map/ppermute | solution.py:74
  77.3 15.2 %collective-permute-start = (bf16[640,1024]{1,0:T(8,128)(2,1)S(1)}, bf16[640,1024]{1,0:T(8,128)(2,1)S(1)}, u32[]{:S(2)}, u32[]{:S(2)}) collective-permute-start(bf16[640,1024]{1,0:T(8,128)(2,1)S(1)} %copy-done.17), channel_id=1, source_target_pairs={{0,1},{1,0},{2,3},{3,2},{4,5},{5,4},{6,7},{7,6},{8,9},{9,8},{10,11... | collective-permute-start | bytes 3932168 | tf_op jit(solution)/shard_map/ppermute | solution.py:28
  88.2 11.5 %collective-permute-start.40 = (bf16[1024,384]{1,0:T(8,128)(2,1)S(1)}, bf16[1024,384]{1,0:T(8,128)(2,1)S(1)}, u32[]{:S(2)}, u32[]{:S(2)}) collective-permute-start(bf16[1024,384]{1,0:T(8,128)(2,1)S(1)} %get-tuple-element.97.rest_6_), channel_id=1, source_target_pairs={{0,32},{32,0},{64,96},{96,64},{1,33},{33,1},{65,97},{97,65},{2,34}... | collective-permute-start | bytes 2359304 | tf_op jit(solution)/shard_map/ppermute | solution.py:74
  90.5 16.7 %collective-permute-start.35 = (bf16[1024,384]{1,0:T(8,128)(2,1)S(1)}, bf16[1024,384]{1,0:T(8,128)(2,1)S(1)}, u32[]{:S(2)}, u32[]{:S(2)}) collective-permute-start(bf16[1024,384]{1,0:T(8,128)(2,1)S(1)} %get-tuple-element.91.rest_8_), channel_id=1, source_target_pairs={{0,6},{2,4},{4,2},{6,0},{1,7},{3,5},{5,3},{7,1},{8,14},{10,12},{12... | collective-permute-start | bytes 2359304 | tf_op jit(solution)/shard_map/ppermute | solution.py:74
  92.2 28.1 %collective-permute-start.31 = (bf16[1024,512]{1,0:T(8,128)(2,1)S(1)}, bf16[1024,512]{1,0:T(8,128)(2,1)S(1)}, u32[]{:S(2)}, u32[]{:S(2)}) collective-permute-start(bf16[1024,512]{1,0:T(8,128)(2,1)S(1)} %get-tuple-element.87.rest_0_), channel_id=1, source_target_pairs={{0,96},{32,64},{64,32},{96,0},{1,97},{33,65},{65,33},{97,1},{2,98}... | collective-permute-start | bytes 3145736 | tf_op jit(solution)/shard_map/ppermute | solution.py:74
  92.2 29.2 %collective-permute-start.32 = (bf16[1024,512]{1,0:T(8,128)(2,1)S(1)}, bf16[1024,512]{1,0:T(8,128)(2,1)S(1)}, u32[]{:S(2)}, u32[]{:S(2)}) collective-permute-start(bf16[1024,512]{1,0:T(8,128)(2,1)S(1)} %get-tuple-element.88.rest_2_), channel_id=1, source_target_pairs={{0,2},{2,0},{4,6},{6,4},{1,3},{3,1},{5,7},{7,5},{8,10},{10,8},{12,... | collective-permute-start | bytes 3145736 | tf_op jit(solution)/shard_map/ppermute | solution.py:74
  92.5 29.0 %collective-permute-start.33 = (bf16[1024,512]{1,0:T(8,128)(2,1)S(1)}, bf16[1024,512]{1,0:T(8,128)(2,1)S(1)}, u32[]{:S(2)}, u32[]{:S(2)}) collective-permute-start(bf16[1024,512]{1,0:T(8,128)(2,1)S(1)} %get-tuple-element.89.rest_4_), channel_id=1, source_target_pairs={{0,8},{8,0},{16,24},{24,16},{1,9},{9,1},{17,25},{25,17},{2,10},{10... | collective-permute-start | bytes 3145736 | tf_op jit(solution)/shard_map/ppermute | solution.py:74
  99.7 22.3 %collective-permute-start.34 = (bf16[1024,512]{1,0:T(8,128)(2,1)S(1)}, bf16[1024,512]{1,0:T(8,128)(2,1)S(1)}, u32[]{:S(2)}, u32[]{:S(2)}) collective-permute-start(bf16[1024,512]{1,0:T(8,128)(2,1)S(1)} %get-tuple-element.90.rest_6_), channel_id=1, source_target_pairs={{0,32},{32,0},{64,96},{96,64},{1,33},{33,1},{65,97},{97,65},{2,34}... | collective-permute-start | bytes 3145736 | tf_op jit(solution)/shard_map/ppermute | solution.py:74
  107.1 12.3 %collective-permute-start.36 = (bf16[1024,384]{1,0:T(8,128)(2,1)S(1)}, bf16[1024,384]{1,0:T(8,128)(2,1)S(1)}, u32[]{:S(2)}, u32[]{:S(2)}) collective-permute-start(bf16[1024,384]{1,0:T(8,128)(2,1)S(1)} %get-tuple-element.92.rest_10_), channel_id=1, source_target_pairs={{0,24},{8,16},{16,8},{24,0},{1,25},{9,17},{17,9},{25,1},{2,26},{10... | collective-permute-start | bytes 2359304 | tf_op jit(solution)/shard_map/ppermute | solution.py:74
  119.5 20.9 %collective-permute-start.37 = (bf16[1024,512]{1,0:T(8,128)(2,1)S(1)}, bf16[1024,512]{1,0:T(8,128)(2,1)}, u32[]{:S(2)}, u32[]{:S(2)}) collective-permute-start(bf16[1024,512]{1,0:T(8,128)(2,1)S(1)} %get-tuple-element.94.rest_0_), channel_id=1, source_target_pairs={{0,96},{32,64},{64,32},{96,0},{1,97},{33,65},{65,33},{97,1},{2,98}... | collective-permute-start | bytes 3145736 | tf_op jit(solution)/shard_map/ppermute | solution.py:74
  120.3 20.1 %collective-permute-start.38 = (bf16[1024,512]{1,0:T(8,128)(2,1)S(1)}, bf16[1024,512]{1,0:T(8,128)(2,1)}, u32[]{:S(2)}, u32[]{:S(2)}) collective-permute-start(bf16[1024,512]{1,0:T(8,128)(2,1)S(1)} %get-tuple-element.95.rest_2_), channel_id=1, source_target_pairs={{0,2},{2,0},{4,6},{6,4},{1,3},{3,1},{5,7},{7,5},{8,10},{10,8},{12,... | collective-permute-start | bytes 3145736 | tf_op jit(solution)/shard_map/ppermute | solution.py:74
  121.4 19.0 %collective-permute-start.39 = (bf16[1024,512]{1,0:T(8,128)(2,1)S(1)}, bf16[1024,512]{1,0:T(8,128)(2,1)}, u32[]{:S(2)}, u32[]{:S(2)}) collective-permute-start(bf16[1024,512]{1,0:T(8,128)(2,1)S(1)} %get-tuple-element.96.rest_4_), channel_id=1, source_target_pairs={{0,8},{8,0},{16,24},{24,16},{1,9},{9,1},{17,25},{25,17},{2,10},{10... | collective-permute-start | bytes 3145736 | tf_op jit(solution)/shard_map/ppermute | solution.py:74
  121.6 18.9 %collective-permute-start.41 = (bf16[1024,512]{1,0:T(8,128)(2,1)}, bf16[1024,512]{1,0:T(8,128)(2,1)}, u32[]{:S(2)}, u32[]{:S(2)}) collective-permute-start(bf16[1024,512]{1,0:T(8,128)(2,1)} %get-tuple-element.98.rest_8_), channel_id=1, source_target_pairs={{0,6},{2,4},{4,2},{6,0},{1,7},{3,5},{5,3},{7,1},{8,14},{10,12},{12... | collective-permute-start | bytes 3145736 | tf_op jit(solution)/shard_map/ppermute | solution.py:74
  123.1 23.6 %collective-permute-start.42 = (bf16[1024,512]{1,0:T(8,128)(2,1)}, bf16[1024,512]{1,0:T(8,128)(2,1)}, u32[]{:S(2)}, u32[]{:S(2)}) collective-permute-start(bf16[1024,512]{1,0:T(8,128)(2,1)} %get-tuple-element.99.rest_10_), channel_id=1, source_target_pairs={{0,24},{8,16},{16,8},{24,0},{1,25},{9,17},{17,9},{25,1},{2,26},{10... | collective-permute-start | bytes 3145736 | tf_op jit(solution)/shard_map/ppermute | solution.py:74
  160.6 27.0 %collective-permute-start.43 = (bf16[640,2048]{1,0:T(8,128)(2,1)}, bf16[640,2048]{1,0:T(8,128)(2,1)S(1)}, u32[]{:S(2)}, u32[]{:S(2)}) collective-permute-start(bf16[640,2048]{1,0:T(8,128)(2,1)} %get-tuple-element.100.term), channel_id=1, source_target_pairs={{0,1},{1,0},{2,3},{3,2},{4,5},{5,4},{6,7},{7,6},{8,9},{9,8},{10,11... | collective-permute-start | bytes 7864328 | tf_op jit(solution)/shard_map/ppermute | solution.py:28
  (44 other events, 491.2 us)
where the time goes:
time: 246 us; the launch traced here: 245 us
  waiting for transfers between devices  78.4 us (32%)
  starting transfers between devices  76.8 us (31%)
  Pallas kernels  75.4 us (31%)
  local copies, waits for them, and re-layouts  10.5 us (4%)
  other arithmetic  3.65 us (1%)
    ppermute x42, waiting for transfers between devices, exchange(): return lax.ppermute(x, axis, [(i, i ^ flip) for i in range(4)])  65.3 us
    ppermute x42, starting transfers between devices, exchange(): return lax.ppermute(x, axis, [(i, i ^ flip) for i in range(4)])  44.3 us
    ppermute x5, starting transfers between devices, other_core(): return lax.ppermute(x, 'tp', [(0, 1), (1, 0)])  32.5 us
    pallas_call x1, Pallas kernels, second_pass(): pl.pallas_call(second_kernel, out_shape=[jax.ShapeDtypeStruct((count, hal...  20.7 us
    pallas_call x1, Pallas kernels, first_hidden(): pl.pallas_call(first_kernel, out_shape=[jax.ShapeDtypeStruct((count, unit...  16.5 us
    pallas_call x1, Pallas kernels, first_down(): pl.pallas_call(down_kernel, out_shape=[jax.ShapeDtypeStruct((count, width...  13.9 us
    ppermute x5, waiting for transfers between devices, other_core(): return lax.ppermute(x, 'tp', [(0, 1), (1, 0)])  13.1 us
    pallas_call x1, Pallas kernels, gates(): pl.pallas_call(gates_kernel, out_shape=[jax.ShapeDtypeStruct((count, widt...  11.9 us
  transfers between devices with their start and end apart: 47, of which 20 were waited for; matrix products, arithmetic and copies ran while one was open for 0% of the time, Pallas kernels for 8%

commit v1 on v0

--- a/solution.py
+++ b/solution.py
@@ -20,6 +20,14 @@
 OTHERS = (4, 4, 4, 3, 4, 4)
 RINGS = (("fs_2", 1), ("fs_1", 1), ("z", 1), ("fs_2", 3), ("fs_1", 3), ("z", 3))
 PLACES = (2, 8, 32, 6, 24, 33)
+ROUNDS = (
+    (0, 4, 5, 3, 2, 1),
+    (0, 4, 3, 5, 1, 2),
+    (1, 5, 4, 2, 3, 0),
+    (1, 5, 2, 4, 0, 3),
+    (2, 3, 1, 0, 5, 4),
+    (2, 3, 0, 1, 4, 5),
+)
 
 EPS = 1e-06
 
@@ -69,7 +77,7 @@
 
 
 def exchange(x, color, turn):
-    name, flip = RINGS[(color + turn) % 6]
+    name, flip = RINGS[ROUNDS[color][turn]]
     axis = ("rep", "fs_0") if name == "z" else name
     return lax.ppermute(x, axis, [(i, i ^ flip) for i in range(4)])
 
@@ -78,7 +86,7 @@
     at = 0
     for turn in range(6):
         if slot >> turn & 1:
-            at ^= PLACES[(color + turn) % 6]
+            at ^= PLACES[ROUNDS[color][turn]]
     return at
 
 
@@ -93,9 +101,16 @@
 PAIRS += [(0, 8), (0, 9), (1, 8), (1, 9), (0, 10), (1, 10)]
 
 
-def prepare_kernel(
-    rep, gate, up, down, u, v, out, gate_s, up_s, down_s, u_s, v_s, out_s, *colors
-):
+def prepare_kernel(rep, *refs):
+    inputs, colors, held, sems = refs[:12], refs[12:15], refs[15:27], refs[27]
+    copies = [
+        pltpu.make_async_copy(x, y, sems.at[k]) for k, (x, y) in enumerate(zip(inputs, held))
+    ]
+    for copy in copies:
+        copy.start()
+    for copy in copies:
+        copy.wait()
+    gate, up, down, u, v, out, gate_s, up_s, down_s, u_s, v_s, out_s = held
     rows = pl.ds(pl.multiple_of(rep[0] * HALF_ROWS, HALF_ROWS), HALF_ROWS)
     low = jnp.bfloat16
 
@@ -120,71 +135,79 @@
         axis=1,
     )
     at, begin = 0, starts(OTHERS)
-    for c, ref in enumerate(colors):
-        mine = firsts[at : at + FIRST[c]] + [rest[:, begin[c] : begin[c + 1]]]
-        ref[...] = jnp.concatenate(mine, axis=1)
+    mine = []
+    for c in range(6):
+        mine.append(firsts[at : at + FIRST[c]] + [rest[:, begin[c] : begin[c + 1]]])
         at += FIRST[c]
+    for pair, ref in enumerate(colors):
+        ref[...] = jnp.concatenate(mine[2 * pair] + mine[2 * pair + 1], axis=1)
+
+
+WIDTHS = [(a + b) * LANES for a, b in zip(FIRST, OTHERS)]
+VMEM = pl.BlockSpec(memory_space=pltpu.VMEM)
+SMEM = pl.BlockSpec(memory_space=pltpu.SMEM)
+HBM = pl.BlockSpec(memory_space=pltpu.HBM)
 
 
 def prepare(rep, *arrays):
+    pairs = [WIDTHS[k] + WIDTHS[k + 1] for k in (0, 2, 4)]
     return pl.pallas_call(
         prepare_kernel,
-        out_shape=[
-            jax.ShapeDtypeStruct((HALF_ROWS, (a + b) * LANES), jnp.bfloat16)
-            for a, b in zip(FIRST, OTHERS)
-        ],
-        grid_spec=pltpu.PrefetchScalarGridSpec(
-            num_scalar_prefetch=1,
-            grid=(1,),
-            in_specs=[whole(a.shape) for a in arrays],
-            out_specs=[whole((HALF_ROWS, (a + b) * LANES)) for a, b in zip(FIRST, OTHERS)],
-        ),
-        compiler_params=params(1),
+        out_shape=[jax.ShapeDtypeStruct((HALF_ROWS, n), jnp.bfloat16) for n in pairs],
+        in_specs=[SMEM] + [HBM] * len(arrays),
+        out_specs=[VMEM] * 3,
+        scratch_shapes=[pltpu.VMEM(x.shape, x.dtype) for x in arrays]
+        + [pltpu.SemaphoreType.DMA((len(arrays),))],
+        compiler_params=pltpu.CompilerParams(vmem_limit_bytes=16 * 1024 * 1024),
         name="prepare",
     )(rep, *arrays)
 
 
-VMEM = pl.BlockSpec(memory_space=pltpu.VMEM)
-
-
 def join_kernel(cuts, *refs):
-    held, arrived, joined = refs[:6], refs[6:12], refs[12:]
-    for c in range(6):
-        begin, end = cuts[c]
-        rows = held[c].shape[0]
-        joined[c][pl.ds(0, rows), :] = held[c][:, begin:end]
-        joined[c][pl.ds(rows, rows), :] = arrived[c][:, begin:end]
+    sources = (len(refs) - len(cuts)) // 2
+    for joined, (source, begin, end) in zip(refs[2 * sources :], cuts):
+        held, arrived = refs[source], refs[sources + source]
+        rows = held.shape[0]
+        joined[pl.ds(0, rows), :] = held[:, begin:end]
+        joined[pl.ds(rows, rows), :] = arrived[:, begin:end]
 
 
 def join(held, arrived, cuts=None):
     rows, low = held[0].shape[0], jnp.bfloat16
     if cuts is None:
-        cuts = [(0, x.shape[1]) for x in held]
+        cuts = [(k, 0, x.shape[1]) for k, x in enumerate(held)]
     return pl.pallas_call(
         functools.partial(join_kernel, cuts),
-        out_shape=[jax.ShapeDtypeStruct((2 * rows, b - a), low) for a, b in cuts],
-        in_specs=[VMEM] * 12,
-        out_specs=[VMEM] * 6,
-        compiler_params=pltpu.CompilerParams(vmem_limit_bytes=32 * 1024 * 1024),
+        out_shape=[jax.ShapeDtypeStruct((2 * rows, b - a), low) for _, a, b in cuts],
+        in_specs=[VMEM] * (2 * len(held)),
+        out_specs=[VMEM] * len(cuts),
+        compiler_params=pltpu.CompilerParams(vmem_limit_bytes=16 * 1024 * 1024),
         name="join",
     )(*held, *arrived)
 
 
-def gather(colors):
-    held = list(colors)
-    for turn in range(5):
-        arrived = [exchange(x, c, turn) for c, x in enumerate(held)]
-        if turn < 4:
-            held = join(held, arrived)
+def gather(pairs):
+    ready = []
+    for p, x in enumerate(pairs):
+        (held,) = join([x], [exchange(x, 2 * p, 0)])
+        edge = WIDTHS[2 * p]
+        cuts = [(0, 0, edge), (0, edge, held.shape[1])]
+        held = join([held], [exchange(held, 2 * p, 1)], cuts)
+        for turn in (2, 3):
+            held = join(held, [exchange(y, 2 * p + k, turn) for k, y in enumerate(held)])
+        ready.append((held, [exchange(y, 2 * p + k, 4) for k, y in enumerate(held)]))
     groups = []
     for g in range(2):
-        edge = [n * LANES for n in FIRST]
-        cuts = [(e, x.shape[1]) if g else (0, e) for e, x in zip(edge, held)]
-        group = join(held, arrived, cuts)
-        last = []
-        for c, x in enumerate(group):
-            last.append(exchange(x, c, 5))
-        groups.append([piece[c] for c in range(6) for piece in (group, last)])
+        pieces = []
+        for p, (held, arrived) in enumerate(ready):
+            cuts = []
+            for k, y in enumerate(held):
+                edge = FIRST[2 * p + k] * LANES
+                cuts.append((k, edge, y.shape[1]) if g else (k, 0, edge))
+            halves = join(held, arrived, cuts)
+            for k, y in enumerate(halves):
+                pieces += [y, exchange(y, 2 * p + k, 5)]
+        groups.append(pieces)
     return groups
 
 

time: 246 us -> 252 us (1.024)
  waiting for transfers between devices: 78.4 us -> 91.7 us
  starting transfers between devices: 76.8 us -> 65 us
  local copies, waits for them, and re-layouts: 10.5 us -> 16.3 us
    ppermute x5, starting transfers between devices: 32.5 us -> 15 us  [other_core(): return lax.ppermute(x, 'tp', [(0, 1), (1, 0)])]
    ppermute x42 -> x36, waiting for transfers between devices: 65.3 us -> 78.6 us  [exchange(): return lax.ppermute(x, axis, [(i, i ^ flip) for i in range(4)])]
    unnamed x59 -> x71, local copies, waits for them, and re-layouts: 10.5 us -> 16.3 us
    ppermute x42 -> x36, starting transfers between devices: 44.3 us -> 50 us  [exchange(): return lax.ppermute(x, axis, [(i, i ^ flip) for i in range(4)])]
  transfers between devices with their start and end apart: 47 -> 41, of which waited for: 20 -> 15; matrix products, arithmetic and copies ran while one was open for 0% -> 0% of each run, Pallas kernels for 8% -> 8%
where the time goes in v1:
time: 252 us
  waiting for transfers between devices  91.7 us (36%)
  Pallas kernels  74.5 us (30%)
  starting transfers between devices  65 us (26%)
  local copies, waits for them, and re-layouts  16.3 us (6%)
  other arithmetic  3.65 us (1%)
    ppermute x36, waiting for transfers between devices, exchange(): return lax.ppermute(x, axis, [(i, i ^ flip) for i in range(4)])  78.6 us
    ppermute x36, starting transfers between devices, exchange(): return lax.ppermute(x, axis, [(i, i ^ flip) for i in range(4)])  50 us
    pallas_call x1, Pallas kernels, second_pass(): pl.pallas_call(second_kernel, out_shape=[jax.ShapeDtypeStruct((count, hal...  20.7 us
    pallas_call x1, Pallas kernels, first_hidden(): pl.pallas_call(first_kernel, out_shape=[jax.ShapeDtypeStruct((count, unit...  16.5 us
    unnamed x71, local copies, waits for them, and re-layouts  16.3 us
    ppermute x5, starting transfers between devices, other_core(): return lax.ppermute(x, 'tp', [(0, 1), (1, 0)])  15 us
    pallas_call x1, Pallas kernels, first_down(): pl.pallas_call(down_kernel, out_shape=[jax.ShapeDtypeStruct((count, width...  13.9 us
    ppermute x5, waiting for transfers between devices, other_core(): return lax.ppermute(x, 'tp', [(0, 1), (1, 0)])  13.1 us
  transfers between devices with their start and end apart: 41, of which 15 were waited for; matrix products, arithmetic and copies ran while one was open for 0% of the time, Pallas kernels for 8%

profile of v1, /device:TPU:1, one launch (start us, length us, event | category | flops | bytes accessed | tf_op | source)
XLA Modules:
  0.0 251.6 jit_solution(7092214556150663076)
XLA Ops:
  10.9 2.5 %collective-permute-start.21 = (bf16[32,1792]{1,0:T(8,128)(2,1)S(1)}, bf16[32,1792]{1,0:T(8,128)(2,1)S(1)}, u32[]{:S(2)}, u32[]{:S(2)}) collective-permute-start(bf16[32,1792]{1,0:T(8,128)(2,1)S(1)} %get-tuple-element.66.refs_0_), channel_id=1, source_target_pairs={{0,32},{32,0},{64,96},{96,64},{1,33},{33,1},{65,97},{97,65},{2,34}... | collective-permute-start | bytes 344072 | tf_op jit(solution)/shard_map/ppermute | solution.py:82
  14.8 1.6 collective-permute-done.21.refs_1_
  16.3 2.5 collective-permute-start.22
  18.8 3.5 %collective-permute-start.12 = (bf16[64,1920]{1,0:T(8,128)(2,1)S(1)}, bf16[64,1920]{1,0:T(8,128)(2,1)S(1)}, u32[]{:S(2)}, u32[]{:S(2)}) collective-permute-start(bf16[64,1920]{1,0:T(8,128)(2,1)S(1)} %join.23.refs_0_), channel_id=1, source_target_pairs={{0,96},{32,64},{64,32},{96,0},{1,97},{33,65},{65,33},{97,1},{2,98}... | collective-permute-start | bytes 737288 | tf_op jit(solution)/shard_map/ppermute | solution.py:82
  22.9 2.8 %collective-permute-start.2 = (bf16[64,2048]{1,0:T(8,128)(2,1)S(1)}, bf16[64,2048]{1,0:T(8,128)(2,1)S(1)}, u32[]{:S(2)}, u32[]{:S(2)}) collective-permute-start(bf16[64,2048]{1,0:T(8,128)(2,1)S(1)} %join.18.refs_0_), channel_id=1, source_target_pairs={{0,24},{8,16},{16,8},{24,0},{1,25},{9,17},{17,9},{25,1},{2,26},{10... | collective-permute-start | bytes 786440 | tf_op jit(solution)/shard_map/ppermute | solution.py:82
  27.4 2.2 collective-permute-start.13
  29.6 3.4 %collective-permute-start.3 = (bf16[128,1024]{1,0:T(8,128)(2,1)S(1)}, bf16[128,1024]{1,0:T(8,128)(2,1)S(1)}, u32[]{:S(2)}, u32[]{:S(2)}) collective-permute-start(bf16[128,1024]{1,0:T(8,128)(2,1)S(1)} %get-tuple-element.49.refs_0_), channel_id=1, source_target_pairs={{0,96},{32,64},{64,32},{96,0},{1,97},{33,65},{65,33},{97,1},{2,98}... | collective-permute-start | bytes 786440 | tf_op jit(solution)/shard_map/ppermute | solution.py:82
  35.8 3.4 %collective-permute-start.16 = (bf16[256,896]{1,0:T(8,128)(2,1)S(1)}, bf16[256,896]{1,0:T(8,128)(2,1)S(1)}, u32[]{:S(2)}, u32[]{:S(2)}) collective-permute-start(bf16[256,896]{1,0:T(8,128)(2,1)S(1)} %get-tuple-element.61.refs_1_), channel_id=1, source_target_pairs={{0,24},{8,16},{16,8},{24,0},{1,25},{9,17},{17,9},{25,1},{2,26},{10... | collective-permute-start | bytes 1376264 | tf_op jit(solution)/shard_map/ppermute | solution.py:82
  41.8 1.9 collective-permute-start.27
  43.7 1.9 collective-permute-start.28
  45.8 3.1 %collective-permute-start.6 = (bf16[256,1024]{1,0:T(8,128)(2,1)S(1)}, bf16[256,1024]{1,0:T(8,128)(2,1)S(1)}, u32[]{:S(2)}, u32[]{:S(2)}) collective-permute-start(bf16[256,1024]{1,0:T(8,128)(2,1)S(1)} %get-tuple-element.52.refs_1_), channel_id=1, source_target_pairs={{0,96},{32,64},{64,32},{96,0},{1,97},{33,65},{65,33},{97,1},{2,98}... | collective-permute-start | bytes 1572872 | tf_op jit(solution)/shard_map/ppermute | solution.py:82
  49.0 1.9 collective-permute-start.18
  51.0 2.1 collective-permute-done.5.refs_2_
  53.1 13.9 %collective-permute-done.6.refs_3_ = bf16[256,1024]{1,0:T(8,128)(2,1)S(1)} collective-permute-done((bf16[256,1024]{1,0:T(8,128)(2,1)S(1)}, bf16[256,1024]{1,0:T(8,128)(2,1)S(1)}, u32[]{:S(2)}, u32[]{:S(2)}) %collective-permute-start.6) | collective-permute-done | bytes 524320 | tf_op jit(solution)/shard_map/ppermute | solution.py:82
  66.9 10.1 %collective-permute-start = (bf16[640,1024]{1,0:T(8,128)(2,1)S(1)}, bf16[640,1024]{1,0:T(8,128)(2,1)S(1)}, u32[]{:S(2)}, u32[]{:S(2)}) collective-permute-start(bf16[640,1024]{1,0:T(8,128)(2,1)S(1)} %copy-done.23), channel_id=1, source_target_pairs={{0,1},{1,0},{2,3},{3,2},{4,5},{5,4},{6,7},{7,6},{8,9},{9,8},{10,11... | collective-permute-start | bytes 3932168 | tf_op jit(solution)/shard_map/ppermute | solution.py:36
  78.7 2.1 collective-permute-start.29
  82.3 19.7 %collective-permute-done.7.refs_2_ = bf16[512,1024]{1,0:T(8,128)(2,1)S(1)} collective-permute-done((bf16[512,1024]{1,0:T(8,128)(2,1)S(1)}, bf16[512,1024]{1,0:T(8,128)(2,1)S(1)}, u32[]{:S(2)}, u32[]{:S(2)}) %collective-permute-start.7) | collective-permute-done | bytes 1048608 | tf_op jit(solution)/shard_map/ppermute | solution.py:82
  108.7 1.6 join.33
  110.3 33.9 %collective-permute-done.34.rest_7_ = bf16[1024,384]{1,0:T(8,128)(2,1)S(1)} collective-permute-done((bf16[1024,384]{1,0:T(8,128)(2,1)S(1)}, bf16[1024,384]{1,0:T(8,128)(2,1)S(1)}, u32[]{:S(2)}, u32[]{:S(2)}) %collective-permute-start.34) | collective-permute-done | bytes 786464 | tf_op jit(solution)/shard_map/ppermute | solution.py:82
  144.2 2.8 %collective-permute-start.35 = (bf16[1024,512]{1,0:T(8,128)(2,1)S(1)}, bf16[1024,512]{1,0:T(8,128)(2,1)}, u32[]{:S(2)}, u32[]{:S(2)}) collective-permute-start(bf16[1024,512]{1,0:T(8,128)(2,1)S(1)} %get-tuple-element.80.rest_8_), channel_id=1, source_target_pairs={{0,24},{8,16},{16,8},{24,0},{1,25},{9,17},{17,9},{25,1},{2,26},{10... | collective-permute-start | bytes 3145736 | tf_op jit(solution)/shard_map/ppermute | solution.py:82
  149.7 16.5 %first_hidden.1 = (bf16[640,1408]{1,0:T(8,128)(2,1)}, bf16[2048,2816]{1,0:T(8,128)(2,1)}) custom-call(s32[1]{0:T(128)} %bitcast.core, s32[1]{0:T(128)} %bitcast.1.at, bf16[640,1024]{1,0:T(8,128)(2,1)} %own.3, bf16[640,1024]{1,0:T(8,128)(2,1)} %copy-done.24, f32[1,2048]{1,0:T(1,128)} %bitcast.17, bf16[1024,512]{1,0:T(8,128)(2,1)} %copy-done.18, ...), custom_call_target="tpu_custom_call" | custom-call | flops 7381975040 | bytes 23068672 | tf_op jit(solution)/shard_map/first_hidden/pallas_call | solution.py:302
  166.2 2.3 collective-permute-done.35.rest_9_
  168.4 2.3 collective-permute-done.36.rest_11_
  171.7 13.9 %first_down.1 = (bf16[640,2048]{1,0:T(8,128)(2,1)}, bf16[2048,2944]{1,0:T(8,128)(2,1)}) custom-call(s32[1]{0:T(128)} %bitcast.1.at, bf16[640,1408]{1,0:T(8,128)(2,1)} %get-tuple-element.75.hidden, bf16[1024,512]{1,0:T(8,128)(2,1)} %get-tuple-element.76.rest_0_, bf16[1024,512]{1,0:T(8,128)(2,1)} %collective-permute-done.31.rest_1_, ...), custom_call_target="tpu_custom_call" | custom-call | flops 3690987520 | bytes 24117248 | tf_op jit(solution)/shard_map/first_down/pallas_call | solution.py:355
  185.6 3.7 %collective-permute-start.37 = (bf16[640,2048]{1,0:T(8,128)(2,1)}, bf16[640,2048]{1,0:T(8,128)(2,1)S(1)}, u32[]{:S(2)}, u32[]{:S(2)}) collective-permute-start(bf16[640,2048]{1,0:T(8,128)(2,1)} %get-tuple-element.82.term), channel_id=1, source_target_pairs={{0,1},{1,0},{2,3},{3,2},{4,5},{5,4},{6,7},{7,6},{8,9},{9,8},{10,11... | collective-permute-start | bytes 7864328 | tf_op jit(solution)/shard_map/ppermute | solution.py:36
  189.3 4.7 %collective-permute-done.37.far = bf16[640,2048]{1,0:T(8,128)(2,1)S(1)} collective-permute-done((bf16[640,2048]{1,0:T(8,128)(2,1)}, bf16[640,2048]{1,0:T(8,128)(2,1)S(1)}, u32[]{:S(2)}, u32[]{:S(2)}) %collective-permute-start.37) | collective-permute-done | bytes 2621472 | tf_op jit(solution)/shard_map/ppermute | solution.py:36
  195.5 11.9 %gates.1 = (bf16[640,2048]{1,0:T(8,128)(2,1)}, f32[2,640,512]{2,1,0:T(8,128)}, f32[640,128]{1,0:T(8,128)}) custom-call(s32[1]{0:T(128)} %bitcast.core, bf16[640,1024]{1,0:T(8,128)(2,1)} %own.3, bf16[640,1024]{1,0:T(8,128)(2,1)} %copy-done.24, bf16[640,2048]{1,0:T(8,128)(2,1)} %get-tuple-element.82.term, bf16[640,2048]{1,0:T(8,128)(2,1)} %copy-done.22, ...), custom_call_target="tpu_custom_call" | custom-call | flops 2684354560 | bytes 4194304 | tf_op jit(solution)/shard_map/gates/pallas_call | solution.py:403
  210.0 7.3 %mix.1.term = bf16[640,2048]{1,0:T(8,128)(2,1)} custom-call(f32[2,640,512]{2,1,0:T(8,128)} %get-tuple-element.85.act, f32[640,128]{1,0:T(8,128)} %get-tuple-element.86.sums, f32[640,128]{1,0:T(8,128)} %copy-done.26, f32[1,512]{1,0:T(1,128)} %bitcast.15, f32[1,512]{1,0:T(1,128)} %bitcast.16, bf16[4,128,128]{2,1,0:T(8,128)(2,1)} %weight.1, f32[128,4]{1,0:T(8,128)} %bitcast.13, ...), custom_call_target="tpu_custom_call" | custom-call | flops 1342177280 | bytes 2097152 | tf_op jit(solution)/shard_map/mix/pallas_call | solution.py:467
  217.6 4.7 %collective-permute-done.39.far = bf16[640,2048]{1,0:T(8,128)(2,1)S(1)} collective-permute-done((bf16[640,2048]{1,0:T(8,128)(2,1)}, bf16[640,2048]{1,0:T(8,128)(2,1)S(1)}, u32[]{:S(2)}, u32[]{:S(2)}) %collective-permute-start.39) | collective-permute-done | bytes 2621472 | tf_op jit(solution)/shard_map/ppermute | solution.py:36
  223.9 20.7 %second_pass.1 = (bf16[640,1024]{1,0:T(8,128)(2,1)}, bf16[640,1024]{1,0:T(8,128)(2,1)}, bf16[640,1024]{1,0:T(8,128)(2,1)}) custom-call(s32[1]{0:T(128)} %bitcast.core, bf16[640,2048]{1,0:T(8,128)(2,1)} %get-tuple-element.84.middle, bf16[640,2048]{1,0:T(8,128)(2,1)} %mix.1.term, bf16[640,2048]{1,0:T(8,128)(2,1)} %copy-done.28, f32[1,2048]{1,0:T(1,128)} %bitcast.18, ...), custom_call_target="tpu_custom_call" | custom-call | flops 11072962560 | bytes 17301504 | tf_op jit(solution)/shard_map/second_pass/pallas_call | solution.py:549
  245.1 2.9 %collective-permute-done.40 = bf16[640,1024]{1,0:T(8,128)(2,1)S(1)} collective-permute-done((bf16[640,1024]{1,0:T(8,128)(2,1)}, bf16[640,1024]{1,0:T(8,128)(2,1)S(1)}, u32[]{:S(2)}, u32[]{:S(2)}) %collective-permute-start.40) | collective-permute-done | bytes 1310752 | tf_op jit(solution)/shard_map/ppermute | solution.py:36
  247.9 3.6 %add_convert_fusion = bf16[640,1024]{1,0:T(8,128)(2,1)} fusion(bf16[640,1024]{1,0:T(8,128)(2,1)S(1)} %collective-permute-done.40, bf16[640,1024]{1,0:T(8,128)(2,1)} %get-tuple-element.89, bf16[640,1024]{1,0:T(8,128)(2,1)} %get-tuple-element.88), kind=kLoop, calls=%fused_computation | loop fusion | flops 4587520 | bytes 5242880 | tf_op jit(solution)/shard_map/convert_element_type | solution.py:651
  (146 shorter events, 39.7 us)
Async XLA Ops:
  16.3 9.4 %collective-permute-start.22 = (bf16[64,1792]{1,0:T(8,128)(2,1)S(1)}, bf16[64,1792]{1,0:T(8,128)(2,1)S(1)}, u32[]{:S(2)}, u32[]{:S(2)}) collective-permute-start(bf16[64,1792]{1,0:T(8,128)(2,1)S(1)} %join.28.refs_0_), channel_id=1, source_target_pairs={{0,6},{2,4},{4,2},{6,0},{1,7},{3,5},{5,3},{7,1},{8,14},{10,12},{12... | collective-permute-start | bytes 688136 | tf_op jit(solution)/shard_map/ppermute | solution.py:82
  18.8 8.0 %collective-permute-start.12 = (bf16[64,1920]{1,0:T(8,128)(2,1)S(1)}, bf16[64,1920]{1,0:T(8,128)(2,1)S(1)}, u32[]{:S(2)}, u32[]{:S(2)}) collective-permute-start(bf16[64,1920]{1,0:T(8,128)(2,1)S(1)} %join.23.refs_0_), channel_id=1, source_target_pairs={{0,96},{32,64},{64,32},{96,0},{1,97},{33,65},{65,33},{97,1},{2,98}... | collective-permute-start | bytes 737288 | tf_op jit(solution)/shard_map/ppermute | solution.py:82
  25.8 7.2 %collective-permute-start.23 = (bf16[128,896]{1,0:T(8,128)(2,1)S(1)}, bf16[128,896]{1,0:T(8,128)(2,1)S(1)}, u32[]{:S(2)}, u32[]{:S(2)}) collective-permute-start(bf16[128,896]{1,0:T(8,128)(2,1)S(1)} %get-tuple-element.67.refs_0_), channel_id=1, source_target_pairs={{0,8},{8,0},{16,24},{24,16},{1,9},{9,1},{17,25},{25,17},{2,10},{10... | collective-permute-start | bytes 688136 | tf_op jit(solution)/shard_map/ppermute | solution.py:82
  25.9 7.2 %collective-permute-start.24 = (bf16[128,896]{1,0:T(8,128)(2,1)S(1)}, bf16[128,896]{1,0:T(8,128)(2,1)S(1)}, u32[]{:S(2)}, u32[]{:S(2)}) collective-permute-start(bf16[128,896]{1,0:T(8,128)(2,1)S(1)} %get-tuple-element.68.refs_1_), channel_id=1, source_target_pairs={{0,2},{2,0},{4,6},{6,4},{1,3},{3,1},{5,7},{7,5},{8,10},{10,8},{12,... | collective-permute-start | bytes 688136 | tf_op jit(solution)/shard_map/ppermute | solution.py:82
  27.4 8.4 %collective-permute-start.13 = (bf16[128,1024]{1,0:T(8,128)(2,1)S(1)}, bf16[128,1024]{1,0:T(8,128)(2,1)S(1)}, u32[]{:S(2)}, u32[]{:S(2)}) collective-permute-start(bf16[128,1024]{1,0:T(8,128)(2,1)S(1)} %get-tuple-element.58.refs_0_), channel_id=1, source_target_pairs={{0,24},{8,16},{16,8},{24,0},{1,25},{9,17},{17,9},{25,1},{2,26},{10... | collective-permute-start | bytes 786440 | tf_op jit(solution)/shard_map/ppermute | solution.py:82
  29.6 9.7 %collective-permute-start.3 = (bf16[128,1024]{1,0:T(8,128)(2,1)S(1)}, bf16[128,1024]{1,0:T(8,128)(2,1)S(1)}, u32[]{:S(2)}, u32[]{:S(2)}) collective-permute-start(bf16[128,1024]{1,0:T(8,128)(2,1)S(1)} %get-tuple-element.49.refs_0_), channel_id=1, source_target_pairs={{0,96},{32,64},{64,32},{96,0},{1,97},{33,65},{65,33},{97,1},{2,98}... | collective-permute-start | bytes 786440 | tf_op jit(solution)/shard_map/ppermute | solution.py:82
  33.1 8.5 %collective-permute-start.25 = (bf16[256,896]{1,0:T(8,128)(2,1)S(1)}, bf16[256,896]{1,0:T(8,128)(2,1)S(1)}, u32[]{:S(2)}, u32[]{:S(2)}) collective-permute-start(bf16[256,896]{1,0:T(8,128)(2,1)S(1)} %get-tuple-element.69.refs_0_), channel_id=1, source_target_pairs={{0,2},{2,0},{4,6},{6,4},{1,3},{3,1},{5,7},{7,5},{8,10},{10,8},{12,... | collective-permute-start | bytes 1376264 | tf_op jit(solution)/shard_map/ppermute | solution.py:82
  33.6 8.0 %collective-permute-start.26 = (bf16[256,896]{1,0:T(8,128)(2,1)S(1)}, bf16[256,896]{1,0:T(8,128)(2,1)S(1)}, u32[]{:S(2)}, u32[]{:S(2)}) collective-permute-start(bf16[256,896]{1,0:T(8,128)(2,1)S(1)} %get-tuple-element.70.refs_1_), channel_id=1, source_target_pairs={{0,8},{8,0},{16,24},{24,16},{1,9},{9,1},{17,25},{25,17},{2,10},{10... | collective-permute-start | bytes 1376264 | tf_op jit(solution)/shard_map/ppermute | solution.py:82
  35.8 10.0 %collective-permute-start.16 = (bf16[256,896]{1,0:T(8,128)(2,1)S(1)}, bf16[256,896]{1,0:T(8,128)(2,1)S(1)}, u32[]{:S(2)}, u32[]{:S(2)}) collective-permute-start(bf16[256,896]{1,0:T(8,128)(2,1)S(1)} %get-tuple-element.61.refs_1_), channel_id=1, source_target_pairs={{0,24},{8,16},{16,8},{24,0},{1,25},{9,17},{17,9},{25,1},{2,26},{10... | collective-permute-start | bytes 1376264 | tf_op jit(solution)/shard_map/ppermute | solution.py:82
  39.3 9.6 %collective-permute-start.15 = (bf16[256,1024]{1,0:T(8,128)(2,1)S(1)}, bf16[256,1024]{1,0:T(8,128)(2,1)S(1)}, u32[]{:S(2)}, u32[]{:S(2)}) collective-permute-start(bf16[256,1024]{1,0:T(8,128)(2,1)S(1)} %get-tuple-element.60.refs_0_), channel_id=1, source_target_pairs={{0,32},{32,0},{64,96},{96,64},{1,33},{33,1},{65,97},{97,65},{2,34}... | collective-permute-start | bytes 1572872 | tf_op jit(solution)/shard_map/ppermute | solution.py:82
  40.7 12.4 %collective-permute-start.5 = (bf16[256,1024]{1,0:T(8,128)(2,1)S(1)}, bf16[256,1024]{1,0:T(8,128)(2,1)S(1)}, u32[]{:S(2)}, u32[]{:S(2)}) collective-permute-start(bf16[256,1024]{1,0:T(8,128)(2,1)S(1)} %get-tuple-element.51.refs_0_), channel_id=1, source_target_pairs={{0,6},{2,4},{4,2},{6,0},{1,7},{3,5},{5,3},{7,1},{8,14},{10,12},{12... | collective-permute-start | bytes 1572872 | tf_op jit(solution)/shard_map/ppermute | solution.py:82
  41.8 35.4 %collective-permute-start.27 = (bf16[512,896]{1,0:T(8,128)(2,1)S(1)}, bf16[512,896]{1,0:T(8,128)(2,1)S(1)}, u32[]{:S(2)}, u32[]{:S(2)}) collective-permute-start(bf16[512,896]{1,0:T(8,128)(2,1)S(1)} %get-tuple-element.71.refs_0_), channel_id=1, source_target_pairs={{0,96},{32,64},{64,32},{96,0},{1,97},{33,65},{65,33},{97,1},{2,98}... | collective-permute-start | bytes 2752520 | tf_op jit(solution)/shard_map/ppermute | solution.py:82
  43.7 33.6 %collective-permute-start.28 = (bf16[512,896]{1,0:T(8,128)(2,1)S(1)}, bf16[512,896]{1,0:T(8,128)(2,1)S(1)}, u32[]{:S(2)}, u32[]{:S(2)}) collective-permute-start(bf16[512,896]{1,0:T(8,128)(2,1)S(1)} %get-tuple-element.72.refs_1_), channel_id=1, source_target_pairs={{0,24},{8,16},{16,8},{24,0},{1,25},{9,17},{17,9},{25,1},{2,26},{10... | collective-permute-start | bytes 2752520 | tf_op jit(solution)/shard_map/ppermute | solution.py:82
  45.8 21.1 %collective-permute-start.6 = (bf16[256,1024]{1,0:T(8,128)(2,1)S(1)}, bf16[256,1024]{1,0:T(8,128)(2,1)S(1)}, u32[]{:S(2)}, u32[]{:S(2)}) collective-permute-start(bf16[256,1024]{1,0:T(8,128)(2,1)S(1)} %get-tuple-element.52.refs_1_), channel_id=1, source_target_pairs={{0,96},{32,64},{64,32},{96,0},{1,97},{33,65},{65,33},{97,1},{2,98}... | collective-permute-start | bytes 1572872 | tf_op jit(solution)/shard_map/ppermute | solution.py:82
  49.0 29.6 %collective-permute-start.18 = (bf16[512,896]{1,0:T(8,128)(2,1)S(1)}, bf16[512,896]{1,0:T(8,128)(2,1)S(1)}, u32[]{:S(2)}, u32[]{:S(2)}) collective-permute-start(bf16[512,896]{1,0:T(8,128)(2,1)S(1)} %get-tuple-element.63.refs_1_), channel_id=1, source_target_pairs={{0,2},{2,0},{4,6},{6,4},{1,3},{3,1},{5,7},{7,5},{8,10},{10,8},{12,... | collective-permute-start | bytes 2752520 | tf_op jit(solution)/shard_map/ppermute | solution.py:82
  53.1 27.7 %collective-permute-start.17 = (bf16[512,1024]{1,0:T(8,128)(2,1)S(1)}, bf16[512,1024]{1,0:T(8,128)(2,1)S(1)}, u32[]{:S(2)}, u32[]{:S(2)}) collective-permute-start(bf16[512,1024]{1,0:T(8,128)(2,1)S(1)} %get-tuple-element.62.refs_0_), channel_id=1, source_target_pairs={{0,6},{2,4},{4,2},{6,0},{1,7},{3,5},{5,3},{7,1},{8,14},{10,12},{12... | collective-permute-start | bytes 3145736 | tf_op jit(solution)/shard_map/ppermute | solution.py:82
  66.9 37.2 %collective-permute-start = (bf16[640,1024]{1,0:T(8,128)(2,1)S(1)}, bf16[640,1024]{1,0:T(8,128)(2,1)S(1)}, u32[]{:S(2)}, u32[]{:S(2)}) collective-permute-start(bf16[640,1024]{1,0:T(8,128)(2,1)S(1)} %copy-done.23), channel_id=1, source_target_pairs={{0,1},{1,0},{2,3},{3,2},{4,5},{5,4},{6,7},{7,6},{8,9},{9,8},{10,11... | collective-permute-start | bytes 3932168 | tf_op jit(solution)/shard_map/ppermute | solution.py:36
  77.2 24.8 %collective-permute-start.7 = (bf16[512,1024]{1,0:T(8,128)(2,1)S(1)}, bf16[512,1024]{1,0:T(8,128)(2,1)S(1)}, u32[]{:S(2)}, u32[]{:S(2)}) collective-permute-start(bf16[512,1024]{1,0:T(8,128)(2,1)S(1)} %get-tuple-element.53.refs_0_), channel_id=1, source_target_pairs={{0,32},{32,0},{64,96},{96,64},{1,33},{33,1},{65,97},{97,65},{2,34}... | collective-permute-start | bytes 3145736 | tf_op jit(solution)/shard_map/ppermute | solution.py:82
  77.3 25.2 %collective-permute-start.8 = (bf16[512,1024]{1,0:T(8,128)(2,1)S(1)}, bf16[512,1024]{1,0:T(8,128)(2,1)S(1)}, u32[]{:S(2)}, u32[]{:S(2)}) collective-permute-start(bf16[512,1024]{1,0:T(8,128)(2,1)S(1)} %get-tuple-element.54.refs_1_), channel_id=1, source_target_pairs={{0,8},{8,0},{16,24},{24,16},{1,9},{9,1},{17,25},{25,17},{2,10},{10... | collective-permute-start | bytes 3145736 | tf_op jit(solution)/shard_map/ppermute | solution.py:82
  78.7 26.7 %collective-permute-start.29 = (bf16[1024,384]{1,0:T(8,128)(2,1)S(1)}, bf16[1024,384]{1,0:T(8,128)(2,1)S(1)}, u32[]{:S(2)}, u32[]{:S(2)}) collective-permute-start(bf16[1024,384]{1,0:T(8,128)(2,1)S(1)} %get-tuple-element.73.rest_8_), channel_id=1, source_target_pairs={{0,24},{8,16},{16,8},{24,0},{1,25},{9,17},{17,9},{25,1},{2,26},{10... | collective-permute-start | bytes 2359304 | tf_op jit(solution)/shard_map/ppermute | solution.py:82
  80.7 26.9 %collective-permute-start.30 = (bf16[1024,384]{1,0:T(8,128)(2,1)S(1)}, bf16[1024,384]{1,0:T(8,128)(2,1)S(1)}, u32[]{:S(2)}, u32[]{:S(2)}) collective-permute-start(bf16[1024,384]{1,0:T(8,128)(2,1)S(1)} %get-tuple-element.74.rest_10_), channel_id=1, source_target_pairs={{0,96},{32,64},{64,32},{96,0},{1,97},{33,65},{65,33},{97,1},{2,98}... | collective-permute-start | bytes 2359304 | tf_op jit(solution)/shard_map/ppermute | solution.py:82
  102.0 45.0 %collective-permute-start.19 = (bf16[1024,512]{1,0:T(8,128)(2,1)S(1)}, bf16[1024,512]{1,0:T(8,128)(2,1)S(1)}, u32[]{:S(2)}, u32[]{:S(2)}) collective-permute-start(bf16[1024,512]{1,0:T(8,128)(2,1)S(1)} %get-tuple-element.64.rest_4_), channel_id=1, source_target_pairs={{0,2},{2,0},{4,6},{6,4},{1,3},{3,1},{5,7},{7,5},{8,10},{10,8},{12,... | collective-permute-start | bytes 3145736 | tf_op jit(solution)/shard_map/ppermute | solution.py:82
  102.6 45.2 %collective-permute-start.20 = (bf16[1024,512]{1,0:T(8,128)(2,1)S(1)}, bf16[1024,512]{1,0:T(8,128)(2,1)S(1)}, u32[]{:S(2)}, u32[]{:S(2)}) collective-permute-start(bf16[1024,512]{1,0:T(8,128)(2,1)S(1)} %get-tuple-element.65.rest_6_), channel_id=1, source_target_pairs={{0,6},{2,4},{4,2},{6,0},{1,7},{3,5},{5,3},{7,1},{8,14},{10,12},{12... | collective-permute-start | bytes 3145736 | tf_op jit(solution)/shard_map/ppermute | solution.py:82
  104.2 43.9 %collective-permute-start.10 = (bf16[1024,512]{1,0:T(8,128)(2,1)S(1)}, bf16[1024,512]{1,0:T(8,128)(2,1)S(1)}, u32[]{:S(2)}, u32[]{:S(2)}) collective-permute-start(bf16[1024,512]{1,0:T(8,128)(2,1)S(1)} %get-tuple-element.56.rest_2_), channel_id=1, source_target_pairs={{0,32},{32,0},{64,96},{96,64},{1,33},{33,1},{65,97},{97,65},{2,34}... | collective-permute-start | bytes 3145736 | tf_op jit(solution)/shard_map/ppermute | solution.py:82
  106.3 42.0 %collective-permute-start.9 = (bf16[1024,512]{1,0:T(8,128)(2,1)S(1)}, bf16[1024,512]{1,0:T(8,128)(2,1)S(1)}, u32[]{:S(2)}, u32[]{:S(2)}) collective-permute-start(bf16[1024,512]{1,0:T(8,128)(2,1)S(1)} %get-tuple-element.55.rest_0_), channel_id=1, source_target_pairs={{0,8},{8,0},{16,24},{24,16},{1,9},{9,1},{17,25},{25,17},{2,10},{10... | collective-permute-start | bytes 3145736 | tf_op jit(solution)/shard_map/ppermute | solution.py:82
  107.7 36.5 %collective-permute-start.34 = (bf16[1024,384]{1,0:T(8,128)(2,1)S(1)}, bf16[1024,384]{1,0:T(8,128)(2,1)S(1)}, u32[]{:S(2)}, u32[]{:S(2)}) collective-permute-start(bf16[1024,384]{1,0:T(8,128)(2,1)S(1)} %get-tuple-element.79.rest_6_), channel_id=1, source_target_pairs={{0,6},{2,4},{4,2},{6,0},{1,7},{3,5},{5,3},{7,1},{8,14},{10,12},{12... | collective-permute-start | bytes 2359304 | tf_op jit(solution)/shard_map/ppermute | solution.py:82
  144.2 24.2 %collective-permute-start.35 = (bf16[1024,512]{1,0:T(8,128)(2,1)S(1)}, bf16[1024,512]{1,0:T(8,128)(2,1)}, u32[]{:S(2)}, u32[]{:S(2)}) collective-permute-start(bf16[1024,512]{1,0:T(8,128)(2,1)S(1)} %get-tuple-element.80.rest_8_), channel_id=1, source_target_pairs={{0,24},{8,16},{16,8},{24,0},{1,25},{9,17},{17,9},{25,1},{2,26},{10... | collective-permute-start | bytes 3145736 | tf_op jit(solution)/shard_map/ppermute | solution.py:82
  147.0 23.8 %collective-permute-start.36 = (bf16[1024,512]{1,0:T(8,128)(2,1)S(1)}, bf16[1024,512]{1,0:T(8,128)(2,1)}, u32[]{:S(2)}, u32[]{:S(2)}) collective-permute-start(bf16[1024,512]{1,0:T(8,128)(2,1)S(1)} %get-tuple-element.81.rest_10_), channel_id=1, source_target_pairs={{0,96},{32,64},{64,32},{96,0},{1,97},{33,65},{65,33},{97,1},{2,98}... | collective-permute-start | bytes 3145736 | tf_op jit(solution)/shard_map/ppermute | solution.py:82
  147.8 23.0 %collective-permute-start.33 = (bf16[1024,512]{1,0:T(8,128)(2,1)S(1)}, bf16[1024,512]{1,0:T(8,128)(2,1)}, u32[]{:S(2)}, u32[]{:S(2)}) collective-permute-start(bf16[1024,512]{1,0:T(8,128)(2,1)S(1)} %get-tuple-element.78.rest_4_), channel_id=1, source_target_pairs={{0,2},{2,0},{4,6},{6,4},{1,3},{3,1},{5,7},{7,5},{8,10},{10,8},{12,... | collective-permute-start | bytes 3145736 | tf_op jit(solution)/shard_map/ppermute | solution.py:82
  148.0 22.7 %collective-permute-start.31 = (bf16[1024,512]{1,0:T(8,128)(2,1)}, bf16[1024,512]{1,0:T(8,128)(2,1)}, u32[]{:S(2)}, u32[]{:S(2)}) collective-permute-start(bf16[1024,512]{1,0:T(8,128)(2,1)} %get-tuple-element.76.rest_0_), channel_id=1, source_target_pairs={{0,8},{8,0},{16,24},{24,16},{1,9},{9,1},{17,25},{25,17},{2,10},{10... | collective-permute-start | bytes 3145736 | tf_op jit(solution)/shard_map/ppermute | solution.py:82
  149.4 22.3 %collective-permute-start.32 = (bf16[1024,512]{1,0:T(8,128)(2,1)}, bf16[1024,512]{1,0:T(8,128)(2,1)}, u32[]{:S(2)}, u32[]{:S(2)}) collective-permute-start(bf16[1024,512]{1,0:T(8,128)(2,1)} %get-tuple-element.77.rest_2_), channel_id=1, source_target_pairs={{0,32},{32,0},{64,96},{96,64},{1,33},{33,1},{65,97},{97,65},{2,34}... | collective-permute-start | bytes 3145736 | tf_op jit(solution)/shard_map/ppermute | solution.py:82
  185.6 8.4 %collective-permute-start.37 = (bf16[640,2048]{1,0:T(8,128)(2,1)}, bf16[640,2048]{1,0:T(8,128)(2,1)S(1)}, u32[]{:S(2)}, u32[]{:S(2)}) collective-permute-start(bf16[640,2048]{1,0:T(8,128)(2,1)} %get-tuple-element.82.term), channel_id=1, source_target_pairs={{0,1},{1,0},{2,3},{3,2},{4,5},{5,4},{6,7},{7,6},{8,9},{9,8},{10,11... | collective-permute-start | bytes 7864328 | tf_op jit(solution)/shard_map/ppermute | solution.py:36
  (44 other events, 387.4 us)

commit v2 on v1

--- a/solution.py
+++ b/solution.py
@@ -16,6 +16,7 @@
 LANES = 128
 WIDE = 512
 HALF_ROWS = 32
+CHUNK = 256
 FIRST = (4, 4, 4, 4, 3, 3)
 OTHERS = (4, 4, 4, 3, 4, 4)
 RINGS = (("fs_2", 1), ("fs_1", 1), ("z", 1), ("fs_2", 3), ("fs_1", 3), ("z", 3))
@@ -66,9 +67,9 @@
 ANY = pl.BlockSpec(memory_space=pl.ANY)
 
 
-def params(steps):
+def params(steps, mib=60):
     return pltpu.CompilerParams(
-        dimension_semantics=("arbitrary",) * steps, vmem_limit_bytes=60 * 1024 * 1024
+        dimension_semantics=("arbitrary",) * steps, vmem_limit_bytes=mib * 1024 * 1024
     )
 
 
@@ -158,7 +159,7 @@
         out_specs=[VMEM] * 3,
         scratch_shapes=[pltpu.VMEM(x.shape, x.dtype) for x in arrays]
         + [pltpu.SemaphoreType.DMA((len(arrays),))],
-        compiler_params=pltpu.CompilerParams(vmem_limit_bytes=16 * 1024 * 1024),
+        compiler_params=pltpu.CompilerParams(vmem_limit_bytes=60 * 1024 * 1024),
         name="prepare",
     )(rep, *arrays)
 
@@ -324,7 +325,7 @@
 
 
 def down_kernel(at, hidden, *rest):
-    pieces, (term, kept, weight, sems, out_sem) = rest[:12], rest[12:]
+    pieces, (early, late, kept, weight, sems, out_sem) = rest[:12], rest[12:]
     step = pl.program_id(0)
     begin = starts(OTHERS)
     copy = pltpu.make_async_copy(weight, kept, out_sem)
@@ -336,7 +337,9 @@
             wait_color(weight, sems, OTHERS, c)
 
     rows = pl.ds(pl.multiple_of(step * WIDE, WIDE), WIDE)
-    term[...] = dot_rows(hidden[...], weight[rows, begin[3] :]).astype(jnp.bfloat16)
+    term = dot_rows(hidden[...], weight[rows, begin[3] :]).astype(jnp.bfloat16)
+    early[...] = term[:CHUNK]
+    late[...] = term[CHUNK:]
 
     @pl.when(step == 0)
     def _():
@@ -355,14 +358,19 @@
     return pl.pallas_call(
         down_kernel,
         out_shape=[
-            jax.ShapeDtypeStruct((count, width), jnp.bfloat16),
+            jax.ShapeDtypeStruct((CHUNK, width), jnp.bfloat16),
+            jax.ShapeDtypeStruct((count - CHUNK, width), jnp.bfloat16),
             jax.ShapeDtypeStruct((width, columns), jnp.bfloat16),
         ],
         grid_spec=pltpu.PrefetchScalarGridSpec(
             num_scalar_prefetch=1,
             grid=(width // WIDE,),
             in_specs=[whole((count, units))] + [ANY] * 12,
-            out_specs=[spec((count, WIDE), lambda j, a: (0, j)), ANY],
+            out_specs=[
+                spec((CHUNK, WIDE), lambda j, a: (0, j)),
+                spec((count - CHUNK, WIDE), lambda j, a: (0, j)),
+                ANY,
+            ],
             scratch_shapes=[
                 pltpu.VMEM((width, columns), jnp.bfloat16),
                 pltpu.SemaphoreType.DMA((6,)),
@@ -579,6 +587,28 @@
     )(core, middle, term, far, gain, first, others)
 
 
+def finish_kernel(base, keep, far, *rest):
+    last = keep[...].astype(jnp.float32) + far[...].astype(jnp.float32)
+    rest[-1][...] = (base[...].astype(jnp.float32) + 0.5 * last).astype(jnp.bfloat16)
+
+
+def finish(base, keep, far, count, row, partial):
+    rows, half = base.shape
+    block = spec((SPAN, half), lambda i: (i, 0))
+    held = [] if partial is None else [partial]
+    return pl.pallas_call(
+        finish_kernel,
+        out_shape=jax.ShapeDtypeStruct((count, half), jnp.bfloat16),
+        grid=(rows // SPAN,),
+        in_specs=[block] * 3 + [ANY] * len(held),
+        out_specs=spec((SPAN, half), lambda i: (i + row // SPAN, 0)),
+        input_output_aliases={3: 0} if held else {},
+        compiler_params=params(1, 8),
+        cost_estimate=cost(4 * rows * half, 8 * rows * half, 0),
+        name="finish",
+    )(base, keep, far, *held)
+
+
 def layer(
     tokens,
     norm_first,
@@ -628,27 +658,40 @@
     )
     one, two = gather(colors)
 
+    count = tokens.shape[0]
+    chunks = (slice(0, CHUNK), slice(CHUNK, count))
     own, other = tokens, other_core(tokens)
     hidden, first = first_hidden(core, at, own, other, norm_first[None], one)
-    term, others = first_down(at, hidden, width, two)
-    middle, act, sums = gates(
-        core, own, other, term, other_core(term), norm_mix[None], others, chans
-    )
-    term = mix(
-        act,
-        sums,
-        other_core(sums),
-        ln_gain[None],
-        ln_bias[None],
-        spatial_weight,
-        spatial_bias.T,
-        others,
-    )
-    send, keep, base = second_pass(
-        core, middle, term, other_core(term), norm_second[None], first, others
-    )
-    last = keep.astype(jnp.float32) + other_core(send).astype(jnp.float32)
-    return (base.astype(jnp.float32) + 0.5 * last).astype(jnp.bfloat16)
+    early, late, others = first_down(at, hidden, width, two)
+
+    fars = [other_core(x) for x in (early, late)]
+    mids = [
+        gates(core, own[c], other[c], term, far, norm_mix[None], others, chans)
+        for c, term, far in zip(chunks, (early, late), fars)
+    ]
+    terms = [
+        mix(
+            act,
+            sums,
+            other_core(sums),
+            ln_gain[None],
+            ln_bias[None],
+            spatial_weight,
+            spatial_bias.T,
+            others,
+        )
+        for _, act, sums in mids
+    ]
+    fars = [other_core(x) for x in terms]
+    ends = [
+        second_pass(core, middle, term, far, norm_second[None], first, others)
+        for (middle, _, _), term, far in zip(mids, terms, fars)
+    ]
+    fars = [other_core(x[0]) for x in ends]
+    result = None
+    for c, far, (_, keep, base) in zip(chunks, fars, ends):
+        result = finish(base, keep, far, count, c.start, result)
+    return result
 
 
 def solution(mesh):

time: 252 us -> 257 us (1.020)
  Pallas kernels: 74.5 us -> 90.6 us
  waiting for transfers between devices: 91.7 us -> 84.5 us
  other arithmetic: 3.65 us -> 0 us
    ppermute x5 -> x9, waiting for transfers between devices: 13.1 us -> 5.13 us  [other_core(): return lax.ppermute(x, 'tp', [(0, 1), (1, 0)])]
    pallas_call x1 -> x2, Pallas kernels: 20.7 us -> 26.4 us  [second_pass(): pl.pallas_call(second_kernel, out_shape=[jax.ShapeDtypeStruct((count, hal...]
    slice x0 -> x4, local copies, waits for them, and re-layouts: none -> 4.63 us  [the longest x2 2.83 us: layer(): other[c]]
    pallas_call x1 -> x2, Pallas kernels: 7.25 us -> 11.1 us  [mix(): pl.pallas_call(mix_kernel, out_shape=jax.ShapeDtypeStruct((count, width),...]
    convert_element_type x1 -> x0, other arithmetic: 3.65 us -> none  [layer(): return (base.astype(jnp.float32) + 0.5 * last).astype(jnp.bfloat16)]
    unnamed x71 -> x69, local copies, waits for them, and re-layouts: 16.3 us -> 12.9 us
    ppermute x36, starting transfers between devices: 50 us -> 47.1 us  [exchange(): return lax.ppermute(x, axis, [(i, i ^ flip) for i in range(4)])]
    pallas_call x1 -> x3, Pallas kernels: 13.9 us -> 16.6 us  [the longest x1 14 us: first_down(): pl.pallas_call(down_kernel, out_shape=[jax.ShapeDtypeStruct((CHUNK, width...]
  transfers between devices with their start and end apart: 41 -> 45, of which waited for: 15 -> 16; matrix products, arithmetic and copies ran while one was open for 0% -> 2% of each run, Pallas kernels for 8% -> 25%
where the time goes in v2:
time: 257 us
  Pallas kernels  90.6 us (35%)
  waiting for transfers between devices  84.5 us (33%)
  starting transfers between devices  63.5 us (25%)
  local copies, waits for them, and re-layouts  17.6 us (7%)
    ppermute x36, waiting for transfers between devices, exchange(): return lax.ppermute(x, axis, [(i, i ^ flip) for i in range(4)])  79.4 us
    ppermute x36, starting transfers between devices, exchange(): return lax.ppermute(x, axis, [(i, i ^ flip) for i in range(4)])  47.1 us
    pallas_call x2, Pallas kernels, second_pass(): pl.pallas_call(second_kernel, out_shape=[jax.ShapeDtypeStruct((count, hal...  26.4 us
    pallas_call x1, Pallas kernels, first_hidden(): pl.pallas_call(first_kernel, out_shape=[jax.ShapeDtypeStruct((count, unit...  16.5 us
    ppermute x9, starting transfers between devices, other_core(): return lax.ppermute(x, 'tp', [(0, 1), (1, 0)])  16.4 us
    pallas_call x2, Pallas kernels, gates(): pl.pallas_call(gates_kernel, out_shape=[jax.ShapeDtypeStruct((count, widt...  14.6 us
    pallas_call x1, Pallas kernels, first_down(): pl.pallas_call(down_kernel, out_shape=[jax.ShapeDtypeStruct((CHUNK, width...  14 us
    unnamed x69, local copies, waits for them, and re-layouts  12.9 us
  transfers between devices with their start and end apart: 45, of which 16 were waited for; matrix products, arithmetic and copies ran while one was open for 2% of the time, Pallas kernels for 25%

profile of v2, /device:TPU:1, one launch (start us, length us, event | category | flops | bytes accessed | tf_op | source)
XLA Modules:
  0.0 256.6 jit_solution(2052214011284438350)
XLA Ops:
  0.0 2.2 prepare.1
  2.3 2.5 collective-permute-start.21
  6.1 1.8 collective-permute-done.21.refs_1_
  8.8 2.5 collective-permute-start.22
  12.2 3.5 %collective-permute-start.12 = (bf16[64,1920]{1,0:T(8,128)(2,1)S(1)}, bf16[64,1920]{1,0:T(8,128)(2,1)S(1)}, u32[]{:S(2)}, u32[]{:S(2)}) collective-permute-start(bf16[64,1920]{1,0:T(8,128)(2,1)S(1)} %join.23.refs_0_), channel_id=1, source_target_pairs={{0,96},{32,64},{64,32},{96,0},{1,97},{33,65},{65,33},{97,1},{2,98}... | collective-permute-start | bytes 737288 | tf_op jit(solution)/shard_map/ppermute | solution.py:83
  16.6 2.8 %collective-permute-start.2 = (bf16[64,2048]{1,0:T(8,128)(2,1)S(1)}, bf16[64,2048]{1,0:T(8,128)(2,1)S(1)}, u32[]{:S(2)}, u32[]{:S(2)}) collective-permute-start(bf16[64,2048]{1,0:T(8,128)(2,1)S(1)} %join.18.refs_0_), channel_id=1, source_target_pairs={{0,24},{8,16},{16,8},{24,0},{1,25},{9,17},{17,9},{25,1},{2,26},{10... | collective-permute-start | bytes 786440 | tf_op jit(solution)/shard_map/ppermute | solution.py:83
  21.2 1.7 collective-permute-start.13
  23.5 3.1 %collective-permute-start.3 = (bf16[128,1024]{1,0:T(8,128)(2,1)S(1)}, bf16[128,1024]{1,0:T(8,128)(2,1)S(1)}, u32[]{:S(2)}, u32[]{:S(2)}) collective-permute-start(bf16[128,1024]{1,0:T(8,128)(2,1)S(1)} %get-tuple-element.56.refs_0_), channel_id=1, source_target_pairs={{0,96},{32,64},{64,32},{96,0},{1,97},{33,65},{65,33},{97,1},{2,98}... | collective-permute-start | bytes 786440 | tf_op jit(solution)/shard_map/ppermute | solution.py:83
  29.4 3.2 %collective-permute-start.16 = (bf16[256,896]{1,0:T(8,128)(2,1)S(1)}, bf16[256,896]{1,0:T(8,128)(2,1)S(1)}, u32[]{:S(2)}, u32[]{:S(2)}) collective-permute-start(bf16[256,896]{1,0:T(8,128)(2,1)S(1)} %get-tuple-element.68.refs_1_), channel_id=1, source_target_pairs={{0,24},{8,16},{16,8},{24,0},{1,25},{9,17},{17,9},{25,1},{2,26},{10... | collective-permute-start | bytes 1376264 | tf_op jit(solution)/shard_map/ppermute | solution.py:83
  35.0 1.9 collective-permute-start.27
  38.7 3.7 %collective-permute-start.6 = (bf16[256,1024]{1,0:T(8,128)(2,1)S(1)}, bf16[256,1024]{1,0:T(8,128)(2,1)S(1)}, u32[]{:S(2)}, u32[]{:S(2)}) collective-permute-start(bf16[256,1024]{1,0:T(8,128)(2,1)S(1)} %get-tuple-element.59.refs_1_), channel_id=1, source_target_pairs={{0,96},{32,64},{64,32},{96,0},{1,97},{33,65},{65,33},{97,1},{2,98}... | collective-permute-start | bytes 1572872 | tf_op jit(solution)/shard_map/ppermute | solution.py:83
  44.2 2.5 collective-permute-done.5.refs_2_
  47.1 12.1 %collective-permute-done.6.refs_3_ = bf16[256,1024]{1,0:T(8,128)(2,1)S(1)} collective-permute-done((bf16[256,1024]{1,0:T(8,128)(2,1)S(1)}, bf16[256,1024]{1,0:T(8,128)(2,1)S(1)}, u32[]{:S(2)}, u32[]{:S(2)}) %collective-permute-start.6) | collective-permute-done | bytes 524320 | tf_op jit(solution)/shard_map/ppermute | solution.py:83
  59.3 11.0 %collective-permute-start = (bf16[640,1024]{1,0:T(8,128)(2,1)S(1)}, bf16[640,1024]{1,0:T(8,128)(2,1)S(1)}, u32[]{:S(2)}, u32[]{:S(2)}) collective-permute-start(bf16[640,1024]{1,0:T(8,128)(2,1)S(1)} %copy-done.19), channel_id=1, source_target_pairs={{0,1},{1,0},{2,3},{3,2},{4,5},{5,4},{6,7},{7,6},{8,9},{9,8},{10,11... | collective-permute-start | bytes 3932168 | tf_op jit(solution)/shard_map/ppermute | solution.py:37
  71.7 2.6 %collective-permute-start.29 = (bf16[1024,384]{1,0:T(8,128)(2,1)S(1)}, bf16[1024,384]{1,0:T(8,128)(2,1)S(1)}, u32[]{:S(2)}, u32[]{:S(2)}) collective-permute-start(bf16[1024,384]{1,0:T(8,128)(2,1)S(1)} %get-tuple-element.80.rest_8_), channel_id=1, source_target_pairs={{0,24},{8,16},{16,8},{24,0},{1,25},{9,17},{17,9},{25,1},{2,26},{10... | collective-permute-start | bytes 2359304 | tf_op jit(solution)/shard_map/ppermute | solution.py:83
  74.8 20.4 %collective-permute-done.7.refs_2_ = bf16[512,1024]{1,0:T(8,128)(2,1)S(1)} collective-permute-done((bf16[512,1024]{1,0:T(8,128)(2,1)S(1)}, bf16[512,1024]{1,0:T(8,128)(2,1)S(1)}, u32[]{:S(2)}, u32[]{:S(2)}) %collective-permute-start.7) | collective-permute-done | bytes 1048608 | tf_op jit(solution)/shard_map/ppermute | solution.py:83
  103.8 34.1 %collective-permute-done.34.rest_7_ = bf16[1024,384]{1,0:T(8,128)(2,1)S(1)} collective-permute-done((bf16[1024,384]{1,0:T(8,128)(2,1)S(1)}, bf16[1024,384]{1,0:T(8,128)(2,1)S(1)}, u32[]{:S(2)}, u32[]{:S(2)}) %collective-permute-start.34) | collective-permute-done | bytes 786464 | tf_op jit(solution)/shard_map/ppermute | solution.py:83
  137.9 2.7 %collective-permute-start.35 = (bf16[1024,512]{1,0:T(8,128)(2,1)S(1)}, bf16[1024,512]{1,0:T(8,128)(2,1)}, u32[]{:S(2)}, u32[]{:S(2)}) collective-permute-start(bf16[1024,512]{1,0:T(8,128)(2,1)S(1)} %get-tuple-element.87.rest_8_), channel_id=1, source_target_pairs={{0,24},{8,16},{16,8},{24,0},{1,25},{9,17},{17,9},{25,1},{2,26},{10... | collective-permute-start | bytes 3145736 | tf_op jit(solution)/shard_map/ppermute | solution.py:83
  143.1 16.5 %first_hidden.1 = (bf16[640,1408]{1,0:T(8,128)(2,1)}, bf16[2048,2816]{1,0:T(8,128)(2,1)}) custom-call(s32[1]{0:T(128)} %bitcast.core, s32[1]{0:T(128)} %bitcast.1.at, bf16[640,1024]{1,0:T(8,128)(2,1)} %own.1, bf16[640,1024]{1,0:T(8,128)(2,1)} %copy-done.21, f32[1,2048]{1,0:T(1,128)} %bitcast.23, bf16[1024,512]{1,0:T(8,128)(2,1)} %copy-done.13, ...), custom_call_target="tpu_custom_call" | custom-call | flops 7381975040 | bytes 23068672 | tf_op jit(solution)/shard_map/first_hidden/pallas_call | solution.py:303
  159.6 2.3 collective-permute-done.35.rest_9_
  161.9 2.5 collective-permute-done.36.rest_11_
  165.2 14.0 %first_down.1 = (bf16[256,2048]{1,0:T(8,128)(2,1)}, bf16[384,2048]{1,0:T(8,128)(2,1)}, bf16[2048,2944]{1,0:T(8,128)(2,1)}) custom-call(s32[1]{0:T(128)} %bitcast.1.at, bf16[640,1408]{1,0:T(8,128)(2,1)} %get-tuple-element.82.hidden, bf16[1024,512]{1,0:T(8,128)(2,1)} %get-tuple-element.83.rest_0_, bf16[1024,512]{1,0:T(8,128)(2,1)} %collective-permute-done.31.rest_1_, ...), custom_call_target="tpu_custom_call" | custom-call | flops 3690987520 | bytes 24117248 | tf_op jit(solution)/shard_map/first_down/pallas_call | solution.py:358
  179.2 3.5 %collective-permute-start.37 = (bf16[384,2048]{1,0:T(8,128)(2,1)}, bf16[384,2048]{1,0:T(8,128)(2,1)S(1)}, u32[]{:S(2)}, u32[]{:S(2)}) collective-permute-start(bf16[384,2048]{1,0:T(8,128)(2,1)} %get-tuple-element.89.term), channel_id=1, source_target_pairs={{0,1},{1,0},{2,3},{3,2},{4,5},{5,4},{6,7},{7,6},{8,9},{9,8},{10,11... | collective-permute-start | bytes 4718600 | tf_op jit(solution)/shard_map/ppermute | solution.py:37
  187.1 8.3 %gates.2 = (bf16[384,2048]{1,0:T(8,128)(2,1)}, f32[2,384,512]{2,1,0:T(8,128)}, f32[384,128]{1,0:T(8,128)}) custom-call(s32[1]{0:T(128)} %bitcast.core, bf16[384,1024]{1,0:T(8,128)(2,1)} %slice.12.own, bf16[384,1024]{1,0:T(8,128)(2,1)} %slice.16.other, bf16[384,2048]{1,0:T(8,128)(2,1)} %get-tuple-element.89.term, bf16[384,2048]{1,0:T(8,128)(2,1)} %copy-done.18, ...), custom_call_target="tpu_custom_call" | custom-call | flops 1610612736 | bytes 4194304 | tf_op jit(solution)/shard_map/gates/pallas_call | solution.py:411
  197.7 5.9 %mix.2.term = bf16[384,2048]{1,0:T(8,128)(2,1)} custom-call(f32[2,384,512]{2,1,0:T(8,128)} %get-tuple-element.92.act, f32[384,128]{1,0:T(8,128)} %get-tuple-element.93.sums, f32[384,128]{1,0:T(8,128)} %copy-done.25, f32[1,512]{1,0:T(1,128)} %bitcast.19, f32[1,512]{1,0:T(1,128)} %bitcast.21, bf16[4,128,128]{2,1,0:T(8,128)(2,1)} %weight.3, f32[128,4]{1,0:T(8,128)} %bitcast.11, ...), custom_call_target="tpu_custom_call" | custom-call | flops 805306368 | bytes 2097152 | tf_op jit(solution)/shard_map/mix/pallas_call | solution.py:475
  204.8 1.9 slice.17.other
  206.7 6.4 %gates.3 = (bf16[256,2048]{1,0:T(8,128)(2,1)}, f32[2,256,512]{2,1,0:T(8,128)}, f32[256,128]{1,0:T(8,128)}) custom-call(s32[1]{0:T(128)} %bitcast.core, bf16[256,1024]{1,0:T(8,128)(2,1)} %slice.14.own, bf16[256,1024]{1,0:T(8,128)(2,1)} %slice.17.other, bf16[256,2048]{1,0:T(8,128)(2,1)} %get-tuple-element.98.term, ...), custom_call_target="tpu_custom_call" | custom-call | flops 1073741824 | bytes 4194304 | tf_op jit(solution)/shard_map/gates/pallas_call | solution.py:411
  215.2 5.2 %mix.3.term = bf16[256,2048]{1,0:T(8,128)(2,1)} custom-call(f32[2,256,512]{2,1,0:T(8,128)} %get-tuple-element.100.act, f32[256,128]{1,0:T(8,128)} %get-tuple-element.101.sums, f32[256,128]{1,0:T(8,128)} %copy-done.26, f32[1,512]{1,0:T(1,128)} %bitcast.20, f32[1,512]{1,0:T(1,128)} %bitcast.22, bf16[4,128,128]{2,1,0:T(8,128)(2,1)} %weight.3, ...), custom_call_target="tpu_custom_call" | custom-call | flops 536870912 | bytes 2097152 | tf_op jit(solution)/shard_map/mix/pallas_call | solution.py:475
  221.8 14.6 %second_pass.2 = (bf16[384,1024]{1,0:T(8,128)(2,1)}, bf16[384,1024]{1,0:T(8,128)(2,1)}, bf16[384,1024]{1,0:T(8,128)(2,1)}) custom-call(s32[1]{0:T(128)} %bitcast.core, bf16[384,2048]{1,0:T(8,128)(2,1)} %get-tuple-element.91.middle, bf16[384,2048]{1,0:T(8,128)(2,1)} %mix.2.term, bf16[384,2048]{1,0:T(8,128)(2,1)} %copy-done.17, f32[1,2048]{1,0:T(1,128)} %bitcast.17, ...), custom_call_target="tpu_custom_call" | custom-call | flops 6643777536 | bytes 17301504 | tf_op jit(solution)/shard_map/second_pass/pallas_call | solution.py:557
  237.9 11.8 %second_pass.3 = (bf16[256,1024]{1,0:T(8,128)(2,1)}, bf16[256,1024]{1,0:T(8,128)(2,1)}, bf16[256,1024]{1,0:T(8,128)(2,1)}) custom-call(s32[1]{0:T(128)} %bitcast.core, bf16[256,2048]{1,0:T(8,128)(2,1)} %get-tuple-element.99.middle, bf16[256,2048]{1,0:T(8,128)(2,1)} %mix.3.term, bf16[256,2048]{1,0:T(8,128)(2,1)} %copy-done.23, f32[1,2048]{1,0:T(1,128)} %bitcast.18, ...), custom_call_target="tpu_custom_call" | custom-call | flops 4429185024 | bytes 17301504 | tf_op jit(solution)/shard_map/second_pass/pallas_call | solution.py:557
  250.0 2.0 collective-permute-done.44.far
  254.9 1.7 finish.3
  (160 shorter events, 45.4 us)
Async XLA Ops:
  8.8 10.6 %collective-permute-start.22 = (bf16[64,1792]{1,0:T(8,128)(2,1)S(1)}, bf16[64,1792]{1,0:T(8,128)(2,1)S(1)}, u32[]{:S(2)}, u32[]{:S(2)}) collective-permute-start(bf16[64,1792]{1,0:T(8,128)(2,1)S(1)} %join.28.refs_0_), channel_id=1, source_target_pairs={{0,6},{2,4},{4,2},{6,0},{1,7},{3,5},{5,3},{7,1},{8,14},{10,12},{12... | collective-permute-start | bytes 688136 | tf_op jit(solution)/shard_map/ppermute | solution.py:83
  12.2 8.9 %collective-permute-start.12 = (bf16[64,1920]{1,0:T(8,128)(2,1)S(1)}, bf16[64,1920]{1,0:T(8,128)(2,1)S(1)}, u32[]{:S(2)}, u32[]{:S(2)}) collective-permute-start(bf16[64,1920]{1,0:T(8,128)(2,1)S(1)} %join.23.refs_0_), channel_id=1, source_target_pairs={{0,96},{32,64},{64,32},{96,0},{1,97},{33,65},{65,33},{97,1},{2,98}... | collective-permute-start | bytes 737288 | tf_op jit(solution)/shard_map/ppermute | solution.py:83
  21.2 8.1 %collective-permute-start.13 = (bf16[128,1024]{1,0:T(8,128)(2,1)S(1)}, bf16[128,1024]{1,0:T(8,128)(2,1)S(1)}, u32[]{:S(2)}, u32[]{:S(2)}) collective-permute-start(bf16[128,1024]{1,0:T(8,128)(2,1)S(1)} %get-tuple-element.65.refs_0_), channel_id=1, source_target_pairs={{0,24},{8,16},{16,8},{24,0},{1,25},{9,17},{17,9},{25,1},{2,26},{10... | collective-permute-start | bytes 786440 | tf_op jit(solution)/shard_map/ppermute | solution.py:83
  23.5 9.1 %collective-permute-start.3 = (bf16[128,1024]{1,0:T(8,128)(2,1)S(1)}, bf16[128,1024]{1,0:T(8,128)(2,1)S(1)}, u32[]{:S(2)}, u32[]{:S(2)}) collective-permute-start(bf16[128,1024]{1,0:T(8,128)(2,1)S(1)} %get-tuple-element.56.refs_0_), channel_id=1, source_target_pairs={{0,96},{32,64},{64,32},{96,0},{1,97},{33,65},{65,33},{97,1},{2,98}... | collective-permute-start | bytes 786440 | tf_op jit(solution)/shard_map/ppermute | solution.py:83
  26.7 8.2 %collective-permute-start.25 = (bf16[256,896]{1,0:T(8,128)(2,1)S(1)}, bf16[256,896]{1,0:T(8,128)(2,1)S(1)}, u32[]{:S(2)}, u32[]{:S(2)}) collective-permute-start(bf16[256,896]{1,0:T(8,128)(2,1)S(1)} %get-tuple-element.76.refs_0_), channel_id=1, source_target_pairs={{0,2},{2,0},{4,6},{6,4},{1,3},{3,1},{5,7},{7,5},{8,10},{10,8},{12,... | collective-permute-start | bytes 1376264 | tf_op jit(solution)/shard_map/ppermute | solution.py:83
  29.4 9.3 %collective-permute-start.16 = (bf16[256,896]{1,0:T(8,128)(2,1)S(1)}, bf16[256,896]{1,0:T(8,128)(2,1)S(1)}, u32[]{:S(2)}, u32[]{:S(2)}) collective-permute-start(bf16[256,896]{1,0:T(8,128)(2,1)S(1)} %get-tuple-element.68.refs_1_), channel_id=1, source_target_pairs={{0,24},{8,16},{16,8},{24,0},{1,25},{9,17},{17,9},{25,1},{2,26},{10... | collective-permute-start | bytes 1376264 | tf_op jit(solution)/shard_map/ppermute | solution.py:83
  32.6 9.9 %collective-permute-start.15 = (bf16[256,1024]{1,0:T(8,128)(2,1)S(1)}, bf16[256,1024]{1,0:T(8,128)(2,1)S(1)}, u32[]{:S(2)}, u32[]{:S(2)}) collective-permute-start(bf16[256,1024]{1,0:T(8,128)(2,1)S(1)} %get-tuple-element.67.refs_0_), channel_id=1, source_target_pairs={{0,32},{32,0},{64,96},{96,64},{1,33},{33,1},{65,97},{97,65},{2,34}... | collective-permute-start | bytes 1572872 | tf_op jit(solution)/shard_map/ppermute | solution.py:83
  34.6 12.1 %collective-permute-start.5 = (bf16[256,1024]{1,0:T(8,128)(2,1)S(1)}, bf16[256,1024]{1,0:T(8,128)(2,1)S(1)}, u32[]{:S(2)}, u32[]{:S(2)}) collective-permute-start(bf16[256,1024]{1,0:T(8,128)(2,1)S(1)} %get-tuple-element.58.refs_0_), channel_id=1, source_target_pairs={{0,6},{2,4},{4,2},{6,0},{1,7},{3,5},{5,3},{7,1},{8,14},{10,12},{12... | collective-permute-start | bytes 1572872 | tf_op jit(solution)/shard_map/ppermute | solution.py:83
  35.0 35.4 %collective-permute-start.27 = (bf16[512,896]{1,0:T(8,128)(2,1)S(1)}, bf16[512,896]{1,0:T(8,128)(2,1)S(1)}, u32[]{:S(2)}, u32[]{:S(2)}) collective-permute-start(bf16[512,896]{1,0:T(8,128)(2,1)S(1)} %get-tuple-element.78.refs_0_), channel_id=1, source_target_pairs={{0,96},{32,64},{64,32},{96,0},{1,97},{33,65},{65,33},{97,1},{2,98}... | collective-permute-start | bytes 2752520 | tf_op jit(solution)/shard_map/ppermute | solution.py:83
  36.9 33.6 %collective-permute-start.28 = (bf16[512,896]{1,0:T(8,128)(2,1)S(1)}, bf16[512,896]{1,0:T(8,128)(2,1)S(1)}, u32[]{:S(2)}, u32[]{:S(2)}) collective-permute-start(bf16[512,896]{1,0:T(8,128)(2,1)S(1)} %get-tuple-element.79.refs_1_), channel_id=1, source_target_pairs={{0,24},{8,16},{16,8},{24,0},{1,25},{9,17},{17,9},{25,1},{2,26},{10... | collective-permute-start | bytes 2752520 | tf_op jit(solution)/shard_map/ppermute | solution.py:83
  38.7 20.5 %collective-permute-start.6 = (bf16[256,1024]{1,0:T(8,128)(2,1)S(1)}, bf16[256,1024]{1,0:T(8,128)(2,1)S(1)}, u32[]{:S(2)}, u32[]{:S(2)}) collective-permute-start(bf16[256,1024]{1,0:T(8,128)(2,1)S(1)} %get-tuple-element.59.refs_1_), channel_id=1, source_target_pairs={{0,96},{32,64},{64,32},{96,0},{1,97},{33,65},{65,33},{97,1},{2,98}... | collective-permute-start | bytes 1572872 | tf_op jit(solution)/shard_map/ppermute | solution.py:83
  42.6 29.1 %collective-permute-start.18 = (bf16[512,896]{1,0:T(8,128)(2,1)S(1)}, bf16[512,896]{1,0:T(8,128)(2,1)S(1)}, u32[]{:S(2)}, u32[]{:S(2)}) collective-permute-start(bf16[512,896]{1,0:T(8,128)(2,1)S(1)} %get-tuple-element.70.refs_1_), channel_id=1, source_target_pairs={{0,2},{2,0},{4,6},{6,4},{1,3},{3,1},{5,7},{7,5},{8,10},{10,8},{12,... | collective-permute-start | bytes 2752520 | tf_op jit(solution)/shard_map/ppermute | solution.py:83
  46.7 27.6 %collective-permute-start.17 = (bf16[512,1024]{1,0:T(8,128)(2,1)S(1)}, bf16[512,1024]{1,0:T(8,128)(2,1)S(1)}, u32[]{:S(2)}, u32[]{:S(2)}) collective-permute-start(bf16[512,1024]{1,0:T(8,128)(2,1)S(1)} %get-tuple-element.69.refs_0_), channel_id=1, source_target_pairs={{0,6},{2,4},{4,2},{6,0},{1,7},{3,5},{5,3},{7,1},{8,14},{10,12},{12... | collective-permute-start | bytes 3145736 | tf_op jit(solution)/shard_map/ppermute | solution.py:83
  59.3 38.7 %collective-permute-start = (bf16[640,1024]{1,0:T(8,128)(2,1)S(1)}, bf16[640,1024]{1,0:T(8,128)(2,1)S(1)}, u32[]{:S(2)}, u32[]{:S(2)}) collective-permute-start(bf16[640,1024]{1,0:T(8,128)(2,1)S(1)} %copy-done.19), channel_id=1, source_target_pairs={{0,1},{1,0},{2,3},{3,2},{4,5},{5,4},{6,7},{7,6},{8,9},{9,8},{10,11... | collective-permute-start | bytes 3932168 | tf_op jit(solution)/shard_map/ppermute | solution.py:37
  70.5 24.8 %collective-permute-start.7 = (bf16[512,1024]{1,0:T(8,128)(2,1)S(1)}, bf16[512,1024]{1,0:T(8,128)(2,1)S(1)}, u32[]{:S(2)}, u32[]{:S(2)}) collective-permute-start(bf16[512,1024]{1,0:T(8,128)(2,1)S(1)} %get-tuple-element.60.refs_0_), channel_id=1, source_target_pairs={{0,32},{32,0},{64,96},{96,64},{1,33},{33,1},{65,97},{97,65},{2,34}... | collective-permute-start | bytes 3145736 | tf_op jit(solution)/shard_map/ppermute | solution.py:83
  70.6 25.6 %collective-permute-start.8 = (bf16[512,1024]{1,0:T(8,128)(2,1)S(1)}, bf16[512,1024]{1,0:T(8,128)(2,1)S(1)}, u32[]{:S(2)}, u32[]{:S(2)}) collective-permute-start(bf16[512,1024]{1,0:T(8,128)(2,1)S(1)} %get-tuple-element.61.refs_1_), channel_id=1, source_target_pairs={{0,8},{8,0},{16,24},{24,16},{1,9},{9,1},{17,25},{25,17},{2,10},{10... | collective-permute-start | bytes 3145736 | tf_op jit(solution)/shard_map/ppermute | solution.py:83
  71.7 27.5 %collective-permute-start.29 = (bf16[1024,384]{1,0:T(8,128)(2,1)S(1)}, bf16[1024,384]{1,0:T(8,128)(2,1)S(1)}, u32[]{:S(2)}, u32[]{:S(2)}) collective-permute-start(bf16[1024,384]{1,0:T(8,128)(2,1)S(1)} %get-tuple-element.80.rest_8_), channel_id=1, source_target_pairs={{0,24},{8,16},{16,8},{24,0},{1,25},{9,17},{17,9},{25,1},{2,26},{10... | collective-permute-start | bytes 2359304 | tf_op jit(solution)/shard_map/ppermute | solution.py:83
  74.3 26.7 %collective-permute-start.30 = (bf16[1024,384]{1,0:T(8,128)(2,1)S(1)}, bf16[1024,384]{1,0:T(8,128)(2,1)S(1)}, u32[]{:S(2)}, u32[]{:S(2)}) collective-permute-start(bf16[1024,384]{1,0:T(8,128)(2,1)S(1)} %get-tuple-element.81.rest_10_), channel_id=1, source_target_pairs={{0,96},{32,64},{64,32},{96,0},{1,97},{33,65},{65,33},{97,1},{2,98}... | collective-permute-start | bytes 2359304 | tf_op jit(solution)/shard_map/ppermute | solution.py:83
  95.2 45.3 %collective-permute-start.19 = (bf16[1024,512]{1,0:T(8,128)(2,1)S(1)}, bf16[1024,512]{1,0:T(8,128)(2,1)S(1)}, u32[]{:S(2)}, u32[]{:S(2)}) collective-permute-start(bf16[1024,512]{1,0:T(8,128)(2,1)S(1)} %get-tuple-element.71.rest_4_), channel_id=1, source_target_pairs={{0,2},{2,0},{4,6},{6,4},{1,3},{3,1},{5,7},{7,5},{8,10},{10,8},{12,... | collective-permute-start | bytes 3145736 | tf_op jit(solution)/shard_map/ppermute | solution.py:83
  96.2 44.8 %collective-permute-start.20 = (bf16[1024,512]{1,0:T(8,128)(2,1)S(1)}, bf16[1024,512]{1,0:T(8,128)(2,1)S(1)}, u32[]{:S(2)}, u32[]{:S(2)}) collective-permute-start(bf16[1024,512]{1,0:T(8,128)(2,1)S(1)} %get-tuple-element.72.rest_6_), channel_id=1, source_target_pairs={{0,6},{2,4},{4,2},{6,0},{1,7},{3,5},{5,3},{7,1},{8,14},{10,12},{12... | collective-permute-start | bytes 3145736 | tf_op jit(solution)/shard_map/ppermute | solution.py:83
  98.0 43.1 %collective-permute-start.10 = (bf16[1024,512]{1,0:T(8,128)(2,1)S(1)}, bf16[1024,512]{1,0:T(8,128)(2,1)S(1)}, u32[]{:S(2)}, u32[]{:S(2)}) collective-permute-start(bf16[1024,512]{1,0:T(8,128)(2,1)S(1)} %get-tuple-element.63.rest_2_), channel_id=1, source_target_pairs={{0,32},{32,0},{64,96},{96,64},{1,33},{33,1},{65,97},{97,65},{2,34}... | collective-permute-start | bytes 3145736 | tf_op jit(solution)/shard_map/ppermute | solution.py:83
  100.2 41.2 %collective-permute-start.9 = (bf16[1024,512]{1,0:T(8,128)(2,1)S(1)}, bf16[1024,512]{1,0:T(8,128)(2,1)S(1)}, u32[]{:S(2)}, u32[]{:S(2)}) collective-permute-start(bf16[1024,512]{1,0:T(8,128)(2,1)S(1)} %get-tuple-element.62.rest_0_), channel_id=1, source_target_pairs={{0,8},{8,0},{16,24},{24,16},{1,9},{9,1},{17,25},{25,17},{2,10},{10... | collective-permute-start | bytes 3145736 | tf_op jit(solution)/shard_map/ppermute | solution.py:83
  101.0 36.8 %collective-permute-start.34 = (bf16[1024,384]{1,0:T(8,128)(2,1)S(1)}, bf16[1024,384]{1,0:T(8,128)(2,1)S(1)}, u32[]{:S(2)}, u32[]{:S(2)}) collective-permute-start(bf16[1024,384]{1,0:T(8,128)(2,1)S(1)} %get-tuple-element.86.rest_6_), channel_id=1, source_target_pairs={{0,6},{2,4},{4,2},{6,0},{1,7},{3,5},{5,3},{7,1},{8,14},{10,12},{12... | collective-permute-start | bytes 2359304 | tf_op jit(solution)/shard_map/ppermute | solution.py:83
  137.9 24.0 %collective-permute-start.35 = (bf16[1024,512]{1,0:T(8,128)(2,1)S(1)}, bf16[1024,512]{1,0:T(8,128)(2,1)}, u32[]{:S(2)}, u32[]{:S(2)}) collective-permute-start(bf16[1024,512]{1,0:T(8,128)(2,1)S(1)} %get-tuple-element.87.rest_8_), channel_id=1, source_target_pairs={{0,24},{8,16},{16,8},{24,0},{1,25},{9,17},{17,9},{25,1},{2,26},{10... | collective-permute-start | bytes 3145736 | tf_op jit(solution)/shard_map/ppermute | solution.py:83
  140.5 23.8 %collective-permute-start.36 = (bf16[1024,512]{1,0:T(8,128)(2,1)S(1)}, bf16[1024,512]{1,0:T(8,128)(2,1)}, u32[]{:S(2)}, u32[]{:S(2)}) collective-permute-start(bf16[1024,512]{1,0:T(8,128)(2,1)S(1)} %get-tuple-element.88.rest_10_), channel_id=1, source_target_pairs={{0,96},{32,64},{64,32},{96,0},{1,97},{33,65},{65,33},{97,1},{2,98}... | collective-permute-start | bytes 3145736 | tf_op jit(solution)/shard_map/ppermute | solution.py:83
  141.0 23.4 %collective-permute-start.33 = (bf16[1024,512]{1,0:T(8,128)(2,1)S(1)}, bf16[1024,512]{1,0:T(8,128)(2,1)}, u32[]{:S(2)}, u32[]{:S(2)}) collective-permute-start(bf16[1024,512]{1,0:T(8,128)(2,1)S(1)} %get-tuple-element.85.rest_4_), channel_id=1, source_target_pairs={{0,2},{2,0},{4,6},{6,4},{1,3},{3,1},{5,7},{7,5},{8,10},{10,8},{12,... | collective-permute-start | bytes 3145736 | tf_op jit(solution)/shard_map/ppermute | solution.py:83
  141.1 23.2 %collective-permute-start.31 = (bf16[1024,512]{1,0:T(8,128)(2,1)}, bf16[1024,512]{1,0:T(8,128)(2,1)}, u32[]{:S(2)}, u32[]{:S(2)}) collective-permute-start(bf16[1024,512]{1,0:T(8,128)(2,1)} %get-tuple-element.83.rest_0_), channel_id=1, source_target_pairs={{0,8},{8,0},{16,24},{24,16},{1,9},{9,1},{17,25},{25,17},{2,10},{10... | collective-permute-start | bytes 3145736 | tf_op jit(solution)/shard_map/ppermute | solution.py:83
  142.7 22.5 %collective-permute-start.32 = (bf16[1024,512]{1,0:T(8,128)(2,1)}, bf16[1024,512]{1,0:T(8,128)(2,1)}, u32[]{:S(2)}, u32[]{:S(2)}) collective-permute-start(bf16[1024,512]{1,0:T(8,128)(2,1)} %get-tuple-element.84.rest_2_), channel_id=1, source_target_pairs={{0,32},{32,0},{64,96},{96,64},{1,33},{33,1},{65,97},{97,65},{2,34}... | collective-permute-start | bytes 3145736 | tf_op jit(solution)/shard_map/ppermute | solution.py:83
  195.7 11.0 %collective-permute-start.41 = (bf16[256,2048]{1,0:T(8,128)(2,1)}, bf16[256,2048]{1,0:T(8,128)(2,1)}, u32[]{:S(2)}, u32[]{:S(2)}) collective-permute-start(bf16[256,2048]{1,0:T(8,128)(2,1)} %get-tuple-element.98.term), channel_id=1, source_target_pairs={{0,1},{1,0},{2,3},{3,2},{4,5},{5,4},{6,7},{7,6},{8,9},{9,8},{10,11... | collective-permute-start | bytes 3145736 | tf_op jit(solution)/shard_map/ppermute | solution.py:37
  203.6 17.1 %collective-permute-start.39 = (bf16[384,2048]{1,0:T(8,128)(2,1)}, bf16[384,2048]{1,0:T(8,128)(2,1)S(1)}, u32[]{:S(2)}, u32[]{:S(2)}) collective-permute-start(bf16[384,2048]{1,0:T(8,128)(2,1)} %mix.2.term), channel_id=1, source_target_pairs={{0,1},{1,0},{2,3},{3,2},{4,5},{5,4},{6,7},{7,6},{8,9},{9,8},{10,11... | collective-permute-start | bytes 4718600 | tf_op jit(solution)/shard_map/ppermute | solution.py:37
  220.5 16.4 %collective-permute-start.43 = (bf16[256,2048]{1,0:T(8,128)(2,1)}, bf16[256,2048]{1,0:T(8,128)(2,1)S(1)}, u32[]{:S(2)}, u32[]{:S(2)}) collective-permute-start(bf16[256,2048]{1,0:T(8,128)(2,1)} %mix.3.term), channel_id=1, source_target_pairs={{0,1},{1,0},{2,3},{3,2},{4,5},{5,4},{6,7},{7,6},{8,9},{9,8},{10,11... | collective-permute-start | bytes 3145736 | tf_op jit(solution)/shard_map/ppermute | solution.py:37
  236.4 18.5 %collective-permute-start.40 = (bf16[384,1024]{1,0:T(8,128)(2,1)}, bf16[384,1024]{1,0:T(8,128)(2,1)S(1)}, u32[]{:S(2)}, u32[]{:S(2)}) collective-permute-start(bf16[384,1024]{1,0:T(8,128)(2,1)} %get-tuple-element.97), channel_id=1, source_target_pairs={{0,1},{1,0},{2,3},{3,2},{4,5},{5,4},{6,7},{7,6},{8,9},{9,8},{10,11... | collective-permute-start | bytes 2359304 | tf_op jit(solution)/shard_map/ppermute | solution.py:37
  (47 other events, 333.4 us)

commit v3 on v1

--- a/solution.py
+++ b/solution.py
@@ -158,7 +158,7 @@
         out_specs=[VMEM] * 3,
         scratch_shapes=[pltpu.VMEM(x.shape, x.dtype) for x in arrays]
         + [pltpu.SemaphoreType.DMA((len(arrays),))],
-        compiler_params=pltpu.CompilerParams(vmem_limit_bytes=16 * 1024 * 1024),
+        compiler_params=pltpu.CompilerParams(vmem_limit_bytes=60 * 1024 * 1024),
         name="prepare",
     )(rep, *arrays)
 
@@ -211,18 +211,18 @@
     return groups
 
 
-def place_blocks(at, pieces, weight, sems, widths, colors):
+def place_blocks(at, pieces, weight, sems, widths, colors, first=0):
     begin = starts(widths)
     for c in colors:
         columns = pl.ds(begin[c], widths[c] * LANES)
         for k in range(2):
 
             def copy_four(high, carry, c=c, k=k, columns=columns):
-                moved = at ^ place(c, 32 * k)
+                moved = at ^ place(first + c, 32 * k)
                 for bit in range(3):
-                    moved = moved ^ ((high >> bit & 1) * place(c, 4 << bit))
+                    moved = moved ^ ((high >> bit & 1) * place(first + c, 4 << bit))
                 for low in range(4):
-                    to = (moved ^ place(c, low)) * HALF_ROWS
+                    to = (moved ^ place(first + c, low)) * HALF_ROWS
                     origin = (high * 4 + low) * HALF_ROWS
                     pltpu.make_async_copy(
                         pieces[2 * c + k].at[
@@ -255,7 +255,7 @@
 
 
 def hidden_step(step, normed, weight, hidden):
-    @pl.when(step < 4)
+    @pl.when((step >= 0) & (step < 4))
     def _():
         columns = pl.ds(pl.multiple_of(step * WIDE, WIDE), WIDE)
         both = dot(normed[...], weight[:, columns])
@@ -323,26 +323,27 @@
     )(core, at, own, other, gain, *pieces)
 
 
+MIXER, DOWN = OTHERS[:3], OTHERS[3:]
+
+
+def place_blocks_of(at, pieces, weight, sems, widths, first):
+    place_blocks(at, pieces, weight, sems, widths, range(len(widths)), first)
+
+
 def down_kernel(at, hidden, *rest):
-    pieces, (term, kept, weight, sems, out_sem) = rest[:12], rest[12:]
+    pieces, (term, kept, weight, sems, out_sem) = rest[:6], rest[6:]
     step = pl.program_id(0)
-    begin = starts(OTHERS)
     copy = pltpu.make_async_copy(weight, kept, out_sem)
 
     @pl.when(step == 0)
     def _():
-        place_blocks(at[0], pieces, weight, sems, OTHERS, (3, 4, 5, 0, 1, 2))
-        for c in (3, 4, 5):
-            wait_color(weight, sems, OTHERS, c)
+        place_blocks_of(at[0], pieces, weight, sems, DOWN, 3)
+        for c in range(3):
+            wait_color(weight, sems, DOWN, c)
+        copy.start()
 
     rows = pl.ds(pl.multiple_of(step * WIDE, WIDE), WIDE)
-    term[...] = dot_rows(hidden[...], weight[rows, begin[3] :]).astype(jnp.bfloat16)
-
-    @pl.when(step == 0)
-    def _():
-        for c in (0, 1, 2):
-            wait_color(weight, sems, OTHERS, c)
-        copy.start()
+    term[...] = dot_rows(hidden[...], weight[rows, :]).astype(jnp.bfloat16)
 
     @pl.when(step == pl.num_programs(0) - 1)
     def _():
@@ -351,32 +352,70 @@
 
 def first_down(at, hidden, width, pieces):
     count, units = hidden.shape
-    columns = sum(OTHERS) * LANES
     return pl.pallas_call(
         down_kernel,
         out_shape=[
             jax.ShapeDtypeStruct((count, width), jnp.bfloat16),
-            jax.ShapeDtypeStruct((width, columns), jnp.bfloat16),
+            jax.ShapeDtypeStruct((width, units), jnp.bfloat16),
         ],
         grid_spec=pltpu.PrefetchScalarGridSpec(
             num_scalar_prefetch=1,
             grid=(width // WIDE,),
-            in_specs=[whole((count, units))] + [ANY] * 12,
+            in_specs=[whole((count, units))] + [ANY] * 6,
             out_specs=[spec((count, WIDE), lambda j, a: (0, j)), ANY],
             scratch_shapes=[
-                pltpu.VMEM((width, columns), jnp.bfloat16),
-                pltpu.SemaphoreType.DMA((6,)),
+                pltpu.VMEM((width, units), jnp.bfloat16),
+                pltpu.SemaphoreType.DMA((3,)),
                 pltpu.SemaphoreType.DMA,
             ],
         ),
         compiler_params=params(1),
-        cost_estimate=cost(2 * count * width * units, 4 * width * columns, 0),
+        cost_estimate=cost(2 * count * width * units, 4 * width * units, 0),
         name="first_down",
     )(at, hidden, *pieces)
 
 
-def gates_kernel(core, own, other, term, far, gain, rows, middle, act, sums, normed):
-    @pl.when(pl.program_id(0) == 0)
+def assemble_kernel(at, *rest):
+    pieces, (kept, weight, sems, out_sems) = rest[:6], rest[6:]
+    place_blocks_of(at[0], pieces, weight, sems, MIXER, 0)
+    begin = starts(MIXER)
+    copies = []
+    for c in range(3):
+        wait_color(weight, sems, MIXER, c)
+        columns = pl.ds(begin[c], MIXER[c] * LANES)
+        copy = pltpu.make_async_copy(weight.at[:, columns], kept.at[:, columns], out_sems.at[c])
+        copy.start()
+        copies.append(copy)
+    for copy in copies:
+        copy.wait()
+
+
+def assemble(at, width, pieces):
+    shape = (width, sum(MIXER) * LANES)
+    return pl.pallas_call(
+        assemble_kernel,
+        out_shape=jax.ShapeDtypeStruct(shape, jnp.bfloat16),
+        grid_spec=pltpu.PrefetchScalarGridSpec(
+            num_scalar_prefetch=1,
+            grid=(1,),
+            in_specs=[ANY] * 6,
+            out_specs=ANY,
+            scratch_shapes=[
+                pltpu.VMEM(shape, jnp.bfloat16),
+                pltpu.SemaphoreType.DMA((3,)),
+                pltpu.SemaphoreType.DMA((3,)),
+            ],
+        ),
+        compiler_params=params(1),
+        cost_estimate=cost(5 * 10**9, 8 * shape[0] * shape[1], 0),
+        name="assemble",
+    )(at, *pieces)
+
+
+def gates_kernel(blocks, core, own, other, term, far, gain, rows, middle, act, sums, normed):
+    step = pl.program_id(0)
+
+    @pl.when(step < blocks)
     def _():
         left = jnp.where(core[0] == 0, own[...], other[...])
         right = jnp.where(core[0] == 0, other[...], own[...])
@@ -384,24 +423,32 @@
         values = values + 0.5 * (term[...].astype(jnp.float32) + far[...].astype(jnp.float32))
         mid = values.astype(jnp.bfloat16)
         middle[...] = mid
-        normed[...] = normed_rows(mid.astype(jnp.float32), gain[...])
-
-    acted = gelu(dot(normed[...], rows[...]))
-    act[0] = acted
-
-    @pl.when(pl.program_id(0) == 0)
-    def _():
-        lane = lax.broadcasted_iota(jnp.int32, sums.shape, 1)
-        total = jnp.sum(acted, axis=1, keepdims=True)
-        squares = jnp.sum(acted * acted, axis=1, keepdims=True)
-        sums[...] = jnp.where(lane == 0, total, squares)
+        block = pl.ds(pl.multiple_of(step * SPAN, SPAN), SPAN)
+        normed[block, :] = normed_rows(mid.astype(jnp.float32), gain[...])
+
+    @pl.when(step >= blocks)
+    def _():
+        acted = gelu(dot(normed[...], rows[...]))
+        act[0] = acted
+
+        @pl.when(step == blocks)
+        def _():
+            lane = lax.broadcasted_iota(jnp.int32, sums.shape, 1)
+            total = jnp.sum(acted, axis=1, keepdims=True)
+            squares = jnp.sum(acted * acted, axis=1, keepdims=True)
+            sums[...] = jnp.where(lane == 0, total, squares)
 
 
 def gates(core, own, other, term, far, gain, weight, chans):
     count, half = own.shape
     width = 2 * half
-    return pl.pallas_call(
-        gates_kernel,
+    blocks = count // SPAN
+
+    def block(columns):
+        return spec((SPAN, columns), lambda i, c: (jnp.minimum(i, blocks - 1), 0))
+
+    return pl.pallas_call(
+        functools.partial(gates_kernel, blocks),
         out_shape=[
             jax.ShapeDtypeStruct((count, width), jnp.bfloat16),
             jax.ShapeDtypeStruct((2, count, chans), jnp.float32),
@@ -409,18 +456,18 @@
         ],
         grid_spec=pltpu.PrefetchScalarGridSpec(
             num_scalar_prefetch=1,
-            grid=(2,),
+            grid=(blocks + 2,),
             in_specs=[
-                whole((count, half)),
-                whole((count, half)),
-                whole((count, width)),
-                whole((count, width)),
+                block(half),
+                block(half),
+                block(width),
+                block(width),
                 whole((1, width)),
-                spec((width, chans), lambda i, c: (0, 2 - i)),
+                spec((width, chans), lambda i, c: (0, 2 - jnp.maximum(i - blocks, 0))),
             ],
             out_specs=[
-                whole((count, width)),
-                spec((1, count, chans), lambda i, c: (i, 0, 0)),
+                block(width),
+                spec((1, count, chans), lambda i, c: (jnp.maximum(i - blocks, 0), 0, 0)),
                 whole((count, LANES)),
             ],
             scratch_shapes=[pltpu.VMEM((count, width), jnp.bfloat16)],
@@ -443,6 +490,10 @@
         ]
         count, chans = mixed.shape
         wide = chans // groups
+        column = [
+            jnp.sum(jnp.where(source == at, shift[g : g + 1, :], 0.0), axis=1, keepdims=True)
+            for g in range(groups)
+        ]
         for n in range(count // SPAN):
             block = pl.ds(n * SPAN, SPAN)
             totals = (sums[block, :] + far[block, :]) / BW
@@ -451,7 +502,7 @@
             v_normed = (act[0, block, :] - v_mean) * lax.rsqrt(v_var + EPS) * gain[...] + bias[...]
             v_normed = v_normed.astype(jnp.bfloat16)
             spatial = [
-                dot(masked[g], v_normed[:, g * wide : (g + 1) * wide]) + shift[:, g : g + 1]
+                dot(masked[g], v_normed[:, g * wide : (g + 1) * wide]) + column[g]
                 for g in range(groups)
             ]
             product = act[1, block, :] * jnp.concatenate(spatial, axis=1)
@@ -475,7 +526,7 @@
             whole((1, chans)),
             whole((1, chans)),
             whole((groups, SPAN, SPAN)),
-            whole((SPAN, groups)),
+            whole((groups, SPAN)),
             spec((WIDE, chans), lambda j: (j, 0)),
         ],
         out_specs=spec((count, WIDE), lambda j: (0, j)),
@@ -487,44 +538,59 @@
 
 
 def second_kernel(
-    core, middle, term, far, gain, first, others, send, keep, base, normed, hidden, wide, down, sems
+    blocks,
+    core,
+    middle,
+    term,
+    far,
+    gain,
+    first,
+    others,
+    send,
+    keep,
+    base,
+    normed,
+    hidden,
+    wide,
+    down,
+    sems,
 ):
     step = pl.program_id(0)
     steps = 5
     outs = down.shape[0] // WIDE
-    begin = starts(OTHERS)[3]
     cuts = [pl.ds(k * WIDE, WIDE) for k in range(4)] + [pl.ds(4 * WIDE, 6 * LANES)]
     copies = [
         pltpu.make_async_copy(first.at[:, cut], wide.at[:, cut], sems.at[k])
         for k, cut in enumerate(cuts)
     ]
-    copies.append(
-        pltpu.make_async_copy(others.at[:, pl.ds(begin, down.shape[1])], down, sems.at[steps])
-    )
-
-    @pl.when(step == 0)
-    def _():
-        for copy in copies:
+    copies.append(pltpu.make_async_copy(others, down, sems.at[steps]))
+
+    for k, copy in enumerate(copies):
+
+        @pl.when(step == k)
+        def _():
             copy.start()
+
+        @pl.when(step == blocks + k)
+        def _():
+            copy.wait()
+
+    @pl.when(step < blocks)
+    def _():
         values = middle[...].astype(jnp.float32) + (
             term[...].astype(jnp.float32) + far[...].astype(jnp.float32)
         )
         second = values.astype(jnp.bfloat16)
         half = second.shape[1] // 2
         base[...] = jnp.where(core[0] == 0, second[:, :half], second[:, half:])
-        normed[...] = normed_rows(second.astype(jnp.float32), gain[...])
-
-    for k, copy in enumerate(copies):
-
-        @pl.when(step == k)
-        def _():
-            copy.wait()
-
-    hidden_step(step, normed, wide, hidden)
-
-    @pl.when(step >= steps)
-    def _():
-        n = step - steps
+        block = pl.ds(pl.multiple_of(step * SPAN, SPAN), SPAN)
+        normed[block, :] = normed_rows(second.astype(jnp.float32), gain[...])
+
+    hidden_step(step - blocks, normed, wide, hidden)
+
+    @pl.when(step >= blocks + steps)
+    def _():
+        n = step - blocks - steps
         mine = jnp.where(n < outs // 2, 1 - core[0], core[0])
         row = mine * (outs // 2) + lax.rem(n, outs // 2)
         rows = pl.ds(pl.multiple_of(row * WIDE, WIDE), WIDE)
@@ -546,24 +612,23 @@
     units = columns // 2
     outs = width // WIDE
     sent = outs // 2
-    return pl.pallas_call(
-        second_kernel,
+    blocks = count // SPAN
+    done = blocks + 5
+
+    def block(size):
+        return spec((SPAN, size), lambda j, c: (jnp.minimum(j, blocks - 1), 0))
+
+    return pl.pallas_call(
+        functools.partial(second_kernel, blocks),
         out_shape=[jax.ShapeDtypeStruct((count, half), jnp.bfloat16)] * 3,
         grid_spec=pltpu.PrefetchScalarGridSpec(
             num_scalar_prefetch=1,
-            grid=(5 + outs,),
-            in_specs=[
-                whole((count, width)),
-                whole((count, width)),
-                whole((count, width)),
-                whole((1, width)),
-                ANY,
-                ANY,
-            ],
+            grid=(done + outs,),
+            in_specs=[block(width)] * 3 + [whole((1, width)), ANY, ANY],
             out_specs=[
-                spec((count, WIDE), lambda j, c: (0, jnp.clip(j - 5, 0, sent - 1))),
-                spec((count, WIDE), lambda j, c: (0, jnp.maximum(j - 5 - sent, 0))),
-                whole((count, half)),
+                spec((count, WIDE), lambda j, c: (0, jnp.clip(j - done, 0, sent - 1))),
+                spec((count, WIDE), lambda j, c: (0, jnp.maximum(j - done - sent, 0))),
+                block(half),
             ],
             scratch_shapes=[
                 pltpu.VMEM((count, width), jnp.bfloat16),
@@ -577,6 +642,26 @@
         cost_estimate=cost(6 * count * width * units, 6 * width * units, count * units),
         name="second_pass",
     )(core, middle, term, far, gain, first, others)
+
+
+def finish_kernel(base, keep, far, result):
+    last = keep[...].astype(jnp.float32) + far[...].astype(jnp.float32)
+    result[...] = (base[...].astype(jnp.float32) + 0.5 * last).astype(jnp.bfloat16)
+
+
+def finish(base, keep, far):
+    count, half = base.shape
+    block = spec((SPAN, half), lambda i: (i, 0))
+    return pl.pallas_call(
+        finish_kernel,
+        out_shape=jax.ShapeDtypeStruct((count, half), jnp.bfloat16),
+        grid=(count // SPAN,),
+        in_specs=[block] * 3,
+        out_specs=block,
+        compiler_params=params(1),
+        cost_estimate=cost(4 * count * half, 8 * count * half, 0),
+        name="finish",
+    )(base, keep, far)
 
 
 def layer(
@@ -630,10 +715,10 @@
 
     own, other = tokens, other_core(tokens)
     hidden, first = first_hidden(core, at, own, other, norm_first[None], one)
-    term, others = first_down(at, hidden, width, two)
-    middle, act, sums = gates(
-        core, own, other, term, other_core(term), norm_mix[None], others, chans
-    )
+    term, down = first_down(at, hidden, width, two[6:])
+    far = other_core(term)
+    mixer = assemble(at, width, two[:6])
+    middle, act, sums = gates(core, own, other, term, far, norm_mix[None], mixer, chans)
     term = mix(
         act,
         sums,
@@ -641,14 +726,13 @@
         ln_gain[None],
         ln_bias[None],
         spatial_weight,
-        spatial_bias.T,
-        others,
+        spatial_bias,
+        mixer,
     )
     send, keep, base = second_pass(
-        core, middle, term, other_core(term), norm_second[None], first, others
+        core, middle, term, other_core(term), norm_second[None], first, down
     )
-    last = keep.astype(jnp.float32) + other_core(send).astype(jnp.float32)
-    return (base.astype(jnp.float32) + 0.5 * last).astype(jnp.bfloat16)
+    return finish(base, keep, other_core(send))
 
 
 def solution(mesh):

time: 252 us -> 259 us (1.028)
  waiting for transfers between devices: 91.7 us -> 109 us
  starting transfers between devices: 65 us -> 51.2 us
  Pallas kernels: 74.5 us -> 85.9 us
  local copies, waits for them, and re-layouts: 16.3 us -> 12.3 us
  other arithmetic: 3.65 us -> 0 us
    ppermute x36, waiting for transfers between devices: 78.6 us -> 99.8 us  [exchange(): return lax.ppermute(x, axis, [(i, i ^ flip) for i in range(4)])]
    ppermute x36, starting transfers between devices: 50 us -> 37.4 us  [exchange(): return lax.ppermute(x, axis, [(i, i ^ flip) for i in range(4)])]
    pallas_call x2 -> x4, Pallas kernels: 32.6 us -> 44.6 us  [the longest x1 22.1 us: second_pass(): pl.pallas_call(functools.partial(second_kernel, blocks), out_shape=[jax.S...]
    ppermute x5, waiting for transfers between devices: 13.1 us -> 9.1 us  [other_core(): return lax.ppermute(x, 'tp', [(0, 1), (1, 0)])]
    unnamed x71 -> x48, local copies, waits for them, and re-layouts: 16.3 us -> 12.3 us
    convert_element_type x1 -> x0, other arithmetic: 3.65 us -> none  [layer(): return (base.astype(jnp.float32) + 0.5 * last).astype(jnp.bfloat16)]
    pallas_call x1, Pallas kernels: 13.9 us -> 10.3 us  [first_down(): pl.pallas_call(down_kernel, out_shape=[jax.ShapeDtypeStruct((count, width...]
  transfers between devices with their start and end apart: 41 -> 41, of which waited for: 15 -> 18; matrix products, arithmetic and copies ran while one was open for 0% -> 0% of each run, Pallas kernels for 8% -> 10%
where the time goes in v3:
time: 259 us
  waiting for transfers between devices  109 us (42%)
  Pallas kernels  85.9 us (33%)
  starting transfers between devices  51.2 us (20%)
  local copies, waits for them, and re-layouts  12.3 us (5%)
    ppermute x36, waiting for transfers between devices, exchange(): return lax.ppermute(x, axis, [(i, i ^ flip) for i in range(4)])  99.8 us
    ppermute x36, starting transfers between devices, exchange(): return lax.ppermute(x, axis, [(i, i ^ flip) for i in range(4)])  37.4 us
    pallas_call x1, Pallas kernels, second_pass(): pl.pallas_call(functools.partial(second_kernel, blocks), out_shape=[jax.S...  22.1 us
    pallas_call x1, Pallas kernels, first_hidden(): pl.pallas_call(first_kernel, out_shape=[jax.ShapeDtypeStruct((count, unit...  16.6 us
    ppermute x5, starting transfers between devices, other_core(): return lax.ppermute(x, 'tp', [(0, 1), (1, 0)])  13.7 us
    pallas_call x1, Pallas kernels, gates(): pl.pallas_call(functools.partial(gates_kernel, blocks), out_shape=[jax.Sh...  12.5 us
    unnamed x48, local copies, waits for them, and re-layouts  12.3 us
    pallas_call x1, Pallas kernels, first_down(): pl.pallas_call(down_kernel, out_shape=[jax.ShapeDtypeStruct((count, width...  10.3 us
  transfers between devices with their start and end apart: 41, of which 18 were waited for; matrix products, arithmetic and copies ran while one was open for 0% of the time, Pallas kernels for 10%

profile of v3, /device:TPU:1, one launch (start us, length us, event | category | flops | bytes accessed | tf_op | source)
XLA Modules:
  0.0 258.5 jit_solution(3912865495765459354)
XLA Ops:
  0.0 2.2 prepare.1
  2.3 2.5 collective-permute-start.21
  4.8 3.1 %collective-permute-done.21.refs_1_ = bf16[32,1792]{1,0:T(8,128)(2,1)S(1)} collective-permute-done((bf16[32,1792]{1,0:T(8,128)(2,1)}, bf16[32,1792]{1,0:T(8,128)(2,1)S(1)}, u32[]{:S(2)}, u32[]{:S(2)}) %collective-permute-start.21) | collective-permute-done | bytes 114720 | tf_op jit(solution)/shard_map/ppermute | solution.py:82
  8.8 2.5 collective-permute-start.22
  12.5 3.5 %collective-permute-done.22.refs_1_ = bf16[64,1792]{1,0:T(8,128)(2,1)S(1)} collective-permute-done((bf16[64,1792]{1,0:T(8,128)(2,1)S(1)}, bf16[64,1792]{1,0:T(8,128)(2,1)S(1)}, u32[]{:S(2)}, u32[]{:S(2)}) %collective-permute-start.22) | collective-permute-done | bytes 229408 | tf_op jit(solution)/shard_map/ppermute | solution.py:82
  18.1 3.3 %collective-permute-start.12 = (bf16[64,1920]{1,0:T(8,128)(2,1)S(1)}, bf16[64,1920]{1,0:T(8,128)(2,1)S(1)}, u32[]{:S(2)}, u32[]{:S(2)}) collective-permute-start(bf16[64,1920]{1,0:T(8,128)(2,1)S(1)} %join.23.refs_0_), channel_id=1, source_target_pairs={{0,96},{32,64},{64,32},{96,0},{1,97},{33,65},{65,33},{97,1},{2,98}... | collective-permute-start | bytes 737288 | tf_op jit(solution)/shard_map/ppermute | solution.py:82
  23.1 3.6 %collective-permute-done.1.refs_1_ = bf16[32,2048]{1,0:T(8,128)(2,1)S(1)} collective-permute-done((bf16[32,2048]{1,0:T(8,128)(2,1)}, bf16[32,2048]{1,0:T(8,128)(2,1)S(1)}, u32[]{:S(2)}, u32[]{:S(2)}) %collective-permute-start.1) | collective-permute-done | bytes 131104 | tf_op jit(solution)/shard_map/ppermute | solution.py:82
  27.6 2.0 collective-permute-start.2
  30.5 3.6 %collective-permute-done.2.refs_1_ = bf16[64,2048]{1,0:T(8,128)(2,1)S(1)} collective-permute-done((bf16[64,2048]{1,0:T(8,128)(2,1)S(1)}, bf16[64,2048]{1,0:T(8,128)(2,1)S(1)}, u32[]{:S(2)}, u32[]{:S(2)}) %collective-permute-start.2) | collective-permute-done | bytes 262176 | tf_op jit(solution)/shard_map/ppermute | solution.py:82
  35.7 2.2 collective-permute-done.13.refs_2_
  40.0 2.8 %collective-permute-start.4 = (bf16[128,1024]{1,0:T(8,128)(2,1)S(1)}, bf16[128,1024]{1,0:T(8,128)(2,1)S(1)}, u32[]{:S(2)}, u32[]{:S(2)}) collective-permute-start(bf16[128,1024]{1,0:T(8,128)(2,1)S(1)} %get-tuple-element.50.refs_1_), channel_id=1, source_target_pairs={{0,6},{2,4},{4,2},{6,0},{1,7},{3,5},{5,3},{7,1},{8,14},{10,12},{12... | collective-permute-start | bytes 786440 | tf_op jit(solution)/shard_map/ppermute | solution.py:82
  43.8 3.0 %collective-permute-done.4.refs_3_ = bf16[128,1024]{1,0:T(8,128)(2,1)S(1)} collective-permute-done((bf16[128,1024]{1,0:T(8,128)(2,1)S(1)}, bf16[128,1024]{1,0:T(8,128)(2,1)S(1)}, u32[]{:S(2)}, u32[]{:S(2)}) %collective-permute-start.4) | collective-permute-done | bytes 262176 | tf_op jit(solution)/shard_map/ppermute | solution.py:82
  46.8 2.8 %collective-permute-start.5 = (bf16[256,1024]{1,0:T(8,128)(2,1)S(1)}, bf16[256,1024]{1,0:T(8,128)(2,1)S(1)}, u32[]{:S(2)}, u32[]{:S(2)}) collective-permute-start(bf16[256,1024]{1,0:T(8,128)(2,1)S(1)} %get-tuple-element.51.refs_0_), channel_id=1, source_target_pairs={{0,6},{2,4},{4,2},{6,0},{1,7},{3,5},{5,3},{7,1},{8,14},{10,12},{12... | collective-permute-start | bytes 1572872 | tf_op jit(solution)/shard_map/ppermute | solution.py:82
  50.4 8.8 %collective-permute-done.5.refs_2_ = bf16[256,1024]{1,0:T(8,128)(2,1)S(1)} collective-permute-done((bf16[256,1024]{1,0:T(8,128)(2,1)S(1)}, bf16[256,1024]{1,0:T(8,128)(2,1)S(1)}, u32[]{:S(2)}, u32[]{:S(2)}) %collective-permute-start.5) | collective-permute-done | bytes 524320 | tf_op jit(solution)/shard_map/ppermute | solution.py:82
  59.3 2.7 %collective-permute-start.17 = (bf16[512,1024]{1,0:T(8,128)(2,1)S(1)}, bf16[512,1024]{1,0:T(8,128)(2,1)S(1)}, u32[]{:S(2)}, u32[]{:S(2)}) collective-permute-start(bf16[512,1024]{1,0:T(8,128)(2,1)S(1)} %get-tuple-element.62.refs_0_), channel_id=1, source_target_pairs={{0,6},{2,4},{4,2},{6,0},{1,7},{3,5},{5,3},{7,1},{8,14},{10,12},{12... | collective-permute-start | bytes 3145736 | tf_op jit(solution)/shard_map/ppermute | solution.py:82
  61.9 8.3 %collective-permute-done.6.refs_3_ = bf16[256,1024]{1,0:T(8,128)(2,1)S(1)} collective-permute-done((bf16[256,1024]{1,0:T(8,128)(2,1)S(1)}, bf16[256,1024]{1,0:T(8,128)(2,1)S(1)}, u32[]{:S(2)}, u32[]{:S(2)}) %collective-permute-start.6) | collective-permute-done | bytes 524320 | tf_op jit(solution)/shard_map/ppermute | solution.py:82
  70.3 8.8 %collective-permute-start = (bf16[640,1024]{1,0:T(8,128)(2,1)S(1)}, bf16[640,1024]{1,0:T(8,128)(2,1)S(1)}, u32[]{:S(2)}, u32[]{:S(2)}) collective-permute-start(bf16[640,1024]{1,0:T(8,128)(2,1)S(1)} %copy-done.13), channel_id=1, source_target_pairs={{0,1},{1,0},{2,3},{3,2},{4,5},{5,4},{6,7},{7,6},{8,9},{9,8},{10,11... | collective-permute-start | bytes 3932168 | tf_op jit(solution)/shard_map/ppermute | solution.py:36
  82.6 21.4 %collective-permute-done.7.refs_2_ = bf16[512,1024]{1,0:T(8,128)(2,1)S(1)} collective-permute-done((bf16[512,1024]{1,0:T(8,128)(2,1)S(1)}, bf16[512,1024]{1,0:T(8,128)(2,1)S(1)}, u32[]{:S(2)}, u32[]{:S(2)}) %collective-permute-start.7) | collective-permute-done | bytes 1048608 | tf_op jit(solution)/shard_map/ppermute | solution.py:82
  110.5 13.0 %collective-permute-done.30.rest_11_ = bf16[1024,384]{1,0:T(8,128)(2,1)S(1)} collective-permute-done((bf16[1024,384]{1,0:T(8,128)(2,1)S(1)}, bf16[1024,384]{1,0:T(8,128)(2,1)S(1)}, u32[]{:S(2)}, u32[]{:S(2)}) %collective-permute-start.30) | collective-permute-done | bytes 786464 | tf_op jit(solution)/shard_map/ppermute | solution.py:82
  128.1 2.5 collective-permute-done.20.rest_7_
  131.9 16.6 %first_hidden.1 = (bf16[640,1408]{1,0:T(8,128)(2,1)}, bf16[2048,2816]{1,0:T(8,128)(2,1)}) custom-call(s32[1]{0:T(128)} %bitcast.core, s32[1]{0:T(128)} %bitcast.1.at, bf16[640,1024]{1,0:T(8,128)(2,1)} %own.3, bf16[640,1024]{1,0:T(8,128)(2,1)} %copy-done.14, f32[1,2048]{1,0:T(1,128)} %bitcast.15, bf16[1024,512]{1,0:T(8,128)(2,1)} %get-tuple-element.55.rest_0_, ...), custom_call_target="tpu_custom_call" | custom-call | flops 7381975040 | bytes 23068672 | tf_op jit(solution)/shard_map/first_hidden/pallas_call | solution.py:302
  148.5 2.0 collective-permute-done.31.rest_1_
  150.5 10.3 %first_down.1 = (bf16[640,2048]{1,0:T(8,128)(2,1)}, bf16[2048,1408]{1,0:T(8,128)(2,1)}) custom-call(s32[1]{0:T(128)} %bitcast.1.at, bf16[640,1408]{1,0:T(8,128)(2,1)} %get-tuple-element.75.hidden, bf16[1024,384]{1,0:T(8,128)(2,1)} %get-tuple-element.76.rest_0_, bf16[1024,384]{1,0:T(8,128)(2,1)} %collective-permute-done.31.rest_1_, ...), custom_call_target="tpu_custom_call" | custom-call | flops 3690987520 | bytes 11534336 | tf_op jit(solution)/shard_map/first_down/pallas_call | solution.py:355
  160.8 2.8 %collective-permute-start.34 = (bf16[640,2048]{1,0:T(8,128)(2,1)}, bf16[640,2048]{1,0:T(8,128)(2,1)}, u32[]{:S(2)}, u32[]{:S(2)}) collective-permute-start(bf16[640,2048]{1,0:T(8,128)(2,1)} %get-tuple-element.79.term), channel_id=1, source_target_pairs={{0,1},{1,0},{2,3},{3,2},{4,5},{5,4},{6,7},{7,6},{8,9},{9,8},{10,11... | collective-permute-start | bytes 7864328 | tf_op jit(solution)/shard_map/ppermute | solution.py:36
  166.0 22.5 %collective-permute-done.37.rest_5_ = bf16[1024,512]{1,0:T(8,128)(2,1)S(1)} collective-permute-done((bf16[1024,512]{1,0:T(8,128)(2,1)}, bf16[1024,512]{1,0:T(8,128)(2,1)S(1)}, u32[]{:S(2)}, u32[]{:S(2)}) %collective-permute-start.37) | collective-permute-done | bytes 1048608 | tf_op jit(solution)/shard_map/ppermute | solution.py:82
  192.3 5.3 %assemble.1.rows = bf16[2048,1536]{1,0:T(8,128)(2,1)} custom-call(s32[1]{0:T(128)} %bitcast.1.at, bf16[1024,512]{1,0:T(8,128)(2,1)} %copy-done.8, bf16[1024,512]{1,0:T(8,128)(2,1)} %copy-done.20, bf16[1024,512]{1,0:T(8,128)(2,1)} %copy-done.9, bf16[1024,512]{1,0:T(8,128)(2,1)} %copy-done.21, bf16[1024,512]{1,0:T(8,128)(2,1)} %copy-done.7, ...), custom_call_target="tpu_custom_call" | custom-call | flops 5000000000 | bytes 25165824 | tf_op jit(solution)/shard_map/assemble/pallas_call | solution.py:395
  197.6 12.5 %gates.1 = (bf16[640,2048]{1,0:T(8,128)(2,1)}, f32[2,640,512]{2,1,0:T(8,128)}, f32[640,128]{1,0:T(8,128)}) custom-call(s32[1]{0:T(128)} %bitcast.core, bf16[640,1024]{1,0:T(8,128)(2,1)} %own.3, bf16[640,1024]{1,0:T(8,128)(2,1)} %copy-done.14, bf16[640,2048]{1,0:T(8,128)(2,1)} %get-tuple-element.79.term, bf16[640,2048]{1,0:T(8,128)(2,1)} %collective-permute-done.34.far, ...), custom_call_target="tpu_custom_call" | custom-call | flops 2684354560 | bytes 4194304 | tf_op jit(solution)/shard_map/gates/pallas_call | solution.py:450
  213.6 7.0 %mix.1.term = bf16[640,2048]{1,0:T(8,128)(2,1)} custom-call(f32[2,640,512]{2,1,0:T(8,128)} %get-tuple-element.84.act, f32[640,128]{1,0:T(8,128)} %get-tuple-element.85.sums, f32[640,128]{1,0:T(8,128)} %copy-done.15, f32[1,512]{1,0:T(1,128)} %bitcast.13, f32[1,512]{1,0:T(1,128)} %bitcast.14, bf16[4,128,128]{2,1,0:T(8,128)(2,1)} %weight.1, f32[4,128]{1,0:T(4,128)} %shift.1, ...), custom_call_target="tpu_custom_call" | custom-call | flops 1342177280 | bytes 2097152 | tf_op jit(solution)/shard_map/mix/pallas_call | solution.py:518
  221.0 4.7 %collective-permute-done.39.far = bf16[640,2048]{1,0:T(8,128)(2,1)S(1)} collective-permute-done((bf16[640,2048]{1,0:T(8,128)(2,1)}, bf16[640,2048]{1,0:T(8,128)(2,1)S(1)}, u32[]{:S(2)}, u32[]{:S(2)}) %collective-permute-start.39) | collective-permute-done | bytes 2621472 | tf_op jit(solution)/shard_map/ppermute | solution.py:36
  227.3 22.1 %second_pass.1 = (bf16[640,1024]{1,0:T(8,128)(2,1)}, bf16[640,1024]{1,0:T(8,128)(2,1)}, bf16[640,1024]{1,0:T(8,128)(2,1)}) custom-call(s32[1]{0:T(128)} %bitcast.core, bf16[640,2048]{1,0:T(8,128)(2,1)} %get-tuple-element.83.middle, bf16[640,2048]{1,0:T(8,128)(2,1)} %mix.1.term, bf16[640,2048]{1,0:T(8,128)(2,1)} %copy-done.16, f32[1,2048]{1,0:T(1,128)} %bitcast.16, ...), custom_call_target="tpu_custom_call" | custom-call | flops 11072962560 | bytes 17301504 | tf_op jit(solution)/shard_map/second_pass/pallas_call | solution.py:621
  249.8 2.9 %collective-permute-done.40.far = bf16[640,1024]{1,0:T(8,128)(2,1)S(1)} collective-permute-done((bf16[640,1024]{1,0:T(8,128)(2,1)}, bf16[640,1024]{1,0:T(8,128)(2,1)S(1)}, u32[]{:S(2)}, u32[]{:S(2)}) %collective-permute-start.40) | collective-permute-done | bytes 1310752 | tf_op jit(solution)/shard_map/ppermute | solution.py:36
  253.8 4.8 %finish.1 = bf16[640,1024]{1,0:T(8,128)(2,1)} custom-call(bf16[640,1024]{1,0:T(8,128)(2,1)} %get-tuple-element.88.base, bf16[640,1024]{1,0:T(8,128)(2,1)} %get-tuple-element.89.keep, bf16[640,1024]{1,0:T(8,128)(2,1)} %copy-done.12), custom_call_target="tpu_custom_call" | custom-call | flops 2621440 | bytes 5242880 | tf_op jit(solution)/shard_map/finish/pallas_call | solution.py:655
  (124 shorter events, 42.3 us)
Async XLA Ops:
  8.8 7.2 %collective-permute-start.22 = (bf16[64,1792]{1,0:T(8,128)(2,1)S(1)}, bf16[64,1792]{1,0:T(8,128)(2,1)S(1)}, u32[]{:S(2)}, u32[]{:S(2)}) collective-permute-start(bf16[64,1792]{1,0:T(8,128)(2,1)S(1)} %join.28.refs_0_), channel_id=1, source_target_pairs={{0,6},{2,4},{4,2},{6,0},{1,7},{3,5},{5,3},{7,1},{8,14},{10,12},{12... | collective-permute-start | bytes 688136 | tf_op jit(solution)/shard_map/ppermute | solution.py:82
  16.0 6.9 %collective-permute-start.23 = (bf16[128,896]{1,0:T(8,128)(2,1)S(1)}, bf16[128,896]{1,0:T(8,128)(2,1)S(1)}, u32[]{:S(2)}, u32[]{:S(2)}) collective-permute-start(bf16[128,896]{1,0:T(8,128)(2,1)S(1)} %get-tuple-element.67.refs_0_), channel_id=1, source_target_pairs={{0,8},{8,0},{16,24},{24,16},{1,9},{9,1},{17,25},{25,17},{2,10},{10... | collective-permute-start | bytes 688136 | tf_op jit(solution)/shard_map/ppermute | solution.py:82
  18.1 11.5 %collective-permute-start.12 = (bf16[64,1920]{1,0:T(8,128)(2,1)S(1)}, bf16[64,1920]{1,0:T(8,128)(2,1)S(1)}, u32[]{:S(2)}, u32[]{:S(2)}) collective-permute-start(bf16[64,1920]{1,0:T(8,128)(2,1)S(1)} %join.23.refs_0_), channel_id=1, source_target_pairs={{0,96},{32,64},{64,32},{96,0},{1,97},{33,65},{65,33},{97,1},{2,98}... | collective-permute-start | bytes 737288 | tf_op jit(solution)/shard_map/ppermute | solution.py:82
  23.0 17.0 %collective-permute-start.25 = (bf16[256,896]{1,0:T(8,128)(2,1)S(1)}, bf16[256,896]{1,0:T(8,128)(2,1)S(1)}, u32[]{:S(2)}, u32[]{:S(2)}) collective-permute-start(bf16[256,896]{1,0:T(8,128)(2,1)S(1)} %get-tuple-element.69.refs_0_), channel_id=1, source_target_pairs={{0,2},{2,0},{4,6},{6,4},{1,3},{3,1},{5,7},{7,5},{8,10},{10,8},{12,... | collective-permute-start | bytes 1376264 | tf_op jit(solution)/shard_map/ppermute | solution.py:82
  29.6 8.2 %collective-permute-start.13 = (bf16[128,1024]{1,0:T(8,128)(2,1)S(1)}, bf16[128,1024]{1,0:T(8,128)(2,1)S(1)}, u32[]{:S(2)}, u32[]{:S(2)}) collective-permute-start(bf16[128,1024]{1,0:T(8,128)(2,1)S(1)} %get-tuple-element.58.refs_0_), channel_id=1, source_target_pairs={{0,24},{8,16},{16,8},{24,0},{1,25},{9,17},{17,9},{25,1},{2,26},{10... | collective-permute-start | bytes 786440 | tf_op jit(solution)/shard_map/ppermute | solution.py:82
  30.5 12.2 %collective-permute-start.26 = (bf16[256,896]{1,0:T(8,128)(2,1)S(1)}, bf16[256,896]{1,0:T(8,128)(2,1)S(1)}, u32[]{:S(2)}, u32[]{:S(2)}) collective-permute-start(bf16[256,896]{1,0:T(8,128)(2,1)S(1)} %get-tuple-element.70.refs_1_), channel_id=1, source_target_pairs={{0,8},{8,0},{16,24},{24,16},{1,9},{9,1},{17,25},{25,17},{2,10},{10... | collective-permute-start | bytes 1376264 | tf_op jit(solution)/shard_map/ppermute | solution.py:82
  34.2 8.8 %collective-permute-start.3 = (bf16[128,1024]{1,0:T(8,128)(2,1)S(1)}, bf16[128,1024]{1,0:T(8,128)(2,1)S(1)}, u32[]{:S(2)}, u32[]{:S(2)}) collective-permute-start(bf16[128,1024]{1,0:T(8,128)(2,1)S(1)} %get-tuple-element.49.refs_0_), channel_id=1, source_target_pairs={{0,96},{32,64},{64,32},{96,0},{1,97},{33,65},{65,33},{97,1},{2,98}... | collective-permute-start | bytes 786440 | tf_op jit(solution)/shard_map/ppermute | solution.py:82
  38.0 11.6 %collective-permute-start.16 = (bf16[256,896]{1,0:T(8,128)(2,1)S(1)}, bf16[256,896]{1,0:T(8,128)(2,1)S(1)}, u32[]{:S(2)}, u32[]{:S(2)}) collective-permute-start(bf16[256,896]{1,0:T(8,128)(2,1)S(1)} %get-tuple-element.61.refs_1_), channel_id=1, source_target_pairs={{0,24},{8,16},{16,8},{24,0},{1,25},{9,17},{17,9},{25,1},{2,26},{10... | collective-permute-start | bytes 1376264 | tf_op jit(solution)/shard_map/ppermute | solution.py:82
  39.9 9.6 %collective-permute-start.15 = (bf16[256,1024]{1,0:T(8,128)(2,1)S(1)}, bf16[256,1024]{1,0:T(8,128)(2,1)S(1)}, u32[]{:S(2)}, u32[]{:S(2)}) collective-permute-start(bf16[256,1024]{1,0:T(8,128)(2,1)S(1)} %get-tuple-element.60.refs_0_), channel_id=1, source_target_pairs={{0,32},{32,0},{64,96},{96,64},{1,33},{33,1},{65,97},{97,65},{2,34}... | collective-permute-start | bytes 1572872 | tf_op jit(solution)/shard_map/ppermute | solution.py:82
  40.0 6.8 %collective-permute-start.4 = (bf16[128,1024]{1,0:T(8,128)(2,1)S(1)}, bf16[128,1024]{1,0:T(8,128)(2,1)S(1)}, u32[]{:S(2)}, u32[]{:S(2)}) collective-permute-start(bf16[128,1024]{1,0:T(8,128)(2,1)S(1)} %get-tuple-element.50.refs_1_), channel_id=1, source_target_pairs={{0,6},{2,4},{4,2},{6,0},{1,7},{3,5},{5,3},{7,1},{8,14},{10,12},{12... | collective-permute-start | bytes 786440 | tf_op jit(solution)/shard_map/ppermute | solution.py:82
  42.8 36.3 %collective-permute-start.27 = (bf16[512,896]{1,0:T(8,128)(2,1)S(1)}, bf16[512,896]{1,0:T(8,128)(2,1)S(1)}, u32[]{:S(2)}, u32[]{:S(2)}) collective-permute-start(bf16[512,896]{1,0:T(8,128)(2,1)S(1)} %get-tuple-element.71.refs_0_), channel_id=1, source_target_pairs={{0,96},{32,64},{64,32},{96,0},{1,97},{33,65},{65,33},{97,1},{2,98}... | collective-permute-start | bytes 2752520 | tf_op jit(solution)/shard_map/ppermute | solution.py:82
  43.0 36.3 %collective-permute-start.28 = (bf16[512,896]{1,0:T(8,128)(2,1)S(1)}, bf16[512,896]{1,0:T(8,128)(2,1)S(1)}, u32[]{:S(2)}, u32[]{:S(2)}) collective-permute-start(bf16[512,896]{1,0:T(8,128)(2,1)S(1)} %get-tuple-element.72.refs_1_), channel_id=1, source_target_pairs={{0,24},{8,16},{16,8},{24,0},{1,25},{9,17},{17,9},{25,1},{2,26},{10... | collective-permute-start | bytes 2752520 | tf_op jit(solution)/shard_map/ppermute | solution.py:82
  46.8 12.4 %collective-permute-start.5 = (bf16[256,1024]{1,0:T(8,128)(2,1)S(1)}, bf16[256,1024]{1,0:T(8,128)(2,1)S(1)}, u32[]{:S(2)}, u32[]{:S(2)}) collective-permute-start(bf16[256,1024]{1,0:T(8,128)(2,1)S(1)} %get-tuple-element.51.refs_0_), channel_id=1, source_target_pairs={{0,6},{2,4},{4,2},{6,0},{1,7},{3,5},{5,3},{7,1},{8,14},{10,12},{12... | collective-permute-start | bytes 1572872 | tf_op jit(solution)/shard_map/ppermute | solution.py:82
  49.6 20.7 %collective-permute-start.6 = (bf16[256,1024]{1,0:T(8,128)(2,1)S(1)}, bf16[256,1024]{1,0:T(8,128)(2,1)S(1)}, u32[]{:S(2)}, u32[]{:S(2)}) collective-permute-start(bf16[256,1024]{1,0:T(8,128)(2,1)S(1)} %get-tuple-element.52.refs_1_), channel_id=1, source_target_pairs={{0,96},{32,64},{64,32},{96,0},{1,97},{33,65},{65,33},{97,1},{2,98}... | collective-permute-start | bytes 1572872 | tf_op jit(solution)/shard_map/ppermute | solution.py:82
  49.7 29.8 %collective-permute-start.18 = (bf16[512,896]{1,0:T(8,128)(2,1)S(1)}, bf16[512,896]{1,0:T(8,128)(2,1)S(1)}, u32[]{:S(2)}, u32[]{:S(2)}) collective-permute-start(bf16[512,896]{1,0:T(8,128)(2,1)S(1)} %get-tuple-element.63.refs_1_), channel_id=1, source_target_pairs={{0,2},{2,0},{4,6},{6,4},{1,3},{3,1},{5,7},{7,5},{8,10},{10,8},{12,... | collective-permute-start | bytes 2752520 | tf_op jit(solution)/shard_map/ppermute | solution.py:82
  59.3 22.3 %collective-permute-start.17 = (bf16[512,1024]{1,0:T(8,128)(2,1)S(1)}, bf16[512,1024]{1,0:T(8,128)(2,1)S(1)}, u32[]{:S(2)}, u32[]{:S(2)}) collective-permute-start(bf16[512,1024]{1,0:T(8,128)(2,1)S(1)} %get-tuple-element.62.refs_0_), channel_id=1, source_target_pairs={{0,6},{2,4},{4,2},{6,0},{1,7},{3,5},{5,3},{7,1},{8,14},{10,12},{12... | collective-permute-start | bytes 3145736 | tf_op jit(solution)/shard_map/ppermute | solution.py:82
  70.3 37.3 %collective-permute-start = (bf16[640,1024]{1,0:T(8,128)(2,1)S(1)}, bf16[640,1024]{1,0:T(8,128)(2,1)S(1)}, u32[]{:S(2)}, u32[]{:S(2)}) collective-permute-start(bf16[640,1024]{1,0:T(8,128)(2,1)S(1)} %copy-done.13), channel_id=1, source_target_pairs={{0,1},{1,0},{2,3},{3,2},{4,5},{5,4},{6,7},{7,6},{8,9},{9,8},{10,11... | collective-permute-start | bytes 3932168 | tf_op jit(solution)/shard_map/ppermute | solution.py:36
  79.2 24.8 %collective-permute-start.7 = (bf16[512,1024]{1,0:T(8,128)(2,1)S(1)}, bf16[512,1024]{1,0:T(8,128)(2,1)S(1)}, u32[]{:S(2)}, u32[]{:S(2)}) collective-permute-start(bf16[512,1024]{1,0:T(8,128)(2,1)S(1)} %get-tuple-element.53.refs_0_), channel_id=1, source_target_pairs={{0,32},{32,0},{64,96},{96,64},{1,33},{33,1},{65,97},{97,65},{2,34}... | collective-permute-start | bytes 3145736 | tf_op jit(solution)/shard_map/ppermute | solution.py:82
  79.3 26.5 %collective-permute-start.8 = (bf16[512,1024]{1,0:T(8,128)(2,1)S(1)}, bf16[512,1024]{1,0:T(8,128)(2,1)S(1)}, u32[]{:S(2)}, u32[]{:S(2)}) collective-permute-start(bf16[512,1024]{1,0:T(8,128)(2,1)S(1)} %get-tuple-element.54.refs_1_), channel_id=1, source_target_pairs={{0,8},{8,0},{16,24},{24,16},{1,9},{9,1},{17,25},{25,17},{2,10},{10... | collective-permute-start | bytes 3145736 | tf_op jit(solution)/shard_map/ppermute | solution.py:82
  79.6 28.3 %collective-permute-start.29 = (bf16[1024,384]{1,0:T(8,128)(2,1)S(1)}, bf16[1024,384]{1,0:T(8,128)(2,1)S(1)}, u32[]{:S(2)}, u32[]{:S(2)}) collective-permute-start(bf16[1024,384]{1,0:T(8,128)(2,1)S(1)} %get-tuple-element.73.rest_8_), channel_id=1, source_target_pairs={{0,24},{8,16},{16,8},{24,0},{1,25},{9,17},{17,9},{25,1},{2,26},{10... | collective-permute-start | bytes 2359304 | tf_op jit(solution)/shard_map/ppermute | solution.py:82
  81.7 43.6 %collective-permute-start.19 = (bf16[1024,512]{1,0:T(8,128)(2,1)S(1)}, bf16[1024,512]{1,0:T(8,128)(2,1)S(1)}, u32[]{:S(2)}, u32[]{:S(2)}) collective-permute-start(bf16[1024,512]{1,0:T(8,128)(2,1)S(1)} %get-tuple-element.64.rest_4_), channel_id=1, source_target_pairs={{0,2},{2,0},{4,6},{6,4},{1,3},{3,1},{5,7},{7,5},{8,10},{10,8},{12,... | collective-permute-start | bytes 3145736 | tf_op jit(solution)/shard_map/ppermute | solution.py:82
  104.0 19.4 %collective-permute-start.30 = (bf16[1024,384]{1,0:T(8,128)(2,1)S(1)}, bf16[1024,384]{1,0:T(8,128)(2,1)S(1)}, u32[]{:S(2)}, u32[]{:S(2)}) collective-permute-start(bf16[1024,384]{1,0:T(8,128)(2,1)S(1)} %get-tuple-element.74.rest_10_), channel_id=1, source_target_pairs={{0,96},{32,64},{64,32},{96,0},{1,97},{33,65},{65,33},{97,1},{2,98}... | collective-permute-start | bytes 2359304 | tf_op jit(solution)/shard_map/ppermute | solution.py:82
  105.8 24.9 %collective-permute-start.20 = (bf16[1024,512]{1,0:T(8,128)(2,1)S(1)}, bf16[1024,512]{1,0:T(8,128)(2,1)S(1)}, u32[]{:S(2)}, u32[]{:S(2)}) collective-permute-start(bf16[1024,512]{1,0:T(8,128)(2,1)S(1)} %get-tuple-element.65.rest_6_), channel_id=1, source_target_pairs={{0,6},{2,4},{4,2},{6,0},{1,7},{3,5},{5,3},{7,1},{8,14},{10,12},{12... | collective-permute-start | bytes 3145736 | tf_op jit(solution)/shard_map/ppermute | solution.py:82
  107.6 24.3 %collective-permute-start.9 = (bf16[1024,512]{1,0:T(8,128)(2,1)}, bf16[1024,512]{1,0:T(8,128)(2,1)}, u32[]{:S(2)}, u32[]{:S(2)}) collective-permute-start(bf16[1024,512]{1,0:T(8,128)(2,1)} %get-tuple-element.55.rest_0_), channel_id=1, source_target_pairs={{0,8},{8,0},{16,24},{24,16},{1,9},{9,1},{17,25},{25,17},{2,10},{10... | collective-permute-start | bytes 3145736 | tf_op jit(solution)/shard_map/ppermute | solution.py:82
  107.9 24.0 %collective-permute-start.10 = (bf16[1024,512]{1,0:T(8,128)(2,1)}, bf16[1024,512]{1,0:T(8,128)(2,1)}, u32[]{:S(2)}, u32[]{:S(2)}) collective-permute-start(bf16[1024,512]{1,0:T(8,128)(2,1)} %get-tuple-element.56.rest_2_), channel_id=1, source_target_pairs={{0,32},{32,0},{64,96},{96,64},{1,33},{33,1},{65,97},{97,65},{2,34}... | collective-permute-start | bytes 3145736 | tf_op jit(solution)/shard_map/ppermute | solution.py:82
  123.4 27.0 %collective-permute-start.32 = (bf16[1024,512]{1,0:T(8,128)(2,1)}, bf16[1024,512]{1,0:T(8,128)(2,1)}, u32[]{:S(2)}, u32[]{:S(2)}) collective-permute-start(bf16[1024,512]{1,0:T(8,128)(2,1)} %get-tuple-element.77.rest_2_), channel_id=1, source_target_pairs={{0,24},{8,16},{16,8},{24,0},{1,25},{9,17},{17,9},{25,1},{2,26},{10... | collective-permute-start | bytes 3145736 | tf_op jit(solution)/shard_map/ppermute | solution.py:82
  125.4 25.1 %collective-permute-start.33 = (bf16[1024,512]{1,0:T(8,128)(2,1)}, bf16[1024,512]{1,0:T(8,128)(2,1)}, u32[]{:S(2)}, u32[]{:S(2)}) collective-permute-start(bf16[1024,512]{1,0:T(8,128)(2,1)} %get-tuple-element.78.rest_4_), channel_id=1, source_target_pairs={{0,96},{32,64},{64,32},{96,0},{1,97},{33,65},{65,33},{97,1},{2,98}... | collective-permute-start | bytes 3145736 | tf_op jit(solution)/shard_map/ppermute | solution.py:82
  131.7 18.7 %collective-permute-start.31 = (bf16[1024,384]{1,0:T(8,128)(2,1)}, bf16[1024,384]{1,0:T(8,128)(2,1)}, u32[]{:S(2)}, u32[]{:S(2)}) collective-permute-start(bf16[1024,384]{1,0:T(8,128)(2,1)} %get-tuple-element.76.rest_0_), channel_id=1, source_target_pairs={{0,6},{2,4},{4,2},{6,0},{1,7},{3,5},{5,3},{7,1},{8,14},{10,12},{12... | collective-permute-start | bytes 2359304 | tf_op jit(solution)/shard_map/ppermute | solution.py:82
  160.8 36.8 %collective-permute-start.34 = (bf16[640,2048]{1,0:T(8,128)(2,1)}, bf16[640,2048]{1,0:T(8,128)(2,1)}, u32[]{:S(2)}, u32[]{:S(2)}) collective-permute-start(bf16[640,2048]{1,0:T(8,128)(2,1)} %get-tuple-element.79.term), channel_id=1, source_target_pairs={{0,1},{1,0},{2,3},{3,2},{4,5},{5,4},{6,7},{7,6},{8,9},{9,8},{10,11... | collective-permute-start | bytes 7864328 | tf_op jit(solution)/shard_map/ppermute | solution.py:36
  163.6 24.8 %collective-permute-start.37 = (bf16[1024,512]{1,0:T(8,128)(2,1)}, bf16[1024,512]{1,0:T(8,128)(2,1)S(1)}, u32[]{:S(2)}, u32[]{:S(2)}) collective-permute-start(bf16[1024,512]{1,0:T(8,128)(2,1)} %copy-done.7), channel_id=1, source_target_pairs={{0,2},{2,0},{4,6},{6,4},{1,3},{3,1},{5,7},{7,5},{8,10},{10,8},{12,... | collective-permute-start | bytes 3145736 | tf_op jit(solution)/shard_map/ppermute | solution.py:82
  166.0 24.3 %collective-permute-start.35 = (bf16[1024,512]{1,0:T(8,128)(2,1)S(1)}, bf16[1024,512]{1,0:T(8,128)(2,1)S(1)}, u32[]{:S(2)}, u32[]{:S(2)}) collective-permute-start(bf16[1024,512]{1,0:T(8,128)(2,1)S(1)} %get-tuple-element.80.rest_0_), channel_id=1, source_target_pairs={{0,8},{8,0},{16,24},{24,16},{1,9},{9,1},{17,25},{25,17},{2,10},{10... | collective-permute-start | bytes 3145736 | tf_op jit(solution)/shard_map/ppermute | solution.py:82
  166.0 24.4 %collective-permute-start.36 = (bf16[1024,512]{1,0:T(8,128)(2,1)S(1)}, bf16[1024,512]{1,0:T(8,128)(2,1)S(1)}, u32[]{:S(2)}, u32[]{:S(2)}) collective-permute-start(bf16[1024,512]{1,0:T(8,128)(2,1)S(1)} %get-tuple-element.81.rest_2_), channel_id=1, source_target_pairs={{0,32},{32,0},{64,96},{96,64},{1,33},{33,1},{65,97},{97,65},{2,34}... | collective-permute-start | bytes 3145736 | tf_op jit(solution)/shard_map/ppermute | solution.py:82
  (33 other events, 286.9 us)

commit v4 on v3

--- a/solution.py
+++ b/solution.py
@@ -172,6 +172,24 @@
         joined[pl.ds(rows, rows), :] = arrived[:, begin:end]
 
 
+def cut_kernel(*refs):
+    for k in range(len(refs) // 2):
+        refs[len(refs) // 2 + k][...] = refs[k][:, : refs[len(refs) // 2 + k].shape[1]]
+
+
+def first_columns(arrays, widths):
+    return pl.pallas_call(
+        cut_kernel,
+        out_shape=[
+            jax.ShapeDtypeStruct((x.shape[0], n * LANES), x.dtype) for x, n in zip(arrays, widths)
+        ],
+        in_specs=[VMEM] * len(arrays),
+        out_specs=[VMEM] * len(arrays),
+        compiler_params=pltpu.CompilerParams(vmem_limit_bytes=16 * 1024 * 1024),
+        name="first_columns",
+    )(*arrays)
+
+
 def join(held, arrived, cuts=None):
     rows, low = held[0].shape[0], jnp.bfloat16
     if cuts is None:
@@ -193,39 +211,42 @@
         edge = WIDTHS[2 * p]
         cuts = [(0, 0, edge), (0, edge, held.shape[1])]
         held = join([held], [exchange(held, 2 * p, 1)], cuts)
-        for turn in (2, 3):
-            held = join(held, [exchange(y, 2 * p + k, turn) for k, y in enumerate(held)])
+        held = join(held, [exchange(y, 2 * p + k, 2) for k, y in enumerate(held)])
+        arrived = [exchange(y, 2 * p + k, 3) for k, y in enumerate(held)]
+        held = join(held, arrived)
         ready.append((held, [exchange(y, 2 * p + k, 4) for k, y in enumerate(held)]))
-    groups = []
-    for g in range(2):
-        pieces = []
-        for p, (held, arrived) in enumerate(ready):
-            cuts = []
-            for k, y in enumerate(held):
-                edge = FIRST[2 * p + k] * LANES
-                cuts.append((k, edge, y.shape[1]) if g else (k, 0, edge))
-            halves = join(held, arrived, cuts)
-            for k, y in enumerate(halves):
-                pieces += [y, exchange(y, 2 * p + k, 5)]
-        groups.append(pieces)
-    return groups
+    one, two = [], []
+    for p, (held, arrived) in enumerate(ready):
+        kept = first_columns(held, FIRST[2 * p : 2 * p + 2])
+        early = [exchange(x, 2 * p + k, 5) for k, x in enumerate(kept)]
+        come = first_columns(arrived, FIRST[2 * p : 2 * p + 2])
+        late = [exchange(x, 2 * p + k, 5) for k, x in enumerate(come)]
+        for k in range(2):
+            one += [kept[k], come[k], early[k], late[k]]
+        cuts = [(k, FIRST[2 * p + k] * LANES, y.shape[1]) for k, y in enumerate(held)]
+        halves = join(held, arrived, cuts)
+        for k, y in enumerate(halves):
+            two += [y, exchange(y, 2 * p + k, 5)]
+    return one, two
 
 
 def place_blocks(at, pieces, weight, sems, widths, colors, first=0):
     begin = starts(widths)
+    parts = len(pieces) // len(widths)
+    slots = 64 // parts
     for c in colors:
         columns = pl.ds(begin[c], widths[c] * LANES)
-        for k in range(2):
+        for k in range(parts):
 
             def copy_four(high, carry, c=c, k=k, columns=columns):
-                moved = at ^ place(first + c, 32 * k)
-                for bit in range(3):
+                moved = at ^ place(first + c, slots * k)
+                for bit in range(slots.bit_length() - 3):
                     moved = moved ^ ((high >> bit & 1) * place(first + c, 4 << bit))
                 for low in range(4):
                     to = (moved ^ place(first + c, low)) * HALF_ROWS
                     origin = (high * 4 + low) * HALF_ROWS
                     pltpu.make_async_copy(
-                        pieces[2 * c + k].at[
+                        pieces[parts * c + k].at[
                             pl.ds(pl.multiple_of(origin, HALF_ROWS), HALF_ROWS), :
                         ],
                         weight.at[pl.ds(pl.multiple_of(to, HALF_ROWS), HALF_ROWS), columns],
@@ -233,7 +254,7 @@
                     ).start()
                 return carry
 
-            lax.fori_loop(0, 8, copy_four, 0)
+            lax.fori_loop(0, slots // 4, copy_four, 0)
 
 
 def wait_color(weight, sems, widths, c):
@@ -268,7 +289,7 @@
 
 
 def first_kernel(core, at, own, other, gain, *rest):
-    pieces, (hidden, kept, weight, normed, sems, out_sem) = rest[:12], rest[12:]
+    pieces, (hidden, kept, weight, normed, sems, out_sem) = rest[:24], rest[24:]
     step = pl.program_id(0)
 
     @pl.when(step == 0)
@@ -308,7 +329,7 @@
         grid_spec=pltpu.PrefetchScalarGridSpec(
             num_scalar_prefetch=2,
             grid=(5,),
-            in_specs=[whole((count, half)), whole((count, half)), whole((1, width))] + [ANY] * 12,
+            in_specs=[whole((count, half)), whole((count, half)), whole((1, width))] + [ANY] * 24,
             out_specs=[whole((count, units)), ANY],
             scratch_shapes=[
                 pltpu.VMEM((width, columns), jnp.bfloat16),
@@ -538,22 +559,7 @@
 
 
 def second_kernel(
-    blocks,
-    core,
-    middle,
-    term,
-    far,
-    gain,
-    first,
-    others,
-    send,
-    keep,
-    base,
-    normed,
-    hidden,
-    wide,
-    down,
-    sems,
+    core, middle, term, far, gain, first, others, send, keep, base, normed, hidden, wide, down, sems
 ):
     step = pl.program_id(0)
     steps = 5
@@ -565,32 +571,29 @@
     ]
     copies.append(pltpu.make_async_copy(others, down, sems.at[steps]))
 
-    for k, copy in enumerate(copies):
-
-        @pl.when(step == k)
-        def _():
+    @pl.when(step == 0)
+    def _():
+        for copy in copies:
             copy.start()
-
-        @pl.when(step == blocks + k)
-        def _():
-            copy.wait()
-
-    @pl.when(step < blocks)
-    def _():
         values = middle[...].astype(jnp.float32) + (
             term[...].astype(jnp.float32) + far[...].astype(jnp.float32)
         )
         second = values.astype(jnp.bfloat16)
         half = second.shape[1] // 2
         base[...] = jnp.where(core[0] == 0, second[:, :half], second[:, half:])
-        block = pl.ds(pl.multiple_of(step * SPAN, SPAN), SPAN)
-        normed[block, :] = normed_rows(second.astype(jnp.float32), gain[...])
-
-    hidden_step(step - blocks, normed, wide, hidden)
-
-    @pl.when(step >= blocks + steps)
-    def _():
-        n = step - blocks - steps
+        normed[...] = normed_rows(second.astype(jnp.float32), gain[...])
+
+    for k, copy in enumerate(copies):
+
+        @pl.when(step == k)
+        def _():
+            copy.wait()
+
+    hidden_step(step, normed, wide, hidden)
+
+    @pl.when(step >= steps)
+    def _():
+        n = step - steps
         mine = jnp.where(n < outs // 2, 1 - core[0], core[0])
         row = mine * (outs // 2) + lax.rem(n, outs // 2)
         rows = pl.ds(pl.multiple_of(row * WIDE, WIDE), WIDE)
@@ -612,23 +615,24 @@
     units = columns // 2
     outs = width // WIDE
     sent = outs // 2
-    blocks = count // SPAN
-    done = blocks + 5
-
-    def block(size):
-        return spec((SPAN, size), lambda j, c: (jnp.minimum(j, blocks - 1), 0))
-
-    return pl.pallas_call(
-        functools.partial(second_kernel, blocks),
+    return pl.pallas_call(
+        second_kernel,
         out_shape=[jax.ShapeDtypeStruct((count, half), jnp.bfloat16)] * 3,
         grid_spec=pltpu.PrefetchScalarGridSpec(
             num_scalar_prefetch=1,
-            grid=(done + outs,),
-            in_specs=[block(width)] * 3 + [whole((1, width)), ANY, ANY],
+            grid=(5 + outs,),
+            in_specs=[
+                whole((count, width)),
+                whole((count, width)),
+                whole((count, width)),
+                whole((1, width)),
+                ANY,
+                ANY,
+            ],
             out_specs=[
-                spec((count, WIDE), lambda j, c: (0, jnp.clip(j - done, 0, sent - 1))),
-                spec((count, WIDE), lambda j, c: (0, jnp.maximum(j - done - sent, 0))),
-                block(half),
+                spec((count, WIDE), lambda j, c: (0, jnp.clip(j - 5, 0, sent - 1))),
+                spec((count, WIDE), lambda j, c: (0, jnp.maximum(j - 5 - sent, 0))),
+                whole((count, half)),
             ],
             scratch_shapes=[
                 pltpu.VMEM((count, width), jnp.bfloat16),
@@ -642,26 +646,6 @@
         cost_estimate=cost(6 * count * width * units, 6 * width * units, count * units),
         name="second_pass",
     )(core, middle, term, far, gain, first, others)
-
-
-def finish_kernel(base, keep, far, result):
-    last = keep[...].astype(jnp.float32) + far[...].astype(jnp.float32)
-    result[...] = (base[...].astype(jnp.float32) + 0.5 * last).astype(jnp.bfloat16)
-
-
-def finish(base, keep, far):
-    count, half = base.shape
-    block = spec((SPAN, half), lambda i: (i, 0))
-    return pl.pallas_call(
-        finish_kernel,
-        out_shape=jax.ShapeDtypeStruct((count, half), jnp.bfloat16),
-        grid=(count // SPAN,),
-        in_specs=[block] * 3,
-        out_specs=block,
-        compiler_params=params(1),
-        cost_estimate=cost(4 * count * half, 8 * count * half, 0),
-        name="finish",
-    )(base, keep, far)
 
 
 def layer(
@@ -732,7 +716,8 @@
     send, keep, base = second_pass(
         core, middle, term, other_core(term), norm_second[None], first, down
     )
-    return finish(base, keep, other_core(send))
+    last = keep.astype(jnp.float32) + other_core(send).astype(jnp.float32)
+    return (base.astype(jnp.float32) + 0.5 * last).astype(jnp.bfloat16)
 
 
 def solution(mesh):

time: 259 us -> 269 us (1.039)
  waiting for transfers between devices: 109 us -> 130 us
  starting transfers between devices: 51.2 us -> 42.6 us
  Pallas kernels: 85.9 us -> 79.5 us
  other arithmetic: 0 us -> 3.65 us
    ppermute x36 -> x42, waiting for transfers between devices: 99.8 us -> 121 us  [exchange(): return lax.ppermute(x, axis, [(i, i ^ flip) for i in range(4)])]
    ppermute x36 -> x42, starting transfers between devices: 37.4 us -> 30.5 us  [exchange(): return lax.ppermute(x, axis, [(i, i ^ flip) for i in range(4)])]
    pallas_call x2 -> x7, Pallas kernels: 26.8 us -> 22.1 us  [the longest x1 20.7 us: second_pass(): pl.pallas_call(second_kernel, out_shape=[jax.ShapeDtypeStruct((count, hal...]
    convert_element_type x0 -> x1, other arithmetic: none -> 3.65 us  [layer(): return (base.astype(jnp.float32) + 0.5 * last).astype(jnp.bfloat16)]
    unnamed x48 -> x68, local copies, waits for them, and re-layouts: 12.3 us -> 12.4 us
  transfers between devices with their start and end apart: 41 -> 47, of which waited for: 18 -> 22; matrix products, arithmetic and copies ran while one was open for 0% -> 0% of each run, Pallas kernels for 10% -> 10%
where the time goes in v4:
time: 269 us; the launch traced here: 268 us
  waiting for transfers between devices  130 us (48%)
  Pallas kernels  79.5 us (30%)
  starting transfers between devices  42.6 us (16%)
  local copies, waits for them, and re-layouts  12.4 us (5%)
  other arithmetic  3.65 us (1%)
    ppermute x42, waiting for transfers between devices, exchange(): return lax.ppermute(x, axis, [(i, i ^ flip) for i in range(4)])  121 us
    ppermute x42, starting transfers between devices, exchange(): return lax.ppermute(x, axis, [(i, i ^ flip) for i in range(4)])  30.5 us
    pallas_call x1, Pallas kernels, second_pass(): pl.pallas_call(second_kernel, out_shape=[jax.ShapeDtypeStruct((count, hal...  20.7 us
    pallas_call x1, Pallas kernels, first_hidden(): pl.pallas_call(first_kernel, out_shape=[jax.ShapeDtypeStruct((count, unit...  16.4 us
    pallas_call x1, Pallas kernels, gates(): pl.pallas_call(functools.partial(gates_kernel, blocks), out_shape=[jax.Sh...  12.5 us
    unnamed x68, local copies, waits for them, and re-layouts  12.4 us
    ppermute x5, starting transfers between devices, other_core(): return lax.ppermute(x, 'tp', [(0, 1), (1, 0)])  12.1 us
    pallas_call x1, Pallas kernels, first_down(): pl.pallas_call(down_kernel, out_shape=[jax.ShapeDtypeStruct((count, width...  10.3 us
  transfers between devices with their start and end apart: 47, of which 22 were waited for; matrix products, arithmetic and copies ran while one was open for 0% of the time, Pallas kernels for 10%

profile of v4, /device:TPU:1, one launch (start us, length us, event | category | flops | bytes accessed | tf_op | source)
XLA Modules:
  0.0 268.5 jit_solution(1773548104852322841)
XLA Ops:
  0.0 2.3 prepare.1
  2.4 2.5 collective-permute-start.25
  4.9 3.1 %collective-permute-done.25.refs_1_ = bf16[32,1792]{1,0:T(8,128)(2,1)S(1)} collective-permute-done((bf16[32,1792]{1,0:T(8,128)(2,1)}, bf16[32,1792]{1,0:T(8,128)(2,1)S(1)}, u32[]{:S(2)}, u32[]{:S(2)}) %collective-permute-start.25) | collective-permute-done | bytes 114720 | tf_op jit(solution)/shard_map/ppermute | solution.py:82
  8.9 2.5 collective-permute-start.26
  12.6 2.9 %collective-permute-done.13.refs_1_ = bf16[32,1920]{1,0:T(8,128)(2,1)S(1)} collective-permute-done((bf16[32,1920]{1,0:T(8,128)(2,1)}, bf16[32,1920]{1,0:T(8,128)(2,1)S(1)}, u32[]{:S(2)}, u32[]{:S(2)}) %collective-permute-start.13) | collective-permute-done | bytes 122912 | tf_op jit(solution)/shard_map/ppermute | solution.py:82
  16.5 3.5 %collective-permute-start.14 = (bf16[64,1920]{1,0:T(8,128)(2,1)S(1)}, bf16[64,1920]{1,0:T(8,128)(2,1)S(1)}, u32[]{:S(2)}, u32[]{:S(2)}) collective-permute-start(bf16[64,1920]{1,0:T(8,128)(2,1)S(1)} %join.19.refs_0_), channel_id=1, source_target_pairs={{0,96},{32,64},{64,32},{96,0},{1,97},{33,65},{65,33},{97,1},{2,98}... | collective-permute-start | bytes 737288 | tf_op jit(solution)/shard_map/ppermute | solution.py:82
  25.2 2.8 %collective-permute-start.2 = (bf16[64,2048]{1,0:T(8,128)(2,1)S(1)}, bf16[64,2048]{1,0:T(8,128)(2,1)S(1)}, u32[]{:S(2)}, u32[]{:S(2)}) collective-permute-start(bf16[64,2048]{1,0:T(8,128)(2,1)S(1)} %join.15.refs_0_), channel_id=1, source_target_pairs={{0,24},{8,16},{16,8},{24,0},{1,25},{9,17},{17,9},{25,1},{2,26},{10... | collective-permute-start | bytes 786440 | tf_op jit(solution)/shard_map/ppermute | solution.py:82
  28.0 4.5 %collective-permute-start = (bf16[640,1024]{1,0:T(8,128)(2,1)S(1)}, bf16[640,1024]{1,0:T(8,128)(2,1)S(1)}, u32[]{:S(2)}, u32[]{:S(2)}) collective-permute-start(bf16[640,1024]{1,0:T(8,128)(2,1)S(1)} %copy-done.18), channel_id=1, source_target_pairs={{0,1},{1,0},{2,3},{3,2},{4,5},{5,4},{6,7},{7,6},{8,9},{9,8},{10,11... | collective-permute-start | bytes 3932168 | tf_op jit(solution)/shard_map/ppermute | solution.py:36
  33.8 6.0 %collective-permute-done.16.refs_3_ = bf16[128,896]{1,0:T(8,128)(2,1)S(1)} collective-permute-done((bf16[128,896]{1,0:T(8,128)(2,1)S(1)}, bf16[128,896]{1,0:T(8,128)(2,1)S(1)}, u32[]{:S(2)}, u32[]{:S(2)}) %collective-permute-start.16) | collective-permute-done | bytes 229408 | tf_op jit(solution)/shard_map/ppermute | solution.py:82
  39.8 2.2 collective-permute-done.15.refs_2_
  42.8 5.1 %collective-permute-done.4.refs_3_ = bf16[128,1024]{1,0:T(8,128)(2,1)S(1)} collective-permute-done((bf16[128,1024]{1,0:T(8,128)(2,1)S(1)}, bf16[128,1024]{1,0:T(8,128)(2,1)S(1)}, u32[]{:S(2)}, u32[]{:S(2)}) %collective-permute-start.4) | collective-permute-done | bytes 262176 | tf_op jit(solution)/shard_map/ppermute | solution.py:82
  48.7 4.7 %collective-permute-done.30.refs_3_ = bf16[256,896]{1,0:T(8,128)(2,1)S(1)} collective-permute-done((bf16[256,896]{1,0:T(8,128)(2,1)S(1)}, bf16[256,896]{1,0:T(8,128)(2,1)S(1)}, u32[]{:S(2)}, u32[]{:S(2)}) %collective-permute-start.30) | collective-permute-done | bytes 458784 | tf_op jit(solution)/shard_map/ppermute | solution.py:82
  53.8 4.9 %collective-permute-done.17.refs_2_ = bf16[256,1024]{1,0:T(8,128)(2,1)S(1)} collective-permute-done((bf16[256,1024]{1,0:T(8,128)(2,1)S(1)}, bf16[256,1024]{1,0:T(8,128)(2,1)S(1)}, u32[]{:S(2)}, u32[]{:S(2)}) %collective-permute-start.17) | collective-permute-done | bytes 524320 | tf_op jit(solution)/shard_map/ppermute | solution.py:82
  58.9 2.3 collective-permute-done.5.refs_2_
  61.2 5.2 %collective-permute-done.6.refs_3_ = bf16[256,1024]{1,0:T(8,128)(2,1)S(1)} collective-permute-done((bf16[256,1024]{1,0:T(8,128)(2,1)S(1)}, bf16[256,1024]{1,0:T(8,128)(2,1)S(1)}, u32[]{:S(2)}, u32[]{:S(2)}) %collective-permute-start.6) | collective-permute-done | bytes 524320 | tf_op jit(solution)/shard_map/ppermute | solution.py:82
  68.1 26.4 %collective-permute-done.35.rest_22_ = bf16[512,384]{1,0:T(8,128)(2,1)S(1)} collective-permute-done((bf16[512,384]{1,0:T(8,128)(2,1)S(1)}, bf16[512,384]{1,0:T(8,128)(2,1)S(1)}, u32[]{:S(2)}, u32[]{:S(2)}) %collective-permute-start.35) | collective-permute-done | bytes 393248 | tf_op jit(solution)/shard_map/ppermute | solution.py:82
  97.3 16.7 %collective-permute-done.20.refs_1_.refs_3_ = bf16[512,896]{1,0:T(8,128)(2,1)S(1)} collective-permute-done((bf16[512,896]{1,0:T(8,128)(2,1)S(1)}, bf16[512,896]{1,0:T(8,128)(2,1)S(1)}, u32[]{:S(2)}, u32[]{:S(2)}) %collective-permute-start.20) | collective-permute-done | bytes 917536 | tf_op jit(solution)/shard_map/ppermute | solution.py:82
  114.1 4.6 %collective-permute-done.19.refs_0_.refs_2_ = bf16[512,1024]{1,0:T(8,128)(2,1)S(1)} collective-permute-done((bf16[512,1024]{1,0:T(8,128)(2,1)S(1)}, bf16[512,1024]{1,0:T(8,128)(2,1)S(1)}, u32[]{:S(2)}, u32[]{:S(2)}) %collective-permute-start.19) | collective-permute-done | bytes 1048608 | tf_op jit(solution)/shard_map/ppermute | solution.py:82
  118.9 10.1 %collective-permute-done.9.rest_2_ = bf16[512,512]{1,0:T(8,128)(2,1)S(1)} collective-permute-done((bf16[512,512]{1,0:T(8,128)(2,1)S(1)}, bf16[512,512]{1,0:T(8,128)(2,1)S(1)}, u32[]{:S(2)}, u32[]{:S(2)}) %collective-permute-start.9) | collective-permute-done | bytes 524320 | tf_op jit(solution)/shard_map/ppermute | solution.py:82
  141.9 2.4 collective-permute-start.37
  144.3 16.4 %first_hidden.1 = (bf16[640,1408]{1,0:T(8,128)(2,1)}, bf16[2048,2816]{1,0:T(8,128)(2,1)}) custom-call(s32[1]{0:T(128)} %bitcast.core, s32[1]{0:T(128)} %bitcast.1.at, bf16[640,1024]{1,0:T(8,128)(2,1)} %own.3, bf16[640,1024]{1,0:T(8,128)(2,1)} %copy-done.19, f32[1,2048]{1,0:T(1,128)} %bitcast.15, bf16[512,512]{1,0:T(8,128)(2,1)} %copy-done.10, ...), custom_call_target="tpu_custom_call" | custom-call | flops 7381975040 | bytes 23068672 | tf_op jit(solution)/shard_map/first_hidden/pallas_call | solution.py:323
  160.8 10.3 %first_down.1 = (bf16[640,2048]{1,0:T(8,128)(2,1)}, bf16[2048,1408]{1,0:T(8,128)(2,1)}) custom-call(s32[1]{0:T(128)} %bitcast.1.at, bf16[640,1408]{1,0:T(8,128)(2,1)} %get-tuple-element.87.hidden, bf16[1024,384]{1,0:T(8,128)(2,1)} %get-tuple-element.88.rest_0_, bf16[1024,384]{1,0:T(8,128)(2,1)} %collective-permute-done.37.rest_1_, ...), custom_call_target="tpu_custom_call" | custom-call | flops 3690987520 | bytes 11534336 | tf_op jit(solution)/shard_map/first_down/pallas_call | solution.py:376
  171.1 5.4 %collective-permute-start.40 = (bf16[640,2048]{1,0:T(8,128)(2,1)}, bf16[640,2048]{1,0:T(8,128)(2,1)}, u32[]{:S(2)}, u32[]{:S(2)}) collective-permute-start(bf16[640,2048]{1,0:T(8,128)(2,1)} %get-tuple-element.91.term), channel_id=1, source_target_pairs={{0,1},{1,0},{2,3},{3,2},{4,5},{5,4},{6,7},{7,6},{8,9},{9,8},{10,11... | collective-permute-start | bytes 7864328 | tf_op jit(solution)/shard_map/ppermute | solution.py:36
  181.0 20.4 %collective-permute-done.43.rest_5_ = bf16[1024,512]{1,0:T(8,128)(2,1)S(1)} collective-permute-done((bf16[1024,512]{1,0:T(8,128)(2,1)}, bf16[1024,512]{1,0:T(8,128)(2,1)S(1)}, u32[]{:S(2)}, u32[]{:S(2)}) %collective-permute-start.43) | collective-permute-done | bytes 1048608 | tf_op jit(solution)/shard_map/ppermute | solution.py:82
  201.4 2.4 collective-permute-done.41.rest_1_
  205.7 5.3 %assemble.1.rows = bf16[2048,1536]{1,0:T(8,128)(2,1)} custom-call(s32[1]{0:T(128)} %bitcast.1.at, bf16[1024,512]{1,0:T(8,128)(2,1)} %copy-done.6, bf16[1024,512]{1,0:T(8,128)(2,1)} %copy-done.23, bf16[1024,512]{1,0:T(8,128)(2,1)} %copy-done.7, bf16[1024,512]{1,0:T(8,128)(2,1)} %copy-done.24, bf16[1024,512]{1,0:T(8,128)(2,1)} %copy-done.5, ...), custom_call_target="tpu_custom_call" | custom-call | flops 5000000000 | bytes 25165824 | tf_op jit(solution)/shard_map/assemble/pallas_call | solution.py:416
  211.1 12.5 %gates.1 = (bf16[640,2048]{1,0:T(8,128)(2,1)}, f32[2,640,512]{2,1,0:T(8,128)}, f32[640,128]{1,0:T(8,128)}) custom-call(s32[1]{0:T(128)} %bitcast.core, bf16[640,1024]{1,0:T(8,128)(2,1)} %own.3, bf16[640,1024]{1,0:T(8,128)(2,1)} %copy-done.19, bf16[640,2048]{1,0:T(8,128)(2,1)} %get-tuple-element.91.term, bf16[640,2048]{1,0:T(8,128)(2,1)} %collective-permute-done.40.far, ...), custom_call_target="tpu_custom_call" | custom-call | flops 2684354560 | bytes 4194304 | tf_op jit(solution)/shard_map/gates/pallas_call | solution.py:471
  227.1 7.0 %mix.1.term = bf16[640,2048]{1,0:T(8,128)(2,1)} custom-call(f32[2,640,512]{2,1,0:T(8,128)} %get-tuple-element.96.act, f32[640,128]{1,0:T(8,128)} %get-tuple-element.97.sums, f32[640,128]{1,0:T(8,128)} %copy-done.20, f32[1,512]{1,0:T(1,128)} %bitcast.13, f32[1,512]{1,0:T(1,128)} %bitcast.14, bf16[4,128,128]{2,1,0:T(8,128)(2,1)} %weight.1, f32[4,128]{1,0:T(4,128)} %shift.1, ...), custom_call_target="tpu_custom_call" | custom-call | flops 1342177280 | bytes 2097152 | tf_op jit(solution)/shard_map/mix/pallas_call | solution.py:539
  234.4 4.7 %collective-permute-done.45.far = bf16[640,2048]{1,0:T(8,128)(2,1)S(1)} collective-permute-done((bf16[640,2048]{1,0:T(8,128)(2,1)}, bf16[640,2048]{1,0:T(8,128)(2,1)S(1)}, u32[]{:S(2)}, u32[]{:S(2)}) %collective-permute-start.45) | collective-permute-done | bytes 2621472 | tf_op jit(solution)/shard_map/ppermute | solution.py:36
  240.8 20.7 %second_pass.1 = (bf16[640,1024]{1,0:T(8,128)(2,1)}, bf16[640,1024]{1,0:T(8,128)(2,1)}, bf16[640,1024]{1,0:T(8,128)(2,1)}) custom-call(s32[1]{0:T(128)} %bitcast.core, bf16[640,2048]{1,0:T(8,128)(2,1)} %get-tuple-element.95.middle, bf16[640,2048]{1,0:T(8,128)(2,1)} %mix.1.term, bf16[640,2048]{1,0:T(8,128)(2,1)} %copy-done.21, f32[1,2048]{1,0:T(1,128)} %bitcast.16, ...), custom_call_target="tpu_custom_call" | custom-call | flops 11072962560 | bytes 17301504 | tf_op jit(solution)/shard_map/second_pass/pallas_call | solution.py:618
  262.0 2.9 %collective-permute-done.46 = bf16[640,1024]{1,0:T(8,128)(2,1)S(1)} collective-permute-done((bf16[640,1024]{1,0:T(8,128)(2,1)}, bf16[640,1024]{1,0:T(8,128)(2,1)S(1)}, u32[]{:S(2)}, u32[]{:S(2)}) %collective-permute-start.46) | collective-permute-done | bytes 1310752 | tf_op jit(solution)/shard_map/ppermute | solution.py:36
  264.8 3.6 %add_convert_fusion = bf16[640,1024]{1,0:T(8,128)(2,1)} fusion(bf16[640,1024]{1,0:T(8,128)(2,1)S(1)} %collective-permute-done.46, bf16[640,1024]{1,0:T(8,128)(2,1)} %get-tuple-element.101, bf16[640,1024]{1,0:T(8,128)(2,1)} %get-tuple-element.100), kind=kLoop, calls=%fused_computation | loop fusion | flops 4587520 | bytes 5242880 | tf_op jit(solution)/shard_map/convert_element_type | solution.py:720
  (159 shorter events, 41.4 us)
Async XLA Ops:
  8.9 11.1 %collective-permute-start.26 = (bf16[64,1792]{1,0:T(8,128)(2,1)S(1)}, bf16[64,1792]{1,0:T(8,128)(2,1)S(1)}, u32[]{:S(2)}, u32[]{:S(2)}) collective-permute-start(bf16[64,1792]{1,0:T(8,128)(2,1)S(1)} %join.23.refs_0_), channel_id=1, source_target_pairs={{0,6},{2,4},{4,2},{6,0},{1,7},{3,5},{5,3},{7,1},{8,14},{10,12},{12... | collective-permute-start | bytes 688136 | tf_op jit(solution)/shard_map/ppermute | solution.py:82
  16.5 16.1 %collective-permute-start.14 = (bf16[64,1920]{1,0:T(8,128)(2,1)S(1)}, bf16[64,1920]{1,0:T(8,128)(2,1)S(1)}, u32[]{:S(2)}, u32[]{:S(2)}) collective-permute-start(bf16[64,1920]{1,0:T(8,128)(2,1)S(1)} %join.19.refs_0_), channel_id=1, source_target_pairs={{0,96},{32,64},{64,32},{96,0},{1,97},{33,65},{65,33},{97,1},{2,98}... | collective-permute-start | bytes 737288 | tf_op jit(solution)/shard_map/ppermute | solution.py:82
  20.0 12.7 %collective-permute-start.27 = (bf16[128,896]{1,0:T(8,128)(2,1)S(1)}, bf16[128,896]{1,0:T(8,128)(2,1)S(1)}, u32[]{:S(2)}, u32[]{:S(2)}) collective-permute-start(bf16[128,896]{1,0:T(8,128)(2,1)S(1)} %get-tuple-element.77.refs_0_), channel_id=1, source_target_pairs={{0,8},{8,0},{16,24},{24,16},{1,9},{9,1},{17,25},{25,17},{2,10},{10... | collective-permute-start | bytes 688136 | tf_op jit(solution)/shard_map/ppermute | solution.py:82
  21.4 11.4 %collective-permute-start.28 = (bf16[128,896]{1,0:T(8,128)(2,1)S(1)}, bf16[128,896]{1,0:T(8,128)(2,1)S(1)}, u32[]{:S(2)}, u32[]{:S(2)}) collective-permute-start(bf16[128,896]{1,0:T(8,128)(2,1)S(1)} %get-tuple-element.78.refs_1_), channel_id=1, source_target_pairs={{0,2},{2,0},{4,6},{6,4},{1,3},{3,1},{5,7},{7,5},{8,10},{10,8},{12,... | collective-permute-start | bytes 688136 | tf_op jit(solution)/shard_map/ppermute | solution.py:82
  28.0 38.5 %collective-permute-start = (bf16[640,1024]{1,0:T(8,128)(2,1)S(1)}, bf16[640,1024]{1,0:T(8,128)(2,1)S(1)}, u32[]{:S(2)}, u32[]{:S(2)}) collective-permute-start(bf16[640,1024]{1,0:T(8,128)(2,1)S(1)} %copy-done.18), channel_id=1, source_target_pairs={{0,1},{1,0},{2,3},{3,2},{4,5},{5,4},{6,7},{7,6},{8,9},{9,8},{10,11... | collective-permute-start | bytes 3932168 | tf_op jit(solution)/shard_map/ppermute | solution.py:36
  32.9 15.7 %collective-permute-start.29 = (bf16[256,896]{1,0:T(8,128)(2,1)S(1)}, bf16[256,896]{1,0:T(8,128)(2,1)S(1)}, u32[]{:S(2)}, u32[]{:S(2)}) collective-permute-start(bf16[256,896]{1,0:T(8,128)(2,1)S(1)} %get-tuple-element.79.refs_0_), channel_id=1, source_target_pairs={{0,2},{2,0},{4,6},{6,4},{1,3},{3,1},{5,7},{7,5},{8,10},{10,8},{12,... | collective-permute-start | bytes 1376264 | tf_op jit(solution)/shard_map/ppermute | solution.py:82
  42.0 11.3 %collective-permute-start.30 = (bf16[256,896]{1,0:T(8,128)(2,1)S(1)}, bf16[256,896]{1,0:T(8,128)(2,1)S(1)}, u32[]{:S(2)}, u32[]{:S(2)}) collective-permute-start(bf16[256,896]{1,0:T(8,128)(2,1)S(1)} %get-tuple-element.80.refs_1_), channel_id=1, source_target_pairs={{0,8},{8,0},{16,24},{24,16},{1,9},{9,1},{17,25},{25,17},{2,10},{10... | collective-permute-start | bytes 1376264 | tf_op jit(solution)/shard_map/ppermute | solution.py:82
  42.1 11.6 %collective-permute-start.18 = (bf16[256,896]{1,0:T(8,128)(2,1)S(1)}, bf16[256,896]{1,0:T(8,128)(2,1)S(1)}, u32[]{:S(2)}, u32[]{:S(2)}) collective-permute-start(bf16[256,896]{1,0:T(8,128)(2,1)S(1)} %get-tuple-element.69.refs_1_), channel_id=1, source_target_pairs={{0,24},{8,16},{16,8},{24,0},{1,25},{9,17},{17,9},{25,1},{2,26},{10... | collective-permute-start | bytes 1376264 | tf_op jit(solution)/shard_map/ppermute | solution.py:82
  47.9 10.8 %collective-permute-start.17 = (bf16[256,1024]{1,0:T(8,128)(2,1)S(1)}, bf16[256,1024]{1,0:T(8,128)(2,1)S(1)}, u32[]{:S(2)}, u32[]{:S(2)}) collective-permute-start(bf16[256,1024]{1,0:T(8,128)(2,1)S(1)} %get-tuple-element.68.refs_0_), channel_id=1, source_target_pairs={{0,32},{32,0},{64,96},{96,64},{1,33},{33,1},{65,97},{97,65},{2,34}... | collective-permute-start | bytes 1572872 | tf_op jit(solution)/shard_map/ppermute | solution.py:82
  48.6 12.6 %collective-permute-start.5 = (bf16[256,1024]{1,0:T(8,128)(2,1)S(1)}, bf16[256,1024]{1,0:T(8,128)(2,1)S(1)}, u32[]{:S(2)}, u32[]{:S(2)}) collective-permute-start(bf16[256,1024]{1,0:T(8,128)(2,1)S(1)} %get-tuple-element.57.refs_0_), channel_id=1, source_target_pairs={{0,6},{2,4},{4,2},{6,0},{1,7},{3,5},{5,3},{7,1},{8,14},{10,12},{12... | collective-permute-start | bytes 1572872 | tf_op jit(solution)/shard_map/ppermute | solution.py:82
  53.4 13.1 %collective-permute-start.6 = (bf16[256,1024]{1,0:T(8,128)(2,1)S(1)}, bf16[256,1024]{1,0:T(8,128)(2,1)S(1)}, u32[]{:S(2)}, u32[]{:S(2)}) collective-permute-start(bf16[256,1024]{1,0:T(8,128)(2,1)S(1)} %get-tuple-element.58.refs_1_), channel_id=1, source_target_pairs={{0,96},{32,64},{64,32},{96,0},{1,97},{33,65},{65,33},{97,1},{2,98}... | collective-permute-start | bytes 1572872 | tf_op jit(solution)/shard_map/ppermute | solution.py:82
  53.7 12.9 %collective-permute-start.33 = (bf16[512,384]{1,0:T(8,128)(2,1)S(1)}, bf16[512,384]{1,0:T(8,128)(2,1)S(1)}, u32[]{:S(2)}, u32[]{:S(2)}) collective-permute-start(bf16[512,384]{1,0:T(8,128)(2,1)S(1)} %get-tuple-element.83.rest_16_), channel_id=1, source_target_pairs={{0,24},{8,16},{16,8},{24,0},{1,25},{9,17},{17,9},{25,1},{2,26},{10... | collective-permute-start | bytes 1179656 | tf_op jit(solution)/shard_map/ppermute | solution.py:82
  58.7 36.9 %collective-permute-start.31 = (bf16[512,896]{1,0:T(8,128)(2,1)S(1)}, bf16[512,896]{1,0:T(8,128)(2,1)S(1)}, u32[]{:S(2)}, u32[]{:S(2)}) collective-permute-start(bf16[512,896]{1,0:T(8,128)(2,1)S(1)} %get-tuple-element.81.refs_0_), channel_id=1, source_target_pairs={{0,96},{32,64},{64,32},{96,0},{1,97},{33,65},{65,33},{97,1},{2,98}... | collective-permute-start | bytes 2752520 | tf_op jit(solution)/shard_map/ppermute | solution.py:82
  61.2 34.1 %collective-permute-start.21 = (bf16[512,512]{1,0:T(8,128)(2,1)S(1)}, bf16[512,512]{1,0:T(8,128)(2,1)}, u32[]{:S(2)}, u32[]{:S(2)}) collective-permute-start(bf16[512,512]{1,0:T(8,128)(2,1)S(1)} %get-tuple-element.72.rest_8_), channel_id=1, source_target_pairs={{0,2},{2,0},{4,6},{6,4},{1,3},{3,1},{5,7},{7,5},{8,10},{10,8},{12,... | collective-permute-start | bytes 1572872 | tf_op jit(solution)/shard_map/ppermute | solution.py:82
  66.5 28.1 %collective-permute-start.35 = (bf16[512,384]{1,0:T(8,128)(2,1)S(1)}, bf16[512,384]{1,0:T(8,128)(2,1)S(1)}, u32[]{:S(2)}, u32[]{:S(2)}) collective-permute-start(bf16[512,384]{1,0:T(8,128)(2,1)S(1)} %get-tuple-element.85.rest_20_), channel_id=1, source_target_pairs={{0,96},{32,64},{64,32},{96,0},{1,97},{33,65},{65,33},{97,1},{2,98}... | collective-permute-start | bytes 1179656 | tf_op jit(solution)/shard_map/ppermute | solution.py:82
  66.6 28.9 %collective-permute-start.23 = (bf16[512,512]{1,0:T(8,128)(2,1)S(1)}, bf16[512,512]{1,0:T(8,128)(2,1)S(1)}, u32[]{:S(2)}, u32[]{:S(2)}) collective-permute-start(bf16[512,512]{1,0:T(8,128)(2,1)S(1)} %get-tuple-element.74.rest_12_), channel_id=1, source_target_pairs={{0,6},{2,4},{4,2},{6,0},{1,7},{3,5},{5,3},{7,1},{8,14},{10,12},{12... | collective-permute-start | bytes 1572872 | tf_op jit(solution)/shard_map/ppermute | solution.py:82
  66.6 29.3 %collective-permute-start.32 = (bf16[512,896]{1,0:T(8,128)(2,1)S(1)}, bf16[512,896]{1,0:T(8,128)(2,1)S(1)}, u32[]{:S(2)}, u32[]{:S(2)}) collective-permute-start(bf16[512,896]{1,0:T(8,128)(2,1)S(1)} %get-tuple-element.82.refs_1_), channel_id=1, source_target_pairs={{0,24},{8,16},{16,8},{24,0},{1,25},{9,17},{17,9},{25,1},{2,26},{10... | collective-permute-start | bytes 2752520 | tf_op jit(solution)/shard_map/ppermute | solution.py:82
  94.5 19.5 %collective-permute-start.20 = (bf16[512,896]{1,0:T(8,128)(2,1)S(1)}, bf16[512,896]{1,0:T(8,128)(2,1)S(1)}, u32[]{:S(2)}, u32[]{:S(2)}) collective-permute-start(bf16[512,896]{1,0:T(8,128)(2,1)S(1)} %get-tuple-element.71.refs_1_), channel_id=1, source_target_pairs={{0,2},{2,0},{4,6},{6,4},{1,3},{3,1},{5,7},{7,5},{8,10},{10,8},{12,... | collective-permute-start | bytes 2752520 | tf_op jit(solution)/shard_map/ppermute | solution.py:82
  95.3 23.4 %collective-permute-start.19 = (bf16[512,1024]{1,0:T(8,128)(2,1)S(1)}, bf16[512,1024]{1,0:T(8,128)(2,1)S(1)}, u32[]{:S(2)}, u32[]{:S(2)}) collective-permute-start(bf16[512,1024]{1,0:T(8,128)(2,1)S(1)} %get-tuple-element.70.refs_0_), channel_id=1, source_target_pairs={{0,6},{2,4},{4,2},{6,0},{1,7},{3,5},{5,3},{7,1},{8,14},{10,12},{12... | collective-permute-start | bytes 3145736 | tf_op jit(solution)/shard_map/ppermute | solution.py:82
  95.5 34.2 %collective-permute-start.7 = (bf16[512,1024]{1,0:T(8,128)(2,1)S(1)}, bf16[512,1024]{1,0:T(8,128)(2,1)S(1)}, u32[]{:S(2)}, u32[]{:S(2)}) collective-permute-start(bf16[512,1024]{1,0:T(8,128)(2,1)S(1)} %get-tuple-element.59.refs_0_), channel_id=1, source_target_pairs={{0,32},{32,0},{64,96},{96,64},{1,33},{33,1},{65,97},{97,65},{2,34}... | collective-permute-start | bytes 3145736 | tf_op jit(solution)/shard_map/ppermute | solution.py:82
  95.6 34.2 %collective-permute-start.8 = (bf16[512,1024]{1,0:T(8,128)(2,1)S(1)}, bf16[512,1024]{1,0:T(8,128)(2,1)S(1)}, u32[]{:S(2)}, u32[]{:S(2)}) collective-permute-start(bf16[512,1024]{1,0:T(8,128)(2,1)S(1)} %get-tuple-element.60.refs_1_), channel_id=1, source_target_pairs={{0,8},{8,0},{16,24},{24,16},{1,9},{9,1},{17,25},{25,17},{2,10},{10... | collective-permute-start | bytes 3145736 | tf_op jit(solution)/shard_map/ppermute | solution.py:82
  95.9 33.1 %collective-permute-start.9 = (bf16[512,512]{1,0:T(8,128)(2,1)S(1)}, bf16[512,512]{1,0:T(8,128)(2,1)S(1)}, u32[]{:S(2)}, u32[]{:S(2)}) collective-permute-start(bf16[512,512]{1,0:T(8,128)(2,1)S(1)} %get-tuple-element.61.rest_0_), channel_id=1, source_target_pairs={{0,8},{8,0},{16,24},{24,16},{1,9},{9,1},{17,25},{25,17},{2,10},{10... | collective-permute-start | bytes 1572872 | tf_op jit(solution)/shard_map/ppermute | solution.py:82
  114.0 19.8 %collective-permute-start.11 = (bf16[512,512]{1,0:T(8,128)(2,1)S(1)}, bf16[512,512]{1,0:T(8,128)(2,1)S(1)}, u32[]{:S(2)}, u32[]{:S(2)}) collective-permute-start(bf16[512,512]{1,0:T(8,128)(2,1)S(1)} %get-tuple-element.63.rest_4_), channel_id=1, source_target_pairs={{0,32},{32,0},{64,96},{96,64},{1,33},{33,1},{65,97},{97,65},{2,34}... | collective-permute-start | bytes 1572872 | tf_op jit(solution)/shard_map/ppermute | solution.py:82
  118.7 16.0 %collective-permute-start.34 = (bf16[512,384]{1,0:T(8,128)(2,1)S(1)}, bf16[512,384]{1,0:T(8,128)(2,1)S(1)}, u32[]{:S(2)}, u32[]{:S(2)}) collective-permute-start(bf16[512,384]{1,0:T(8,128)(2,1)S(1)} %get-tuple-element.84.rest_17_), channel_id=1, source_target_pairs={{0,24},{8,16},{16,8},{24,0},{1,25},{9,17},{17,9},{25,1},{2,26},{10... | collective-permute-start | bytes 1179656 | tf_op jit(solution)/shard_map/ppermute | solution.py:82
  129.8 11.3 %collective-permute-start.24 = (bf16[512,512]{1,0:T(8,128)(2,1)S(1)}, bf16[512,512]{1,0:T(8,128)(2,1)S(1)}, u32[]{:S(2)}, u32[]{:S(2)}) collective-permute-start(bf16[512,512]{1,0:T(8,128)(2,1)S(1)} %get-tuple-element.75.rest_13_), channel_id=1, source_target_pairs={{0,6},{2,4},{4,2},{6,0},{1,7},{3,5},{5,3},{7,1},{8,14},{10,12},{12... | collective-permute-start | bytes 1572872 | tf_op jit(solution)/shard_map/ppermute | solution.py:82
  137.6 23.2 %collective-permute-start.38 = (bf16[1024,512]{1,0:T(8,128)(2,1)}, bf16[1024,512]{1,0:T(8,128)(2,1)}, u32[]{:S(2)}, u32[]{:S(2)}) collective-permute-start(bf16[1024,512]{1,0:T(8,128)(2,1)} %get-tuple-element.89.rest_2_), channel_id=1, source_target_pairs={{0,24},{8,16},{16,8},{24,0},{1,25},{9,17},{17,9},{25,1},{2,26},{10... | collective-permute-start | bytes 3145736 | tf_op jit(solution)/shard_map/ppermute | solution.py:82
  138.9 21.9 %collective-permute-start.39 = (bf16[1024,512]{1,0:T(8,128)(2,1)}, bf16[1024,512]{1,0:T(8,128)(2,1)}, u32[]{:S(2)}, u32[]{:S(2)}) collective-permute-start(bf16[1024,512]{1,0:T(8,128)(2,1)} %get-tuple-element.90.rest_4_), channel_id=1, source_target_pairs={{0,96},{32,64},{64,32},{96,0},{1,97},{33,65},{65,33},{97,1},{2,98}... | collective-permute-start | bytes 3145736 | tf_op jit(solution)/shard_map/ppermute | solution.py:82
  141.9 18.9 %collective-permute-start.37 = (bf16[1024,384]{1,0:T(8,128)(2,1)}, bf16[1024,384]{1,0:T(8,128)(2,1)}, u32[]{:S(2)}, u32[]{:S(2)}) collective-permute-start(bf16[1024,384]{1,0:T(8,128)(2,1)} %get-tuple-element.88.rest_0_), channel_id=1, source_target_pairs={{0,6},{2,4},{4,2},{6,0},{1,7},{3,5},{5,3},{7,1},{8,14},{10,12},{12... | collective-permute-start | bytes 2359304 | tf_op jit(solution)/shard_map/ppermute | solution.py:82
  171.1 40.0 %collective-permute-start.40 = (bf16[640,2048]{1,0:T(8,128)(2,1)}, bf16[640,2048]{1,0:T(8,128)(2,1)}, u32[]{:S(2)}, u32[]{:S(2)}) collective-permute-start(bf16[640,2048]{1,0:T(8,128)(2,1)} %get-tuple-element.91.term), channel_id=1, source_target_pairs={{0,1},{1,0},{2,3},{3,2},{4,5},{5,4},{6,7},{7,6},{8,9},{9,8},{10,11... | collective-permute-start | bytes 7864328 | tf_op jit(solution)/shard_map/ppermute | solution.py:36
  176.5 24.8 %collective-permute-start.43 = (bf16[1024,512]{1,0:T(8,128)(2,1)}, bf16[1024,512]{1,0:T(8,128)(2,1)S(1)}, u32[]{:S(2)}, u32[]{:S(2)}) collective-permute-start(bf16[1024,512]{1,0:T(8,128)(2,1)} %copy-done.5), channel_id=1, source_target_pairs={{0,2},{2,0},{4,6},{6,4},{1,3},{3,1},{5,7},{7,5},{8,10},{10,8},{12,... | collective-permute-start | bytes 3145736 | tf_op jit(solution)/shard_map/ppermute | solution.py:82
  179.4 24.3 %collective-permute-start.41 = (bf16[1024,512]{1,0:T(8,128)(2,1)S(1)}, bf16[1024,512]{1,0:T(8,128)(2,1)S(1)}, u32[]{:S(2)}, u32[]{:S(2)}) collective-permute-start(bf16[1024,512]{1,0:T(8,128)(2,1)S(1)} %get-tuple-element.92.rest_0_), channel_id=1, source_target_pairs={{0,8},{8,0},{16,24},{24,16},{1,9},{9,1},{17,25},{25,17},{2,10},{10... | collective-permute-start | bytes 3145736 | tf_op jit(solution)/shard_map/ppermute | solution.py:82
  179.9 24.1 %collective-permute-start.42 = (bf16[1024,512]{1,0:T(8,128)(2,1)S(1)}, bf16[1024,512]{1,0:T(8,128)(2,1)S(1)}, u32[]{:S(2)}, u32[]{:S(2)}) collective-permute-start(bf16[1024,512]{1,0:T(8,128)(2,1)S(1)} %get-tuple-element.93.rest_2_), channel_id=1, source_target_pairs={{0,32},{32,0},{64,96},{96,64},{1,33},{33,1},{65,97},{97,65},{2,34}... | collective-permute-start | bytes 3145736 | tf_op jit(solution)/shard_map/ppermute | solution.py:82
  (49 other events, 646.3 us)

commit v5 on v4

--- a/solution.py
+++ b/solution.py
@@ -66,9 +66,9 @@
 ANY = pl.BlockSpec(memory_space=pl.ANY)
 
 
-def params(steps):
+def params(steps, mib=60):
     return pltpu.CompilerParams(
-        dimension_semantics=("arbitrary",) * steps, vmem_limit_bytes=60 * 1024 * 1024
+        dimension_semantics=("arbitrary",) * steps, vmem_limit_bytes=mib * 1024 * 1024
     )
 
 
@@ -288,36 +288,65 @@
         hidden[:, 2 * WIDE :] = narrow_step(normed[...], weight[:, 4 * WIDE :])
 
 
-def first_kernel(core, at, own, other, gain, *rest):
-    pieces, (hidden, kept, weight, normed, sems, out_sem) = rest[:24], rest[24:]
+def norm_kernel(core, own, other, gain, normed):
+    left = jnp.where(core[0] == 0, own[...], other[...])
+    right = jnp.where(core[0] == 0, other[...], own[...])
+    values = jnp.concatenate([left, right], axis=1).astype(jnp.float32)
+    normed[...] = normed_rows(values, gain[...])
+
+
+def first_norm(core, own, other, gain):
+    count, half = own.shape
+    block = spec((SPAN, half), lambda i, c: (i, 0))
+    return pl.pallas_call(
+        norm_kernel,
+        out_shape=jax.ShapeDtypeStruct((count, 2 * half), jnp.bfloat16),
+        grid_spec=pltpu.PrefetchScalarGridSpec(
+            num_scalar_prefetch=1,
+            grid=(count // SPAN,),
+            in_specs=[block, block, whole((1, 2 * half))],
+            out_specs=spec((SPAN, 2 * half), lambda i, c: (i, 0)),
+        ),
+        compiler_params=params(1),
+        cost_estimate=cost(5 * 10**9, 8 * count * half, count),
+        name="first_norm",
+    )(core, own, other, gain)
+
+
+def first_kernel(at, normed, *rest):
+    pieces, (hidden, kept, weight, sems, out_sems) = rest[:24], rest[24:]
     step = pl.program_id(0)
-
-    @pl.when(step == 0)
-    def _():
-        place_blocks(at[0], pieces, weight, sems, FIRST, range(6))
-        left = jnp.where(core[0] == 0, own[...], other[...])
-        right = jnp.where(core[0] == 0, other[...], own[...])
-        values = jnp.concatenate([left, right], axis=1).astype(jnp.float32)
-        normed[...] = normed_rows(values, gain[...])
+    begin = starts(FIRST)
+    copies = []
+    for c in range(6):
+        columns = pl.ds(begin[c], FIRST[c] * LANES)
+        copies.append(
+            pltpu.make_async_copy(weight.at[:, columns], kept.at[:, columns], out_sems.at[c])
+        )
+
+    for k, colors in enumerate(((0, 1, 2), (3,), (4,), (5,))):
+
+        @pl.when(step == k)
+        def _():
+            place_blocks(at[0], pieces, weight, sems, FIRST, colors)
 
     for c in range(6):
 
         @pl.when(step == min(c, 4))
         def _():
             wait_color(weight, sems, FIRST, c)
+            copies[c].start()
 
     hidden_step(step, normed, weight, hidden)
 
     @pl.when(step == 4)
     def _():
-        copy = pltpu.make_async_copy(weight, kept, out_sem)
-        copy.start()
-        copy.wait()
-
-
-def first_hidden(core, at, own, other, gain, pieces):
-    count, half = own.shape
-    width = 2 * half
+        for copy in copies:
+            copy.wait()
+
+
+def first_hidden(at, normed, pieces):
+    count, width = normed.shape
     columns = sum(FIRST) * LANES
     units = columns // 2
     return pl.pallas_call(
@@ -327,21 +356,20 @@
             jax.ShapeDtypeStruct((width, columns), jnp.bfloat16),
         ],
         grid_spec=pltpu.PrefetchScalarGridSpec(
-            num_scalar_prefetch=2,
+            num_scalar_prefetch=1,
             grid=(5,),
-            in_specs=[whole((count, half)), whole((count, half)), whole((1, width))] + [ANY] * 24,
+            in_specs=[whole((count, width))] + [ANY] * 24,
             out_specs=[whole((count, units)), ANY],
             scratch_shapes=[
                 pltpu.VMEM((width, columns), jnp.bfloat16),
-                pltpu.VMEM((count, width), jnp.bfloat16),
                 pltpu.SemaphoreType.DMA((6,)),
-                pltpu.SemaphoreType.DMA,
+                pltpu.SemaphoreType.DMA((6,)),
             ],
         ),
         compiler_params=params(1),
         cost_estimate=cost(2 * count * width * columns, 4 * width * columns, count * units),
         name="first_hidden",
-    )(core, at, own, other, gain, *pieces)
+    )(at, normed, *pieces)
 
 
 MIXER, DOWN = OTHERS[:3], OTHERS[3:]
@@ -433,7 +461,9 @@
     )(at, *pieces)
 
 
-def gates_kernel(blocks, core, own, other, term, far, gain, rows, middle, act, sums, normed):
+def gates_kernel(
+    blocks, core, own, other, term, far, gain, u_rows, v_rows, middle, act, sums, normed
+):
     step = pl.program_id(0)
 
     @pl.when(step < blocks)
@@ -447,17 +477,17 @@
         block = pl.ds(pl.multiple_of(step * SPAN, SPAN), SPAN)
         normed[block, :] = normed_rows(mid.astype(jnp.float32), gain[...])
 
-    @pl.when(step >= blocks)
-    def _():
-        acted = gelu(dot(normed[...], rows[...]))
-        act[0] = acted
-
-        @pl.when(step == blocks)
-        def _():
-            lane = lax.broadcasted_iota(jnp.int32, sums.shape, 1)
-            total = jnp.sum(acted, axis=1, keepdims=True)
-            squares = jnp.sum(acted * acted, axis=1, keepdims=True)
-            sums[...] = jnp.where(lane == 0, total, squares)
+    @pl.when(step == blocks)
+    def _():
+        v_pre = dot(normed[...], v_rows[...])
+        u_pre = dot(normed[...], u_rows[...])
+        v_act = gelu(v_pre)
+        act[0] = v_act
+        lane = lax.broadcasted_iota(jnp.int32, sums.shape, 1)
+        total = jnp.sum(v_act, axis=1, keepdims=True)
+        squares = jnp.sum(v_act * v_act, axis=1, keepdims=True)
+        sums[...] = jnp.where(lane == 0, total, squares)
+        act[1] = gelu(u_pre)
 
 
 def gates(core, own, other, term, far, gain, weight, chans):
@@ -477,26 +507,23 @@
         ],
         grid_spec=pltpu.PrefetchScalarGridSpec(
             num_scalar_prefetch=1,
-            grid=(blocks + 2,),
+            grid=(blocks + 1,),
             in_specs=[
                 block(half),
                 block(half),
                 block(width),
                 block(width),
                 whole((1, width)),
-                spec((width, chans), lambda i, c: (0, 2 - jnp.maximum(i - blocks, 0))),
+                spec((width, chans), lambda i, c: (0, 1)),
+                spec((width, chans), lambda i, c: (0, 2)),
             ],
-            out_specs=[
-                block(width),
-                spec((1, count, chans), lambda i, c: (jnp.maximum(i - blocks, 0), 0, 0)),
-                whole((count, LANES)),
-            ],
+            out_specs=[block(width), whole((2, count, chans)), whole((count, LANES))],
             scratch_shapes=[pltpu.VMEM((count, width), jnp.bfloat16)],
         ),
         compiler_params=params(1),
         cost_estimate=cost(4 * count * width * chans, 4 * width * chans, 2 * count * chans),
         name="gates",
-    )(core, own, other, term, far, gain, weight)
+    )(core, own, other, term, far, gain, weight, weight)
 
 
 def mix_kernel(act, sums, far, gain, bias, weight, shift, rows, term, mixed):
@@ -698,7 +725,8 @@
     one, two = gather(colors)
 
     own, other = tokens, other_core(tokens)
-    hidden, first = first_hidden(core, at, own, other, norm_first[None], one)
+    normed = first_norm(core, own, other, norm_first[None])
+    hidden, first = first_hidden(at, normed, one)
     term, down = first_down(at, hidden, width, two[6:])
     far = other_core(term)
     mixer = assemble(at, width, two[:6])

time: 269 us -> 258 us (0.959)
  waiting for transfers between devices: 130 us -> 75 us
  starting transfers between devices: 42.6 us -> 73.1 us
  local copies, waits for them, and re-layouts: 12.4 us -> 19.7 us
  Pallas kernels: 79.5 us -> 84.7 us
    ppermute x42, waiting for transfers between devices: 121 us -> 65.9 us  [exchange(): return lax.ppermute(x, axis, [(i, i ^ flip) for i in range(4)])]
    ppermute x42, starting transfers between devices: 30.5 us -> 61.4 us  [exchange(): return lax.ppermute(x, axis, [(i, i ^ flip) for i in range(4)])]
    unnamed x68 -> x88, local copies, waits for them, and re-layouts: 12.4 us -> 19.7 us
    pallas_call x0 -> x1, Pallas kernels: none -> 5.26 us  [first_norm(): pl.pallas_call(norm_kernel, out_shape=jax.ShapeDtypeStruct((count, 2 * ha...]
  transfers between devices with their start and end apart: 47 -> 47, of which waited for: 22 -> 18; matrix products, arithmetic and copies ran while one was open for 0% -> 0% of each run, Pallas kernels for 10% -> 12%
where the time goes in v5:
time: 258 us; the launch traced here: 257 us
  Pallas kernels  84.7 us (33%)
  waiting for transfers between devices  75 us (29%)
  starting transfers between devices  73.1 us (28%)
  local copies, waits for them, and re-layouts  19.7 us (8%)
  other arithmetic  3.65 us (1%)
    ppermute x42, waiting for transfers between devices, exchange(): return lax.ppermute(x, axis, [(i, i ^ flip) for i in range(4)])  65.9 us
    ppermute x42, starting transfers between devices, exchange(): return lax.ppermute(x, axis, [(i, i ^ flip) for i in range(4)])  61.4 us
    pallas_call x1, Pallas kernels, second_pass(): pl.pallas_call(second_kernel, out_shape=[jax.ShapeDtypeStruct((count, hal...  20.8 us
    unnamed x88, local copies, waits for them, and re-layouts  19.7 us
    pallas_call x1, Pallas kernels, first_hidden(): pl.pallas_call(first_kernel, out_shape=[jax.ShapeDtypeStruct((count, unit...  14.2 us
    pallas_call x1, Pallas kernels, gates(): pl.pallas_call(functools.partial(gates_kernel, blocks), out_shape=[jax.Sh...  13 us
    ppermute x5, starting transfers between devices, other_core(): return lax.ppermute(x, 'tp', [(0, 1), (1, 0)])  11.7 us
    pallas_call x1, Pallas kernels, first_down(): pl.pallas_call(down_kernel, out_shape=[jax.ShapeDtypeStruct((count, width...  10.2 us
  transfers between devices with their start and end apart: 47, of which 18 were waited for; matrix products, arithmetic and copies ran while one was open for 0% of the time, Pallas kernels for 12%

profile of v5, /device:TPU:1, one launch (start us, length us, event | category | flops | bytes accessed | tf_op | source)
XLA Modules:
  0.0 256.6 jit_solution(13639800130721085658)
XLA Ops:
  0.0 2.3 prepare.1
  2.4 2.5 collective-permute-start.25
  8.9 2.5 collective-permute-start.26
  12.3 3.5 %collective-permute-start.14 = (bf16[64,1920]{1,0:T(8,128)(2,1)S(1)}, bf16[64,1920]{1,0:T(8,128)(2,1)S(1)}, u32[]{:S(2)}, u32[]{:S(2)}) collective-permute-start(bf16[64,1920]{1,0:T(8,128)(2,1)S(1)} %join.19.refs_0_), channel_id=1, source_target_pairs={{0,96},{32,64},{64,32},{96,0},{1,97},{33,65},{65,33},{97,1},{2,98}... | collective-permute-start | bytes 737288 | tf_op jit(solution)/shard_map/ppermute | solution.py:82
  16.7 2.8 %collective-permute-start.2 = (bf16[64,2048]{1,0:T(8,128)(2,1)S(1)}, bf16[64,2048]{1,0:T(8,128)(2,1)S(1)}, u32[]{:S(2)}, u32[]{:S(2)}) collective-permute-start(bf16[64,2048]{1,0:T(8,128)(2,1)S(1)} %join.15.refs_0_), channel_id=1, source_target_pairs={{0,24},{8,16},{16,8},{24,0},{1,25},{9,17},{17,9},{25,1},{2,26},{10... | collective-permute-start | bytes 786440 | tf_op jit(solution)/shard_map/ppermute | solution.py:82
  19.7 2.6 %collective-permute-start = (bf16[640,1024]{1,0:T(8,128)(2,1)S(1)}, bf16[640,1024]{1,0:T(8,128)(2,1)S(1)}, u32[]{:S(2)}, u32[]{:S(2)}) collective-permute-start(bf16[640,1024]{1,0:T(8,128)(2,1)S(1)} %copy-done.31), channel_id=1, source_target_pairs={{0,1},{1,0},{2,3},{3,2},{4,5},{5,4},{6,7},{7,6},{8,9},{9,8},{10,11... | collective-permute-start | bytes 3932168 | tf_op jit(solution)/shard_map/ppermute | solution.py:36
  25.7 2.2 collective-permute-start.4
  36.4 3.5 %collective-permute-start.5 = (bf16[256,1024]{1,0:T(8,128)(2,1)S(1)}, bf16[256,1024]{1,0:T(8,128)(2,1)S(1)}, u32[]{:S(2)}, u32[]{:S(2)}) collective-permute-start(bf16[256,1024]{1,0:T(8,128)(2,1)S(1)} %get-tuple-element.57.refs_0_), channel_id=1, source_target_pairs={{0,6},{2,4},{4,2},{6,0},{1,7},{3,5},{5,3},{7,1},{8,14},{10,12},{12... | collective-permute-start | bytes 1572872 | tf_op jit(solution)/shard_map/ppermute | solution.py:82
  40.7 5.4 %collective-permute-start.6 = (bf16[256,1024]{1,0:T(8,128)(2,1)S(1)}, bf16[256,1024]{1,0:T(8,128)(2,1)S(1)}, u32[]{:S(2)}, u32[]{:S(2)}) collective-permute-start(bf16[256,1024]{1,0:T(8,128)(2,1)S(1)} %get-tuple-element.58.refs_1_), channel_id=1, source_target_pairs={{0,96},{32,64},{64,32},{96,0},{1,97},{33,65},{65,33},{97,1},{2,98}... | collective-permute-start | bytes 1572872 | tf_op jit(solution)/shard_map/ppermute | solution.py:82
  48.1 8.5 %collective-permute-start.35 = (bf16[512,384]{1,0:T(8,128)(2,1)S(1)}, bf16[512,384]{1,0:T(8,128)(2,1)S(1)}, u32[]{:S(2)}, u32[]{:S(2)}) collective-permute-start(bf16[512,384]{1,0:T(8,128)(2,1)S(1)} %get-tuple-element.85.rest_20_), channel_id=1, source_target_pairs={{0,96},{32,64},{64,32},{96,0},{1,97},{33,65},{65,33},{97,1},{2,98}... | collective-permute-start | bytes 1179656 | tf_op jit(solution)/shard_map/ppermute | solution.py:82
  57.2 2.2 collective-permute-start.23
  59.8 5.3 %collective-permute-done.35.rest_22_ = bf16[512,384]{1,0:T(8,128)(2,1)S(1)} collective-permute-done((bf16[512,384]{1,0:T(8,128)(2,1)S(1)}, bf16[512,384]{1,0:T(8,128)(2,1)S(1)}, u32[]{:S(2)}, u32[]{:S(2)}) %collective-permute-start.35) | collective-permute-done | bytes 393248 | tf_op jit(solution)/shard_map/ppermute | solution.py:82
  65.9 10.5 %collective-permute-done.21.rest_10_ = bf16[512,512]{1,0:T(8,128)(2,1)S(1)} collective-permute-done((bf16[512,512]{1,0:T(8,128)(2,1)S(1)}, bf16[512,512]{1,0:T(8,128)(2,1)S(1)}, u32[]{:S(2)}, u32[]{:S(2)}) %collective-permute-start.21) | collective-permute-done | bytes 524320 | tf_op jit(solution)/shard_map/ppermute | solution.py:82
  77.3 2.1 collective-permute-start.8
  81.0 10.5 %collective-permute-done.19.refs_0_.refs_2_ = bf16[512,1024]{1,0:T(8,128)(2,1)S(1)} collective-permute-done((bf16[512,1024]{1,0:T(8,128)(2,1)S(1)}, bf16[512,1024]{1,0:T(8,128)(2,1)S(1)}, u32[]{:S(2)}, u32[]{:S(2)}) %collective-permute-start.19) | collective-permute-done | bytes 1048608 | tf_op jit(solution)/shard_map/ppermute | solution.py:82
  92.7 6.5 %collective-permute-done.31.refs_0_.refs_2_ = bf16[512,896]{1,0:T(8,128)(2,1)S(1)} collective-permute-done((bf16[512,896]{1,0:T(8,128)(2,1)S(1)}, bf16[512,896]{1,0:T(8,128)(2,1)S(1)}, u32[]{:S(2)}, u32[]{:S(2)}) %collective-permute-start.31) | collective-permute-done | bytes 917536 | tf_op jit(solution)/shard_map/ppermute | solution.py:82
  99.2 2.9 %collective-permute-start.24 = (bf16[512,512]{1,0:T(8,128)(2,1)}, bf16[512,512]{1,0:T(8,128)(2,1)}, u32[]{:S(2)}, u32[]{:S(2)}) collective-permute-start(bf16[512,512]{1,0:T(8,128)(2,1)} %get-tuple-element.75.rest_13_), channel_id=1, source_target_pairs={{0,6},{2,4},{4,2},{6,0},{1,7},{3,5},{5,3},{7,1},{8,14},{10,12},{12... | collective-permute-start | bytes 1572872 | tf_op jit(solution)/shard_map/ppermute | solution.py:82
  108.3 3.2 %collective-permute-start.10 = (bf16[512,512]{1,0:T(8,128)(2,1)}, bf16[512,512]{1,0:T(8,128)(2,1)}, u32[]{:S(2)}, u32[]{:S(2)}) collective-permute-start(bf16[512,512]{1,0:T(8,128)(2,1)} %get-tuple-element.62.rest_1_), channel_id=1, source_target_pairs={{0,8},{8,0},{16,24},{24,16},{1,9},{9,1},{17,25},{25,17},{2,10},{10... | collective-permute-start | bytes 1572872 | tf_op jit(solution)/shard_map/ppermute | solution.py:82
  125.0 2.2 collective-permute-start.37
  127.2 5.3 %first_norm.1.normed = bf16[640,2048]{1,0:T(8,128)(2,1)} custom-call(s32[1]{0:T(128)} %bitcast.core, bf16[640,1024]{1,0:T(8,128)(2,1)} %own.3, bf16[640,1024]{1,0:T(8,128)(2,1)} %copy-done.32, f32[1,2048]{1,0:T(1,128)} %bitcast.15), custom_call_target="tpu_custom_call" | custom-call | flops 5000000000 | bytes 5242880 | tf_op jit(solution)/shard_map/first_norm/pallas_call | solution.py:301
  132.5 14.2 %first_hidden.1 = (bf16[640,1408]{1,0:T(8,128)(2,1)}, bf16[2048,2816]{1,0:T(8,128)(2,1)}) custom-call(s32[1]{0:T(128)} %bitcast.1.at, bf16[640,2048]{1,0:T(8,128)(2,1)} %first_norm.1.normed, bf16[512,512]{1,0:T(8,128)(2,1)} %copy-done.26, bf16[512,512]{1,0:T(8,128)(2,1)} %get-tuple-element.62.rest_1_, bf16[512,512]{1,0:T(8,128)(2,1)} %copy-done.39, ...), custom_call_target="tpu_custom_call" | custom-call | flops 7381975040 | bytes 23068672 | tf_op jit(solution)/shard_map/first_hidden/pallas_call | solution.py:352
  146.7 10.2 %first_down.1 = (bf16[640,2048]{1,0:T(8,128)(2,1)}, bf16[2048,1408]{1,0:T(8,128)(2,1)}) custom-call(s32[1]{0:T(128)} %bitcast.1.at, bf16[640,1408]{1,0:T(8,128)(2,1)} %get-tuple-element.87.hidden, bf16[1024,384]{1,0:T(8,128)(2,1)} %get-tuple-element.88.rest_0_, bf16[1024,384]{1,0:T(8,128)(2,1)} %collective-permute-done.37.rest_1_, ...), custom_call_target="tpu_custom_call" | custom-call | flops 3690987520 | bytes 11534336 | tf_op jit(solution)/shard_map/first_down/pallas_call | solution.py:404
  157.0 7.0 %collective-permute-start.40 = (bf16[640,2048]{1,0:T(8,128)(2,1)}, bf16[640,2048]{1,0:T(8,128)(2,1)}, u32[]{:S(2)}, u32[]{:S(2)}) collective-permute-start(bf16[640,2048]{1,0:T(8,128)(2,1)} %get-tuple-element.91.term), channel_id=1, source_target_pairs={{0,1},{1,0},{2,3},{3,2},{4,5},{5,4},{6,7},{7,6},{8,9},{9,8},{10,11... | collective-permute-start | bytes 7864328 | tf_op jit(solution)/shard_map/ppermute | solution.py:36
  167.2 21.6 %collective-permute-done.43.rest_5_ = bf16[1024,512]{1,0:T(8,128)(2,1)S(1)} collective-permute-done((bf16[1024,512]{1,0:T(8,128)(2,1)}, bf16[1024,512]{1,0:T(8,128)(2,1)S(1)}, u32[]{:S(2)}, u32[]{:S(2)}) %collective-permute-start.43) | collective-permute-done | bytes 1048608 | tf_op jit(solution)/shard_map/ppermute | solution.py:82
  188.8 2.7 %collective-permute-done.41.rest_1_ = bf16[1024,512]{1,0:T(8,128)(2,1)S(1)} collective-permute-done((bf16[1024,512]{1,0:T(8,128)(2,1)S(1)}, bf16[1024,512]{1,0:T(8,128)(2,1)S(1)}, u32[]{:S(2)}, u32[]{:S(2)}) %collective-permute-start.41) | collective-permute-done | bytes 1048608 | tf_op jit(solution)/shard_map/ppermute | solution.py:82
  193.5 5.3 %assemble.1.u_rows.v_rows.rows = bf16[2048,1536]{1,0:T(8,128)(2,1)} custom-call(s32[1]{0:T(128)} %bitcast.1.at, bf16[1024,512]{1,0:T(8,128)(2,1)} %copy-done.22, bf16[1024,512]{1,0:T(8,128)(2,1)} %copy-done.36, bf16[1024,512]{1,0:T(8,128)(2,1)} %copy-done.23, bf16[1024,512]{1,0:T(8,128)(2,1)} %copy-done.37, bf16[1024,512]{1,0:T(8,128)(2,1)} %copy-done.21, ...), custom_call_target="tpu_custom_call" | custom-call | flops 5000000000 | bytes 25165824 | tf_op jit(solution)/shard_map/assemble/pallas_call | solution.py:444
  198.8 13.0 %gates.1 = (bf16[640,2048]{1,0:T(8,128)(2,1)}, f32[2,640,512]{2,1,0:T(8,128)}, f32[640,128]{1,0:T(8,128)}) custom-call(s32[1]{0:T(128)} %bitcast.core, bf16[640,1024]{1,0:T(8,128)(2,1)} %own.3, bf16[640,1024]{1,0:T(8,128)(2,1)} %copy-done.32, bf16[640,2048]{1,0:T(8,128)(2,1)} %get-tuple-element.91.term, bf16[640,2048]{1,0:T(8,128)(2,1)} %collective-permute-done.40.far, ...), custom_call_target="tpu_custom_call" | custom-call | flops 2684354560 | bytes 4194304 | tf_op jit(solution)/shard_map/gates/pallas_call | solution.py:501
  215.2 7.0 %mix.1.term = bf16[640,2048]{1,0:T(8,128)(2,1)} custom-call(f32[2,640,512]{2,1,0:T(8,128)} %get-tuple-element.96.act, f32[640,128]{1,0:T(8,128)} %get-tuple-element.97.sums, f32[640,128]{1,0:T(8,128)} %copy-done.33, f32[1,512]{1,0:T(1,128)} %bitcast.13, f32[1,512]{1,0:T(1,128)} %bitcast.14, bf16[4,128,128]{2,1,0:T(8,128)(2,1)} %weight.1, f32[4,128]{1,0:T(4,128)} %shift.1, ...), custom_call_target="tpu_custom_call" | custom-call | flops 1342177280 | bytes 2097152 | tf_op jit(solution)/shard_map/mix/pallas_call | solution.py:566
  222.5 4.7 %collective-permute-done.45.far = bf16[640,2048]{1,0:T(8,128)(2,1)S(1)} collective-permute-done((bf16[640,2048]{1,0:T(8,128)(2,1)}, bf16[640,2048]{1,0:T(8,128)(2,1)S(1)}, u32[]{:S(2)}, u32[]{:S(2)}) %collective-permute-start.45) | collective-permute-done | bytes 2621472 | tf_op jit(solution)/shard_map/ppermute | solution.py:36
  228.8 20.8 %second_pass.1 = (bf16[640,1024]{1,0:T(8,128)(2,1)}, bf16[640,1024]{1,0:T(8,128)(2,1)}, bf16[640,1024]{1,0:T(8,128)(2,1)}) custom-call(s32[1]{0:T(128)} %bitcast.core, bf16[640,2048]{1,0:T(8,128)(2,1)} %get-tuple-element.95.middle, bf16[640,2048]{1,0:T(8,128)(2,1)} %mix.1.term, bf16[640,2048]{1,0:T(8,128)(2,1)} %copy-done.34, f32[1,2048]{1,0:T(1,128)} %bitcast.16, ...), custom_call_target="tpu_custom_call" | custom-call | flops 11072962560 | bytes 17301504 | tf_op jit(solution)/shard_map/second_pass/pallas_call | solution.py:645
  250.0 2.9 %collective-permute-done.46 = bf16[640,1024]{1,0:T(8,128)(2,1)S(1)} collective-permute-done((bf16[640,1024]{1,0:T(8,128)(2,1)}, bf16[640,1024]{1,0:T(8,128)(2,1)S(1)}, u32[]{:S(2)}, u32[]{:S(2)}) %collective-permute-start.46) | collective-permute-done | bytes 1310752 | tf_op jit(solution)/shard_map/ppermute | solution.py:36
  252.9 3.6 %add_convert_fusion = bf16[640,1024]{1,0:T(8,128)(2,1)} fusion(bf16[640,1024]{1,0:T(8,128)(2,1)S(1)} %collective-permute-done.46, bf16[640,1024]{1,0:T(8,128)(2,1)} %get-tuple-element.101, bf16[640,1024]{1,0:T(8,128)(2,1)} %get-tuple-element.100), kind=kLoop, calls=%fused_computation | loop fusion | flops 4587520 | bytes 5242880 | tf_op jit(solution)/shard_map/convert_element_type | solution.py:748
  (180 shorter events, 56.3 us)
Async XLA Ops:
  6.2 9.6 %collective-permute-start.1 = (bf16[32,2048]{1,0:T(8,128)(2,1)}, bf16[32,2048]{1,0:T(8,128)(2,1)S(1)}, u32[]{:S(2)}, u32[]{:S(2)}) collective-permute-start(bf16[32,2048]{1,0:T(8,128)(2,1)} %get-tuple-element.54.refs_0_), channel_id=1, source_target_pairs={{0,2},{2,0},{4,6},{6,4},{1,3},{3,1},{5,7},{7,5},{8,10},{10,8},{12,... | collective-permute-start | bytes 393224 | tf_op jit(solution)/shard_map/ppermute | solution.py:82
  8.9 10.6 %collective-permute-start.26 = (bf16[64,1792]{1,0:T(8,128)(2,1)S(1)}, bf16[64,1792]{1,0:T(8,128)(2,1)S(1)}, u32[]{:S(2)}, u32[]{:S(2)}) collective-permute-start(bf16[64,1792]{1,0:T(8,128)(2,1)S(1)} %join.23.refs_0_), channel_id=1, source_target_pairs={{0,6},{2,4},{4,2},{6,0},{1,7},{3,5},{5,3},{7,1},{8,14},{10,12},{12... | collective-permute-start | bytes 688136 | tf_op jit(solution)/shard_map/ppermute | solution.py:82
  12.3 10.1 %collective-permute-start.14 = (bf16[64,1920]{1,0:T(8,128)(2,1)S(1)}, bf16[64,1920]{1,0:T(8,128)(2,1)S(1)}, u32[]{:S(2)}, u32[]{:S(2)}) collective-permute-start(bf16[64,1920]{1,0:T(8,128)(2,1)S(1)} %join.19.refs_0_), channel_id=1, source_target_pairs={{0,96},{32,64},{64,32},{96,0},{1,97},{33,65},{65,33},{97,1},{2,98}... | collective-permute-start | bytes 737288 | tf_op jit(solution)/shard_map/ppermute | solution.py:82
  19.7 37.5 %collective-permute-start = (bf16[640,1024]{1,0:T(8,128)(2,1)S(1)}, bf16[640,1024]{1,0:T(8,128)(2,1)S(1)}, u32[]{:S(2)}, u32[]{:S(2)}) collective-permute-start(bf16[640,1024]{1,0:T(8,128)(2,1)S(1)} %copy-done.31), channel_id=1, source_target_pairs={{0,1},{1,0},{2,3},{3,2},{4,5},{5,4},{6,7},{7,6},{8,9},{9,8},{10,11... | collective-permute-start | bytes 3932168 | tf_op jit(solution)/shard_map/ppermute | solution.py:36
  32.0 14.4 %collective-permute-start.17 = (bf16[256,1024]{1,0:T(8,128)(2,1)S(1)}, bf16[256,1024]{1,0:T(8,128)(2,1)S(1)}, u32[]{:S(2)}, u32[]{:S(2)}) collective-permute-start(bf16[256,1024]{1,0:T(8,128)(2,1)S(1)} %get-tuple-element.68.refs_0_), channel_id=1, source_target_pairs={{0,32},{32,0},{64,96},{96,64},{1,33},{33,1},{65,97},{97,65},{2,34}... | collective-permute-start | bytes 1572872 | tf_op jit(solution)/shard_map/ppermute | solution.py:82
  32.5 13.8 %collective-permute-start.18 = (bf16[256,896]{1,0:T(8,128)(2,1)S(1)}, bf16[256,896]{1,0:T(8,128)(2,1)S(1)}, u32[]{:S(2)}, u32[]{:S(2)}) collective-permute-start(bf16[256,896]{1,0:T(8,128)(2,1)S(1)} %get-tuple-element.69.refs_1_), channel_id=1, source_target_pairs={{0,24},{8,16},{16,8},{24,0},{1,25},{9,17},{17,9},{25,1},{2,26},{10... | collective-permute-start | bytes 1376264 | tf_op jit(solution)/shard_map/ppermute | solution.py:82
  36.4 11.7 %collective-permute-start.5 = (bf16[256,1024]{1,0:T(8,128)(2,1)S(1)}, bf16[256,1024]{1,0:T(8,128)(2,1)S(1)}, u32[]{:S(2)}, u32[]{:S(2)}) collective-permute-start(bf16[256,1024]{1,0:T(8,128)(2,1)S(1)} %get-tuple-element.57.refs_0_), channel_id=1, source_target_pairs={{0,6},{2,4},{4,2},{6,0},{1,7},{3,5},{5,3},{7,1},{8,14},{10,12},{12... | collective-permute-start | bytes 1572872 | tf_op jit(solution)/shard_map/ppermute | solution.py:82
  40.7 16.0 %collective-permute-start.6 = (bf16[256,1024]{1,0:T(8,128)(2,1)S(1)}, bf16[256,1024]{1,0:T(8,128)(2,1)S(1)}, u32[]{:S(2)}, u32[]{:S(2)}) collective-permute-start(bf16[256,1024]{1,0:T(8,128)(2,1)S(1)} %get-tuple-element.58.refs_1_), channel_id=1, source_target_pairs={{0,96},{32,64},{64,32},{96,0},{1,97},{33,65},{65,33},{97,1},{2,98}... | collective-permute-start | bytes 1572872 | tf_op jit(solution)/shard_map/ppermute | solution.py:82
  46.3 13.1 %collective-permute-start.33 = (bf16[512,384]{1,0:T(8,128)(2,1)S(1)}, bf16[512,384]{1,0:T(8,128)(2,1)S(1)}, u32[]{:S(2)}, u32[]{:S(2)}) collective-permute-start(bf16[512,384]{1,0:T(8,128)(2,1)S(1)} %get-tuple-element.83.rest_16_), channel_id=1, source_target_pairs={{0,24},{8,16},{16,8},{24,0},{1,25},{9,17},{17,9},{25,1},{2,26},{10... | collective-permute-start | bytes 1179656 | tf_op jit(solution)/shard_map/ppermute | solution.py:82
  46.6 32.9 %collective-permute-start.20 = (bf16[512,896]{1,0:T(8,128)(2,1)S(1)}, bf16[512,896]{1,0:T(8,128)(2,1)S(1)}, u32[]{:S(2)}, u32[]{:S(2)}) collective-permute-start(bf16[512,896]{1,0:T(8,128)(2,1)S(1)} %get-tuple-element.71.refs_1_), channel_id=1, source_target_pairs={{0,2},{2,0},{4,6},{6,4},{1,3},{3,1},{5,7},{7,5},{8,10},{10,8},{12,... | collective-permute-start | bytes 2752520 | tf_op jit(solution)/shard_map/ppermute | solution.py:82
  48.1 17.0 %collective-permute-start.35 = (bf16[512,384]{1,0:T(8,128)(2,1)S(1)}, bf16[512,384]{1,0:T(8,128)(2,1)S(1)}, u32[]{:S(2)}, u32[]{:S(2)}) collective-permute-start(bf16[512,384]{1,0:T(8,128)(2,1)S(1)} %get-tuple-element.85.rest_20_), channel_id=1, source_target_pairs={{0,96},{32,64},{64,32},{96,0},{1,97},{33,65},{65,33},{97,1},{2,98}... | collective-permute-start | bytes 1179656 | tf_op jit(solution)/shard_map/ppermute | solution.py:82
  56.6 19.8 %collective-permute-start.21 = (bf16[512,512]{1,0:T(8,128)(2,1)S(1)}, bf16[512,512]{1,0:T(8,128)(2,1)S(1)}, u32[]{:S(2)}, u32[]{:S(2)}) collective-permute-start(bf16[512,512]{1,0:T(8,128)(2,1)S(1)} %get-tuple-element.72.rest_8_), channel_id=1, source_target_pairs={{0,2},{2,0},{4,6},{6,4},{1,3},{3,1},{5,7},{7,5},{8,10},{10,8},{12,... | collective-permute-start | bytes 1572872 | tf_op jit(solution)/shard_map/ppermute | solution.py:82
  57.2 20.0 %collective-permute-start.23 = (bf16[512,512]{1,0:T(8,128)(2,1)S(1)}, bf16[512,512]{1,0:T(8,128)(2,1)}, u32[]{:S(2)}, u32[]{:S(2)}) collective-permute-start(bf16[512,512]{1,0:T(8,128)(2,1)S(1)} %get-tuple-element.74.rest_12_), channel_id=1, source_target_pairs={{0,6},{2,4},{4,2},{6,0},{1,7},{3,5},{5,3},{7,1},{8,14},{10,12},{12... | collective-permute-start | bytes 1572872 | tf_op jit(solution)/shard_map/ppermute | solution.py:82
  59.4 20.0 %collective-permute-start.9 = (bf16[512,512]{1,0:T(8,128)(2,1)S(1)}, bf16[512,512]{1,0:T(8,128)(2,1)S(1)}, u32[]{:S(2)}, u32[]{:S(2)}) collective-permute-start(bf16[512,512]{1,0:T(8,128)(2,1)S(1)} %get-tuple-element.61.rest_0_), channel_id=1, source_target_pairs={{0,8},{8,0},{16,24},{24,16},{1,9},{9,1},{17,25},{25,17},{2,10},{10... | collective-permute-start | bytes 1572872 | tf_op jit(solution)/shard_map/ppermute | solution.py:82
  65.2 26.4 %collective-permute-start.19 = (bf16[512,1024]{1,0:T(8,128)(2,1)S(1)}, bf16[512,1024]{1,0:T(8,128)(2,1)S(1)}, u32[]{:S(2)}, u32[]{:S(2)}) collective-permute-start(bf16[512,1024]{1,0:T(8,128)(2,1)S(1)} %get-tuple-element.70.refs_0_), channel_id=1, source_target_pairs={{0,6},{2,4},{4,2},{6,0},{1,7},{3,5},{5,3},{7,1},{8,14},{10,12},{12... | collective-permute-start | bytes 3145736 | tf_op jit(solution)/shard_map/ppermute | solution.py:82
  76.5 26.4 %collective-permute-start.7 = (bf16[512,1024]{1,0:T(8,128)(2,1)S(1)}, bf16[512,1024]{1,0:T(8,128)(2,1)S(1)}, u32[]{:S(2)}, u32[]{:S(2)}) collective-permute-start(bf16[512,1024]{1,0:T(8,128)(2,1)S(1)} %get-tuple-element.59.refs_0_), channel_id=1, source_target_pairs={{0,32},{32,0},{64,96},{96,64},{1,33},{33,1},{65,97},{97,65},{2,34}... | collective-permute-start | bytes 3145736 | tf_op jit(solution)/shard_map/ppermute | solution.py:82
  77.3 25.6 %collective-permute-start.8 = (bf16[512,1024]{1,0:T(8,128)(2,1)S(1)}, bf16[512,1024]{1,0:T(8,128)(2,1)S(1)}, u32[]{:S(2)}, u32[]{:S(2)}) collective-permute-start(bf16[512,1024]{1,0:T(8,128)(2,1)S(1)} %get-tuple-element.60.refs_1_), channel_id=1, source_target_pairs={{0,8},{8,0},{16,24},{24,16},{1,9},{9,1},{17,25},{25,17},{2,10},{10... | collective-permute-start | bytes 3145736 | tf_op jit(solution)/shard_map/ppermute | solution.py:82
  79.4 19.8 %collective-permute-start.31 = (bf16[512,896]{1,0:T(8,128)(2,1)S(1)}, bf16[512,896]{1,0:T(8,128)(2,1)S(1)}, u32[]{:S(2)}, u32[]{:S(2)}) collective-permute-start(bf16[512,896]{1,0:T(8,128)(2,1)S(1)} %get-tuple-element.81.refs_0_), channel_id=1, source_target_pairs={{0,96},{32,64},{64,32},{96,0},{1,97},{33,65},{65,33},{97,1},{2,98}... | collective-permute-start | bytes 2752520 | tf_op jit(solution)/shard_map/ppermute | solution.py:82
  79.5 19.7 %collective-permute-start.32 = (bf16[512,896]{1,0:T(8,128)(2,1)S(1)}, bf16[512,896]{1,0:T(8,128)(2,1)S(1)}, u32[]{:S(2)}, u32[]{:S(2)}) collective-permute-start(bf16[512,896]{1,0:T(8,128)(2,1)S(1)} %get-tuple-element.82.refs_1_), channel_id=1, source_target_pairs={{0,24},{8,16},{16,8},{24,0},{1,25},{9,17},{17,9},{25,1},{2,26},{10... | collective-permute-start | bytes 2752520 | tf_op jit(solution)/shard_map/ppermute | solution.py:82
  91.5 16.8 %collective-permute-start.11 = (bf16[512,512]{1,0:T(8,128)(2,1)S(1)}, bf16[512,512]{1,0:T(8,128)(2,1)S(1)}, u32[]{:S(2)}, u32[]{:S(2)}) collective-permute-start(bf16[512,512]{1,0:T(8,128)(2,1)S(1)} %get-tuple-element.63.rest_4_), channel_id=1, source_target_pairs={{0,32},{32,0},{64,96},{96,64},{1,33},{33,1},{65,97},{97,65},{2,34}... | collective-permute-start | bytes 1572872 | tf_op jit(solution)/shard_map/ppermute | solution.py:82
  99.2 25.8 %collective-permute-start.22 = (bf16[512,512]{1,0:T(8,128)(2,1)}, bf16[512,512]{1,0:T(8,128)(2,1)}, u32[]{:S(2)}, u32[]{:S(2)}) collective-permute-start(bf16[512,512]{1,0:T(8,128)(2,1)} %get-tuple-element.73.rest_9_), channel_id=1, source_target_pairs={{0,2},{2,0},{4,6},{6,4},{1,3},{3,1},{5,7},{7,5},{8,10},{10,8},{12,... | collective-permute-start | bytes 1572872 | tf_op jit(solution)/shard_map/ppermute | solution.py:82
  99.2 25.8 %collective-permute-start.24 = (bf16[512,512]{1,0:T(8,128)(2,1)}, bf16[512,512]{1,0:T(8,128)(2,1)}, u32[]{:S(2)}, u32[]{:S(2)}) collective-permute-start(bf16[512,512]{1,0:T(8,128)(2,1)} %get-tuple-element.75.rest_13_), channel_id=1, source_target_pairs={{0,6},{2,4},{4,2},{6,0},{1,7},{3,5},{5,3},{7,1},{8,14},{10,12},{12... | collective-permute-start | bytes 1572872 | tf_op jit(solution)/shard_map/ppermute | solution.py:82
  102.9 20.2 %collective-permute-start.36 = (bf16[512,384]{1,0:T(8,128)(2,1)}, bf16[512,384]{1,0:T(8,128)(2,1)}, u32[]{:S(2)}, u32[]{:S(2)}) collective-permute-start(bf16[512,384]{1,0:T(8,128)(2,1)} %get-tuple-element.86.rest_21_), channel_id=1, source_target_pairs={{0,96},{32,64},{64,32},{96,0},{1,97},{33,65},{65,33},{97,1},{2,98}... | collective-permute-start | bytes 1179656 | tf_op jit(solution)/shard_map/ppermute | solution.py:82
  108.3 24.1 %collective-permute-start.10 = (bf16[512,512]{1,0:T(8,128)(2,1)}, bf16[512,512]{1,0:T(8,128)(2,1)}, u32[]{:S(2)}, u32[]{:S(2)}) collective-permute-start(bf16[512,512]{1,0:T(8,128)(2,1)} %get-tuple-element.62.rest_1_), channel_id=1, source_target_pairs={{0,8},{8,0},{16,24},{24,16},{1,9},{9,1},{17,25},{25,17},{2,10},{10... | collective-permute-start | bytes 1572872 | tf_op jit(solution)/shard_map/ppermute | solution.py:82
  112.3 20.1 %collective-permute-start.12 = (bf16[512,512]{1,0:T(8,128)(2,1)}, bf16[512,512]{1,0:T(8,128)(2,1)}, u32[]{:S(2)}, u32[]{:S(2)}) collective-permute-start(bf16[512,512]{1,0:T(8,128)(2,1)} %get-tuple-element.64.rest_5_), channel_id=1, source_target_pairs={{0,32},{32,0},{64,96},{96,64},{1,33},{33,1},{65,97},{97,65},{2,34}... | collective-permute-start | bytes 1572872 | tf_op jit(solution)/shard_map/ppermute | solution.py:82
  123.1 23.6 %collective-permute-start.38 = (bf16[1024,512]{1,0:T(8,128)(2,1)}, bf16[1024,512]{1,0:T(8,128)(2,1)}, u32[]{:S(2)}, u32[]{:S(2)}) collective-permute-start(bf16[1024,512]{1,0:T(8,128)(2,1)} %get-tuple-element.89.rest_2_), channel_id=1, source_target_pairs={{0,24},{8,16},{16,8},{24,0},{1,25},{9,17},{17,9},{25,1},{2,26},{10... | collective-permute-start | bytes 3145736 | tf_op jit(solution)/shard_map/ppermute | solution.py:82
  125.0 21.8 %collective-permute-start.39 = (bf16[1024,512]{1,0:T(8,128)(2,1)}, bf16[1024,512]{1,0:T(8,128)(2,1)}, u32[]{:S(2)}, u32[]{:S(2)}) collective-permute-start(bf16[1024,512]{1,0:T(8,128)(2,1)} %get-tuple-element.90.rest_4_), channel_id=1, source_target_pairs={{0,96},{32,64},{64,32},{96,0},{1,97},{33,65},{65,33},{97,1},{2,98}... | collective-permute-start | bytes 3145736 | tf_op jit(solution)/shard_map/ppermute | solution.py:82
  125.0 21.7 %collective-permute-start.37 = (bf16[1024,384]{1,0:T(8,128)(2,1)}, bf16[1024,384]{1,0:T(8,128)(2,1)}, u32[]{:S(2)}, u32[]{:S(2)}) collective-permute-start(bf16[1024,384]{1,0:T(8,128)(2,1)} %get-tuple-element.88.rest_0_), channel_id=1, source_target_pairs={{0,6},{2,4},{4,2},{6,0},{1,7},{3,5},{5,3},{7,1},{8,14},{10,12},{12... | collective-permute-start | bytes 2359304 | tf_op jit(solution)/shard_map/ppermute | solution.py:82
  157.0 41.8 %collective-permute-start.40 = (bf16[640,2048]{1,0:T(8,128)(2,1)}, bf16[640,2048]{1,0:T(8,128)(2,1)}, u32[]{:S(2)}, u32[]{:S(2)}) collective-permute-start(bf16[640,2048]{1,0:T(8,128)(2,1)} %get-tuple-element.91.term), channel_id=1, source_target_pairs={{0,1},{1,0},{2,3},{3,2},{4,5},{5,4},{6,7},{7,6},{8,9},{9,8},{10,11... | collective-permute-start | bytes 7864328 | tf_op jit(solution)/shard_map/ppermute | solution.py:36
  164.0 24.8 %collective-permute-start.43 = (bf16[1024,512]{1,0:T(8,128)(2,1)}, bf16[1024,512]{1,0:T(8,128)(2,1)S(1)}, u32[]{:S(2)}, u32[]{:S(2)}) collective-permute-start(bf16[1024,512]{1,0:T(8,128)(2,1)} %copy-done.21), channel_id=1, source_target_pairs={{0,2},{2,0},{4,6},{6,4},{1,3},{3,1},{5,7},{7,5},{8,10},{10,8},{12,... | collective-permute-start | bytes 3145736 | tf_op jit(solution)/shard_map/ppermute | solution.py:82
  167.2 24.3 %collective-permute-start.41 = (bf16[1024,512]{1,0:T(8,128)(2,1)S(1)}, bf16[1024,512]{1,0:T(8,128)(2,1)S(1)}, u32[]{:S(2)}, u32[]{:S(2)}) collective-permute-start(bf16[1024,512]{1,0:T(8,128)(2,1)S(1)} %get-tuple-element.92.rest_0_), channel_id=1, source_target_pairs={{0,8},{8,0},{16,24},{24,16},{1,9},{9,1},{17,25},{25,17},{2,10},{10... | collective-permute-start | bytes 3145736 | tf_op jit(solution)/shard_map/ppermute | solution.py:82
  167.2 24.4 %collective-permute-start.42 = (bf16[1024,512]{1,0:T(8,128)(2,1)S(1)}, bf16[1024,512]{1,0:T(8,128)(2,1)S(1)}, u32[]{:S(2)}, u32[]{:S(2)}) collective-permute-start(bf16[1024,512]{1,0:T(8,128)(2,1)S(1)} %get-tuple-element.93.rest_2_), channel_id=1, source_target_pairs={{0,32},{32,0},{64,96},{96,64},{1,33},{33,1},{65,97},{97,65},{2,34}... | collective-permute-start | bytes 3145736 | tf_op jit(solution)/shard_map/ppermute | solution.py:82
  (59 other events, 637.4 us)

commit v6 on v4

--- a/solution.py
+++ b/solution.py
@@ -289,12 +289,24 @@
 
 
 def first_kernel(core, at, own, other, gain, *rest):
-    pieces, (hidden, kept, weight, normed, sems, out_sem) = rest[:24], rest[24:]
+    pieces, (hidden, kept, weight, normed, sems, out_sems) = rest[:24], rest[24:]
     step = pl.program_id(0)
+    begin = starts(FIRST)
+    copies = []
+    for c in range(6):
+        columns = pl.ds(begin[c], FIRST[c] * LANES)
+        copies.append(
+            pltpu.make_async_copy(weight.at[:, columns], kept.at[:, columns], out_sems.at[c])
+        )
+
+    for k, colors in enumerate(((0, 1, 2), (3,), (4,), (5,))):
+
+        @pl.when(step == k)
+        def _():
+            place_blocks(at[0], pieces, weight, sems, FIRST, colors)
 
     @pl.when(step == 0)
     def _():
-        place_blocks(at[0], pieces, weight, sems, FIRST, range(6))
         left = jnp.where(core[0] == 0, own[...], other[...])
         right = jnp.where(core[0] == 0, other[...], own[...])
         values = jnp.concatenate([left, right], axis=1).astype(jnp.float32)
@@ -305,14 +317,14 @@
         @pl.when(step == min(c, 4))
         def _():
             wait_color(weight, sems, FIRST, c)
+            copies[c].start()
 
     hidden_step(step, normed, weight, hidden)
 
     @pl.when(step == 4)
     def _():
-        copy = pltpu.make_async_copy(weight, kept, out_sem)
-        copy.start()
-        copy.wait()
+        for copy in copies:
+            copy.wait()
 
 
 def first_hidden(core, at, own, other, gain, pieces):
@@ -335,7 +347,7 @@
                 pltpu.VMEM((width, columns), jnp.bfloat16),
                 pltpu.VMEM((count, width), jnp.bfloat16),
                 pltpu.SemaphoreType.DMA((6,)),
-                pltpu.SemaphoreType.DMA,
+                pltpu.SemaphoreType.DMA((6,)),
             ],
         ),
         compiler_params=params(1),
@@ -433,10 +445,8 @@
     )(at, *pieces)
 
 
-def gates_kernel(blocks, core, own, other, term, far, gain, rows, middle, act, sums, normed):
-    step = pl.program_id(0)
-
-    @pl.when(step < blocks)
+def gates_kernel(core, own, other, term, far, gain, rows, middle, act, sums, normed):
+    @pl.when(pl.program_id(0) == 0)
     def _():
         left = jnp.where(core[0] == 0, own[...], other[...])
         right = jnp.where(core[0] == 0, other[...], own[...])
@@ -444,32 +454,24 @@
         values = values + 0.5 * (term[...].astype(jnp.float32) + far[...].astype(jnp.float32))
         mid = values.astype(jnp.bfloat16)
         middle[...] = mid
-        block = pl.ds(pl.multiple_of(step * SPAN, SPAN), SPAN)
-        normed[block, :] = normed_rows(mid.astype(jnp.float32), gain[...])
-
-    @pl.when(step >= blocks)
-    def _():
-        acted = gelu(dot(normed[...], rows[...]))
-        act[0] = acted
-
-        @pl.when(step == blocks)
-        def _():
-            lane = lax.broadcasted_iota(jnp.int32, sums.shape, 1)
-            total = jnp.sum(acted, axis=1, keepdims=True)
-            squares = jnp.sum(acted * acted, axis=1, keepdims=True)
-            sums[...] = jnp.where(lane == 0, total, squares)
+        normed[...] = normed_rows(mid.astype(jnp.float32), gain[...])
+
+    acted = gelu(dot(normed[...], rows[...]))
+    act[0] = acted
+
+    @pl.when(pl.program_id(0) == 0)
+    def _():
+        lane = lax.broadcasted_iota(jnp.int32, sums.shape, 1)
+        total = jnp.sum(acted, axis=1, keepdims=True)
+        squares = jnp.sum(acted * acted, axis=1, keepdims=True)
+        sums[...] = jnp.where(lane == 0, total, squares)
 
 
 def gates(core, own, other, term, far, gain, weight, chans):
     count, half = own.shape
     width = 2 * half
-    blocks = count // SPAN
-
-    def block(columns):
-        return spec((SPAN, columns), lambda i, c: (jnp.minimum(i, blocks - 1), 0))
-
-    return pl.pallas_call(
-        functools.partial(gates_kernel, blocks),
+    return pl.pallas_call(
+        gates_kernel,
         out_shape=[
             jax.ShapeDtypeStruct((count, width), jnp.bfloat16),
             jax.ShapeDtypeStruct((2, count, chans), jnp.float32),
@@ -477,18 +479,18 @@
         ],
         grid_spec=pltpu.PrefetchScalarGridSpec(
             num_scalar_prefetch=1,
-            grid=(blocks + 2,),
+            grid=(2,),
             in_specs=[
-                block(half),
-                block(half),
-                block(width),
-                block(width),
+                whole((count, half)),
+                whole((count, half)),
+                whole((count, width)),
+                whole((count, width)),
                 whole((1, width)),
-                spec((width, chans), lambda i, c: (0, 2 - jnp.maximum(i - blocks, 0))),
+                spec((width, chans), lambda i, c: (0, 2 - i)),
             ],
             out_specs=[
-                block(width),
-                spec((1, count, chans), lambda i, c: (jnp.maximum(i - blocks, 0), 0, 0)),
+                whole((count, width)),
+                spec((1, count, chans), lambda i, c: (i, 0, 0)),
                 whole((count, LANES)),
             ],
             scratch_shapes=[pltpu.VMEM((count, width), jnp.bfloat16)],

time: 269 us -> 268 us (level)
  transfers between devices with their start and end apart: 47 -> 47, of which waited for: 22 -> 22; matrix products, arithmetic and copies ran while one was open for 0% -> 0% of each run, Pallas kernels for 10% -> 9%
where the time goes in v6:
time: 268 us
  waiting for transfers between devices  132 us (49%)
  Pallas kernels  77 us (29%)
  starting transfers between devices  41.8 us (16%)
  local copies, waits for them, and re-layouts  12.6 us (5%)
  other arithmetic  3.65 us (1%)
    ppermute x42, waiting for transfers between devices, exchange(): return lax.ppermute(x, axis, [(i, i ^ flip) for i in range(4)])  123 us
    ppermute x42, starting transfers between devices, exchange(): return lax.ppermute(x, axis, [(i, i ^ flip) for i in range(4)])  29.4 us
    pallas_call x1, Pallas kernels, second_pass(): pl.pallas_call(second_kernel, out_shape=[jax.ShapeDtypeStruct((count, hal...  20.7 us
    pallas_call x1, Pallas kernels, first_hidden(): pl.pallas_call(first_kernel, out_shape=[jax.ShapeDtypeStruct((count, unit...  14.7 us
    unnamed x68, local copies, waits for them, and re-layouts  12.6 us
    ppermute x5, starting transfers between devices, other_core(): return lax.ppermute(x, 'tp', [(0, 1), (1, 0)])  12.4 us
    pallas_call x1, Pallas kernels, gates(): pl.pallas_call(gates_kernel, out_shape=[jax.ShapeDtypeStruct((count, widt...  11.9 us
    pallas_call x1, Pallas kernels, first_down(): pl.pallas_call(down_kernel, out_shape=[jax.ShapeDtypeStruct((count, width...  10.2 us
  transfers between devices with their start and end apart: 47, of which 22 were waited for; matrix products, arithmetic and copies ran while one was open for 0% of the time, Pallas kernels for 9%

profile of v6, /device:TPU:1, one launch (start us, length us, event | category | flops | bytes accessed | tf_op | source)
XLA Modules:
  0.0 267.8 jit_solution(3958728418785406617)
XLA Ops:
  0.0 2.3 prepare.1
  2.4 2.5 collective-permute-start.25
  4.9 3.1 %collective-permute-done.25.refs_1_ = bf16[32,1792]{1,0:T(8,128)(2,1)S(1)} collective-permute-done((bf16[32,1792]{1,0:T(8,128)(2,1)}, bf16[32,1792]{1,0:T(8,128)(2,1)S(1)}, u32[]{:S(2)}, u32[]{:S(2)}) %collective-permute-start.25) | collective-permute-done | bytes 114720 | tf_op jit(solution)/shard_map/ppermute | solution.py:82
  8.9 2.5 collective-permute-start.26
  12.6 2.9 %collective-permute-done.13.refs_1_ = bf16[32,1920]{1,0:T(8,128)(2,1)S(1)} collective-permute-done((bf16[32,1920]{1,0:T(8,128)(2,1)}, bf16[32,1920]{1,0:T(8,128)(2,1)S(1)}, u32[]{:S(2)}, u32[]{:S(2)}) %collective-permute-start.13) | collective-permute-done | bytes 122912 | tf_op jit(solution)/shard_map/ppermute | solution.py:82
  16.5 3.5 %collective-permute-start.14 = (bf16[64,1920]{1,0:T(8,128)(2,1)S(1)}, bf16[64,1920]{1,0:T(8,128)(2,1)S(1)}, u32[]{:S(2)}, u32[]{:S(2)}) collective-permute-start(bf16[64,1920]{1,0:T(8,128)(2,1)S(1)} %join.19.refs_0_), channel_id=1, source_target_pairs={{0,96},{32,64},{64,32},{96,0},{1,97},{33,65},{65,33},{97,1},{2,98}... | collective-permute-start | bytes 737288 | tf_op jit(solution)/shard_map/ppermute | solution.py:82
  25.2 2.8 %collective-permute-start.2 = (bf16[64,2048]{1,0:T(8,128)(2,1)S(1)}, bf16[64,2048]{1,0:T(8,128)(2,1)S(1)}, u32[]{:S(2)}, u32[]{:S(2)}) collective-permute-start(bf16[64,2048]{1,0:T(8,128)(2,1)S(1)} %join.15.refs_0_), channel_id=1, source_target_pairs={{0,24},{8,16},{16,8},{24,0},{1,25},{9,17},{17,9},{25,1},{2,26},{10... | collective-permute-start | bytes 786440 | tf_op jit(solution)/shard_map/ppermute | solution.py:82
  28.0 4.5 %collective-permute-start = (bf16[640,1024]{1,0:T(8,128)(2,1)S(1)}, bf16[640,1024]{1,0:T(8,128)(2,1)S(1)}, u32[]{:S(2)}, u32[]{:S(2)}) collective-permute-start(bf16[640,1024]{1,0:T(8,128)(2,1)S(1)} %copy-done.18), channel_id=1, source_target_pairs={{0,1},{1,0},{2,3},{3,2},{4,5},{5,4},{6,7},{7,6},{8,9},{9,8},{10,11... | collective-permute-start | bytes 3932168 | tf_op jit(solution)/shard_map/ppermute | solution.py:36
  33.8 6.0 %collective-permute-done.16.refs_3_ = bf16[128,896]{1,0:T(8,128)(2,1)S(1)} collective-permute-done((bf16[128,896]{1,0:T(8,128)(2,1)S(1)}, bf16[128,896]{1,0:T(8,128)(2,1)S(1)}, u32[]{:S(2)}, u32[]{:S(2)}) %collective-permute-start.16) | collective-permute-done | bytes 229408 | tf_op jit(solution)/shard_map/ppermute | solution.py:82
  39.8 2.2 collective-permute-done.15.refs_2_
  42.8 5.1 %collective-permute-done.4.refs_3_ = bf16[128,1024]{1,0:T(8,128)(2,1)S(1)} collective-permute-done((bf16[128,1024]{1,0:T(8,128)(2,1)S(1)}, bf16[128,1024]{1,0:T(8,128)(2,1)S(1)}, u32[]{:S(2)}, u32[]{:S(2)}) %collective-permute-start.4) | collective-permute-done | bytes 262176 | tf_op jit(solution)/shard_map/ppermute | solution.py:82
  48.7 4.7 %collective-permute-done.30.refs_3_ = bf16[256,896]{1,0:T(8,128)(2,1)S(1)} collective-permute-done((bf16[256,896]{1,0:T(8,128)(2,1)S(1)}, bf16[256,896]{1,0:T(8,128)(2,1)S(1)}, u32[]{:S(2)}, u32[]{:S(2)}) %collective-permute-start.30) | collective-permute-done | bytes 458784 | tf_op jit(solution)/shard_map/ppermute | solution.py:82
  53.8 4.9 %collective-permute-done.17.refs_2_ = bf16[256,1024]{1,0:T(8,128)(2,1)S(1)} collective-permute-done((bf16[256,1024]{1,0:T(8,128)(2,1)S(1)}, bf16[256,1024]{1,0:T(8,128)(2,1)S(1)}, u32[]{:S(2)}, u32[]{:S(2)}) %collective-permute-start.17) | collective-permute-done | bytes 524320 | tf_op jit(solution)/shard_map/ppermute | solution.py:82
  58.9 2.3 collective-permute-done.5.refs_2_
  61.2 5.2 %collective-permute-done.6.refs_3_ = bf16[256,1024]{1,0:T(8,128)(2,1)S(1)} collective-permute-done((bf16[256,1024]{1,0:T(8,128)(2,1)S(1)}, bf16[256,1024]{1,0:T(8,128)(2,1)S(1)}, u32[]{:S(2)}, u32[]{:S(2)}) %collective-permute-start.6) | collective-permute-done | bytes 524320 | tf_op jit(solution)/shard_map/ppermute | solution.py:82
  68.1 26.4 %collective-permute-done.35.rest_22_ = bf16[512,384]{1,0:T(8,128)(2,1)S(1)} collective-permute-done((bf16[512,384]{1,0:T(8,128)(2,1)S(1)}, bf16[512,384]{1,0:T(8,128)(2,1)S(1)}, u32[]{:S(2)}, u32[]{:S(2)}) %collective-permute-start.35) | collective-permute-done | bytes 393248 | tf_op jit(solution)/shard_map/ppermute | solution.py:82
  97.3 16.7 %collective-permute-done.20.refs_1_.refs_3_ = bf16[512,896]{1,0:T(8,128)(2,1)S(1)} collective-permute-done((bf16[512,896]{1,0:T(8,128)(2,1)S(1)}, bf16[512,896]{1,0:T(8,128)(2,1)S(1)}, u32[]{:S(2)}, u32[]{:S(2)}) %collective-permute-start.20) | collective-permute-done | bytes 917536 | tf_op jit(solution)/shard_map/ppermute | solution.py:82
  114.1 4.6 %collective-permute-done.19.refs_0_.refs_2_ = bf16[512,1024]{1,0:T(8,128)(2,1)S(1)} collective-permute-done((bf16[512,1024]{1,0:T(8,128)(2,1)S(1)}, bf16[512,1024]{1,0:T(8,128)(2,1)S(1)}, u32[]{:S(2)}, u32[]{:S(2)}) %collective-permute-start.19) | collective-permute-done | bytes 1048608 | tf_op jit(solution)/shard_map/ppermute | solution.py:82
  118.9 10.1 %collective-permute-done.9.rest_2_ = bf16[512,512]{1,0:T(8,128)(2,1)S(1)} collective-permute-done((bf16[512,512]{1,0:T(8,128)(2,1)S(1)}, bf16[512,512]{1,0:T(8,128)(2,1)S(1)}, u32[]{:S(2)}, u32[]{:S(2)}) %collective-permute-start.9) | collective-permute-done | bytes 524320 | tf_op jit(solution)/shard_map/ppermute | solution.py:82
  141.9 2.4 collective-permute-start.37
  144.3 14.7 %first_hidden.1 = (bf16[640,1408]{1,0:T(8,128)(2,1)}, bf16[2048,2816]{1,0:T(8,128)(2,1)}) custom-call(s32[1]{0:T(128)} %bitcast.core, s32[1]{0:T(128)} %bitcast.1.at, bf16[640,1024]{1,0:T(8,128)(2,1)} %own.3, bf16[640,1024]{1,0:T(8,128)(2,1)} %copy-done.19, f32[1,2048]{1,0:T(1,128)} %bitcast.15, bf16[512,512]{1,0:T(8,128)(2,1)} %copy-done.10, ...), custom_call_target="tpu_custom_call" | custom-call | flops 7381975040 | bytes 23068672 | tf_op jit(solution)/shard_map/first_hidden/pallas_call | solution.py:335
  160.2 10.2 %first_down.1 = (bf16[640,2048]{1,0:T(8,128)(2,1)}, bf16[2048,1408]{1,0:T(8,128)(2,1)}) custom-call(s32[1]{0:T(128)} %bitcast.1.at, bf16[640,1408]{1,0:T(8,128)(2,1)} %get-tuple-element.87.hidden, bf16[1024,384]{1,0:T(8,128)(2,1)} %get-tuple-element.88.rest_0_, bf16[1024,384]{1,0:T(8,128)(2,1)} %collective-permute-done.37.rest_1_, ...), custom_call_target="tpu_custom_call" | custom-call | flops 3690987520 | bytes 11534336 | tf_op jit(solution)/shard_map/first_down/pallas_call | solution.py:388
  170.5 5.8 %collective-permute-start.40 = (bf16[640,2048]{1,0:T(8,128)(2,1)}, bf16[640,2048]{1,0:T(8,128)(2,1)}, u32[]{:S(2)}, u32[]{:S(2)}) collective-permute-start(bf16[640,2048]{1,0:T(8,128)(2,1)} %get-tuple-element.91.term), channel_id=1, source_target_pairs={{0,1},{1,0},{2,3},{3,2},{4,5},{5,4},{6,7},{7,6},{8,9},{9,8},{10,11... | collective-permute-start | bytes 7864328 | tf_op jit(solution)/shard_map/ppermute | solution.py:36
  179.6 21.6 %collective-permute-done.43.rest_5_ = bf16[1024,512]{1,0:T(8,128)(2,1)S(1)} collective-permute-done((bf16[1024,512]{1,0:T(8,128)(2,1)}, bf16[1024,512]{1,0:T(8,128)(2,1)S(1)}, u32[]{:S(2)}, u32[]{:S(2)}) %collective-permute-start.43) | collective-permute-done | bytes 1048608 | tf_op jit(solution)/shard_map/ppermute | solution.py:82
  201.1 2.6 collective-permute-done.41.rest_1_
  205.7 5.3 %assemble.1.rows = bf16[2048,1536]{1,0:T(8,128)(2,1)} custom-call(s32[1]{0:T(128)} %bitcast.1.at, bf16[1024,512]{1,0:T(8,128)(2,1)} %copy-done.6, bf16[1024,512]{1,0:T(8,128)(2,1)} %copy-done.23, bf16[1024,512]{1,0:T(8,128)(2,1)} %copy-done.7, bf16[1024,512]{1,0:T(8,128)(2,1)} %copy-done.24, bf16[1024,512]{1,0:T(8,128)(2,1)} %copy-done.5, ...), custom_call_target="tpu_custom_call" | custom-call | flops 5000000000 | bytes 25165824 | tf_op jit(solution)/shard_map/assemble/pallas_call | solution.py:428
  211.1 11.9 %gates.1 = (bf16[640,2048]{1,0:T(8,128)(2,1)}, f32[2,640,512]{2,1,0:T(8,128)}, f32[640,128]{1,0:T(8,128)}) custom-call(s32[1]{0:T(128)} %bitcast.core, bf16[640,1024]{1,0:T(8,128)(2,1)} %own.3, bf16[640,1024]{1,0:T(8,128)(2,1)} %copy-done.19, bf16[640,2048]{1,0:T(8,128)(2,1)} %get-tuple-element.91.term, bf16[640,2048]{1,0:T(8,128)(2,1)} %collective-permute-done.40.far, ...), custom_call_target="tpu_custom_call" | custom-call | flops 2684354560 | bytes 4194304 | tf_op jit(solution)/shard_map/gates/pallas_call | solution.py:473
  226.4 7.0 %mix.1.term = bf16[640,2048]{1,0:T(8,128)(2,1)} custom-call(f32[2,640,512]{2,1,0:T(8,128)} %get-tuple-element.96.act, f32[640,128]{1,0:T(8,128)} %get-tuple-element.97.sums, f32[640,128]{1,0:T(8,128)} %copy-done.20, f32[1,512]{1,0:T(1,128)} %bitcast.13, f32[1,512]{1,0:T(1,128)} %bitcast.14, bf16[4,128,128]{2,1,0:T(8,128)(2,1)} %weight.1, f32[4,128]{1,0:T(4,128)} %shift.1, ...), custom_call_target="tpu_custom_call" | custom-call | flops 1342177280 | bytes 2097152 | tf_op jit(solution)/shard_map/mix/pallas_call | solution.py:541
  233.8 4.7 %collective-permute-done.45.far = bf16[640,2048]{1,0:T(8,128)(2,1)S(1)} collective-permute-done((bf16[640,2048]{1,0:T(8,128)(2,1)}, bf16[640,2048]{1,0:T(8,128)(2,1)S(1)}, u32[]{:S(2)}, u32[]{:S(2)}) %collective-permute-start.45) | collective-permute-done | bytes 2621472 | tf_op jit(solution)/shard_map/ppermute | solution.py:36
  240.1 20.7 %second_pass.1 = (bf16[640,1024]{1,0:T(8,128)(2,1)}, bf16[640,1024]{1,0:T(8,128)(2,1)}, bf16[640,1024]{1,0:T(8,128)(2,1)}) custom-call(s32[1]{0:T(128)} %bitcast.core, bf16[640,2048]{1,0:T(8,128)(2,1)} %get-tuple-element.95.middle, bf16[640,2048]{1,0:T(8,128)(2,1)} %mix.1.term, bf16[640,2048]{1,0:T(8,128)(2,1)} %copy-done.21, f32[1,2048]{1,0:T(1,128)} %bitcast.16, ...), custom_call_target="tpu_custom_call" | custom-call | flops 11072962560 | bytes 17301504 | tf_op jit(solution)/shard_map/second_pass/pallas_call | solution.py:620
  261.3 2.9 %collective-permute-done.46 = bf16[640,1024]{1,0:T(8,128)(2,1)S(1)} collective-permute-done((bf16[640,1024]{1,0:T(8,128)(2,1)}, bf16[640,1024]{1,0:T(8,128)(2,1)S(1)}, u32[]{:S(2)}, u32[]{:S(2)}) %collective-permute-start.46) | collective-permute-done | bytes 1310752 | tf_op jit(solution)/shard_map/ppermute | solution.py:36
  264.1 3.6 %add_convert_fusion = bf16[640,1024]{1,0:T(8,128)(2,1)} fusion(bf16[640,1024]{1,0:T(8,128)(2,1)S(1)} %collective-permute-done.46, bf16[640,1024]{1,0:T(8,128)(2,1)} %get-tuple-element.101, bf16[640,1024]{1,0:T(8,128)(2,1)} %get-tuple-element.100), kind=kLoop, calls=%fused_computation | loop fusion | flops 4587520 | bytes 5242880 | tf_op jit(solution)/shard_map/convert_element_type | solution.py:722
  (159 shorter events, 41.4 us)
Async XLA Ops:
  8.9 11.1 %collective-permute-start.26 = (bf16[64,1792]{1,0:T(8,128)(2,1)S(1)}, bf16[64,1792]{1,0:T(8,128)(2,1)S(1)}, u32[]{:S(2)}, u32[]{:S(2)}) collective-permute-start(bf16[64,1792]{1,0:T(8,128)(2,1)S(1)} %join.23.refs_0_), channel_id=1, source_target_pairs={{0,6},{2,4},{4,2},{6,0},{1,7},{3,5},{5,3},{7,1},{8,14},{10,12},{12... | collective-permute-start | bytes 688136 | tf_op jit(solution)/shard_map/ppermute | solution.py:82
  16.5 16.1 %collective-permute-start.14 = (bf16[64,1920]{1,0:T(8,128)(2,1)S(1)}, bf16[64,1920]{1,0:T(8,128)(2,1)S(1)}, u32[]{:S(2)}, u32[]{:S(2)}) collective-permute-start(bf16[64,1920]{1,0:T(8,128)(2,1)S(1)} %join.19.refs_0_), channel_id=1, source_target_pairs={{0,96},{32,64},{64,32},{96,0},{1,97},{33,65},{65,33},{97,1},{2,98}... | collective-permute-start | bytes 737288 | tf_op jit(solution)/shard_map/ppermute | solution.py:82
  20.0 12.7 %collective-permute-start.27 = (bf16[128,896]{1,0:T(8,128)(2,1)S(1)}, bf16[128,896]{1,0:T(8,128)(2,1)S(1)}, u32[]{:S(2)}, u32[]{:S(2)}) collective-permute-start(bf16[128,896]{1,0:T(8,128)(2,1)S(1)} %get-tuple-element.77.refs_0_), channel_id=1, source_target_pairs={{0,8},{8,0},{16,24},{24,16},{1,9},{9,1},{17,25},{25,17},{2,10},{10... | collective-permute-start | bytes 688136 | tf_op jit(solution)/shard_map/ppermute | solution.py:82
  21.4 11.4 %collective-permute-start.28 = (bf16[128,896]{1,0:T(8,128)(2,1)S(1)}, bf16[128,896]{1,0:T(8,128)(2,1)S(1)}, u32[]{:S(2)}, u32[]{:S(2)}) collective-permute-start(bf16[128,896]{1,0:T(8,128)(2,1)S(1)} %get-tuple-element.78.refs_1_), channel_id=1, source_target_pairs={{0,2},{2,0},{4,6},{6,4},{1,3},{3,1},{5,7},{7,5},{8,10},{10,8},{12,... | collective-permute-start | bytes 688136 | tf_op jit(solution)/shard_map/ppermute | solution.py:82
  28.0 38.5 %collective-permute-start = (bf16[640,1024]{1,0:T(8,128)(2,1)S(1)}, bf16[640,1024]{1,0:T(8,128)(2,1)S(1)}, u32[]{:S(2)}, u32[]{:S(2)}) collective-permute-start(bf16[640,1024]{1,0:T(8,128)(2,1)S(1)} %copy-done.18), channel_id=1, source_target_pairs={{0,1},{1,0},{2,3},{3,2},{4,5},{5,4},{6,7},{7,6},{8,9},{9,8},{10,11... | collective-permute-start | bytes 3932168 | tf_op jit(solution)/shard_map/ppermute | solution.py:36
  32.9 15.7 %collective-permute-start.29 = (bf16[256,896]{1,0:T(8,128)(2,1)S(1)}, bf16[256,896]{1,0:T(8,128)(2,1)S(1)}, u32[]{:S(2)}, u32[]{:S(2)}) collective-permute-start(bf16[256,896]{1,0:T(8,128)(2,1)S(1)} %get-tuple-element.79.refs_0_), channel_id=1, source_target_pairs={{0,2},{2,0},{4,6},{6,4},{1,3},{3,1},{5,7},{7,5},{8,10},{10,8},{12,... | collective-permute-start | bytes 1376264 | tf_op jit(solution)/shard_map/ppermute | solution.py:82
  42.0 11.3 %collective-permute-start.30 = (bf16[256,896]{1,0:T(8,128)(2,1)S(1)}, bf16[256,896]{1,0:T(8,128)(2,1)S(1)}, u32[]{:S(2)}, u32[]{:S(2)}) collective-permute-start(bf16[256,896]{1,0:T(8,128)(2,1)S(1)} %get-tuple-element.80.refs_1_), channel_id=1, source_target_pairs={{0,8},{8,0},{16,24},{24,16},{1,9},{9,1},{17,25},{25,17},{2,10},{10... | collective-permute-start | bytes 1376264 | tf_op jit(solution)/shard_map/ppermute | solution.py:82
  42.1 11.6 %collective-permute-start.18 = (bf16[256,896]{1,0:T(8,128)(2,1)S(1)}, bf16[256,896]{1,0:T(8,128)(2,1)S(1)}, u32[]{:S(2)}, u32[]{:S(2)}) collective-permute-start(bf16[256,896]{1,0:T(8,128)(2,1)S(1)} %get-tuple-element.69.refs_1_), channel_id=1, source_target_pairs={{0,24},{8,16},{16,8},{24,0},{1,25},{9,17},{17,9},{25,1},{2,26},{10... | collective-permute-start | bytes 1376264 | tf_op jit(solution)/shard_map/ppermute | solution.py:82
  47.9 10.8 %collective-permute-start.17 = (bf16[256,1024]{1,0:T(8,128)(2,1)S(1)}, bf16[256,1024]{1,0:T(8,128)(2,1)S(1)}, u32[]{:S(2)}, u32[]{:S(2)}) collective-permute-start(bf16[256,1024]{1,0:T(8,128)(2,1)S(1)} %get-tuple-element.68.refs_0_), channel_id=1, source_target_pairs={{0,32},{32,0},{64,96},{96,64},{1,33},{33,1},{65,97},{97,65},{2,34}... | collective-permute-start | bytes 1572872 | tf_op jit(solution)/shard_map/ppermute | solution.py:82
  48.6 12.6 %collective-permute-start.5 = (bf16[256,1024]{1,0:T(8,128)(2,1)S(1)}, bf16[256,1024]{1,0:T(8,128)(2,1)S(1)}, u32[]{:S(2)}, u32[]{:S(2)}) collective-permute-start(bf16[256,1024]{1,0:T(8,128)(2,1)S(1)} %get-tuple-element.57.refs_0_), channel_id=1, source_target_pairs={{0,6},{2,4},{4,2},{6,0},{1,7},{3,5},{5,3},{7,1},{8,14},{10,12},{12... | collective-permute-start | bytes 1572872 | tf_op jit(solution)/shard_map/ppermute | solution.py:82
  53.4 13.1 %collective-permute-start.6 = (bf16[256,1024]{1,0:T(8,128)(2,1)S(1)}, bf16[256,1024]{1,0:T(8,128)(2,1)S(1)}, u32[]{:S(2)}, u32[]{:S(2)}) collective-permute-start(bf16[256,1024]{1,0:T(8,128)(2,1)S(1)} %get-tuple-element.58.refs_1_), channel_id=1, source_target_pairs={{0,96},{32,64},{64,32},{96,0},{1,97},{33,65},{65,33},{97,1},{2,98}... | collective-permute-start | bytes 1572872 | tf_op jit(solution)/shard_map/ppermute | solution.py:82
  53.7 12.9 %collective-permute-start.33 = (bf16[512,384]{1,0:T(8,128)(2,1)S(1)}, bf16[512,384]{1,0:T(8,128)(2,1)S(1)}, u32[]{:S(2)}, u32[]{:S(2)}) collective-permute-start(bf16[512,384]{1,0:T(8,128)(2,1)S(1)} %get-tuple-element.83.rest_16_), channel_id=1, source_target_pairs={{0,24},{8,16},{16,8},{24,0},{1,25},{9,17},{17,9},{25,1},{2,26},{10... | collective-permute-start | bytes 1179656 | tf_op jit(solution)/shard_map/ppermute | solution.py:82
  58.7 36.9 %collective-permute-start.31 = (bf16[512,896]{1,0:T(8,128)(2,1)S(1)}, bf16[512,896]{1,0:T(8,128)(2,1)S(1)}, u32[]{:S(2)}, u32[]{:S(2)}) collective-permute-start(bf16[512,896]{1,0:T(8,128)(2,1)S(1)} %get-tuple-element.81.refs_0_), channel_id=1, source_target_pairs={{0,96},{32,64},{64,32},{96,0},{1,97},{33,65},{65,33},{97,1},{2,98}... | collective-permute-start | bytes 2752520 | tf_op jit(solution)/shard_map/ppermute | solution.py:82
  61.2 34.1 %collective-permute-start.21 = (bf16[512,512]{1,0:T(8,128)(2,1)S(1)}, bf16[512,512]{1,0:T(8,128)(2,1)}, u32[]{:S(2)}, u32[]{:S(2)}) collective-permute-start(bf16[512,512]{1,0:T(8,128)(2,1)S(1)} %get-tuple-element.72.rest_8_), channel_id=1, source_target_pairs={{0,2},{2,0},{4,6},{6,4},{1,3},{3,1},{5,7},{7,5},{8,10},{10,8},{12,... | collective-permute-start | bytes 1572872 | tf_op jit(solution)/shard_map/ppermute | solution.py:82
  66.5 28.1 %collective-permute-start.35 = (bf16[512,384]{1,0:T(8,128)(2,1)S(1)}, bf16[512,384]{1,0:T(8,128)(2,1)S(1)}, u32[]{:S(2)}, u32[]{:S(2)}) collective-permute-start(bf16[512,384]{1,0:T(8,128)(2,1)S(1)} %get-tuple-element.85.rest_20_), channel_id=1, source_target_pairs={{0,96},{32,64},{64,32},{96,0},{1,97},{33,65},{65,33},{97,1},{2,98}... | collective-permute-start | bytes 1179656 | tf_op jit(solution)/shard_map/ppermute | solution.py:82
  66.6 28.9 %collective-permute-start.23 = (bf16[512,512]{1,0:T(8,128)(2,1)S(1)}, bf16[512,512]{1,0:T(8,128)(2,1)S(1)}, u32[]{:S(2)}, u32[]{:S(2)}) collective-permute-start(bf16[512,512]{1,0:T(8,128)(2,1)S(1)} %get-tuple-element.74.rest_12_), channel_id=1, source_target_pairs={{0,6},{2,4},{4,2},{6,0},{1,7},{3,5},{5,3},{7,1},{8,14},{10,12},{12... | collective-permute-start | bytes 1572872 | tf_op jit(solution)/shard_map/ppermute | solution.py:82
  66.6 29.3 %collective-permute-start.32 = (bf16[512,896]{1,0:T(8,128)(2,1)S(1)}, bf16[512,896]{1,0:T(8,128)(2,1)S(1)}, u32[]{:S(2)}, u32[]{:S(2)}) collective-permute-start(bf16[512,896]{1,0:T(8,128)(2,1)S(1)} %get-tuple-element.82.refs_1_), channel_id=1, source_target_pairs={{0,24},{8,16},{16,8},{24,0},{1,25},{9,17},{17,9},{25,1},{2,26},{10... | collective-permute-start | bytes 2752520 | tf_op jit(solution)/shard_map/ppermute | solution.py:82
  94.5 19.5 %collective-permute-start.20 = (bf16[512,896]{1,0:T(8,128)(2,1)S(1)}, bf16[512,896]{1,0:T(8,128)(2,1)S(1)}, u32[]{:S(2)}, u32[]{:S(2)}) collective-permute-start(bf16[512,896]{1,0:T(8,128)(2,1)S(1)} %get-tuple-element.71.refs_1_), channel_id=1, source_target_pairs={{0,2},{2,0},{4,6},{6,4},{1,3},{3,1},{5,7},{7,5},{8,10},{10,8},{12,... | collective-permute-start | bytes 2752520 | tf_op jit(solution)/shard_map/ppermute | solution.py:82
  95.3 23.4 %collective-permute-start.19 = (bf16[512,1024]{1,0:T(8,128)(2,1)S(1)}, bf16[512,1024]{1,0:T(8,128)(2,1)S(1)}, u32[]{:S(2)}, u32[]{:S(2)}) collective-permute-start(bf16[512,1024]{1,0:T(8,128)(2,1)S(1)} %get-tuple-element.70.refs_0_), channel_id=1, source_target_pairs={{0,6},{2,4},{4,2},{6,0},{1,7},{3,5},{5,3},{7,1},{8,14},{10,12},{12... | collective-permute-start | bytes 3145736 | tf_op jit(solution)/shard_map/ppermute | solution.py:82
  95.5 34.2 %collective-permute-start.7 = (bf16[512,1024]{1,0:T(8,128)(2,1)S(1)}, bf16[512,1024]{1,0:T(8,128)(2,1)S(1)}, u32[]{:S(2)}, u32[]{:S(2)}) collective-permute-start(bf16[512,1024]{1,0:T(8,128)(2,1)S(1)} %get-tuple-element.59.refs_0_), channel_id=1, source_target_pairs={{0,32},{32,0},{64,96},{96,64},{1,33},{33,1},{65,97},{97,65},{2,34}... | collective-permute-start | bytes 3145736 | tf_op jit(solution)/shard_map/ppermute | solution.py:82
  95.6 34.2 %collective-permute-start.8 = (bf16[512,1024]{1,0:T(8,128)(2,1)S(1)}, bf16[512,1024]{1,0:T(8,128)(2,1)S(1)}, u32[]{:S(2)}, u32[]{:S(2)}) collective-permute-start(bf16[512,1024]{1,0:T(8,128)(2,1)S(1)} %get-tuple-element.60.refs_1_), channel_id=1, source_target_pairs={{0,8},{8,0},{16,24},{24,16},{1,9},{9,1},{17,25},{25,17},{2,10},{10... | collective-permute-start | bytes 3145736 | tf_op jit(solution)/shard_map/ppermute | solution.py:82
  95.9 33.1 %collective-permute-start.9 = (bf16[512,512]{1,0:T(8,128)(2,1)S(1)}, bf16[512,512]{1,0:T(8,128)(2,1)S(1)}, u32[]{:S(2)}, u32[]{:S(2)}) collective-permute-start(bf16[512,512]{1,0:T(8,128)(2,1)S(1)} %get-tuple-element.61.rest_0_), channel_id=1, source_target_pairs={{0,8},{8,0},{16,24},{24,16},{1,9},{9,1},{17,25},{25,17},{2,10},{10... | collective-permute-start | bytes 1572872 | tf_op jit(solution)/shard_map/ppermute | solution.py:82
  114.0 19.8 %collective-permute-start.11 = (bf16[512,512]{1,0:T(8,128)(2,1)S(1)}, bf16[512,512]{1,0:T(8,128)(2,1)S(1)}, u32[]{:S(2)}, u32[]{:S(2)}) collective-permute-start(bf16[512,512]{1,0:T(8,128)(2,1)S(1)} %get-tuple-element.63.rest_4_), channel_id=1, source_target_pairs={{0,32},{32,0},{64,96},{96,64},{1,33},{33,1},{65,97},{97,65},{2,34}... | collective-permute-start | bytes 1572872 | tf_op jit(solution)/shard_map/ppermute | solution.py:82
  118.7 16.0 %collective-permute-start.34 = (bf16[512,384]{1,0:T(8,128)(2,1)S(1)}, bf16[512,384]{1,0:T(8,128)(2,1)S(1)}, u32[]{:S(2)}, u32[]{:S(2)}) collective-permute-start(bf16[512,384]{1,0:T(8,128)(2,1)S(1)} %get-tuple-element.84.rest_17_), channel_id=1, source_target_pairs={{0,24},{8,16},{16,8},{24,0},{1,25},{9,17},{17,9},{25,1},{2,26},{10... | collective-permute-start | bytes 1179656 | tf_op jit(solution)/shard_map/ppermute | solution.py:82
  129.8 11.3 %collective-permute-start.24 = (bf16[512,512]{1,0:T(8,128)(2,1)S(1)}, bf16[512,512]{1,0:T(8,128)(2,1)S(1)}, u32[]{:S(2)}, u32[]{:S(2)}) collective-permute-start(bf16[512,512]{1,0:T(8,128)(2,1)S(1)} %get-tuple-element.75.rest_13_), channel_id=1, source_target_pairs={{0,6},{2,4},{4,2},{6,0},{1,7},{3,5},{5,3},{7,1},{8,14},{10,12},{12... | collective-permute-start | bytes 1572872 | tf_op jit(solution)/shard_map/ppermute | solution.py:82
  137.6 21.5 %collective-permute-start.38 = (bf16[1024,512]{1,0:T(8,128)(2,1)}, bf16[1024,512]{1,0:T(8,128)(2,1)}, u32[]{:S(2)}, u32[]{:S(2)}) collective-permute-start(bf16[1024,512]{1,0:T(8,128)(2,1)} %get-tuple-element.89.rest_2_), channel_id=1, source_target_pairs={{0,24},{8,16},{16,8},{24,0},{1,25},{9,17},{17,9},{25,1},{2,26},{10... | collective-permute-start | bytes 3145736 | tf_op jit(solution)/shard_map/ppermute | solution.py:82
  138.9 21.3 %collective-permute-start.39 = (bf16[1024,512]{1,0:T(8,128)(2,1)}, bf16[1024,512]{1,0:T(8,128)(2,1)}, u32[]{:S(2)}, u32[]{:S(2)}) collective-permute-start(bf16[1024,512]{1,0:T(8,128)(2,1)} %get-tuple-element.90.rest_4_), channel_id=1, source_target_pairs={{0,96},{32,64},{64,32},{96,0},{1,97},{33,65},{65,33},{97,1},{2,98}... | collective-permute-start | bytes 3145736 | tf_op jit(solution)/shard_map/ppermute | solution.py:82
  141.9 17.1 %collective-permute-start.37 = (bf16[1024,384]{1,0:T(8,128)(2,1)}, bf16[1024,384]{1,0:T(8,128)(2,1)}, u32[]{:S(2)}, u32[]{:S(2)}) collective-permute-start(bf16[1024,384]{1,0:T(8,128)(2,1)} %get-tuple-element.88.rest_0_), channel_id=1, source_target_pairs={{0,6},{2,4},{4,2},{6,0},{1,7},{3,5},{5,3},{7,1},{8,14},{10,12},{12... | collective-permute-start | bytes 2359304 | tf_op jit(solution)/shard_map/ppermute | solution.py:82
  170.5 40.6 %collective-permute-start.40 = (bf16[640,2048]{1,0:T(8,128)(2,1)}, bf16[640,2048]{1,0:T(8,128)(2,1)}, u32[]{:S(2)}, u32[]{:S(2)}) collective-permute-start(bf16[640,2048]{1,0:T(8,128)(2,1)} %get-tuple-element.91.term), channel_id=1, source_target_pairs={{0,1},{1,0},{2,3},{3,2},{4,5},{5,4},{6,7},{7,6},{8,9},{9,8},{10,11... | collective-permute-start | bytes 7864328 | tf_op jit(solution)/shard_map/ppermute | solution.py:36
  176.3 24.8 %collective-permute-start.43 = (bf16[1024,512]{1,0:T(8,128)(2,1)}, bf16[1024,512]{1,0:T(8,128)(2,1)S(1)}, u32[]{:S(2)}, u32[]{:S(2)}) collective-permute-start(bf16[1024,512]{1,0:T(8,128)(2,1)} %copy-done.5), channel_id=1, source_target_pairs={{0,2},{2,0},{4,6},{6,4},{1,3},{3,1},{5,7},{7,5},{8,10},{10,8},{12,... | collective-permute-start | bytes 3145736 | tf_op jit(solution)/shard_map/ppermute | solution.py:82
  179.4 24.3 %collective-permute-start.41 = (bf16[1024,512]{1,0:T(8,128)(2,1)S(1)}, bf16[1024,512]{1,0:T(8,128)(2,1)S(1)}, u32[]{:S(2)}, u32[]{:S(2)}) collective-permute-start(bf16[1024,512]{1,0:T(8,128)(2,1)S(1)} %get-tuple-element.92.rest_0_), channel_id=1, source_target_pairs={{0,8},{8,0},{16,24},{24,16},{1,9},{9,1},{17,25},{25,17},{2,10},{10... | collective-permute-start | bytes 3145736 | tf_op jit(solution)/shard_map/ppermute | solution.py:82
  179.6 24.2 %collective-permute-start.42 = (bf16[1024,512]{1,0:T(8,128)(2,1)S(1)}, bf16[1024,512]{1,0:T(8,128)(2,1)S(1)}, u32[]{:S(2)}, u32[]{:S(2)}) collective-permute-start(bf16[1024,512]{1,0:T(8,128)(2,1)S(1)} %get-tuple-element.93.rest_2_), channel_id=1, source_target_pairs={{0,32},{32,0},{64,96},{96,64},{1,33},{33,1},{65,97},{97,65},{2,34}... | collective-permute-start | bytes 3145736 | tf_op jit(solution)/shard_map/ppermute | solution.py:82
  (49 other events, 646.4 us)

commit v7 on v6

--- a/solution.py
+++ b/solution.py
@@ -363,24 +363,54 @@
     place_blocks(at, pieces, weight, sems, widths, range(len(widths)), first)
 
 
+QUARTER = WIDE // HALF_ROWS
+
+
 def down_kernel(at, hidden, *rest):
-    pieces, (term, kept, weight, sems, out_sem) = rest[:6], rest[6:]
+    pieces, (term, kept, weight, sems, out_sems) = rest[:6], rest[6:]
     step = pl.program_id(0)
-    copy = pltpu.make_async_copy(weight, kept, out_sem)
+    begin = starts(DOWN)
 
     @pl.when(step == 0)
     def _():
-        place_blocks_of(at[0], pieces, weight, sems, DOWN, 3)
-        for c in range(3):
-            wait_color(weight, sems, DOWN, c)
-        copy.start()
-
-    rows = pl.ds(pl.multiple_of(step * WIDE, WIDE), WIDE)
-    term[...] = dot_rows(hidden[...], weight[rows, :]).astype(jnp.bfloat16)
-
-    @pl.when(step == pl.num_programs(0) - 1)
-    def _():
-        copy.wait()
+        for quarter in range(4):
+            for c in range(3):
+                columns = pl.ds(begin[c], DOWN[c] * LANES)
+                for slot in range(64):
+                    moved = place(3 + c, slot)
+                    if moved // QUARTER != quarter:
+                        continue
+                    to = pl.multiple_of((at[0] ^ moved) * HALF_ROWS, HALF_ROWS)
+                    pltpu.make_async_copy(
+                        pieces[2 * c + slot // 32].at[
+                            pl.ds(slot % 32 * HALF_ROWS, HALF_ROWS), :
+                        ],
+                        weight.at[pl.ds(to, HALF_ROWS), columns],
+                        sems.at[quarter],
+                    ).start()
+
+    def rows_of(quarter):
+        block = ((at[0] // QUARTER) ^ quarter) * WIDE
+        return pl.ds(pl.multiple_of(block, WIDE), WIDE)
+
+    copies = []
+    for quarter in range(4):
+        part = weight.at[rows_of(quarter), :]
+        copy = pltpu.make_async_copy(part, kept.at[rows_of(quarter), :], out_sems.at[quarter])
+        copies.append(copy)
+
+        @pl.when(step == quarter)
+        def _():
+            pltpu.make_async_copy(part, part, sems.at[quarter]).wait()
+            copy.start()
+
+    part = weight[rows_of(step), :]
+    term[...] = dot_rows(hidden[...], part).astype(jnp.bfloat16)
+
+    @pl.when(step == 3)
+    def _():
+        for copy in copies:
+            copy.wait()
 
 
 def first_down(at, hidden, width, pieces):
@@ -395,11 +425,11 @@
             num_scalar_prefetch=1,
             grid=(width // WIDE,),
             in_specs=[whole((count, units))] + [ANY] * 6,
-            out_specs=[spec((count, WIDE), lambda j, a: (0, j)), ANY],
+            out_specs=[spec((count, WIDE), lambda j, a: (0, (a[0] // QUARTER) ^ j)), ANY],
             scratch_shapes=[
                 pltpu.VMEM((width, units), jnp.bfloat16),
-                pltpu.SemaphoreType.DMA((3,)),
-                pltpu.SemaphoreType.DMA,
+                pltpu.SemaphoreType.DMA((4,)),
+                pltpu.SemaphoreType.DMA((4,)),
             ],
         ),
         compiler_params=params(1),

time: 268 us -> 267 us (level)
  no operation moved by 1% of the time
where the time goes in v7:
time: 267 us; the launch traced here: 266 us
  waiting for transfers between devices  132 us (49%)
  Pallas kernels  75.7 us (28%)
  starting transfers between devices  41.8 us (16%)
  local copies, waits for them, and re-layouts  12.6 us (5%)
  other arithmetic  3.65 us (1%)
    ppermute x42, waiting for transfers between devices, exchange(): return lax.ppermute(x, axis, [(i, i ^ flip) for i in range(4)])  123 us
    ppermute x42, starting transfers between devices, exchange(): return lax.ppermute(x, axis, [(i, i ^ flip) for i in range(4)])  29.4 us
    pallas_call x1, Pallas kernels, second_pass(): pl.pallas_call(second_kernel, out_shape=[jax.ShapeDtypeStruct((count, hal...  20.7 us
    pallas_call x1, Pallas kernels, first_hidden(): pl.pallas_call(first_kernel, out_shape=[jax.ShapeDtypeStruct((count, unit...  14.7 us
    unnamed x68, local copies, waits for them, and re-layouts  12.6 us
    ppermute x5, starting transfers between devices, other_core(): return lax.ppermute(x, 'tp', [(0, 1), (1, 0)])  12.4 us
    pallas_call x1, Pallas kernels, gates(): pl.pallas_call(gates_kernel, out_shape=[jax.ShapeDtypeStruct((count, widt...  11.9 us
    ppermute x5, waiting for transfers between devices, other_core(): return lax.ppermute(x, 'tp', [(0, 1), (1, 0)])  9.09 us
  transfers between devices with their start and end apart: 47, of which 22 were waited for; matrix products, arithmetic and copies ran while one was open for 0% of the time, Pallas kernels for 9%

profile of v7, /device:TPU:1, one launch (start us, length us, event | category | flops | bytes accessed | tf_op | source)
XLA Modules:
  0.0 266.5 jit_solution(13451581758926960791)
XLA Ops:
  0.0 2.3 prepare.1
  2.4 2.5 collective-permute-start.25
  4.9 3.1 %collective-permute-done.25.refs_1_ = bf16[32,1792]{1,0:T(8,128)(2,1)S(1)} collective-permute-done((bf16[32,1792]{1,0:T(8,128)(2,1)}, bf16[32,1792]{1,0:T(8,128)(2,1)S(1)}, u32[]{:S(2)}, u32[]{:S(2)}) %collective-permute-start.25) | collective-permute-done | bytes 114720 | tf_op jit(solution)/shard_map/ppermute | solution.py:82
  8.9 2.5 collective-permute-start.26
  12.6 2.9 %collective-permute-done.13.refs_1_ = bf16[32,1920]{1,0:T(8,128)(2,1)S(1)} collective-permute-done((bf16[32,1920]{1,0:T(8,128)(2,1)}, bf16[32,1920]{1,0:T(8,128)(2,1)S(1)}, u32[]{:S(2)}, u32[]{:S(2)}) %collective-permute-start.13) | collective-permute-done | bytes 122912 | tf_op jit(solution)/shard_map/ppermute | solution.py:82
  16.5 3.5 %collective-permute-start.14 = (bf16[64,1920]{1,0:T(8,128)(2,1)S(1)}, bf16[64,1920]{1,0:T(8,128)(2,1)S(1)}, u32[]{:S(2)}, u32[]{:S(2)}) collective-permute-start(bf16[64,1920]{1,0:T(8,128)(2,1)S(1)} %join.19.refs_0_), channel_id=1, source_target_pairs={{0,96},{32,64},{64,32},{96,0},{1,97},{33,65},{65,33},{97,1},{2,98}... | collective-permute-start | bytes 737288 | tf_op jit(solution)/shard_map/ppermute | solution.py:82
  25.2 2.8 %collective-permute-start.2 = (bf16[64,2048]{1,0:T(8,128)(2,1)S(1)}, bf16[64,2048]{1,0:T(8,128)(2,1)S(1)}, u32[]{:S(2)}, u32[]{:S(2)}) collective-permute-start(bf16[64,2048]{1,0:T(8,128)(2,1)S(1)} %join.15.refs_0_), channel_id=1, source_target_pairs={{0,24},{8,16},{16,8},{24,0},{1,25},{9,17},{17,9},{25,1},{2,26},{10... | collective-permute-start | bytes 786440 | tf_op jit(solution)/shard_map/ppermute | solution.py:82
  28.0 4.5 %collective-permute-start = (bf16[640,1024]{1,0:T(8,128)(2,1)S(1)}, bf16[640,1024]{1,0:T(8,128)(2,1)S(1)}, u32[]{:S(2)}, u32[]{:S(2)}) collective-permute-start(bf16[640,1024]{1,0:T(8,128)(2,1)S(1)} %copy-done.18), channel_id=1, source_target_pairs={{0,1},{1,0},{2,3},{3,2},{4,5},{5,4},{6,7},{7,6},{8,9},{9,8},{10,11... | collective-permute-start | bytes 3932168 | tf_op jit(solution)/shard_map/ppermute | solution.py:36
  33.8 6.0 %collective-permute-done.16.refs_3_ = bf16[128,896]{1,0:T(8,128)(2,1)S(1)} collective-permute-done((bf16[128,896]{1,0:T(8,128)(2,1)S(1)}, bf16[128,896]{1,0:T(8,128)(2,1)S(1)}, u32[]{:S(2)}, u32[]{:S(2)}) %collective-permute-start.16) | collective-permute-done | bytes 229408 | tf_op jit(solution)/shard_map/ppermute | solution.py:82
  39.8 2.2 collective-permute-done.15.refs_2_
  42.8 5.1 %collective-permute-done.4.refs_3_ = bf16[128,1024]{1,0:T(8,128)(2,1)S(1)} collective-permute-done((bf16[128,1024]{1,0:T(8,128)(2,1)S(1)}, bf16[128,1024]{1,0:T(8,128)(2,1)S(1)}, u32[]{:S(2)}, u32[]{:S(2)}) %collective-permute-start.4) | collective-permute-done | bytes 262176 | tf_op jit(solution)/shard_map/ppermute | solution.py:82
  48.7 4.7 %collective-permute-done.30.refs_3_ = bf16[256,896]{1,0:T(8,128)(2,1)S(1)} collective-permute-done((bf16[256,896]{1,0:T(8,128)(2,1)S(1)}, bf16[256,896]{1,0:T(8,128)(2,1)S(1)}, u32[]{:S(2)}, u32[]{:S(2)}) %collective-permute-start.30) | collective-permute-done | bytes 458784 | tf_op jit(solution)/shard_map/ppermute | solution.py:82
  53.8 4.9 %collective-permute-done.17.refs_2_ = bf16[256,1024]{1,0:T(8,128)(2,1)S(1)} collective-permute-done((bf16[256,1024]{1,0:T(8,128)(2,1)S(1)}, bf16[256,1024]{1,0:T(8,128)(2,1)S(1)}, u32[]{:S(2)}, u32[]{:S(2)}) %collective-permute-start.17) | collective-permute-done | bytes 524320 | tf_op jit(solution)/shard_map/ppermute | solution.py:82
  58.9 2.3 collective-permute-done.5.refs_2_
  61.2 5.2 %collective-permute-done.6.refs_3_ = bf16[256,1024]{1,0:T(8,128)(2,1)S(1)} collective-permute-done((bf16[256,1024]{1,0:T(8,128)(2,1)S(1)}, bf16[256,1024]{1,0:T(8,128)(2,1)S(1)}, u32[]{:S(2)}, u32[]{:S(2)}) %collective-permute-start.6) | collective-permute-done | bytes 524320 | tf_op jit(solution)/shard_map/ppermute | solution.py:82
  68.1 26.4 %collective-permute-done.35.rest_22_ = bf16[512,384]{1,0:T(8,128)(2,1)S(1)} collective-permute-done((bf16[512,384]{1,0:T(8,128)(2,1)S(1)}, bf16[512,384]{1,0:T(8,128)(2,1)S(1)}, u32[]{:S(2)}, u32[]{:S(2)}) %collective-permute-start.35) | collective-permute-done | bytes 393248 | tf_op jit(solution)/shard_map/ppermute | solution.py:82
  97.3 16.7 %collective-permute-done.20.refs_1_.refs_3_ = bf16[512,896]{1,0:T(8,128)(2,1)S(1)} collective-permute-done((bf16[512,896]{1,0:T(8,128)(2,1)S(1)}, bf16[512,896]{1,0:T(8,128)(2,1)S(1)}, u32[]{:S(2)}, u32[]{:S(2)}) %collective-permute-start.20) | collective-permute-done | bytes 917536 | tf_op jit(solution)/shard_map/ppermute | solution.py:82
  114.1 4.6 %collective-permute-done.19.refs_0_.refs_2_ = bf16[512,1024]{1,0:T(8,128)(2,1)S(1)} collective-permute-done((bf16[512,1024]{1,0:T(8,128)(2,1)S(1)}, bf16[512,1024]{1,0:T(8,128)(2,1)S(1)}, u32[]{:S(2)}, u32[]{:S(2)}) %collective-permute-start.19) | collective-permute-done | bytes 1048608 | tf_op jit(solution)/shard_map/ppermute | solution.py:82
  118.9 10.1 %collective-permute-done.9.rest_2_ = bf16[512,512]{1,0:T(8,128)(2,1)S(1)} collective-permute-done((bf16[512,512]{1,0:T(8,128)(2,1)S(1)}, bf16[512,512]{1,0:T(8,128)(2,1)S(1)}, u32[]{:S(2)}, u32[]{:S(2)}) %collective-permute-start.9) | collective-permute-done | bytes 524320 | tf_op jit(solution)/shard_map/ppermute | solution.py:82
  141.9 2.4 collective-permute-start.37
  144.3 14.7 %first_hidden.1 = (bf16[640,1408]{1,0:T(8,128)(2,1)}, bf16[2048,2816]{1,0:T(8,128)(2,1)}) custom-call(s32[1]{0:T(128)} %bitcast.core, s32[1]{0:T(128)} %bitcast.1.at, bf16[640,1024]{1,0:T(8,128)(2,1)} %own.3, bf16[640,1024]{1,0:T(8,128)(2,1)} %copy-done.19, f32[1,2048]{1,0:T(1,128)} %bitcast.15, bf16[512,512]{1,0:T(8,128)(2,1)} %copy-done.10, ...), custom_call_target="tpu_custom_call" | custom-call | flops 7381975040 | bytes 23068672 | tf_op jit(solution)/shard_map/first_hidden/pallas_call | solution.py:335
  160.2 8.9 %first_down.1 = (bf16[640,2048]{1,0:T(8,128)(2,1)}, bf16[2048,1408]{1,0:T(8,128)(2,1)}) custom-call(s32[1]{0:T(128)} %bitcast.1.at, bf16[640,1408]{1,0:T(8,128)(2,1)} %get-tuple-element.87.hidden, bf16[1024,384]{1,0:T(8,128)(2,1)} %get-tuple-element.88.rest_0_, bf16[1024,384]{1,0:T(8,128)(2,1)} %collective-permute-done.37.rest_1_, ...), custom_call_target="tpu_custom_call" | custom-call | flops 3690987520 | bytes 11534336 | tf_op jit(solution)/shard_map/first_down/pallas_call | solution.py:418
  169.2 5.8 %collective-permute-start.40 = (bf16[640,2048]{1,0:T(8,128)(2,1)}, bf16[640,2048]{1,0:T(8,128)(2,1)}, u32[]{:S(2)}, u32[]{:S(2)}) collective-permute-start(bf16[640,2048]{1,0:T(8,128)(2,1)} %get-tuple-element.91.term), channel_id=1, source_target_pairs={{0,1},{1,0},{2,3},{3,2},{4,5},{5,4},{6,7},{7,6},{8,9},{9,8},{10,11... | collective-permute-start | bytes 7864328 | tf_op jit(solution)/shard_map/ppermute | solution.py:36
  178.3 21.6 %collective-permute-done.43.rest_5_ = bf16[1024,512]{1,0:T(8,128)(2,1)S(1)} collective-permute-done((bf16[1024,512]{1,0:T(8,128)(2,1)}, bf16[1024,512]{1,0:T(8,128)(2,1)S(1)}, u32[]{:S(2)}, u32[]{:S(2)}) %collective-permute-start.43) | collective-permute-done | bytes 1048608 | tf_op jit(solution)/shard_map/ppermute | solution.py:82
  199.8 2.6 collective-permute-done.41.rest_1_
  204.4 5.3 %assemble.1.rows = bf16[2048,1536]{1,0:T(8,128)(2,1)} custom-call(s32[1]{0:T(128)} %bitcast.1.at, bf16[1024,512]{1,0:T(8,128)(2,1)} %copy-done.6, bf16[1024,512]{1,0:T(8,128)(2,1)} %copy-done.23, bf16[1024,512]{1,0:T(8,128)(2,1)} %copy-done.7, bf16[1024,512]{1,0:T(8,128)(2,1)} %copy-done.24, bf16[1024,512]{1,0:T(8,128)(2,1)} %copy-done.5, ...), custom_call_target="tpu_custom_call" | custom-call | flops 5000000000 | bytes 25165824 | tf_op jit(solution)/shard_map/assemble/pallas_call | solution.py:458
  209.8 11.9 %gates.1 = (bf16[640,2048]{1,0:T(8,128)(2,1)}, f32[2,640,512]{2,1,0:T(8,128)}, f32[640,128]{1,0:T(8,128)}) custom-call(s32[1]{0:T(128)} %bitcast.core, bf16[640,1024]{1,0:T(8,128)(2,1)} %own.3, bf16[640,1024]{1,0:T(8,128)(2,1)} %copy-done.19, bf16[640,2048]{1,0:T(8,128)(2,1)} %get-tuple-element.91.term, bf16[640,2048]{1,0:T(8,128)(2,1)} %collective-permute-done.40.far, ...), custom_call_target="tpu_custom_call" | custom-call | flops 2684354560 | bytes 4194304 | tf_op jit(solution)/shard_map/gates/pallas_call | solution.py:503
  225.1 7.0 %mix.1.term = bf16[640,2048]{1,0:T(8,128)(2,1)} custom-call(f32[2,640,512]{2,1,0:T(8,128)} %get-tuple-element.96.act, f32[640,128]{1,0:T(8,128)} %get-tuple-element.97.sums, f32[640,128]{1,0:T(8,128)} %copy-done.20, f32[1,512]{1,0:T(1,128)} %bitcast.13, f32[1,512]{1,0:T(1,128)} %bitcast.14, bf16[4,128,128]{2,1,0:T(8,128)(2,1)} %weight.1, f32[4,128]{1,0:T(4,128)} %shift.1, ...), custom_call_target="tpu_custom_call" | custom-call | flops 1342177280 | bytes 2097152 | tf_op jit(solution)/shard_map/mix/pallas_call | solution.py:571
  232.4 4.7 %collective-permute-done.45.far = bf16[640,2048]{1,0:T(8,128)(2,1)S(1)} collective-permute-done((bf16[640,2048]{1,0:T(8,128)(2,1)}, bf16[640,2048]{1,0:T(8,128)(2,1)S(1)}, u32[]{:S(2)}, u32[]{:S(2)}) %collective-permute-start.45) | collective-permute-done | bytes 2621472 | tf_op jit(solution)/shard_map/ppermute | solution.py:36
  238.8 20.7 %second_pass.1 = (bf16[640,1024]{1,0:T(8,128)(2,1)}, bf16[640,1024]{1,0:T(8,128)(2,1)}, bf16[640,1024]{1,0:T(8,128)(2,1)}) custom-call(s32[1]{0:T(128)} %bitcast.core, bf16[640,2048]{1,0:T(8,128)(2,1)} %get-tuple-element.95.middle, bf16[640,2048]{1,0:T(8,128)(2,1)} %mix.1.term, bf16[640,2048]{1,0:T(8,128)(2,1)} %copy-done.21, f32[1,2048]{1,0:T(1,128)} %bitcast.16, ...), custom_call_target="tpu_custom_call" | custom-call | flops 11072962560 | bytes 17301504 | tf_op jit(solution)/shard_map/second_pass/pallas_call | solution.py:650
  260.0 2.9 %collective-permute-done.46 = bf16[640,1024]{1,0:T(8,128)(2,1)S(1)} collective-permute-done((bf16[640,1024]{1,0:T(8,128)(2,1)}, bf16[640,1024]{1,0:T(8,128)(2,1)S(1)}, u32[]{:S(2)}, u32[]{:S(2)}) %collective-permute-start.46) | collective-permute-done | bytes 1310752 | tf_op jit(solution)/shard_map/ppermute | solution.py:36
  262.8 3.6 %add_convert_fusion = bf16[640,1024]{1,0:T(8,128)(2,1)} fusion(bf16[640,1024]{1,0:T(8,128)(2,1)S(1)} %collective-permute-done.46, bf16[640,1024]{1,0:T(8,128)(2,1)} %get-tuple-element.101, bf16[640,1024]{1,0:T(8,128)(2,1)} %get-tuple-element.100), kind=kLoop, calls=%fused_computation | loop fusion | flops 4587520 | bytes 5242880 | tf_op jit(solution)/shard_map/convert_element_type | solution.py:752
  (159 shorter events, 41.4 us)
Async XLA Ops:
  8.9 11.1 %collective-permute-start.26 = (bf16[64,1792]{1,0:T(8,128)(2,1)S(1)}, bf16[64,1792]{1,0:T(8,128)(2,1)S(1)}, u32[]{:S(2)}, u32[]{:S(2)}) collective-permute-start(bf16[64,1792]{1,0:T(8,128)(2,1)S(1)} %join.23.refs_0_), channel_id=1, source_target_pairs={{0,6},{2,4},{4,2},{6,0},{1,7},{3,5},{5,3},{7,1},{8,14},{10,12},{12... | collective-permute-start | bytes 688136 | tf_op jit(solution)/shard_map/ppermute | solution.py:82
  16.5 16.1 %collective-permute-start.14 = (bf16[64,1920]{1,0:T(8,128)(2,1)S(1)}, bf16[64,1920]{1,0:T(8,128)(2,1)S(1)}, u32[]{:S(2)}, u32[]{:S(2)}) collective-permute-start(bf16[64,1920]{1,0:T(8,128)(2,1)S(1)} %join.19.refs_0_), channel_id=1, source_target_pairs={{0,96},{32,64},{64,32},{96,0},{1,97},{33,65},{65,33},{97,1},{2,98}... | collective-permute-start | bytes 737288 | tf_op jit(solution)/shard_map/ppermute | solution.py:82
  20.0 12.7 %collective-permute-start.27 = (bf16[128,896]{1,0:T(8,128)(2,1)S(1)}, bf16[128,896]{1,0:T(8,128)(2,1)S(1)}, u32[]{:S(2)}, u32[]{:S(2)}) collective-permute-start(bf16[128,896]{1,0:T(8,128)(2,1)S(1)} %get-tuple-element.77.refs_0_), channel_id=1, source_target_pairs={{0,8},{8,0},{16,24},{24,16},{1,9},{9,1},{17,25},{25,17},{2,10},{10... | collective-permute-start | bytes 688136 | tf_op jit(solution)/shard_map/ppermute | solution.py:82
  21.4 11.4 %collective-permute-start.28 = (bf16[128,896]{1,0:T(8,128)(2,1)S(1)}, bf16[128,896]{1,0:T(8,128)(2,1)S(1)}, u32[]{:S(2)}, u32[]{:S(2)}) collective-permute-start(bf16[128,896]{1,0:T(8,128)(2,1)S(1)} %get-tuple-element.78.refs_1_), channel_id=1, source_target_pairs={{0,2},{2,0},{4,6},{6,4},{1,3},{3,1},{5,7},{7,5},{8,10},{10,8},{12,... | collective-permute-start | bytes 688136 | tf_op jit(solution)/shard_map/ppermute | solution.py:82
  28.0 38.5 %collective-permute-start = (bf16[640,1024]{1,0:T(8,128)(2,1)S(1)}, bf16[640,1024]{1,0:T(8,128)(2,1)S(1)}, u32[]{:S(2)}, u32[]{:S(2)}) collective-permute-start(bf16[640,1024]{1,0:T(8,128)(2,1)S(1)} %copy-done.18), channel_id=1, source_target_pairs={{0,1},{1,0},{2,3},{3,2},{4,5},{5,4},{6,7},{7,6},{8,9},{9,8},{10,11... | collective-permute-start | bytes 3932168 | tf_op jit(solution)/shard_map/ppermute | solution.py:36
  32.9 15.7 %collective-permute-start.29 = (bf16[256,896]{1,0:T(8,128)(2,1)S(1)}, bf16[256,896]{1,0:T(8,128)(2,1)S(1)}, u32[]{:S(2)}, u32[]{:S(2)}) collective-permute-start(bf16[256,896]{1,0:T(8,128)(2,1)S(1)} %get-tuple-element.79.refs_0_), channel_id=1, source_target_pairs={{0,2},{2,0},{4,6},{6,4},{1,3},{3,1},{5,7},{7,5},{8,10},{10,8},{12,... | collective-permute-start | bytes 1376264 | tf_op jit(solution)/shard_map/ppermute | solution.py:82
  42.0 11.3 %collective-permute-start.30 = (bf16[256,896]{1,0:T(8,128)(2,1)S(1)}, bf16[256,896]{1,0:T(8,128)(2,1)S(1)}, u32[]{:S(2)}, u32[]{:S(2)}) collective-permute-start(bf16[256,896]{1,0:T(8,128)(2,1)S(1)} %get-tuple-element.80.refs_1_), channel_id=1, source_target_pairs={{0,8},{8,0},{16,24},{24,16},{1,9},{9,1},{17,25},{25,17},{2,10},{10... | collective-permute-start | bytes 1376264 | tf_op jit(solution)/shard_map/ppermute | solution.py:82
  42.1 11.6 %collective-permute-start.18 = (bf16[256,896]{1,0:T(8,128)(2,1)S(1)}, bf16[256,896]{1,0:T(8,128)(2,1)S(1)}, u32[]{:S(2)}, u32[]{:S(2)}) collective-permute-start(bf16[256,896]{1,0:T(8,128)(2,1)S(1)} %get-tuple-element.69.refs_1_), channel_id=1, source_target_pairs={{0,24},{8,16},{16,8},{24,0},{1,25},{9,17},{17,9},{25,1},{2,26},{10... | collective-permute-start | bytes 1376264 | tf_op jit(solution)/shard_map/ppermute | solution.py:82
  47.9 10.8 %collective-permute-start.17 = (bf16[256,1024]{1,0:T(8,128)(2,1)S(1)}, bf16[256,1024]{1,0:T(8,128)(2,1)S(1)}, u32[]{:S(2)}, u32[]{:S(2)}) collective-permute-start(bf16[256,1024]{1,0:T(8,128)(2,1)S(1)} %get-tuple-element.68.refs_0_), channel_id=1, source_target_pairs={{0,32},{32,0},{64,96},{96,64},{1,33},{33,1},{65,97},{97,65},{2,34}... | collective-permute-start | bytes 1572872 | tf_op jit(solution)/shard_map/ppermute | solution.py:82
  48.6 12.6 %collective-permute-start.5 = (bf16[256,1024]{1,0:T(8,128)(2,1)S(1)}, bf16[256,1024]{1,0:T(8,128)(2,1)S(1)}, u32[]{:S(2)}, u32[]{:S(2)}) collective-permute-start(bf16[256,1024]{1,0:T(8,128)(2,1)S(1)} %get-tuple-element.57.refs_0_), channel_id=1, source_target_pairs={{0,6},{2,4},{4,2},{6,0},{1,7},{3,5},{5,3},{7,1},{8,14},{10,12},{12... | collective-permute-start | bytes 1572872 | tf_op jit(solution)/shard_map/ppermute | solution.py:82
  53.4 13.1 %collective-permute-start.6 = (bf16[256,1024]{1,0:T(8,128)(2,1)S(1)}, bf16[256,1024]{1,0:T(8,128)(2,1)S(1)}, u32[]{:S(2)}, u32[]{:S(2)}) collective-permute-start(bf16[256,1024]{1,0:T(8,128)(2,1)S(1)} %get-tuple-element.58.refs_1_), channel_id=1, source_target_pairs={{0,96},{32,64},{64,32},{96,0},{1,97},{33,65},{65,33},{97,1},{2,98}... | collective-permute-start | bytes 1572872 | tf_op jit(solution)/shard_map/ppermute | solution.py:82
  53.7 12.9 %collective-permute-start.33 = (bf16[512,384]{1,0:T(8,128)(2,1)S(1)}, bf16[512,384]{1,0:T(8,128)(2,1)S(1)}, u32[]{:S(2)}, u32[]{:S(2)}) collective-permute-start(bf16[512,384]{1,0:T(8,128)(2,1)S(1)} %get-tuple-element.83.rest_16_), channel_id=1, source_target_pairs={{0,24},{8,16},{16,8},{24,0},{1,25},{9,17},{17,9},{25,1},{2,26},{10... | collective-permute-start | bytes 1179656 | tf_op jit(solution)/shard_map/ppermute | solution.py:82
  58.7 36.9 %collective-permute-start.31 = (bf16[512,896]{1,0:T(8,128)(2,1)S(1)}, bf16[512,896]{1,0:T(8,128)(2,1)S(1)}, u32[]{:S(2)}, u32[]{:S(2)}) collective-permute-start(bf16[512,896]{1,0:T(8,128)(2,1)S(1)} %get-tuple-element.81.refs_0_), channel_id=1, source_target_pairs={{0,96},{32,64},{64,32},{96,0},{1,97},{33,65},{65,33},{97,1},{2,98}... | collective-permute-start | bytes 2752520 | tf_op jit(solution)/shard_map/ppermute | solution.py:82
  61.2 34.1 %collective-permute-start.21 = (bf16[512,512]{1,0:T(8,128)(2,1)S(1)}, bf16[512,512]{1,0:T(8,128)(2,1)}, u32[]{:S(2)}, u32[]{:S(2)}) collective-permute-start(bf16[512,512]{1,0:T(8,128)(2,1)S(1)} %get-tuple-element.72.rest_8_), channel_id=1, source_target_pairs={{0,2},{2,0},{4,6},{6,4},{1,3},{3,1},{5,7},{7,5},{8,10},{10,8},{12,... | collective-permute-start | bytes 1572872 | tf_op jit(solution)/shard_map/ppermute | solution.py:82
  66.5 28.1 %collective-permute-start.35 = (bf16[512,384]{1,0:T(8,128)(2,1)S(1)}, bf16[512,384]{1,0:T(8,128)(2,1)S(1)}, u32[]{:S(2)}, u32[]{:S(2)}) collective-permute-start(bf16[512,384]{1,0:T(8,128)(2,1)S(1)} %get-tuple-element.85.rest_20_), channel_id=1, source_target_pairs={{0,96},{32,64},{64,32},{96,0},{1,97},{33,65},{65,33},{97,1},{2,98}... | collective-permute-start | bytes 1179656 | tf_op jit(solution)/shard_map/ppermute | solution.py:82
  66.6 28.9 %collective-permute-start.23 = (bf16[512,512]{1,0:T(8,128)(2,1)S(1)}, bf16[512,512]{1,0:T(8,128)(2,1)S(1)}, u32[]{:S(2)}, u32[]{:S(2)}) collective-permute-start(bf16[512,512]{1,0:T(8,128)(2,1)S(1)} %get-tuple-element.74.rest_12_), channel_id=1, source_target_pairs={{0,6},{2,4},{4,2},{6,0},{1,7},{3,5},{5,3},{7,1},{8,14},{10,12},{12... | collective-permute-start | bytes 1572872 | tf_op jit(solution)/shard_map/ppermute | solution.py:82
  66.6 29.3 %collective-permute-start.32 = (bf16[512,896]{1,0:T(8,128)(2,1)S(1)}, bf16[512,896]{1,0:T(8,128)(2,1)S(1)}, u32[]{:S(2)}, u32[]{:S(2)}) collective-permute-start(bf16[512,896]{1,0:T(8,128)(2,1)S(1)} %get-tuple-element.82.refs_1_), channel_id=1, source_target_pairs={{0,24},{8,16},{16,8},{24,0},{1,25},{9,17},{17,9},{25,1},{2,26},{10... | collective-permute-start | bytes 2752520 | tf_op jit(solution)/shard_map/ppermute | solution.py:82
  94.5 19.5 %collective-permute-start.20 = (bf16[512,896]{1,0:T(8,128)(2,1)S(1)}, bf16[512,896]{1,0:T(8,128)(2,1)S(1)}, u32[]{:S(2)}, u32[]{:S(2)}) collective-permute-start(bf16[512,896]{1,0:T(8,128)(2,1)S(1)} %get-tuple-element.71.refs_1_), channel_id=1, source_target_pairs={{0,2},{2,0},{4,6},{6,4},{1,3},{3,1},{5,7},{7,5},{8,10},{10,8},{12,... | collective-permute-start | bytes 2752520 | tf_op jit(solution)/shard_map/ppermute | solution.py:82
  95.3 23.4 %collective-permute-start.19 = (bf16[512,1024]{1,0:T(8,128)(2,1)S(1)}, bf16[512,1024]{1,0:T(8,128)(2,1)S(1)}, u32[]{:S(2)}, u32[]{:S(2)}) collective-permute-start(bf16[512,1024]{1,0:T(8,128)(2,1)S(1)} %get-tuple-element.70.refs_0_), channel_id=1, source_target_pairs={{0,6},{2,4},{4,2},{6,0},{1,7},{3,5},{5,3},{7,1},{8,14},{10,12},{12... | collective-permute-start | bytes 3145736 | tf_op jit(solution)/shard_map/ppermute | solution.py:82
  95.5 34.2 %collective-permute-start.7 = (bf16[512,1024]{1,0:T(8,128)(2,1)S(1)}, bf16[512,1024]{1,0:T(8,128)(2,1)S(1)}, u32[]{:S(2)}, u32[]{:S(2)}) collective-permute-start(bf16[512,1024]{1,0:T(8,128)(2,1)S(1)} %get-tuple-element.59.refs_0_), channel_id=1, source_target_pairs={{0,32},{32,0},{64,96},{96,64},{1,33},{33,1},{65,97},{97,65},{2,34}... | collective-permute-start | bytes 3145736 | tf_op jit(solution)/shard_map/ppermute | solution.py:82
  95.6 34.2 %collective-permute-start.8 = (bf16[512,1024]{1,0:T(8,128)(2,1)S(1)}, bf16[512,1024]{1,0:T(8,128)(2,1)S(1)}, u32[]{:S(2)}, u32[]{:S(2)}) collective-permute-start(bf16[512,1024]{1,0:T(8,128)(2,1)S(1)} %get-tuple-element.60.refs_1_), channel_id=1, source_target_pairs={{0,8},{8,0},{16,24},{24,16},{1,9},{9,1},{17,25},{25,17},{2,10},{10... | collective-permute-start | bytes 3145736 | tf_op jit(solution)/shard_map/ppermute | solution.py:82
  95.9 33.1 %collective-permute-start.9 = (bf16[512,512]{1,0:T(8,128)(2,1)S(1)}, bf16[512,512]{1,0:T(8,128)(2,1)S(1)}, u32[]{:S(2)}, u32[]{:S(2)}) collective-permute-start(bf16[512,512]{1,0:T(8,128)(2,1)S(1)} %get-tuple-element.61.rest_0_), channel_id=1, source_target_pairs={{0,8},{8,0},{16,24},{24,16},{1,9},{9,1},{17,25},{25,17},{2,10},{10... | collective-permute-start | bytes 1572872 | tf_op jit(solution)/shard_map/ppermute | solution.py:82
  114.0 19.8 %collective-permute-start.11 = (bf16[512,512]{1,0:T(8,128)(2,1)S(1)}, bf16[512,512]{1,0:T(8,128)(2,1)S(1)}, u32[]{:S(2)}, u32[]{:S(2)}) collective-permute-start(bf16[512,512]{1,0:T(8,128)(2,1)S(1)} %get-tuple-element.63.rest_4_), channel_id=1, source_target_pairs={{0,32},{32,0},{64,96},{96,64},{1,33},{33,1},{65,97},{97,65},{2,34}... | collective-permute-start | bytes 1572872 | tf_op jit(solution)/shard_map/ppermute | solution.py:82
  118.7 16.0 %collective-permute-start.34 = (bf16[512,384]{1,0:T(8,128)(2,1)S(1)}, bf16[512,384]{1,0:T(8,128)(2,1)S(1)}, u32[]{:S(2)}, u32[]{:S(2)}) collective-permute-start(bf16[512,384]{1,0:T(8,128)(2,1)S(1)} %get-tuple-element.84.rest_17_), channel_id=1, source_target_pairs={{0,24},{8,16},{16,8},{24,0},{1,25},{9,17},{17,9},{25,1},{2,26},{10... | collective-permute-start | bytes 1179656 | tf_op jit(solution)/shard_map/ppermute | solution.py:82
  129.8 11.3 %collective-permute-start.24 = (bf16[512,512]{1,0:T(8,128)(2,1)S(1)}, bf16[512,512]{1,0:T(8,128)(2,1)S(1)}, u32[]{:S(2)}, u32[]{:S(2)}) collective-permute-start(bf16[512,512]{1,0:T(8,128)(2,1)S(1)} %get-tuple-element.75.rest_13_), channel_id=1, source_target_pairs={{0,6},{2,4},{4,2},{6,0},{1,7},{3,5},{5,3},{7,1},{8,14},{10,12},{12... | collective-permute-start | bytes 1572872 | tf_op jit(solution)/shard_map/ppermute | solution.py:82
  137.6 21.5 %collective-permute-start.38 = (bf16[1024,512]{1,0:T(8,128)(2,1)}, bf16[1024,512]{1,0:T(8,128)(2,1)}, u32[]{:S(2)}, u32[]{:S(2)}) collective-permute-start(bf16[1024,512]{1,0:T(8,128)(2,1)} %get-tuple-element.89.rest_2_), channel_id=1, source_target_pairs={{0,24},{8,16},{16,8},{24,0},{1,25},{9,17},{17,9},{25,1},{2,26},{10... | collective-permute-start | bytes 3145736 | tf_op jit(solution)/shard_map/ppermute | solution.py:82
  138.9 21.3 %collective-permute-start.39 = (bf16[1024,512]{1,0:T(8,128)(2,1)}, bf16[1024,512]{1,0:T(8,128)(2,1)}, u32[]{:S(2)}, u32[]{:S(2)}) collective-permute-start(bf16[1024,512]{1,0:T(8,128)(2,1)} %get-tuple-element.90.rest_4_), channel_id=1, source_target_pairs={{0,96},{32,64},{64,32},{96,0},{1,97},{33,65},{65,33},{97,1},{2,98}... | collective-permute-start | bytes 3145736 | tf_op jit(solution)/shard_map/ppermute | solution.py:82
  141.9 17.1 %collective-permute-start.37 = (bf16[1024,384]{1,0:T(8,128)(2,1)}, bf16[1024,384]{1,0:T(8,128)(2,1)}, u32[]{:S(2)}, u32[]{:S(2)}) collective-permute-start(bf16[1024,384]{1,0:T(8,128)(2,1)} %get-tuple-element.88.rest_0_), channel_id=1, source_target_pairs={{0,6},{2,4},{4,2},{6,0},{1,7},{3,5},{5,3},{7,1},{8,14},{10,12},{12... | collective-permute-start | bytes 2359304 | tf_op jit(solution)/shard_map/ppermute | solution.py:82
  169.2 40.6 %collective-permute-start.40 = (bf16[640,2048]{1,0:T(8,128)(2,1)}, bf16[640,2048]{1,0:T(8,128)(2,1)}, u32[]{:S(2)}, u32[]{:S(2)}) collective-permute-start(bf16[640,2048]{1,0:T(8,128)(2,1)} %get-tuple-element.91.term), channel_id=1, source_target_pairs={{0,1},{1,0},{2,3},{3,2},{4,5},{5,4},{6,7},{7,6},{8,9},{9,8},{10,11... | collective-permute-start | bytes 7864328 | tf_op jit(solution)/shard_map/ppermute | solution.py:36
  175.0 24.8 %collective-permute-start.43 = (bf16[1024,512]{1,0:T(8,128)(2,1)}, bf16[1024,512]{1,0:T(8,128)(2,1)S(1)}, u32[]{:S(2)}, u32[]{:S(2)}) collective-permute-start(bf16[1024,512]{1,0:T(8,128)(2,1)} %copy-done.5), channel_id=1, source_target_pairs={{0,2},{2,0},{4,6},{6,4},{1,3},{3,1},{5,7},{7,5},{8,10},{10,8},{12,... | collective-permute-start | bytes 3145736 | tf_op jit(solution)/shard_map/ppermute | solution.py:82
  178.1 24.3 %collective-permute-start.41 = (bf16[1024,512]{1,0:T(8,128)(2,1)S(1)}, bf16[1024,512]{1,0:T(8,128)(2,1)S(1)}, u32[]{:S(2)}, u32[]{:S(2)}) collective-permute-start(bf16[1024,512]{1,0:T(8,128)(2,1)S(1)} %get-tuple-element.92.rest_0_), channel_id=1, source_target_pairs={{0,8},{8,0},{16,24},{24,16},{1,9},{9,1},{17,25},{25,17},{2,10},{10... | collective-permute-start | bytes 3145736 | tf_op jit(solution)/shard_map/ppermute | solution.py:82
  178.3 24.2 %collective-permute-start.42 = (bf16[1024,512]{1,0:T(8,128)(2,1)S(1)}, bf16[1024,512]{1,0:T(8,128)(2,1)S(1)}, u32[]{:S(2)}, u32[]{:S(2)}) collective-permute-start(bf16[1024,512]{1,0:T(8,128)(2,1)S(1)} %get-tuple-element.93.rest_2_), channel_id=1, source_target_pairs={{0,32},{32,0},{64,96},{96,64},{1,33},{33,1},{65,97},{97,65},{2,34}... | collective-permute-start | bytes 3145736 | tf_op jit(solution)/shard_map/ppermute | solution.py:82
  (49 other events, 646.4 us)

commit v8 on v7

--- a/solution.py
+++ b/solution.py
@@ -637,7 +637,8 @@
 
         @pl.when(n >= outs // 2)
         def _():
-            keep[...] = part
+            columns = pl.ds(pl.multiple_of((n - outs // 2) * WIDE, WIDE), WIDE)
+            keep[...] = base[:, columns].astype(jnp.float32) + 0.5 * part.astype(jnp.float32)
 
 
 def second_pass(core, middle, term, far, gain, first, others):
@@ -649,7 +650,7 @@
     sent = outs // 2
     return pl.pallas_call(
         second_kernel,
-        out_shape=[jax.ShapeDtypeStruct((count, half), jnp.bfloat16)] * 3,
+        out_shape=[jax.ShapeDtypeStruct((count, half), x) for x in (jnp.bfloat16, jnp.float32)],
         grid_spec=pltpu.PrefetchScalarGridSpec(
             num_scalar_prefetch=1,
             grid=(5 + outs,),
@@ -664,9 +665,9 @@
             out_specs=[
                 spec((count, WIDE), lambda j, c: (0, jnp.clip(j - 5, 0, sent - 1))),
                 spec((count, WIDE), lambda j, c: (0, jnp.maximum(j - 5 - sent, 0))),
-                whole((count, half)),
             ],
             scratch_shapes=[
+                pltpu.VMEM((count, half), jnp.bfloat16),
                 pltpu.VMEM((count, width), jnp.bfloat16),
                 pltpu.VMEM((count, units), jnp.bfloat16),
                 pltpu.VMEM((width, columns), jnp.bfloat16),
@@ -745,11 +746,10 @@
         spatial_bias,
         mixer,
     )
-    send, keep, base = second_pass(
+    send, keep = second_pass(
         core, middle, term, other_core(term), norm_second[None], first, down
     )
-    last = keep.astype(jnp.float32) + other_core(send).astype(jnp.float32)
-    return (base.astype(jnp.float32) + 0.5 * last).astype(jnp.bfloat16)
+    return (keep + 0.5 * other_core(send).astype(jnp.float32)).astype(jnp.bfloat16)
 
 
 def solution(mesh):

time: 267 us -> 267 us (level)
  no operation moved by 1% of the time
where the time goes in v8:
time: 267 us; the launch traced here: 266 us
  waiting for transfers between devices  132 us (49%)
  Pallas kernels  75.7 us (28%)
  starting transfers between devices  41.8 us (16%)
  local copies, waits for them, and re-layouts  12.6 us (5%)
  other arithmetic  3.31 us (1%)
    ppermute x42, waiting for transfers between devices, exchange(): return lax.ppermute(x, axis, [(i, i ^ flip) for i in range(4)])  123 us
    ppermute x42, starting transfers between devices, exchange(): return lax.ppermute(x, axis, [(i, i ^ flip) for i in range(4)])  29.4 us
    pallas_call x1, Pallas kernels, second_pass(): pl.pallas_call(second_kernel, out_shape=[jax.ShapeDtypeStruct((count, hal...  20.7 us
    pallas_call x1, Pallas kernels, first_hidden(): pl.pallas_call(first_kernel, out_shape=[jax.ShapeDtypeStruct((count, unit...  14.7 us
    unnamed x68, local copies, waits for them, and re-layouts  12.6 us
    ppermute x5, starting transfers between devices, other_core(): return lax.ppermute(x, 'tp', [(0, 1), (1, 0)])  12.4 us
    pallas_call x1, Pallas kernels, gates(): pl.pallas_call(gates_kernel, out_shape=[jax.ShapeDtypeStruct((count, widt...  11.9 us
    ppermute x5, waiting for transfers between devices, other_core(): return lax.ppermute(x, 'tp', [(0, 1), (1, 0)])  9.09 us
  transfers between devices with their start and end apart: 47, of which 22 were waited for; matrix products, arithmetic and copies ran while one was open for 0% of the time, Pallas kernels for 9%

profile of v8, /device:TPU:1, one launch (start us, length us, event | category | flops | bytes accessed | tf_op | source)
XLA Modules:
  0.0 266.1 jit_solution(1587867800517550176)
XLA Ops:
  0.0 2.3 prepare.1
  2.4 2.5 collective-permute-start.25
  4.9 3.1 %collective-permute-done.25.refs_1_ = bf16[32,1792]{1,0:T(8,128)(2,1)S(1)} collective-permute-done((bf16[32,1792]{1,0:T(8,128)(2,1)}, bf16[32,1792]{1,0:T(8,128)(2,1)S(1)}, u32[]{:S(2)}, u32[]{:S(2)}) %collective-permute-start.25) | collective-permute-done | bytes 114720 | tf_op jit(solution)/shard_map/ppermute | solution.py:82
  8.9 2.5 collective-permute-start.26
  12.6 2.9 %collective-permute-done.13.refs_1_ = bf16[32,1920]{1,0:T(8,128)(2,1)S(1)} collective-permute-done((bf16[32,1920]{1,0:T(8,128)(2,1)}, bf16[32,1920]{1,0:T(8,128)(2,1)S(1)}, u32[]{:S(2)}, u32[]{:S(2)}) %collective-permute-start.13) | collective-permute-done | bytes 122912 | tf_op jit(solution)/shard_map/ppermute | solution.py:82
  16.5 3.5 %collective-permute-start.14 = (bf16[64,1920]{1,0:T(8,128)(2,1)S(1)}, bf16[64,1920]{1,0:T(8,128)(2,1)S(1)}, u32[]{:S(2)}, u32[]{:S(2)}) collective-permute-start(bf16[64,1920]{1,0:T(8,128)(2,1)S(1)} %join.19.refs_0_), channel_id=1, source_target_pairs={{0,96},{32,64},{64,32},{96,0},{1,97},{33,65},{65,33},{97,1},{2,98}... | collective-permute-start | bytes 737288 | tf_op jit(solution)/shard_map/ppermute | solution.py:82
  25.2 2.8 %collective-permute-start.2 = (bf16[64,2048]{1,0:T(8,128)(2,1)S(1)}, bf16[64,2048]{1,0:T(8,128)(2,1)S(1)}, u32[]{:S(2)}, u32[]{:S(2)}) collective-permute-start(bf16[64,2048]{1,0:T(8,128)(2,1)S(1)} %join.15.refs_0_), channel_id=1, source_target_pairs={{0,24},{8,16},{16,8},{24,0},{1,25},{9,17},{17,9},{25,1},{2,26},{10... | collective-permute-start | bytes 786440 | tf_op jit(solution)/shard_map/ppermute | solution.py:82
  28.0 4.5 %collective-permute-start = (bf16[640,1024]{1,0:T(8,128)(2,1)S(1)}, bf16[640,1024]{1,0:T(8,128)(2,1)S(1)}, u32[]{:S(2)}, u32[]{:S(2)}) collective-permute-start(bf16[640,1024]{1,0:T(8,128)(2,1)S(1)} %copy-done.18), channel_id=1, source_target_pairs={{0,1},{1,0},{2,3},{3,2},{4,5},{5,4},{6,7},{7,6},{8,9},{9,8},{10,11... | collective-permute-start | bytes 3932168 | tf_op jit(solution)/shard_map/ppermute | solution.py:36
  33.8 6.0 %collective-permute-done.16.refs_3_ = bf16[128,896]{1,0:T(8,128)(2,1)S(1)} collective-permute-done((bf16[128,896]{1,0:T(8,128)(2,1)S(1)}, bf16[128,896]{1,0:T(8,128)(2,1)S(1)}, u32[]{:S(2)}, u32[]{:S(2)}) %collective-permute-start.16) | collective-permute-done | bytes 229408 | tf_op jit(solution)/shard_map/ppermute | solution.py:82
  39.8 2.2 collective-permute-done.15.refs_2_
  42.8 5.1 %collective-permute-done.4.refs_3_ = bf16[128,1024]{1,0:T(8,128)(2,1)S(1)} collective-permute-done((bf16[128,1024]{1,0:T(8,128)(2,1)S(1)}, bf16[128,1024]{1,0:T(8,128)(2,1)S(1)}, u32[]{:S(2)}, u32[]{:S(2)}) %collective-permute-start.4) | collective-permute-done | bytes 262176 | tf_op jit(solution)/shard_map/ppermute | solution.py:82
  48.7 4.7 %collective-permute-done.30.refs_3_ = bf16[256,896]{1,0:T(8,128)(2,1)S(1)} collective-permute-done((bf16[256,896]{1,0:T(8,128)(2,1)S(1)}, bf16[256,896]{1,0:T(8,128)(2,1)S(1)}, u32[]{:S(2)}, u32[]{:S(2)}) %collective-permute-start.30) | collective-permute-done | bytes 458784 | tf_op jit(solution)/shard_map/ppermute | solution.py:82
  53.8 4.9 %collective-permute-done.17.refs_2_ = bf16[256,1024]{1,0:T(8,128)(2,1)S(1)} collective-permute-done((bf16[256,1024]{1,0:T(8,128)(2,1)S(1)}, bf16[256,1024]{1,0:T(8,128)(2,1)S(1)}, u32[]{:S(2)}, u32[]{:S(2)}) %collective-permute-start.17) | collective-permute-done | bytes 524320 | tf_op jit(solution)/shard_map/ppermute | solution.py:82
  58.9 2.3 collective-permute-done.5.refs_2_
  61.2 5.2 %collective-permute-done.6.refs_3_ = bf16[256,1024]{1,0:T(8,128)(2,1)S(1)} collective-permute-done((bf16[256,1024]{1,0:T(8,128)(2,1)S(1)}, bf16[256,1024]{1,0:T(8,128)(2,1)S(1)}, u32[]{:S(2)}, u32[]{:S(2)}) %collective-permute-start.6) | collective-permute-done | bytes 524320 | tf_op jit(solution)/shard_map/ppermute | solution.py:82
  68.1 26.4 %collective-permute-done.35.rest_22_ = bf16[512,384]{1,0:T(8,128)(2,1)S(1)} collective-permute-done((bf16[512,384]{1,0:T(8,128)(2,1)S(1)}, bf16[512,384]{1,0:T(8,128)(2,1)S(1)}, u32[]{:S(2)}, u32[]{:S(2)}) %collective-permute-start.35) | collective-permute-done | bytes 393248 | tf_op jit(solution)/shard_map/ppermute | solution.py:82
  97.3 16.7 %collective-permute-done.20.refs_1_.refs_3_ = bf16[512,896]{1,0:T(8,128)(2,1)S(1)} collective-permute-done((bf16[512,896]{1,0:T(8,128)(2,1)S(1)}, bf16[512,896]{1,0:T(8,128)(2,1)S(1)}, u32[]{:S(2)}, u32[]{:S(2)}) %collective-permute-start.20) | collective-permute-done | bytes 917536 | tf_op jit(solution)/shard_map/ppermute | solution.py:82
  114.1 4.6 %collective-permute-done.19.refs_0_.refs_2_ = bf16[512,1024]{1,0:T(8,128)(2,1)S(1)} collective-permute-done((bf16[512,1024]{1,0:T(8,128)(2,1)S(1)}, bf16[512,1024]{1,0:T(8,128)(2,1)S(1)}, u32[]{:S(2)}, u32[]{:S(2)}) %collective-permute-start.19) | collective-permute-done | bytes 1048608 | tf_op jit(solution)/shard_map/ppermute | solution.py:82
  118.9 10.1 %collective-permute-done.9.rest_2_ = bf16[512,512]{1,0:T(8,128)(2,1)S(1)} collective-permute-done((bf16[512,512]{1,0:T(8,128)(2,1)S(1)}, bf16[512,512]{1,0:T(8,128)(2,1)S(1)}, u32[]{:S(2)}, u32[]{:S(2)}) %collective-permute-start.9) | collective-permute-done | bytes 524320 | tf_op jit(solution)/shard_map/ppermute | solution.py:82
  141.9 2.4 collective-permute-start.37
  144.3 14.7 %first_hidden.1 = (bf16[640,1408]{1,0:T(8,128)(2,1)}, bf16[2048,2816]{1,0:T(8,128)(2,1)}) custom-call(s32[1]{0:T(128)} %bitcast.core, s32[1]{0:T(128)} %bitcast.1.at, bf16[640,1024]{1,0:T(8,128)(2,1)} %own.3, bf16[640,1024]{1,0:T(8,128)(2,1)} %copy-done.19, f32[1,2048]{1,0:T(1,128)} %bitcast.15, bf16[512,512]{1,0:T(8,128)(2,1)} %copy-done.10, ...), custom_call_target="tpu_custom_call" | custom-call | flops 7381975040 | bytes 23068672 | tf_op jit(solution)/shard_map/first_hidden/pallas_call | solution.py:335
  160.2 8.9 %first_down.1 = (bf16[640,2048]{1,0:T(8,128)(2,1)}, bf16[2048,1408]{1,0:T(8,128)(2,1)}) custom-call(s32[1]{0:T(128)} %bitcast.1.at, bf16[640,1408]{1,0:T(8,128)(2,1)} %get-tuple-element.86.hidden, bf16[1024,384]{1,0:T(8,128)(2,1)} %get-tuple-element.87.rest_0_, bf16[1024,384]{1,0:T(8,128)(2,1)} %collective-permute-done.37.rest_1_, ...), custom_call_target="tpu_custom_call" | custom-call | flops 3690987520 | bytes 11534336 | tf_op jit(solution)/shard_map/first_down/pallas_call | solution.py:418
  169.2 5.8 %collective-permute-start.40 = (bf16[640,2048]{1,0:T(8,128)(2,1)}, bf16[640,2048]{1,0:T(8,128)(2,1)}, u32[]{:S(2)}, u32[]{:S(2)}) collective-permute-start(bf16[640,2048]{1,0:T(8,128)(2,1)} %get-tuple-element.90.term), channel_id=1, source_target_pairs={{0,1},{1,0},{2,3},{3,2},{4,5},{5,4},{6,7},{7,6},{8,9},{9,8},{10,11... | collective-permute-start | bytes 7864328 | tf_op jit(solution)/shard_map/ppermute | solution.py:36
  178.3 21.6 %collective-permute-done.43.rest_5_ = bf16[1024,512]{1,0:T(8,128)(2,1)S(1)} collective-permute-done((bf16[1024,512]{1,0:T(8,128)(2,1)}, bf16[1024,512]{1,0:T(8,128)(2,1)S(1)}, u32[]{:S(2)}, u32[]{:S(2)}) %collective-permute-start.43) | collective-permute-done | bytes 1048608 | tf_op jit(solution)/shard_map/ppermute | solution.py:82
  199.8 2.6 collective-permute-done.41.rest_1_
  204.4 5.3 %assemble.1.rows = bf16[2048,1536]{1,0:T(8,128)(2,1)} custom-call(s32[1]{0:T(128)} %bitcast.1.at, bf16[1024,512]{1,0:T(8,128)(2,1)} %copy-done.6, bf16[1024,512]{1,0:T(8,128)(2,1)} %copy-done.23, bf16[1024,512]{1,0:T(8,128)(2,1)} %copy-done.7, bf16[1024,512]{1,0:T(8,128)(2,1)} %copy-done.24, bf16[1024,512]{1,0:T(8,128)(2,1)} %copy-done.5, ...), custom_call_target="tpu_custom_call" | custom-call | flops 5000000000 | bytes 25165824 | tf_op jit(solution)/shard_map/assemble/pallas_call | solution.py:458
  209.8 11.9 %gates.1 = (bf16[640,2048]{1,0:T(8,128)(2,1)}, f32[2,640,512]{2,1,0:T(8,128)}, f32[640,128]{1,0:T(8,128)}) custom-call(s32[1]{0:T(128)} %bitcast.core, bf16[640,1024]{1,0:T(8,128)(2,1)} %own.3, bf16[640,1024]{1,0:T(8,128)(2,1)} %copy-done.19, bf16[640,2048]{1,0:T(8,128)(2,1)} %get-tuple-element.90.term, bf16[640,2048]{1,0:T(8,128)(2,1)} %collective-permute-done.40.far, ...), custom_call_target="tpu_custom_call" | custom-call | flops 2684354560 | bytes 4194304 | tf_op jit(solution)/shard_map/gates/pallas_call | solution.py:503
  225.1 7.0 %mix.1.term = bf16[640,2048]{1,0:T(8,128)(2,1)} custom-call(f32[2,640,512]{2,1,0:T(8,128)} %get-tuple-element.95.act, f32[640,128]{1,0:T(8,128)} %get-tuple-element.96.sums, f32[640,128]{1,0:T(8,128)} %copy-done.20, f32[1,512]{1,0:T(1,128)} %bitcast.13, f32[1,512]{1,0:T(1,128)} %bitcast.14, bf16[4,128,128]{2,1,0:T(8,128)(2,1)} %weight.1, f32[4,128]{1,0:T(4,128)} %shift.1, ...), custom_call_target="tpu_custom_call" | custom-call | flops 1342177280 | bytes 2097152 | tf_op jit(solution)/shard_map/mix/pallas_call | solution.py:571
  232.4 4.7 %collective-permute-done.45.far = bf16[640,2048]{1,0:T(8,128)(2,1)S(1)} collective-permute-done((bf16[640,2048]{1,0:T(8,128)(2,1)}, bf16[640,2048]{1,0:T(8,128)(2,1)S(1)}, u32[]{:S(2)}, u32[]{:S(2)}) %collective-permute-start.45) | collective-permute-done | bytes 2621472 | tf_op jit(solution)/shard_map/ppermute | solution.py:36
  238.8 20.7 %second_pass.1 = (bf16[640,1024]{1,0:T(8,128)(2,1)}, f32[640,1024]{1,0:T(8,128)}) custom-call(s32[1]{0:T(128)} %bitcast.core, bf16[640,2048]{1,0:T(8,128)(2,1)} %get-tuple-element.94.middle, bf16[640,2048]{1,0:T(8,128)(2,1)} %mix.1.term, bf16[640,2048]{1,0:T(8,128)(2,1)} %copy-done.21, f32[1,2048]{1,0:T(1,128)} %bitcast.16, ...), custom_call_target="tpu_custom_call" | custom-call | flops 11072962560 | bytes 17301504 | tf_op jit(solution)/shard_map/second_pass/pallas_call | solution.py:651
  259.9 2.9 %collective-permute-done.46 = bf16[640,1024]{1,0:T(8,128)(2,1)S(1)} collective-permute-done((bf16[640,1024]{1,0:T(8,128)(2,1)}, bf16[640,1024]{1,0:T(8,128)(2,1)S(1)}, u32[]{:S(2)}, u32[]{:S(2)}) %collective-permute-start.46) | collective-permute-done | bytes 1310752 | tf_op jit(solution)/shard_map/ppermute | solution.py:36
  262.8 3.3 %add_convert_fusion = bf16[640,1024]{1,0:T(8,128)(2,1)} fusion(f32[640,1024]{1,0:T(8,128)} %get-tuple-element.99, bf16[640,1024]{1,0:T(8,128)(2,1)S(1)} %collective-permute-done.46), kind=kLoop, calls=%fused_computation | loop fusion | flops 2621440 | bytes 5242880 | tf_op jit(solution)/shard_map/convert_element_type | solution.py:752
  (159 shorter events, 41.4 us)
Async XLA Ops:
  8.9 11.1 %collective-permute-start.26 = (bf16[64,1792]{1,0:T(8,128)(2,1)S(1)}, bf16[64,1792]{1,0:T(8,128)(2,1)S(1)}, u32[]{:S(2)}, u32[]{:S(2)}) collective-permute-start(bf16[64,1792]{1,0:T(8,128)(2,1)S(1)} %join.23.refs_0_), channel_id=1, source_target_pairs={{0,6},{2,4},{4,2},{6,0},{1,7},{3,5},{5,3},{7,1},{8,14},{10,12},{12... | collective-permute-start | bytes 688136 | tf_op jit(solution)/shard_map/ppermute | solution.py:82
  16.5 16.1 %collective-permute-start.14 = (bf16[64,1920]{1,0:T(8,128)(2,1)S(1)}, bf16[64,1920]{1,0:T(8,128)(2,1)S(1)}, u32[]{:S(2)}, u32[]{:S(2)}) collective-permute-start(bf16[64,1920]{1,0:T(8,128)(2,1)S(1)} %join.19.refs_0_), channel_id=1, source_target_pairs={{0,96},{32,64},{64,32},{96,0},{1,97},{33,65},{65,33},{97,1},{2,98}... | collective-permute-start | bytes 737288 | tf_op jit(solution)/shard_map/ppermute | solution.py:82
  20.0 12.7 %collective-permute-start.27 = (bf16[128,896]{1,0:T(8,128)(2,1)S(1)}, bf16[128,896]{1,0:T(8,128)(2,1)S(1)}, u32[]{:S(2)}, u32[]{:S(2)}) collective-permute-start(bf16[128,896]{1,0:T(8,128)(2,1)S(1)} %get-tuple-element.76.refs_0_), channel_id=1, source_target_pairs={{0,8},{8,0},{16,24},{24,16},{1,9},{9,1},{17,25},{25,17},{2,10},{10... | collective-permute-start | bytes 688136 | tf_op jit(solution)/shard_map/ppermute | solution.py:82
  21.4 11.4 %collective-permute-start.28 = (bf16[128,896]{1,0:T(8,128)(2,1)S(1)}, bf16[128,896]{1,0:T(8,128)(2,1)S(1)}, u32[]{:S(2)}, u32[]{:S(2)}) collective-permute-start(bf16[128,896]{1,0:T(8,128)(2,1)S(1)} %get-tuple-element.77.refs_1_), channel_id=1, source_target_pairs={{0,2},{2,0},{4,6},{6,4},{1,3},{3,1},{5,7},{7,5},{8,10},{10,8},{12,... | collective-permute-start | bytes 688136 | tf_op jit(solution)/shard_map/ppermute | solution.py:82
  28.0 38.5 %collective-permute-start = (bf16[640,1024]{1,0:T(8,128)(2,1)S(1)}, bf16[640,1024]{1,0:T(8,128)(2,1)S(1)}, u32[]{:S(2)}, u32[]{:S(2)}) collective-permute-start(bf16[640,1024]{1,0:T(8,128)(2,1)S(1)} %copy-done.18), channel_id=1, source_target_pairs={{0,1},{1,0},{2,3},{3,2},{4,5},{5,4},{6,7},{7,6},{8,9},{9,8},{10,11... | collective-permute-start | bytes 3932168 | tf_op jit(solution)/shard_map/ppermute | solution.py:36
  32.9 15.7 %collective-permute-start.29 = (bf16[256,896]{1,0:T(8,128)(2,1)S(1)}, bf16[256,896]{1,0:T(8,128)(2,1)S(1)}, u32[]{:S(2)}, u32[]{:S(2)}) collective-permute-start(bf16[256,896]{1,0:T(8,128)(2,1)S(1)} %get-tuple-element.78.refs_0_), channel_id=1, source_target_pairs={{0,2},{2,0},{4,6},{6,4},{1,3},{3,1},{5,7},{7,5},{8,10},{10,8},{12,... | collective-permute-start | bytes 1376264 | tf_op jit(solution)/shard_map/ppermute | solution.py:82
  42.0 11.3 %collective-permute-start.30 = (bf16[256,896]{1,0:T(8,128)(2,1)S(1)}, bf16[256,896]{1,0:T(8,128)(2,1)S(1)}, u32[]{:S(2)}, u32[]{:S(2)}) collective-permute-start(bf16[256,896]{1,0:T(8,128)(2,1)S(1)} %get-tuple-element.79.refs_1_), channel_id=1, source_target_pairs={{0,8},{8,0},{16,24},{24,16},{1,9},{9,1},{17,25},{25,17},{2,10},{10... | collective-permute-start | bytes 1376264 | tf_op jit(solution)/shard_map/ppermute | solution.py:82
  42.1 11.6 %collective-permute-start.18 = (bf16[256,896]{1,0:T(8,128)(2,1)S(1)}, bf16[256,896]{1,0:T(8,128)(2,1)S(1)}, u32[]{:S(2)}, u32[]{:S(2)}) collective-permute-start(bf16[256,896]{1,0:T(8,128)(2,1)S(1)} %get-tuple-element.68.refs_1_), channel_id=1, source_target_pairs={{0,24},{8,16},{16,8},{24,0},{1,25},{9,17},{17,9},{25,1},{2,26},{10... | collective-permute-start | bytes 1376264 | tf_op jit(solution)/shard_map/ppermute | solution.py:82
  47.9 10.8 %collective-permute-start.17 = (bf16[256,1024]{1,0:T(8,128)(2,1)S(1)}, bf16[256,1024]{1,0:T(8,128)(2,1)S(1)}, u32[]{:S(2)}, u32[]{:S(2)}) collective-permute-start(bf16[256,1024]{1,0:T(8,128)(2,1)S(1)} %get-tuple-element.67.refs_0_), channel_id=1, source_target_pairs={{0,32},{32,0},{64,96},{96,64},{1,33},{33,1},{65,97},{97,65},{2,34}... | collective-permute-start | bytes 1572872 | tf_op jit(solution)/shard_map/ppermute | solution.py:82
  48.6 12.6 %collective-permute-start.5 = (bf16[256,1024]{1,0:T(8,128)(2,1)S(1)}, bf16[256,1024]{1,0:T(8,128)(2,1)S(1)}, u32[]{:S(2)}, u32[]{:S(2)}) collective-permute-start(bf16[256,1024]{1,0:T(8,128)(2,1)S(1)} %get-tuple-element.56.refs_0_), channel_id=1, source_target_pairs={{0,6},{2,4},{4,2},{6,0},{1,7},{3,5},{5,3},{7,1},{8,14},{10,12},{12... | collective-permute-start | bytes 1572872 | tf_op jit(solution)/shard_map/ppermute | solution.py:82
  53.4 13.1 %collective-permute-start.6 = (bf16[256,1024]{1,0:T(8,128)(2,1)S(1)}, bf16[256,1024]{1,0:T(8,128)(2,1)S(1)}, u32[]{:S(2)}, u32[]{:S(2)}) collective-permute-start(bf16[256,1024]{1,0:T(8,128)(2,1)S(1)} %get-tuple-element.57.refs_1_), channel_id=1, source_target_pairs={{0,96},{32,64},{64,32},{96,0},{1,97},{33,65},{65,33},{97,1},{2,98}... | collective-permute-start | bytes 1572872 | tf_op jit(solution)/shard_map/ppermute | solution.py:82
  53.7 12.9 %collective-permute-start.33 = (bf16[512,384]{1,0:T(8,128)(2,1)S(1)}, bf16[512,384]{1,0:T(8,128)(2,1)S(1)}, u32[]{:S(2)}, u32[]{:S(2)}) collective-permute-start(bf16[512,384]{1,0:T(8,128)(2,1)S(1)} %get-tuple-element.82.rest_16_), channel_id=1, source_target_pairs={{0,24},{8,16},{16,8},{24,0},{1,25},{9,17},{17,9},{25,1},{2,26},{10... | collective-permute-start | bytes 1179656 | tf_op jit(solution)/shard_map/ppermute | solution.py:82
  58.7 36.9 %collective-permute-start.31 = (bf16[512,896]{1,0:T(8,128)(2,1)S(1)}, bf16[512,896]{1,0:T(8,128)(2,1)S(1)}, u32[]{:S(2)}, u32[]{:S(2)}) collective-permute-start(bf16[512,896]{1,0:T(8,128)(2,1)S(1)} %get-tuple-element.80.refs_0_), channel_id=1, source_target_pairs={{0,96},{32,64},{64,32},{96,0},{1,97},{33,65},{65,33},{97,1},{2,98}... | collective-permute-start | bytes 2752520 | tf_op jit(solution)/shard_map/ppermute | solution.py:82
  61.2 34.1 %collective-permute-start.21 = (bf16[512,512]{1,0:T(8,128)(2,1)S(1)}, bf16[512,512]{1,0:T(8,128)(2,1)}, u32[]{:S(2)}, u32[]{:S(2)}) collective-permute-start(bf16[512,512]{1,0:T(8,128)(2,1)S(1)} %get-tuple-element.71.rest_8_), channel_id=1, source_target_pairs={{0,2},{2,0},{4,6},{6,4},{1,3},{3,1},{5,7},{7,5},{8,10},{10,8},{12,... | collective-permute-start | bytes 1572872 | tf_op jit(solution)/shard_map/ppermute | solution.py:82
  66.5 28.1 %collective-permute-start.35 = (bf16[512,384]{1,0:T(8,128)(2,1)S(1)}, bf16[512,384]{1,0:T(8,128)(2,1)S(1)}, u32[]{:S(2)}, u32[]{:S(2)}) collective-permute-start(bf16[512,384]{1,0:T(8,128)(2,1)S(1)} %get-tuple-element.84.rest_20_), channel_id=1, source_target_pairs={{0,96},{32,64},{64,32},{96,0},{1,97},{33,65},{65,33},{97,1},{2,98}... | collective-permute-start | bytes 1179656 | tf_op jit(solution)/shard_map/ppermute | solution.py:82
  66.6 28.9 %collective-permute-start.23 = (bf16[512,512]{1,0:T(8,128)(2,1)S(1)}, bf16[512,512]{1,0:T(8,128)(2,1)S(1)}, u32[]{:S(2)}, u32[]{:S(2)}) collective-permute-start(bf16[512,512]{1,0:T(8,128)(2,1)S(1)} %get-tuple-element.73.rest_12_), channel_id=1, source_target_pairs={{0,6},{2,4},{4,2},{6,0},{1,7},{3,5},{5,3},{7,1},{8,14},{10,12},{12... | collective-permute-start | bytes 1572872 | tf_op jit(solution)/shard_map/ppermute | solution.py:82
  66.6 29.3 %collective-permute-start.32 = (bf16[512,896]{1,0:T(8,128)(2,1)S(1)}, bf16[512,896]{1,0:T(8,128)(2,1)S(1)}, u32[]{:S(2)}, u32[]{:S(2)}) collective-permute-start(bf16[512,896]{1,0:T(8,128)(2,1)S(1)} %get-tuple-element.81.refs_1_), channel_id=1, source_target_pairs={{0,24},{8,16},{16,8},{24,0},{1,25},{9,17},{17,9},{25,1},{2,26},{10... | collective-permute-start | bytes 2752520 | tf_op jit(solution)/shard_map/ppermute | solution.py:82
  94.5 19.5 %collective-permute-start.20 = (bf16[512,896]{1,0:T(8,128)(2,1)S(1)}, bf16[512,896]{1,0:T(8,128)(2,1)S(1)}, u32[]{:S(2)}, u32[]{:S(2)}) collective-permute-start(bf16[512,896]{1,0:T(8,128)(2,1)S(1)} %get-tuple-element.70.refs_1_), channel_id=1, source_target_pairs={{0,2},{2,0},{4,6},{6,4},{1,3},{3,1},{5,7},{7,5},{8,10},{10,8},{12,... | collective-permute-start | bytes 2752520 | tf_op jit(solution)/shard_map/ppermute | solution.py:82
  95.3 23.4 %collective-permute-start.19 = (bf16[512,1024]{1,0:T(8,128)(2,1)S(1)}, bf16[512,1024]{1,0:T(8,128)(2,1)S(1)}, u32[]{:S(2)}, u32[]{:S(2)}) collective-permute-start(bf16[512,1024]{1,0:T(8,128)(2,1)S(1)} %get-tuple-element.69.refs_0_), channel_id=1, source_target_pairs={{0,6},{2,4},{4,2},{6,0},{1,7},{3,5},{5,3},{7,1},{8,14},{10,12},{12... | collective-permute-start | bytes 3145736 | tf_op jit(solution)/shard_map/ppermute | solution.py:82
  95.5 34.2 %collective-permute-start.7 = (bf16[512,1024]{1,0:T(8,128)(2,1)S(1)}, bf16[512,1024]{1,0:T(8,128)(2,1)S(1)}, u32[]{:S(2)}, u32[]{:S(2)}) collective-permute-start(bf16[512,1024]{1,0:T(8,128)(2,1)S(1)} %get-tuple-element.58.refs_0_), channel_id=1, source_target_pairs={{0,32},{32,0},{64,96},{96,64},{1,33},{33,1},{65,97},{97,65},{2,34}... | collective-permute-start | bytes 3145736 | tf_op jit(solution)/shard_map/ppermute | solution.py:82
  95.6 34.2 %collective-permute-start.8 = (bf16[512,1024]{1,0:T(8,128)(2,1)S(1)}, bf16[512,1024]{1,0:T(8,128)(2,1)S(1)}, u32[]{:S(2)}, u32[]{:S(2)}) collective-permute-start(bf16[512,1024]{1,0:T(8,128)(2,1)S(1)} %get-tuple-element.59.refs_1_), channel_id=1, source_target_pairs={{0,8},{8,0},{16,24},{24,16},{1,9},{9,1},{17,25},{25,17},{2,10},{10... | collective-permute-start | bytes 3145736 | tf_op jit(solution)/shard_map/ppermute | solution.py:82
  95.9 33.1 %collective-permute-start.9 = (bf16[512,512]{1,0:T(8,128)(2,1)S(1)}, bf16[512,512]{1,0:T(8,128)(2,1)S(1)}, u32[]{:S(2)}, u32[]{:S(2)}) collective-permute-start(bf16[512,512]{1,0:T(8,128)(2,1)S(1)} %get-tuple-element.60.rest_0_), channel_id=1, source_target_pairs={{0,8},{8,0},{16,24},{24,16},{1,9},{9,1},{17,25},{25,17},{2,10},{10... | collective-permute-start | bytes 1572872 | tf_op jit(solution)/shard_map/ppermute | solution.py:82
  114.0 19.8 %collective-permute-start.11 = (bf16[512,512]{1,0:T(8,128)(2,1)S(1)}, bf16[512,512]{1,0:T(8,128)(2,1)S(1)}, u32[]{:S(2)}, u32[]{:S(2)}) collective-permute-start(bf16[512,512]{1,0:T(8,128)(2,1)S(1)} %get-tuple-element.62.rest_4_), channel_id=1, source_target_pairs={{0,32},{32,0},{64,96},{96,64},{1,33},{33,1},{65,97},{97,65},{2,34}... | collective-permute-start | bytes 1572872 | tf_op jit(solution)/shard_map/ppermute | solution.py:82
  118.7 16.0 %collective-permute-start.34 = (bf16[512,384]{1,0:T(8,128)(2,1)S(1)}, bf16[512,384]{1,0:T(8,128)(2,1)S(1)}, u32[]{:S(2)}, u32[]{:S(2)}) collective-permute-start(bf16[512,384]{1,0:T(8,128)(2,1)S(1)} %get-tuple-element.83.rest_17_), channel_id=1, source_target_pairs={{0,24},{8,16},{16,8},{24,0},{1,25},{9,17},{17,9},{25,1},{2,26},{10... | collective-permute-start | bytes 1179656 | tf_op jit(solution)/shard_map/ppermute | solution.py:82
  129.8 11.3 %collective-permute-start.24 = (bf16[512,512]{1,0:T(8,128)(2,1)S(1)}, bf16[512,512]{1,0:T(8,128)(2,1)S(1)}, u32[]{:S(2)}, u32[]{:S(2)}) collective-permute-start(bf16[512,512]{1,0:T(8,128)(2,1)S(1)} %get-tuple-element.74.rest_13_), channel_id=1, source_target_pairs={{0,6},{2,4},{4,2},{6,0},{1,7},{3,5},{5,3},{7,1},{8,14},{10,12},{12... | collective-permute-start | bytes 1572872 | tf_op jit(solution)/shard_map/ppermute | solution.py:82
  137.6 21.5 %collective-permute-start.38 = (bf16[1024,512]{1,0:T(8,128)(2,1)}, bf16[1024,512]{1,0:T(8,128)(2,1)}, u32[]{:S(2)}, u32[]{:S(2)}) collective-permute-start(bf16[1024,512]{1,0:T(8,128)(2,1)} %get-tuple-element.88.rest_2_), channel_id=1, source_target_pairs={{0,24},{8,16},{16,8},{24,0},{1,25},{9,17},{17,9},{25,1},{2,26},{10... | collective-permute-start | bytes 3145736 | tf_op jit(solution)/shard_map/ppermute | solution.py:82
  138.9 21.3 %collective-permute-start.39 = (bf16[1024,512]{1,0:T(8,128)(2,1)}, bf16[1024,512]{1,0:T(8,128)(2,1)}, u32[]{:S(2)}, u32[]{:S(2)}) collective-permute-start(bf16[1024,512]{1,0:T(8,128)(2,1)} %get-tuple-element.89.rest_4_), channel_id=1, source_target_pairs={{0,96},{32,64},{64,32},{96,0},{1,97},{33,65},{65,33},{97,1},{2,98}... | collective-permute-start | bytes 3145736 | tf_op jit(solution)/shard_map/ppermute | solution.py:82
  141.9 17.1 %collective-permute-start.37 = (bf16[1024,384]{1,0:T(8,128)(2,1)}, bf16[1024,384]{1,0:T(8,128)(2,1)}, u32[]{:S(2)}, u32[]{:S(2)}) collective-permute-start(bf16[1024,384]{1,0:T(8,128)(2,1)} %get-tuple-element.87.rest_0_), channel_id=1, source_target_pairs={{0,6},{2,4},{4,2},{6,0},{1,7},{3,5},{5,3},{7,1},{8,14},{10,12},{12... | collective-permute-start | bytes 2359304 | tf_op jit(solution)/shard_map/ppermute | solution.py:82
  169.2 40.6 %collective-permute-start.40 = (bf16[640,2048]{1,0:T(8,128)(2,1)}, bf16[640,2048]{1,0:T(8,128)(2,1)}, u32[]{:S(2)}, u32[]{:S(2)}) collective-permute-start(bf16[640,2048]{1,0:T(8,128)(2,1)} %get-tuple-element.90.term), channel_id=1, source_target_pairs={{0,1},{1,0},{2,3},{3,2},{4,5},{5,4},{6,7},{7,6},{8,9},{9,8},{10,11... | collective-permute-start | bytes 7864328 | tf_op jit(solution)/shard_map/ppermute | solution.py:36
  175.0 24.8 %collective-permute-start.43 = (bf16[1024,512]{1,0:T(8,128)(2,1)}, bf16[1024,512]{1,0:T(8,128)(2,1)S(1)}, u32[]{:S(2)}, u32[]{:S(2)}) collective-permute-start(bf16[1024,512]{1,0:T(8,128)(2,1)} %copy-done.5), channel_id=1, source_target_pairs={{0,2},{2,0},{4,6},{6,4},{1,3},{3,1},{5,7},{7,5},{8,10},{10,8},{12,... | collective-permute-start | bytes 3145736 | tf_op jit(solution)/shard_map/ppermute | solution.py:82
  178.1 24.3 %collective-permute-start.41 = (bf16[1024,512]{1,0:T(8,128)(2,1)S(1)}, bf16[1024,512]{1,0:T(8,128)(2,1)S(1)}, u32[]{:S(2)}, u32[]{:S(2)}) collective-permute-start(bf16[1024,512]{1,0:T(8,128)(2,1)S(1)} %get-tuple-element.91.rest_0_), channel_id=1, source_target_pairs={{0,8},{8,0},{16,24},{24,16},{1,9},{9,1},{17,25},{25,17},{2,10},{10... | collective-permute-start | bytes 3145736 | tf_op jit(solution)/shard_map/ppermute | solution.py:82
  178.3 24.2 %collective-permute-start.42 = (bf16[1024,512]{1,0:T(8,128)(2,1)S(1)}, bf16[1024,512]{1,0:T(8,128)(2,1)S(1)}, u32[]{:S(2)}, u32[]{:S(2)}) collective-permute-start(bf16[1024,512]{1,0:T(8,128)(2,1)S(1)} %get-tuple-element.92.rest_2_), channel_id=1, source_target_pairs={{0,32},{32,0},{64,96},{96,64},{1,33},{33,1},{65,97},{97,65},{2,34}... | collective-permute-start | bytes 3145736 | tf_op jit(solution)/shard_map/ppermute | solution.py:82
  (49 other events, 646.4 us)
